TPU v7x, 128 devices: a whole 4x4x4 slice. The times are simulated.
128 devices in a mesh: sp: 16 (over z, y), tp: 8 (over x, core).
Axes of the slice: x: 4, y: 4, z: 4, core: 2. Of those that a mesh axis runs over, the one named last changes fastest.
Arguments:
- latents: bfloat16 [4096, 4096], P('sp'), may hold values from -0.4375 to 0.4375
- query_heads: bfloat16 [4096, 16, 128], P('sp', 'tp'), may hold values from -8 to 8
- key_heads: bfloat16 [4096, 16, 128], P('sp', 'tp'), may hold values from -8 to 8
- value_heads: bfloat16 [4096, 16, 128], P('sp', 'tp'), may hold values from -6 to 6
- map_outputs: bfloat16 [4096, 2, 16, 128], P('sp', None, 'tp'), may hold values from -6 to 6
- log_sums: float32 [4096, 16, 2], P('sp', 'tp'), may hold values from -600 to 600, as said below
- out_grad: bfloat16 [4096, 16, 128], P('sp', 'tp'), may hold values from -6 to 6
- mix_lambda: float32 [16], P('tp'), may hold values from 0.3 to 0.8
- norm_gain: float32 [128], replicated, may hold values from 0.1 to 1.9
Outputs:
- query_grad: bfloat16 [4096, 16, 128], P('sp', 'tp')
- key_grad: bfloat16 [4096, 16, 128], P('sp', 'tp')
- value_grad: bfloat16 [4096, 16, 128], P('sp', 'tp')
- weight_grad: float32 [4096, 2048], P('sp', 'tp')
Inputs may be any that keep to these rules, and one draw needn't show every extreme that they name: query_heads, key_heads and value_heads together with map_outputs and log_sums are one consistent causal forward pass: log_sums is the row's log-sum of exp(score_m) over keys at or before the row, and map_outputs[:, m] is prob_m times value_heads rounded to bfloat16.
All inputs are finite; a program needn't handle non-finite values.
Results may differ from a plain program's by a relative error of at most 0.019.
Values may be sent and summed in bfloat16 or wider, within the bound.
No kernel may reach another device: no remote copies, remote signals or barrier semaphores. Data moves between devices by JAX's collectives and lax.ppermute only.
A program may use at most 64 MiB of HBM per device.

v0:
```python
import jax
import jax.numpy as jnp
from jax import lax
from jax.experimental import pallas as pl
from jax.experimental.pallas import tpu as pltpu
from jax.sharding import PartitionSpec as P


DH = 64
EPSILON = 1e-05
SIDE = 4
ROWS = 256
HALF = ROWS // 2
WIDE = 1024
STAT_ROWS = 32
QG = 2 * ROWS + STAT_ROWS
SLOT = QG + 2 * ROWS
LOG2E = 1.4426950408889634
NT = (((1,), (1,)), ((), ()))
BF = jnp.bfloat16
F32 = jnp.float32


def iota(shape, dim):
    return lax.broadcasted_iota(jnp.int32, shape, dim)


def one_hot(hit):
    return jnp.where(hit, 1.0, 0.0).astype(BF)


def exact(a, b):
    return jnp.dot(a, b, preferred_element_type=F32)


def turned(eye, x):
    return lax.dot_general(eye, x, NT, preferred_element_type=F32)


def two_heads(spread, first, second):
    parts = []
    for half in range(2):
        rows = pl.ds(half * ROWS, ROWS)
        parts.append(exact(spread, jnp.concatenate([first[rows], second[rows]], axis=1)))
    found = []
    for lanes in (slice(0, 128), slice(128, 256)):
        for head in range(2):
            keep = slice(head * HALF, (head + 1) * HALF)
            found.append(jnp.concatenate([part[keep, lanes] for part in parts], axis=0))
    return found


def prepare_kernel(
    place, lam, q_hbm, k_hbm, v_hbm, maps_hbm, lse_hbm, out_hbm, gain_hbm, lat_hbm,
    yown, zown, plus, minus, far, lat_own, lat_plus, lat_minus, lat_far,
    q_in, k_in, v_in, maps_in, lse_in, out_in, gain_in, sems,
):
    z = place[0]
    core = place[2]
    pairs = [
        (maps_hbm, maps_in), (out_hbm, out_in), (gain_hbm, gain_in), (lse_hbm, lse_in),
        (q_hbm, q_in), (k_hbm, k_in), (v_hbm, v_in),
    ]
    copies = [pltpu.make_async_copy(a, b, sems.at[n]) for n, (a, b) in enumerate(pairs)]
    tokens = pl.ds(pl.multiple_of(core * HALF, HALF), HALF)
    for ref, step in ((lat_plus, 1), (lat_minus, SIDE - 1), (lat_far, 2)):
        columns = pl.ds(pl.multiple_of((z + step) % SIDE * WIDE, WIDE), WIDE)
        copies.append(
            pltpu.make_async_copy(lat_hbm.at[tokens, columns], ref, sems.at[len(copies)])
        )
    columns = pl.ds(pl.multiple_of(z * WIDE, WIDE), WIDE)
    copies.append(pltpu.make_async_copy(lat_hbm.at[:, columns], lat_own, sems.at[len(copies)]))
    for copy in copies:
        copy.start()
    row = iota((ROWS, ROWS), 0)
    col = iota((ROWS, ROWS), 1)
    spread = one_hot(col == 2 * (row % HALF) + row // HALF)
    deal = one_hot(col == 4 * (row % DH) + row // DH)
    for copy in copies[:4]:
        copy.wait()
    left = exact(deal, jnp.concatenate([maps_in[0:256], maps_in[256:512]], axis=1))
    right = exact(deal, jnp.concatenate([maps_in[512:768], maps_in[768:1024]], axis=1))

    def map_rows(which, head):
        rows = slice((which * 2 + head) * DH, (which * 2 + head + 1) * DH)
        return jnp.concatenate(
            [left[rows, 0:128], left[rows, 128:], right[rows, 0:128], right[rows, 128:]], axis=0
        )

    outs = []
    for half in range(2):
        outs.append(exact(spread, out_in[half * ROWS : (half + 1) * ROWS]))
    gain = gain_in[...]
    for head, ref in ((1, yown), (0, zown)):
        first = map_rows(0, head)
        second = map_rows(1, head)
        rows = slice(head * HALF, (head + 1) * HALF)
        cotangent = jnp.concatenate([outs[0][rows], outs[1][rows]], axis=0)
        combined = first - lam[head] * second
        inverse = lax.rsqrt(jnp.mean(combined * combined, axis=-1, keepdims=True) + EPSILON)
        weighted = gain * cotangent
        dot = jnp.mean(combined * weighted, axis=-1, keepdims=True)
        grad = (inverse * weighted - inverse * inverse * inverse * combined * dot).astype(BF)
        wide = grad.astype(F32)
        term1 = jnp.sum((wide * first).T, axis=0, keepdims=True)
        term2 = jnp.sum((wide * second).T, axis=0, keepdims=True)
        lse = lse_in[head]
        table = jnp.concatenate([lse[0:1], lse[1:2], term1, term2], axis=0)
        high = table.astype(BF).astype(F32)
        middle = (table - high).astype(BF).astype(F32)
        low = table - high - middle
        packed = jnp.concatenate([high, middle, low, jnp.zeros_like(table)], axis=0).astype(BF)
        ref[ROWS : 2 * ROWS] = grad
        ref[2 * ROWS : 2 * ROWS + 16] = packed[:, 0:128]
        ref[2 * ROWS + 16 : QG] = packed[:, 128:256]
    for copy in copies[4:7]:
        copy.wait()
    q0, q1, k0, k1 = two_heads(spread, q_in, k_in)
    v0, v1, _, _ = two_heads(spread, v_in, v_in)
    yown[0:ROWS] = q1.astype(BF)
    yown[QG : QG + ROWS] = k0.astype(BF)
    yown[QG + ROWS : SLOT] = v0.astype(BF)
    zown[0:ROWS] = q0.astype(BF)
    zown[QG : QG + ROWS] = k1.astype(BF)
    zown[QG + ROWS : SLOT] = v1.astype(BF)

    def send(ref, keys):
        @pl.when(keys)
        def _():
            ref[0 : 2 * ROWS] = zown[QG:SLOT]
            ref[2 * ROWS : QG] = jnp.zeros((STAT_ROWS, 128), BF)

        @pl.when(jnp.logical_not(keys))
        def _():
            ref[...] = zown[0:QG]

    send(plus, z < SIDE - 1)
    send(minus, z == 0)
    send(far, z < SIDE // 2)
    for copy in copies[7:]:
        copy.wait()


def attend_kernel(
    place, lam, yown, yleft, yright, ytop, ybottom, zown, plus, minus, far,
    q_left, q_right, q_far, q_plus, q_minus, q_zfar,
    kv_left, kv_right, kv_far, v_plus, v_minus, v_zfar, own_q, own_k, own_v,
    buf, stat, kpad, kturn, qpad, dq, dk, dv,
):
    z = place[0]
    y = place[1]
    buf[0] = yown[...]
    buf[1] = yleft[...]
    buf[2] = yright[...]
    buf[3, 0 : SLOT // 2] = ytop[...]
    buf[3, SLOT // 2 :] = ybottom[...]
    buf[SIDE] = zown[...]
    keys_plus = (z > 0).astype(jnp.int32)
    keys_minus = (z == SIDE - 1).astype(jnp.int32)
    keys_far = (z >= SIDE // 2).astype(jnp.int32)
    for slot, (ref, keys) in enumerate(((plus, keys_plus), (minus, keys_minus), (far, keys_far))):
        @pl.when(keys == 1)
        def _():
            buf[SIDE + 1 + slot, QG:SLOT] = ref[0 : 2 * ROWS]

        @pl.when(keys == 0)
        def _():
            buf[SIDE + 1 + slot, 0:QG] = ref[...]

    row = iota((128, 128), 0)
    col = iota((128, 128), 1)
    eye_first = one_hot(jnp.logical_and(row == col, row < DH))
    eye_second = one_hot(jnp.logical_and(row == col, row >= DH))

    def ready(slot, carry):
        lane = iota((ROWS, 128), 1)
        q = buf[slot, 0:ROWS]
        k = buf[slot, QG : QG + ROWS]
        zero = jnp.zeros_like(q)
        qpad[slot, 0:ROWS] = jnp.where(lane < DH, q, zero)
        qpad[slot, ROWS:] = jnp.where(lane < DH, zero, q)
        kpad[slot, 0:ROWS] = jnp.where(lane < DH, k, zero)
        kpad[slot, ROWS:] = jnp.where(lane < DH, zero, k)
        kturn[slot, :, 0:ROWS] = turned(eye_first, k).astype(BF)
        kturn[slot, :, ROWS:] = turned(eye_second, k).astype(BF)
        left = buf[slot, 2 * ROWS : 2 * ROWS + 16].astype(F32)
        right = buf[slot, 2 * ROWS + 16 : QG].astype(F32)
        pieces = jnp.concatenate([left, right], axis=1)
        rows = pieces[0:4] + pieces[4:8] + pieces[8:12]
        stat[slot, 0:2] = rows[0:2] * LOG2E
        stat[slot, 2:4] = rows[2:4]
        dq[slot] = jnp.zeros((128, ROWS), F32)
        dk[slot] = jnp.zeros((ROWS, 128), F32)
        dv[slot] = jnp.zeros((ROWS, 128), F32)
        return carry

    lax.fori_loop(0, 2 * SIDE, ready, 0)

    def pair(zslot, yslot, kind, shift):
        qs = jnp.where(kind == 0, zslot, yslot)
        ks = jnp.where(kind == 0, yslot, zslot)
        factor = lam[kind]
        q = buf[qs, 0:ROWS]
        g = buf[qs, ROWS : 2 * ROWS]
        v = buf[ks, QG + ROWS : SLOT]
        rows = stat[qs]
        scores = lax.dot_general(kpad[ks], q, NT, preferred_element_type=F32)
        mixed = lax.dot_general(v, g, NT, preferred_element_type=F32)
        scale = DH ** (-0.5) * LOG2E
        power1 = scores[0:ROWS] * scale - rows[0:1]
        power2 = scores[ROWS:] * scale - rows[1:2]
        seen = iota((ROWS, ROWS), 0) <= iota((ROWS, ROWS), 1) + shift
        gone = jnp.full((ROWS, ROWS), -1e30, F32)
        prob1 = jnp.exp2(jnp.where(seen, power1, gone))
        prob2 = factor * jnp.exp2(jnp.where(seen, power2, gone))
        weights = (prob1 - prob2).astype(BF)
        score1 = (prob1 * (mixed - rows[2:3])).astype(BF)
        score2 = (prob2 * (rows[3:4] - mixed)).astype(BF)
        dv[ks] += exact(weights, g)
        dk[ks] += exact(jnp.concatenate([score1, score2], axis=1), qpad[qs])
        dq[qs] += exact(kturn[ks], jnp.concatenate([score1, score2], axis=0))

    def step(item, carry):
        own = item < SIDE + 1
        rest = item - SIDE - 1
        zslot = jnp.where(own, SIDE, SIDE + 1 + rest // SIDE)
        yslot = jnp.where(own, jnp.maximum(item - 1, 0), rest % SIDE)
        offset = jnp.where(yslot == 1, SIDE - 1, jnp.where(yslot == 2, 1, yslot - 1))
        behind = jnp.where(
            yslot == 0, item == 0, (y + offset) % SIDE < y
        )
        kind = jnp.where(
            own,
            1 - behind.astype(jnp.int32),
            jnp.where(
                zslot == SIDE + 1, keys_plus, jnp.where(zslot == SIDE + 2, keys_minus, keys_far)
            ),
        )
        shift = jnp.where(item < 2, 0, 2 * ROWS)
        pair(zslot, yslot, kind, shift)
        return carry

    lax.fori_loop(0, SIDE * SIDE + 1, step, 0)

    scale = DH ** (-0.5)

    def put_q(ref, slot):
        value = (dq[slot] * scale).astype(BF)
        ref[0:HALF] = value[:, 0:128]
        ref[HALF:] = value[:, 128:]

    for slot, (ref, kv) in enumerate(((q_left, kv_left), (q_right, kv_right), (q_far, kv_far))):
        put_q(ref, slot + 1)
        kv[0:ROWS] = (dk[slot + 1] * scale).astype(BF)
        kv[ROWS:] = dv[slot + 1].astype(BF)
    for slot, (ref, ref_v, keys) in enumerate(
        ((q_plus, v_plus, keys_plus), (q_minus, v_minus, keys_minus), (q_zfar, v_zfar, keys_far))
    ):
        @pl.when(keys == 1)
        def _():
            ref[...] = (dk[SIDE + 1 + slot] * scale).astype(BF)

        @pl.when(keys == 0)
        def _():
            put_q(ref, SIDE + 1 + slot)

        ref_v[...] = dv[SIDE + 1 + slot].astype(BF)

    own_q[0] = dq[SIDE] * scale
    own_q[1] = dq[0] * scale
    own_k[0] = dk[0] * scale
    own_k[1] = dk[SIDE] * scale
    own_v[0] = dv[0]
    own_v[1] = dv[SIDE]


def queries_kernel(place, own_q, y1, y2, y3, z1, z2, z3, turned_out, rows_out, acc):
    z = place[0]

    def lanes(ref):
        return jnp.concatenate([ref[0:HALF].astype(F32), ref[HALF:].astype(F32)], axis=1)

    acc[...] = own_q[0]
    for ref, keys in ((z1, z < SIDE - 1), (z2, z == 0), (z3, z < SIDE // 2)):
        @pl.when(jnp.logical_not(keys))
        def _():
            acc[...] += lanes(ref)

    first = acc[...].astype(BF)
    second = (own_q[1] + lanes(y1) + lanes(y2) + lanes(y3)).astype(BF)
    turned_out[0:128] = first
    turned_out[128:256] = second
    row = iota((ROWS, ROWS), 0)
    col = iota((ROWS, ROWS), 1)
    weave = one_hot(col == row % 2 * HALF + row // 2)
    for half in range(2):
        keep = slice(half * HALF, (half + 1) * HALF)
        both = jnp.concatenate([first[:, keep], second[:, keep]], axis=1)
        rows_out[half * ROWS : (half + 1) * ROWS] = turned(weave, both).astype(BF)


def keys_kernel(
    place, own_k, own_v, y1, y2, y3, a1, a2, a3, b1, b2, b3, k_out, v_out, acc_k, acc_v
):
    z = place[0]
    acc_k[...] = own_k[1]
    acc_v[...] = own_v[1]
    for ref, ref_v, keys in (
        (a1, b1, z < SIDE - 1), (a2, b2, z == 0), (a3, b3, z < SIDE // 2)
    ):
        @pl.when(keys)
        def _():
            acc_k[...] += ref[...].astype(F32)
            acc_v[...] += ref_v[...].astype(F32)

    row = iota((ROWS, ROWS), 0)
    col = iota((ROWS, ROWS), 1)
    weave = one_hot(col == row % 2 * HALF + row // 2)
    k0 = own_k[0]
    v0 = own_v[0]
    for ref in (y1, y2, y3):
        k0 += ref[0:ROWS].astype(F32)
        v0 += ref[ROWS:].astype(F32)
    k1 = acc_k[...].astype(BF)
    v1 = acc_v[...].astype(BF)
    zero = jnp.concatenate([k0.astype(BF), v0.astype(BF)], axis=1)
    one = jnp.concatenate([k1, v1], axis=1)
    for half in range(2):
        keep = slice(half * HALF, (half + 1) * HALF)
        woven = exact(weave, jnp.concatenate([zero[keep], one[keep]], axis=0)).astype(BF)
        k_out[half * ROWS : (half + 1) * ROWS] = woven[:, 0:128]
        v_out[half * ROWS : (half + 1) * ROWS] = woven[:, 128:256]


def project_kernel(
    place, g0, g1, g2, g3, lat0, m1, m2, m3, s1, s2, s3, own, to_plus, to_minus, to_far, lat
):
    y = place[1]
    core = place[2]
    lat[0:ROWS] = lat0[...]
    for n, (mine, swap) in enumerate(((m1, s1), (m2, s2), (m3, s3))):
        base = (n + 1) * ROWS
        for part in range(2):
            rows = slice(base + part * HALF, base + (part + 1) * HALF)

            @pl.when(core == part)
            def _():
                lat[rows] = mine[...]

            @pl.when(core != part)
            def _():
                lat[rows] = swap[...]

    grads = jnp.concatenate([g0[...], g1[...], g2[...], g3[...]], axis=1)
    for ref, step in ((to_plus, 1), (to_minus, SIDE - 1), (to_far, 2), (own, 0)):
        columns = pl.ds(pl.multiple_of((y + step) % SIDE * ROWS, ROWS), ROWS)
        ref[...] = exact(grads, lat[:, columns]).astype(ref.dtype)


def total_kernel(own, t1, t2, t3, out):
    whole = own[...] + t1[...].astype(F32) + t2[...].astype(F32) + t3[...].astype(F32)
    out[...] = whole.T


def moved(x, dz, dy):
    pairs = []
    for z in range(SIDE):
        for y in range(SIDE):
            pairs.append((z * SIDE + y, (z + dz) % SIDE * SIDE + (y + dy) % SIDE))
    return lax.ppermute(x, "sp", pairs)


def partner(x):
    return lax.ppermute(x, "tp", [(t, t ^ 1) for t in range(lax.axis_size("tp"))])


def shape(*dims, dtype=BF):
    return jax.ShapeDtypeStruct(dims, dtype)


def call(kernel, outs, scalars, hbm, vmem, scratch, flops, mib=16):
    return pl.pallas_call(
        kernel,
        out_shape=outs,
        in_specs=[pl.BlockSpec(memory_space=pltpu.SMEM)] * scalars
        + [pl.BlockSpec(memory_space=pltpu.HBM)] * hbm
        + [pl.BlockSpec(memory_space=pltpu.VMEM)] * vmem,
        out_specs=jax.tree.map(lambda _: pl.BlockSpec(memory_space=pltpu.VMEM), outs),
        scratch_shapes=scratch,
        compiler_params=pltpu.CompilerParams(vmem_limit_bytes=mib * 2**20),
        cost_estimate=pl.CostEstimate(flops=flops, bytes_accessed=10**6, transcendentals=0),
    )


def body(
    latents,
    query_heads,
    key_heads,
    value_heads,
    map_outputs,
    log_sums,
    out_grad,
    mix_lambda,
    norm_gain,
):
    index = lax.axis_index("sp")
    place = jnp.stack([index // SIDE, index % SIDE, lax.axis_index("tp") % 2]).astype(jnp.int32)
    part = shape(HALF, WIDE)
    yown, zown, plus, minus, far, lat_own, lat_plus, lat_minus, lat_far = call(
        prepare_kernel,
        (shape(SLOT, 128),) * 2 + (shape(QG, 128),) * 3 + (shape(ROWS, WIDE), part, part, part),
        2,
        8,
        0,
        [pltpu.VMEM((2 * ROWS, 128), BF)] * 3
        + [
            pltpu.VMEM((4 * ROWS, 128), BF),
            pltpu.VMEM((2, 2, ROWS), F32),
            pltpu.VMEM((2 * ROWS, 128), BF),
            pltpu.VMEM((1, 128), F32),
            pltpu.SemaphoreType.DMA((11,)),
        ],
        10**8,
        54,
    )(
        place,
        mix_lambda,
        query_heads.reshape(2 * ROWS, 128),
        key_heads.reshape(2 * ROWS, 128),
        value_heads.reshape(2 * ROWS, 128),
        map_outputs.reshape(4 * ROWS, 128),
        jnp.transpose(log_sums, (1, 2, 0)),
        out_grad.reshape(2 * ROWS, 128),
        norm_gain.reshape(1, 128),
        latents,
    )
    yleft = moved(yown, 0, 1)
    yright = moved(yown, 0, -1)
    zplus = moved(plus, 1, 0)
    zminus = moved(minus, -1, 0)
    zfar = moved(far, 2, 0)
    ytop = moved(yleft[0 : SLOT // 2], 0, 1)
    ybottom = moved(yright[SLOT // 2 :], 0, -1)
    mine = (moved(lat_plus, 1, 0), moved(lat_minus, -1, 0), moved(lat_far, 2, 0))
    swap = tuple(partner(x) for x in mine)

    slots = 2 * SIDE
    small = shape(ROWS, 128)
    both = shape(2 * ROWS, 128)
    results = call(
        attend_kernel,
        (small,) * 6
        + (both,) * 3
        + (small,) * 3
        + (shape(2, 128, ROWS, dtype=F32),)
        + (shape(2, ROWS, 128, dtype=F32),) * 2,
        2,
        0,
        9,
        [
            pltpu.VMEM((slots, SLOT, 128), BF),
            pltpu.VMEM((slots, 8, ROWS), F32),
            pltpu.VMEM((slots, 2 * ROWS, 128), BF),
            pltpu.VMEM((slots, 128, 2 * ROWS), BF),
            pltpu.VMEM((slots, 2 * ROWS, 128), BF),
            pltpu.VMEM((slots, 128, ROWS), F32),
            pltpu.VMEM((slots, ROWS, 128), F32),
            pltpu.VMEM((slots, ROWS, 128), F32),
        ],
        17 * 10 * ROWS * ROWS * 128,
        24,
    )(place, mix_lambda, yown, yleft, yright, ytop, ybottom, zown, zplus, zminus, zfar)
    q_left, q_right, q_far, q_plus, q_minus, q_zfar = results[0:6]
    kv_left, kv_right, kv_far, v_plus, v_minus, v_zfar = results[6:12]
    own_q, own_k, own_v = results[12:15]
    q_back = (
        moved(q_left, 0, -1),
        moved(q_right, 0, 1),
        moved(q_far, 0, 2),
        moved(q_plus, -1, 0),
        moved(q_minus, 1, 0),
        moved(q_zfar, 2, 0),
    )
    turned_grad, query_rows = call(
        queries_kernel,
        (shape(ROWS, ROWS), shape(2 * ROWS, 128)),
        1,
        0,
        7,
        [pltpu.VMEM((128, ROWS), F32)],
        10**7,
    )(place, own_q, *q_back)
    grads = (
        turned_grad, moved(turned_grad, 1, 0), moved(turned_grad, -1, 0), moved(turned_grad, 2, 0)
    )
    kv_back = (moved(kv_left, 0, -1), moved(kv_right, 0, 1), moved(kv_far, 0, 2))
    v_back = (moved(v_plus, -1, 0), moved(v_minus, 1, 0), moved(v_zfar, 2, 0))
    key_rows, value_rows = call(
        keys_kernel,
        (shape(2 * ROWS, 128),) * 2,
        1,
        0,
        11,
        [pltpu.VMEM((ROWS, 128), F32)] * 2,
        10**7,
    )(place, own_k, own_v, *kv_back, *q_back[3:], *v_back)
    square = shape(ROWS, ROWS)
    own, to_plus, to_minus, to_far = call(
        project_kernel,
        (shape(ROWS, ROWS, dtype=F32), square, square, square),
        1,
        0,
        11,
        [pltpu.VMEM((WIDE, WIDE), BF)],
        2 * WIDE * WIDE * ROWS,
    )(place, *grads, lat_own, *mine, *swap)
    weight_grad = call(total_kernel, shape(ROWS, ROWS, dtype=F32), 0, 0, 4, [], 10**6)(
        own, moved(to_plus, 0, 1), moved(to_minus, 0, -1), moved(to_far, 0, 2)
    )
    whole = (ROWS, 2, 128)
    return (
        query_rows.reshape(whole),
        key_rows.reshape(whole),
        value_rows.reshape(whole),
        weight_grad,
    )


def solution(mesh):
    placed = (
        P("sp", None),
        P("sp", "tp", None),
        P("sp", "tp", None),
        P("sp", "tp", None),
        P("sp", None, "tp", None),
        P("sp", "tp", None),
        P("sp", "tp", None),
        P("tp"),
        P(),
    )
    return jax.shard_map(
        body,
        mesh=mesh,
        in_specs=placed,
        out_specs=(P("sp", "tp", None), P("sp", "tp", None), P("sp", "tp", None), P("sp", "tp")),
        check_vma=False,
    )
```

profile of v0, /device:TPU:0, one launch (start us, length us, event | category | flops | bytes accessed | tf_op | source)
XLA Modules:
  0.0 83.1 jit_solution(14169956088238594023)
XLA Ops:
  0.6 0.0 copy-start.2
  0.7 0.7 pad_add_fusion.place
  1.3 4.1 %shard_map.120 = (bf16[1056,128]{1,0:T(8,128)(2,1)}, bf16[1056,128]{1,0:T(8,128)(2,1)}, bf16[544,128]{1,0:T(8,128)(2,1)}, bf16[544,128]{1,0:T(8,128)(2,1)}, bf16...) custom-call(s32[3]{0:T(128)} %pad_add_fusion.place, ...), custom_call_target="tpu_custom_call" | custom-call | flops 100000000 | bytes 1000000 | tf_op jit(solution)/shard_map/pallas_call | solution.py:409
  5.5 1.8 %collective-permute-start = (bf16[1056,128]{1,0:T(8,128)(2,1)}, bf16[1056,128]{1,0:T(8,128)(2,1)S(1)}, u32[]{:S(2)}, u32[]{:S(2)}) collective-permute-start(bf16[1056,128]{1,0:T(8,128)(2,1)} %get-tuple-element.36.yown), channel_id=1, source_target_pairs={{0,8},{8,16},{16,24},{24,0},{32,40},{40,48},{48,56},{56,32},{64,72... | collective-permute-start | bytes 811016 | tf_op jit(solution)/shard_map/ppermute | solution.py:370
  7.2 1.5 %collective-permute-start.1 = (bf16[1056,128]{1,0:T(8,128)(2,1)}, bf16[1056,128]{1,0:T(8,128)(2,1)S(1)}, u32[]{:S(2)}, u32[]{:S(2)}) collective-permute-start(bf16[1056,128]{1,0:T(8,128)(2,1)} %get-tuple-element.36.yown), channel_id=1, source_target_pairs={{0,24},{8,0},{16,8},{24,16},{32,56},{40,32},{48,40},{56,48},{64,88... | collective-permute-start | bytes 811016 | tf_op jit(solution)/shard_map/ppermute | solution.py:370
  8.8 2.0 %collective-permute-start.4 = (bf16[544,128]{1,0:T(8,128)(2,1)}, bf16[544,128]{1,0:T(8,128)(2,1)S(1)}, u32[]{:S(2)}, u32[]{:S(2)}) collective-permute-start(bf16[544,128]{1,0:T(8,128)(2,1)} %get-tuple-element.38), channel_id=1, source_target_pairs={{0,32},{8,40},{16,48},{24,56},{32,64},{40,72},{48,80},{56,88},{64,... | collective-permute-start | bytes 417800 | tf_op jit(solution)/shard_map/ppermute | solution.py:370
  10.8 2.1 %collective-permute-start.5 = (bf16[544,128]{1,0:T(8,128)(2,1)}, bf16[544,128]{1,0:T(8,128)(2,1)S(1)}, u32[]{:S(2)}, u32[]{:S(2)}) collective-permute-start(bf16[544,128]{1,0:T(8,128)(2,1)} %get-tuple-element.39), channel_id=1, source_target_pairs={{0,96},{8,104},{16,112},{24,120},{32,0},{40,8},{48,16},{56,24},{64... | collective-permute-start | bytes 417800 | tf_op jit(solution)/shard_map/ppermute | solution.py:370
  12.9 2.4 %collective-permute-done.yleft = bf16[1056,128]{1,0:T(8,128)(2,1)S(1)} collective-permute-done((bf16[1056,128]{1,0:T(8,128)(2,1)}, bf16[1056,128]{1,0:T(8,128)(2,1)S(1)}, u32[]{:S(2)}, u32[]{:S(2)}) %collective-permute-start) | collective-permute-done | bytes 270368 | tf_op jit(solution)/shard_map/ppermute | solution.py:370
  15.4 3.9 %collective-permute-start.6 = (bf16[544,128]{1,0:T(8,128)(2,1)}, bf16[544,128]{1,0:T(8,128)(2,1)S(1)}, u32[]{:S(2)}, u32[]{:S(2)}) collective-permute-start(bf16[544,128]{1,0:T(8,128)(2,1)} %get-tuple-element.40), channel_id=1, source_target_pairs={{0,64},{8,72},{16,80},{24,88},{32,96},{40,104},{48,112},{56,120},{... | collective-permute-start | bytes 417800 | tf_op jit(solution)/shard_map/ppermute | solution.py:370
  19.3 0.4 collective-permute-start.2
  19.6 0.0 collective-permute-done.4.plus
  19.6 3.0 %collective-permute-start.3 = (bf16[528,128]{1,0:T(8,128)(2,1)S(1)}, bf16[528,128]{1,0:T(8,128)(2,1)S(1)}, u32[]{:S(2)}, u32[]{:S(2)}) collective-permute-start(bf16[528,128]{1,0:T(8,128)(2,1)S(1)} %slice.9), channel_id=1, source_target_pairs={{0,24},{8,0},{16,8},{24,16},{32,56},{40,32},{48,40},{56,48},{64,88... | collective-permute-start | bytes 405512 | tf_op jit(solution)/shard_map/ppermute | solution.py:370
  22.7 0.7 collective-permute-start.23
  23.4 2.8 %collective-permute-done.6.far = bf16[544,128]{1,0:T(8,128)(2,1)S(1)} collective-permute-done((bf16[544,128]{1,0:T(8,128)(2,1)}, bf16[544,128]{1,0:T(8,128)(2,1)S(1)}, u32[]{:S(2)}, u32[]{:S(2)}) %collective-permute-start.6) | collective-permute-done | bytes 139296 | tf_op jit(solution)/shard_map/ppermute | solution.py:370
  26.2 0.1 collective-permute-start.24
  26.3 0.9 %copy-done.3 = bf16[1056,128]{1,0:T(8,128)(2,1)S(1)} copy-done((bf16[1056,128]{1,0:T(8,128)(2,1)S(1)}, bf16[1056,128]{1,0:T(8,128)(2,1)}, u32[]{:S(2)}) %copy-start.3) | copy-done | bytes 270360
  27.3 1.0 %copy-done.4 = bf16[1056,128]{1,0:T(8,128)(2,1)S(1)} copy-done((bf16[1056,128]{1,0:T(8,128)(2,1)S(1)}, bf16[1056,128]{1,0:T(8,128)(2,1)}, u32[]{:S(2)}) %copy-start.4) | copy-done | bytes 270360
  28.2 12.1 %shard_map.121 = (bf16[256,128]{1,0:T(8,128)(2,1)S(1)}, bf16[256,128]{1,0:T(8,128)(2,1)S(1)}, bf16[256,128]{1,0:T(8,128)(2,1)S(1)}, bf16[256,128]{1,0:T(8,128)(2...) custom-call(s32[3]{0:T(128)S(1)} %copy-done.1, ...), custom_call_target="tpu_custom_call" | custom-call | flops 1426063360 | bytes 1000000 | tf_op jit(solution)/shard_map/pallas_call | solution.py:450
  40.3 1.2 %collective-permute-start.10 = (bf16[256,128]{1,0:T(8,128)(2,1)S(1)}, bf16[256,128]{1,0:T(8,128)(2,1)S(1)}, u32[]{:S(2)}, u32[]{:S(2)}) collective-permute-start(bf16[256,128]{1,0:T(8,128)(2,1)S(1)} %get-tuple-element.45), channel_id=1, source_target_pairs={{0,96},{8,104},{16,112},{24,120},{32,0},{40,8},{48,16},{56,24},{64... | collective-permute-start | bytes 196616 | tf_op jit(solution)/shard_map/ppermute | solution.py:370
  41.5 0.9 %collective-permute-start.11 = (bf16[256,128]{1,0:T(8,128)(2,1)S(1)}, bf16[256,128]{1,0:T(8,128)(2,1)S(1)}, u32[]{:S(2)}, u32[]{:S(2)}) collective-permute-start(bf16[256,128]{1,0:T(8,128)(2,1)S(1)} %get-tuple-element.46), channel_id=1, source_target_pairs={{0,32},{8,40},{16,48},{24,56},{32,64},{40,72},{48,80},{56,88},{64,... | collective-permute-start | bytes 196616 | tf_op jit(solution)/shard_map/ppermute | solution.py:370
  42.4 3.5 %collective-permute-start.12 = (bf16[256,128]{1,0:T(8,128)(2,1)S(1)}, bf16[256,128]{1,0:T(8,128)(2,1)S(1)}, u32[]{:S(2)}, u32[]{:S(2)}) collective-permute-start(bf16[256,128]{1,0:T(8,128)(2,1)S(1)} %get-tuple-element.47), channel_id=1, source_target_pairs={{0,64},{8,72},{16,80},{24,88},{32,96},{40,104},{48,112},{56,120},{... | collective-permute-start | bytes 196616 | tf_op jit(solution)/shard_map/ppermute | solution.py:370
  45.9 1.7 %collective-permute-start.7 = (bf16[256,128]{1,0:T(8,128)(2,1)S(1)}, bf16[256,128]{1,0:T(8,128)(2,1)S(1)}, u32[]{:S(2)}, u32[]{:S(2)}) collective-permute-start(bf16[256,128]{1,0:T(8,128)(2,1)S(1)} %get-tuple-element.42), channel_id=1, source_target_pairs={{0,24},{8,0},{16,8},{24,16},{32,56},{40,32},{48,40},{56,48},{64,88... | collective-permute-start | bytes 196616 | tf_op jit(solution)/shard_map/ppermute | solution.py:370
  47.6 1.8 %collective-permute-done.12.z3.a3 = bf16[256,128]{1,0:T(8,128)(2,1)S(1)} collective-permute-done((bf16[256,128]{1,0:T(8,128)(2,1)S(1)}, bf16[256,128]{1,0:T(8,128)(2,1)S(1)}, u32[]{:S(2)}, u32[]{:S(2)}) %collective-permute-start.12) | collective-permute-done | bytes 65568 | tf_op jit(solution)/shard_map/ppermute | solution.py:370
  49.4 0.2 collective-permute-start.8
  49.6 0.5 collective-permute-done.7.y1
  50.2 2.4 %collective-permute-start.9 = (bf16[256,128]{1,0:T(8,128)(2,1)S(1)}, bf16[256,128]{1,0:T(8,128)(2,1)S(1)}, u32[]{:S(2)}, u32[]{:S(2)}) collective-permute-start(bf16[256,128]{1,0:T(8,128)(2,1)S(1)} %get-tuple-element.44), channel_id=1, source_target_pairs={{0,16},{8,24},{16,0},{24,8},{32,48},{40,56},{48,32},{56,40},{64,80... | collective-permute-start | bytes 196616 | tf_op jit(solution)/shard_map/ppermute | solution.py:370
  52.6 2.4 %collective-permute-done.8.y2 = bf16[256,128]{1,0:T(8,128)(2,1)S(1)} collective-permute-done((bf16[256,128]{1,0:T(8,128)(2,1)S(1)}, bf16[256,128]{1,0:T(8,128)(2,1)S(1)}, u32[]{:S(2)}, u32[]{:S(2)}) %collective-permute-start.8) | collective-permute-done | bytes 65568 | tf_op jit(solution)/shard_map/ppermute | solution.py:370
  55.0 1.6 %collective-permute-start.16 = (bf16[256,128]{1,0:T(8,128)(2,1)S(1)}, bf16[256,128]{1,0:T(8,128)(2,1)S(1)}, u32[]{:S(2)}, u32[]{:S(2)}) collective-permute-start(bf16[256,128]{1,0:T(8,128)(2,1)S(1)} %get-tuple-element.54), channel_id=1, source_target_pairs={{0,96},{8,104},{16,112},{24,120},{32,0},{40,8},{48,16},{56,24},{64... | collective-permute-start | bytes 196616 | tf_op jit(solution)/shard_map/ppermute | solution.py:370
  56.6 1.5 %shard_map.122 = (bf16[256,256]{1,0:T(8,128)(2,1)S(1)}, bf16[512,128]{1,0:T(8,128)(2,1)}) custom-call(s32[3]{0:T(128)S(1)} %copy-done.1, f32[2,128,256]{2,1,0:T(8,128)S(1)} %get-tuple-element.41.own_q, bf16[256,128]{1,0:T(8,128)(2,1)S(1)} %collective-permute-done.7.y1, bf16[256,128]{1,0:T(8,128)(2,1)S(1)} %collective-permute-done.8.y2, ...), custom_call_target="tpu_custom_call" | custom-call | flops 10000000 | bytes 1000000 | tf_op jit(solution)/shard_map/pallas_call | solution.py:484
  58.1 0.4 collective-permute-start.19
  58.5 1.4 %collective-permute-done.16.b1 = bf16[256,128]{1,0:T(8,128)(2,1)S(1)} collective-permute-done((bf16[256,128]{1,0:T(8,128)(2,1)S(1)}, bf16[256,128]{1,0:T(8,128)(2,1)S(1)}, u32[]{:S(2)}, u32[]{:S(2)}) %collective-permute-start.16) | collective-permute-done | bytes 65568 | tf_op jit(solution)/shard_map/ppermute | solution.py:370
  59.9 2.2 %collective-permute-start.20 = (bf16[256,256]{1,0:T(8,128)(2,1)S(1)}, bf16[256,256]{1,0:T(8,128)(2,1)S(1)}, u32[]{:S(2)}, u32[]{:S(2)}) collective-permute-start(bf16[256,256]{1,0:T(8,128)(2,1)S(1)} %get-tuple-element.59.g0), channel_id=1, source_target_pairs={{0,96},{8,104},{16,112},{24,120},{32,0},{40,8},{48,16},{56,24},{64... | collective-permute-start | bytes 393224 | tf_op jit(solution)/shard_map/ppermute | solution.py:370
  62.1 2.6 %collective-permute-start.13 = (bf16[512,128]{1,0:T(8,128)(2,1)S(1)}, bf16[512,128]{1,0:T(8,128)(2,1)S(1)}, u32[]{:S(2)}, u32[]{:S(2)}) collective-permute-start(bf16[512,128]{1,0:T(8,128)(2,1)S(1)} %get-tuple-element.51), channel_id=1, source_target_pairs={{0,24},{8,0},{16,8},{24,16},{32,56},{40,32},{48,40},{56,48},{64,88... | collective-permute-start | bytes 393224 | tf_op jit(solution)/shard_map/ppermute | solution.py:370
  64.7 0.1 collective-permute-start.17
  64.8 1.8 %collective-permute-done.19.g1 = bf16[256,256]{1,0:T(8,128)(2,1)S(1)} collective-permute-done((bf16[256,256]{1,0:T(8,128)(2,1)S(1)}, bf16[256,256]{1,0:T(8,128)(2,1)S(1)}, u32[]{:S(2)}, u32[]{:S(2)}) %collective-permute-start.19) | collective-permute-done | bytes 131104 | tf_op jit(solution)/shard_map/ppermute | solution.py:370
  66.7 0.7 collective-permute-start.18
  67.3 0.7 collective-permute-start.14
  68.1 0.5 collective-permute-done.21.g3
  68.6 2.5 %collective-permute-start.15 = (bf16[512,128]{1,0:T(8,128)(2,1)S(1)}, bf16[512,128]{1,0:T(8,128)(2,1)S(1)}, u32[]{:S(2)}, u32[]{:S(2)}) collective-permute-start(bf16[512,128]{1,0:T(8,128)(2,1)S(1)} %get-tuple-element.53), channel_id=1, source_target_pairs={{0,16},{8,24},{16,0},{24,8},{32,48},{40,56},{48,32},{56,40},{64,80... | collective-permute-start | bytes 393224 | tf_op jit(solution)/shard_map/ppermute | solution.py:370
  71.0 1.4 %shard_map.124 = (f32[256,256]{1,0:T(8,128)S(1)}, bf16[256,256]{1,0:T(8,128)(2,1)S(1)}, bf16[256,256]{1,0:T(8,128)(2,1)S(1)}, bf16[256,256]{1,0:T(8,128)(2,1)S(1)}) custom-call(s32[3]{0:T(128)S(1)} %copy-done.1, bf16[256,256]{1,0:T(8,128)(2,1)S(1)} %get-tuple-element.59.g0, bf16[256,256]{1,0:T(8,128)(2,1)S(1)} %collective-permute-done.19.g1, ...), custom_call_target="tpu_custom_call" | custom-call | flops 536870912 | bytes 1000000 | tf_op jit(solution)/shard_map/pallas_call | solution.py:508
  72.5 0.5 collective-permute-start.28
  73.0 2.8 %collective-permute-start.29 = (bf16[256,256]{1,0:T(8,128)(2,1)S(1)}, bf16[256,256]{1,0:T(8,128)(2,1)S(1)}, u32[]{:S(2)}, u32[]{:S(2)}) collective-permute-start(bf16[256,256]{1,0:T(8,128)(2,1)S(1)} %get-tuple-element.66), channel_id=1, source_target_pairs={{0,24},{8,0},{16,8},{24,16},{32,56},{40,32},{48,40},{56,48},{64,88... | collective-permute-start | bytes 393224 | tf_op jit(solution)/shard_map/ppermute | solution.py:370
  75.8 1.6 %collective-permute-done.14.y2 = bf16[512,128]{1,0:T(8,128)(2,1)S(1)} collective-permute-done((bf16[512,128]{1,0:T(8,128)(2,1)S(1)}, bf16[512,128]{1,0:T(8,128)(2,1)S(1)}, u32[]{:S(2)}, u32[]{:S(2)}) %collective-permute-start.14) | collective-permute-done | bytes 131104 | tf_op jit(solution)/shard_map/ppermute | solution.py:370
  77.4 1.6 %shard_map.123 = (bf16[512,128]{1,0:T(8,128)(2,1)}, bf16[512,128]{1,0:T(8,128)(2,1)}) custom-call(s32[3]{0:T(128)S(1)} %copy-done.1, f32[2,256,128]{2,1,0:T(8,128)S(1)} %get-tuple-element.49.own_k, f32[2,256,128]{2,1,0:T(8,128)S(1)} %get-tuple-element.50.own_v, bf16[512,128]{1,0:T(8,128)(2,1)S(1)} %collective-permute-done.13.y1, ...), custom_call_target="tpu_custom_call" | custom-call | flops 10000000 | bytes 1000000 | tf_op jit(solution)/shard_map/pallas_call | solution.py:498
  79.1 0.1 collective-permute-done.28.t1
  79.1 0.6 collective-permute-done.29.t2
  79.7 2.6 %collective-permute-done.30.t3 = bf16[256,256]{1,0:T(8,128)(2,1)S(1)} collective-permute-done((bf16[256,256]{1,0:T(8,128)(2,1)S(1)}, bf16[256,256]{1,0:T(8,128)(2,1)S(1)}, u32[]{:S(2)}, u32[]{:S(2)}) %collective-permute-start.30) | collective-permute-done | bytes 131104 | tf_op jit(solution)/shard_map/ppermute | solution.py:370
  82.3 0.8 %shard_map.125 = f32[256,256]{1,0:T(8,128)} custom-call(f32[256,256]{1,0:T(8,128)S(1)} %get-tuple-element.64.own, bf16[256,256]{1,0:T(8,128)(2,1)S(1)} %collective-permute-done.28.t1, bf16[256,256]{1,0:T(8,128)(2,1)S(1)} %collective-permute-done.29.t2, bf16[256,256]{1,0:T(8,128)(2,1)S(1)} %collective-permute-done.30.t3), custom_call_target="tpu_custom_call" | custom-call | flops 1000000 | bytes 1000000 | tf_op jit(solution)/shard_map/pallas_call | solution.py:517
  (33 shorter events, 0.1 us)
Async XLA Ops:
  0.6 25.7 %copy-start.2 = (f32[2]{0:T(128)S(1)}, f32[2]{0:T(128)}, u32[]{:S(2)}) copy-start(f32[2]{0:T(128)} %lam.3) | copy-start | bytes 28
  1.3 25.0 %copy-start.1 = (s32[3]{0:T(128)S(1)}, s32[3]{0:T(128)}, u32[]{:S(2)}) copy-start(s32[3]{0:T(128)} %pad_add_fusion.place) | copy-start | bytes 40
  5.5 9.9 %collective-permute-start = (bf16[1056,128]{1,0:T(8,128)(2,1)}, bf16[1056,128]{1,0:T(8,128)(2,1)S(1)}, u32[]{:S(2)}, u32[]{:S(2)}) collective-permute-start(bf16[1056,128]{1,0:T(8,128)(2,1)} %get-tuple-element.36.yown), channel_id=1, source_target_pairs={{0,8},{8,16},{16,24},{24,0},{32,40},{40,48},{48,56},{56,32},{64,72... | collective-permute-start | bytes 811016 | tf_op jit(solution)/shard_map/ppermute | solution.py:370
  7.2 12.0 %collective-permute-start.1 = (bf16[1056,128]{1,0:T(8,128)(2,1)}, bf16[1056,128]{1,0:T(8,128)(2,1)S(1)}, u32[]{:S(2)}, u32[]{:S(2)}) collective-permute-start(bf16[1056,128]{1,0:T(8,128)(2,1)} %get-tuple-element.36.yown), channel_id=1, source_target_pairs={{0,24},{8,0},{16,8},{24,16},{32,56},{40,32},{48,40},{56,48},{64,88... | collective-permute-start | bytes 811016 | tf_op jit(solution)/shard_map/ppermute | solution.py:370
  8.8 10.9 %collective-permute-start.4 = (bf16[544,128]{1,0:T(8,128)(2,1)}, bf16[544,128]{1,0:T(8,128)(2,1)S(1)}, u32[]{:S(2)}, u32[]{:S(2)}) collective-permute-start(bf16[544,128]{1,0:T(8,128)(2,1)} %get-tuple-element.38), channel_id=1, source_target_pairs={{0,32},{8,40},{16,48},{24,56},{32,64},{40,72},{48,80},{56,88},{64,... | collective-permute-start | bytes 417800 | tf_op jit(solution)/shard_map/ppermute | solution.py:370
  10.8 11.9 %collective-permute-start.5 = (bf16[544,128]{1,0:T(8,128)(2,1)}, bf16[544,128]{1,0:T(8,128)(2,1)S(1)}, u32[]{:S(2)}, u32[]{:S(2)}) collective-permute-start(bf16[544,128]{1,0:T(8,128)(2,1)} %get-tuple-element.39), channel_id=1, source_target_pairs={{0,96},{8,104},{16,112},{24,120},{32,0},{40,8},{48,16},{56,24},{64... | collective-permute-start | bytes 417800 | tf_op jit(solution)/shard_map/ppermute | solution.py:370
  12.9 13.4 %collective-permute-start.22 = (bf16[128,1024]{1,0:T(8,128)(2,1)}, bf16[128,1024]{1,0:T(8,128)(2,1)S(1)}, u32[]{:S(2)}, u32[]{:S(2)}) collective-permute-start(bf16[128,1024]{1,0:T(8,128)(2,1)} %get-tuple-element.61), channel_id=1, source_target_pairs={{0,32},{8,40},{16,48},{24,56},{32,64},{40,72},{48,80},{56,88},{64,... | collective-permute-start | bytes 786440 | tf_op jit(solution)/shard_map/ppermute | solution.py:370
  15.4 10.8 %collective-permute-start.6 = (bf16[544,128]{1,0:T(8,128)(2,1)}, bf16[544,128]{1,0:T(8,128)(2,1)S(1)}, u32[]{:S(2)}, u32[]{:S(2)}) collective-permute-start(bf16[544,128]{1,0:T(8,128)(2,1)} %get-tuple-element.40), channel_id=1, source_target_pairs={{0,64},{8,72},{16,80},{24,88},{32,96},{40,104},{48,112},{56,120},{... | collective-permute-start | bytes 417800 | tf_op jit(solution)/shard_map/ppermute | solution.py:370
  19.3 7.0 %collective-permute-start.2 = (bf16[528,128]{1,0:T(8,128)(2,1)S(1)}, bf16[528,128]{1,0:T(8,128)(2,1)S(1)}, u32[]{:S(2)}, u32[]{:S(2)}) collective-permute-start(bf16[528,128]{1,0:T(8,128)(2,1)S(1)} %slice.8), channel_id=1, source_target_pairs={{0,8},{8,16},{16,24},{24,0},{32,40},{40,48},{48,56},{56,32},{64,72... | collective-permute-start | bytes 405512 | tf_op jit(solution)/shard_map/ppermute | solution.py:370
  19.6 6.6 %collective-permute-start.3 = (bf16[528,128]{1,0:T(8,128)(2,1)S(1)}, bf16[528,128]{1,0:T(8,128)(2,1)S(1)}, u32[]{:S(2)}, u32[]{:S(2)}) collective-permute-start(bf16[528,128]{1,0:T(8,128)(2,1)S(1)} %slice.9), channel_id=1, source_target_pairs={{0,24},{8,0},{16,8},{24,16},{32,56},{40,32},{48,40},{56,48},{64,88... | collective-permute-start | bytes 405512 | tf_op jit(solution)/shard_map/ppermute | solution.py:370
  22.7 19.8 %collective-permute-start.23 = (bf16[128,1024]{1,0:T(8,128)(2,1)}, bf16[128,1024]{1,0:T(8,128)(2,1)S(1)}, u32[]{:S(2)}, u32[]{:S(2)}) collective-permute-start(bf16[128,1024]{1,0:T(8,128)(2,1)} %get-tuple-element.62), channel_id=1, source_target_pairs={{0,96},{8,104},{16,112},{24,120},{32,0},{40,8},{48,16},{56,24},{64... | collective-permute-start | bytes 786440 | tf_op jit(solution)/shard_map/ppermute | solution.py:370
  26.2 16.3 %collective-permute-start.24 = (bf16[128,1024]{1,0:T(8,128)(2,1)}, bf16[128,1024]{1,0:T(8,128)(2,1)S(1)}, u32[]{:S(2)}, u32[]{:S(2)}) collective-permute-start(bf16[128,1024]{1,0:T(8,128)(2,1)} %get-tuple-element.63), channel_id=1, source_target_pairs={{0,64},{8,72},{16,80},{24,88},{32,96},{40,104},{48,112},{56,120},{... | collective-permute-start | bytes 786440 | tf_op jit(solution)/shard_map/ppermute | solution.py:370
  26.3 35.8 %collective-permute-start.25 = (bf16[128,1024]{1,0:T(8,128)(2,1)S(1)}, bf16[128,1024]{1,0:T(8,128)(2,1)S(1)}, u32[]{:S(2)}, u32[]{:S(2)}) collective-permute-start(bf16[128,1024]{1,0:T(8,128)(2,1)S(1)} %collective-permute-done.22.m1), channel_id=1, source_target_pairs={{0,1},{1,0},{2,3},{3,2},{4,5},{5,4},{6,7},{7,6},{8,9},{9,8},{10,11... | collective-permute-start | bytes 786440 | tf_op jit(solution)/shard_map/ppermute | solution.py:374
  26.3 1.0 %copy-start.3 = (bf16[1056,128]{1,0:T(8,128)(2,1)S(1)}, bf16[1056,128]{1,0:T(8,128)(2,1)}, u32[]{:S(2)}) copy-start(bf16[1056,128]{1,0:T(8,128)(2,1)} %get-tuple-element.36.yown) | copy-start | bytes 811012
  27.3 1.0 %copy-start.4 = (bf16[1056,128]{1,0:T(8,128)(2,1)S(1)}, bf16[1056,128]{1,0:T(8,128)(2,1)}, u32[]{:S(2)}) copy-start(bf16[1056,128]{1,0:T(8,128)(2,1)} %get-tuple-element.37.zown) | copy-start | bytes 811012
  28.2 42.8 %copy-start = (bf16[256,1024]{1,0:T(8,128)(2,1)S(1)}, bf16[256,1024]{1,0:T(8,128)(2,1)}, u32[]{:S(2)}) copy-start(bf16[256,1024]{1,0:T(8,128)(2,1)} %get-tuple-element.60.lat0) | copy-start | bytes 1572868
  40.3 5.6 %collective-permute-start.10 = (bf16[256,128]{1,0:T(8,128)(2,1)S(1)}, bf16[256,128]{1,0:T(8,128)(2,1)S(1)}, u32[]{:S(2)}, u32[]{:S(2)}) collective-permute-start(bf16[256,128]{1,0:T(8,128)(2,1)S(1)} %get-tuple-element.45), channel_id=1, source_target_pairs={{0,96},{8,104},{16,112},{24,120},{32,0},{40,8},{48,16},{56,24},{64... | collective-permute-start | bytes 196616 | tf_op jit(solution)/shard_map/ppermute | solution.py:370
  41.5 6.1 %collective-permute-start.11 = (bf16[256,128]{1,0:T(8,128)(2,1)S(1)}, bf16[256,128]{1,0:T(8,128)(2,1)S(1)}, u32[]{:S(2)}, u32[]{:S(2)}) collective-permute-start(bf16[256,128]{1,0:T(8,128)(2,1)S(1)} %get-tuple-element.46), channel_id=1, source_target_pairs={{0,32},{8,40},{16,48},{24,56},{32,64},{40,72},{48,80},{56,88},{64,... | collective-permute-start | bytes 196616 | tf_op jit(solution)/shard_map/ppermute | solution.py:370
  42.4 19.7 %collective-permute-start.26 = (bf16[128,1024]{1,0:T(8,128)(2,1)S(1)}, bf16[128,1024]{1,0:T(8,128)(2,1)S(1)}, u32[]{:S(2)}, u32[]{:S(2)}) collective-permute-start(bf16[128,1024]{1,0:T(8,128)(2,1)S(1)} %collective-permute-done.23.m2), channel_id=1, source_target_pairs={{0,1},{1,0},{2,3},{3,2},{4,5},{5,4},{6,7},{7,6},{8,9},{9,8},{10,11... | collective-permute-start | bytes 786440 | tf_op jit(solution)/shard_map/ppermute | solution.py:374
  42.4 7.0 %collective-permute-start.12 = (bf16[256,128]{1,0:T(8,128)(2,1)S(1)}, bf16[256,128]{1,0:T(8,128)(2,1)S(1)}, u32[]{:S(2)}, u32[]{:S(2)}) collective-permute-start(bf16[256,128]{1,0:T(8,128)(2,1)S(1)} %get-tuple-element.47), channel_id=1, source_target_pairs={{0,64},{8,72},{16,80},{24,88},{32,96},{40,104},{48,112},{56,120},{... | collective-permute-start | bytes 196616 | tf_op jit(solution)/shard_map/ppermute | solution.py:370
  45.9 4.3 %collective-permute-start.7 = (bf16[256,128]{1,0:T(8,128)(2,1)S(1)}, bf16[256,128]{1,0:T(8,128)(2,1)S(1)}, u32[]{:S(2)}, u32[]{:S(2)}) collective-permute-start(bf16[256,128]{1,0:T(8,128)(2,1)S(1)} %get-tuple-element.42), channel_id=1, source_target_pairs={{0,24},{8,0},{16,8},{24,16},{32,56},{40,32},{48,40},{56,48},{64,88... | collective-permute-start | bytes 196616 | tf_op jit(solution)/shard_map/ppermute | solution.py:370
  47.6 17.1 %collective-permute-start.27 = (bf16[128,1024]{1,0:T(8,128)(2,1)S(1)}, bf16[128,1024]{1,0:T(8,128)(2,1)S(1)}, u32[]{:S(2)}, u32[]{:S(2)}) collective-permute-start(bf16[128,1024]{1,0:T(8,128)(2,1)S(1)} %collective-permute-done.24.m3), channel_id=1, source_target_pairs={{0,1},{1,0},{2,3},{3,2},{4,5},{5,4},{6,7},{7,6},{8,9},{9,8},{10,11... | collective-permute-start | bytes 786440 | tf_op jit(solution)/shard_map/ppermute | solution.py:374
  49.4 5.6 %collective-permute-start.8 = (bf16[256,128]{1,0:T(8,128)(2,1)S(1)}, bf16[256,128]{1,0:T(8,128)(2,1)S(1)}, u32[]{:S(2)}, u32[]{:S(2)}) collective-permute-start(bf16[256,128]{1,0:T(8,128)(2,1)S(1)} %get-tuple-element.43), channel_id=1, source_target_pairs={{0,8},{8,16},{16,24},{24,0},{32,40},{40,48},{48,56},{56,32},{64,72... | collective-permute-start | bytes 196616 | tf_op jit(solution)/shard_map/ppermute | solution.py:370
  50.2 6.4 %collective-permute-start.9 = (bf16[256,128]{1,0:T(8,128)(2,1)S(1)}, bf16[256,128]{1,0:T(8,128)(2,1)S(1)}, u32[]{:S(2)}, u32[]{:S(2)}) collective-permute-start(bf16[256,128]{1,0:T(8,128)(2,1)S(1)} %get-tuple-element.44), channel_id=1, source_target_pairs={{0,16},{8,24},{16,0},{24,8},{32,48},{40,56},{48,32},{56,40},{64,80... | collective-permute-start | bytes 196616 | tf_op jit(solution)/shard_map/ppermute | solution.py:370
  55.0 4.9 %collective-permute-start.16 = (bf16[256,128]{1,0:T(8,128)(2,1)S(1)}, bf16[256,128]{1,0:T(8,128)(2,1)S(1)}, u32[]{:S(2)}, u32[]{:S(2)}) collective-permute-start(bf16[256,128]{1,0:T(8,128)(2,1)S(1)} %get-tuple-element.54), channel_id=1, source_target_pairs={{0,96},{8,104},{16,112},{24,120},{32,0},{40,8},{48,16},{56,24},{64... | collective-permute-start | bytes 196616 | tf_op jit(solution)/shard_map/ppermute | solution.py:370
  58.1 8.6 %collective-permute-start.19 = (bf16[256,256]{1,0:T(8,128)(2,1)S(1)}, bf16[256,256]{1,0:T(8,128)(2,1)S(1)}, u32[]{:S(2)}, u32[]{:S(2)}) collective-permute-start(bf16[256,256]{1,0:T(8,128)(2,1)S(1)} %get-tuple-element.59.g0), channel_id=1, source_target_pairs={{0,32},{8,40},{16,48},{24,56},{32,64},{40,72},{48,80},{56,88},{64,... | collective-permute-start | bytes 393224 | tf_op jit(solution)/shard_map/ppermute | solution.py:370
  59.9 7.5 %collective-permute-start.20 = (bf16[256,256]{1,0:T(8,128)(2,1)S(1)}, bf16[256,256]{1,0:T(8,128)(2,1)S(1)}, u32[]{:S(2)}, u32[]{:S(2)}) collective-permute-start(bf16[256,256]{1,0:T(8,128)(2,1)S(1)} %get-tuple-element.59.g0), channel_id=1, source_target_pairs={{0,96},{8,104},{16,112},{24,120},{32,0},{40,8},{48,16},{56,24},{64... | collective-permute-start | bytes 393224 | tf_op jit(solution)/shard_map/ppermute | solution.py:370
  62.1 6.5 %collective-permute-start.21 = (bf16[256,256]{1,0:T(8,128)(2,1)S(1)}, bf16[256,256]{1,0:T(8,128)(2,1)S(1)}, u32[]{:S(2)}, u32[]{:S(2)}) collective-permute-start(bf16[256,256]{1,0:T(8,128)(2,1)S(1)} %get-tuple-element.59.g0), channel_id=1, source_target_pairs={{0,64},{8,72},{16,80},{24,88},{32,96},{40,104},{48,112},{56,120},{... | collective-permute-start | bytes 393224 | tf_op jit(solution)/shard_map/ppermute | solution.py:370
  62.1 13.7 %collective-permute-start.13 = (bf16[512,128]{1,0:T(8,128)(2,1)S(1)}, bf16[512,128]{1,0:T(8,128)(2,1)S(1)}, u32[]{:S(2)}, u32[]{:S(2)}) collective-permute-start(bf16[512,128]{1,0:T(8,128)(2,1)S(1)} %get-tuple-element.51), channel_id=1, source_target_pairs={{0,24},{8,0},{16,8},{24,16},{32,56},{40,32},{48,40},{56,48},{64,88... | collective-permute-start | bytes 393224 | tf_op jit(solution)/shard_map/ppermute | solution.py:370
  64.7 7.8 %collective-permute-start.17 = (bf16[256,128]{1,0:T(8,128)(2,1)S(1)}, bf16[256,128]{1,0:T(8,128)(2,1)S(1)}, u32[]{:S(2)}, u32[]{:S(2)}) collective-permute-start(bf16[256,128]{1,0:T(8,128)(2,1)S(1)} %get-tuple-element.55), channel_id=1, source_target_pairs={{0,32},{8,40},{16,48},{24,56},{32,64},{40,72},{48,80},{56,88},{64,... | collective-permute-start | bytes 196616 | tf_op jit(solution)/shard_map/ppermute | solution.py:370
  66.7 6.4 %collective-permute-start.18 = (bf16[256,128]{1,0:T(8,128)(2,1)S(1)}, bf16[256,128]{1,0:T(8,128)(2,1)S(1)}, u32[]{:S(2)}, u32[]{:S(2)}) collective-permute-start(bf16[256,128]{1,0:T(8,128)(2,1)S(1)} %get-tuple-element.56), channel_id=1, source_target_pairs={{0,64},{8,72},{16,80},{24,88},{32,96},{40,104},{48,112},{56,120},{... | collective-permute-start | bytes 196616 | tf_op jit(solution)/shard_map/ppermute | solution.py:370
  67.3 10.1 %collective-permute-start.14 = (bf16[512,128]{1,0:T(8,128)(2,1)S(1)}, bf16[512,128]{1,0:T(8,128)(2,1)S(1)}, u32[]{:S(2)}, u32[]{:S(2)}) collective-permute-start(bf16[512,128]{1,0:T(8,128)(2,1)S(1)} %get-tuple-element.52), channel_id=1, source_target_pairs={{0,8},{8,16},{16,24},{24,0},{32,40},{40,48},{48,56},{56,32},{64,72... | collective-permute-start | bytes 393224 | tf_op jit(solution)/shard_map/ppermute | solution.py:370
  68.6 8.9 %collective-permute-start.15 = (bf16[512,128]{1,0:T(8,128)(2,1)S(1)}, bf16[512,128]{1,0:T(8,128)(2,1)S(1)}, u32[]{:S(2)}, u32[]{:S(2)}) collective-permute-start(bf16[512,128]{1,0:T(8,128)(2,1)S(1)} %get-tuple-element.53), channel_id=1, source_target_pairs={{0,16},{8,24},{16,0},{24,8},{32,48},{40,56},{48,32},{56,40},{64,80... | collective-permute-start | bytes 393224 | tf_op jit(solution)/shard_map/ppermute | solution.py:370
  72.5 6.6 %collective-permute-start.28 = (bf16[256,256]{1,0:T(8,128)(2,1)S(1)}, bf16[256,256]{1,0:T(8,128)(2,1)S(1)}, u32[]{:S(2)}, u32[]{:S(2)}) collective-permute-start(bf16[256,256]{1,0:T(8,128)(2,1)S(1)} %get-tuple-element.65), channel_id=1, source_target_pairs={{0,8},{8,16},{16,24},{24,0},{32,40},{40,48},{48,56},{56,32},{64,72... | collective-permute-start | bytes 393224 | tf_op jit(solution)/shard_map/ppermute | solution.py:370
  73.0 6.7 %collective-permute-start.29 = (bf16[256,256]{1,0:T(8,128)(2,1)S(1)}, bf16[256,256]{1,0:T(8,128)(2,1)S(1)}, u32[]{:S(2)}, u32[]{:S(2)}) collective-permute-start(bf16[256,256]{1,0:T(8,128)(2,1)S(1)} %get-tuple-element.66), channel_id=1, source_target_pairs={{0,24},{8,0},{16,8},{24,16},{32,56},{40,32},{48,40},{56,48},{64,88... | collective-permute-start | bytes 393224 | tf_op jit(solution)/shard_map/ppermute | solution.py:370
  75.8 6.5 %collective-permute-start.30 = (bf16[256,256]{1,0:T(8,128)(2,1)S(1)}, bf16[256,256]{1,0:T(8,128)(2,1)S(1)}, u32[]{:S(2)}, u32[]{:S(2)}) collective-permute-start(bf16[256,256]{1,0:T(8,128)(2,1)S(1)} %get-tuple-element.67), channel_id=1, source_target_pairs={{0,16},{8,24},{16,0},{24,8},{32,48},{40,56},{48,32},{56,40},{64,80... | collective-permute-start | bytes 393224 | tf_op jit(solution)/shard_map/ppermute | solution.py:370
where the time goes:
time: 83.3 us; the launch traced here: 83.1 us
  starting transfers between devices  39.6 us (48%)
  Pallas kernels  21.6 us (26%)
  waiting for transfers between devices  18.6 us (22%)
  local copies, waits for them, and re-layouts  1.93 us (2%)
    ppermute x28, starting transfers between devices, moved(): return lax.ppermute(x, 'sp', pairs)  39.6 us
    ppermute x28, waiting for transfers between devices, moved(): return lax.ppermute(x, 'sp', pairs)  18.6 us
    pallas_call x1, Pallas kernels, body(): call(attend_kernel, (small,) * 6 + (both,) * 3 + (small,) * 3 + (shape(2,...  12.1 us
    pallas_call x1, Pallas kernels, body(): call(prepare_kernel, (shape(SLOT, 128),) * 2 + (shape(QG, 128),) * 3 + (s...  4.14 us
    unnamed x10, local copies, waits for them, and re-layouts  1.91 us
  transfers between devices with their start and end apart: 31, of which 12 were waited for; matrix products, arithmetic and copies ran while one was open for 0% of the time, Pallas kernels for 20%

commit v1 on v0

--- a/solution.py
+++ b/solution.py
@@ -50,26 +50,22 @@
     return found
 
 
+def position():
+    index = lax.axis_index("sp")
+    return index // SIDE, lax.rem(index, SIDE), lax.rem(lax.axis_index("tp"), 2)
+
+
 def prepare_kernel(
-    place, lam, q_hbm, k_hbm, v_hbm, maps_hbm, lse_hbm, out_hbm, gain_hbm, lat_hbm,
-    yown, zown, plus, minus, far, lat_own, lat_plus, lat_minus, lat_far,
+    lam, q_hbm, k_hbm, v_hbm, maps_hbm, lse_hbm, out_hbm, gain_hbm,
+    yown, zown, plus, minus, far,
     q_in, k_in, v_in, maps_in, lse_in, out_in, gain_in, sems,
 ):
-    z = place[0]
-    core = place[2]
+    z, _, _ = position()
     pairs = [
         (maps_hbm, maps_in), (out_hbm, out_in), (gain_hbm, gain_in), (lse_hbm, lse_in),
         (q_hbm, q_in), (k_hbm, k_in), (v_hbm, v_in),
     ]
     copies = [pltpu.make_async_copy(a, b, sems.at[n]) for n, (a, b) in enumerate(pairs)]
-    tokens = pl.ds(pl.multiple_of(core * HALF, HALF), HALF)
-    for ref, step in ((lat_plus, 1), (lat_minus, SIDE - 1), (lat_far, 2)):
-        columns = pl.ds(pl.multiple_of((z + step) % SIDE * WIDE, WIDE), WIDE)
-        copies.append(
-            pltpu.make_async_copy(lat_hbm.at[tokens, columns], ref, sems.at[len(copies)])
-        )
-    columns = pl.ds(pl.multiple_of(z * WIDE, WIDE), WIDE)
-    copies.append(pltpu.make_async_copy(lat_hbm.at[:, columns], lat_own, sems.at[len(copies)]))
     for copy in copies:
         copy.start()
     row = iota((ROWS, ROWS), 0)
@@ -137,18 +133,34 @@
     send(plus, z < SIDE - 1)
     send(minus, z == 0)
     send(far, z < SIDE // 2)
-    for copy in copies[7:]:
+
+
+def fetch_kernel(lat_hbm, lat_own, lat_near, lat_far, sems):
+    z, _, core = position()
+
+    def columns(block):
+        return pl.ds(pl.multiple_of(lax.rem(block, SIDE) * WIDE, WIDE), WIDE)
+
+    tokens = pl.ds(pl.multiple_of(core * HALF, HALF), HALF)
+    near = jnp.where(core == 0, z + 1, z + SIDE - 1)
+    copies = (
+        pltpu.make_async_copy(lat_hbm.at[:, columns(near)], lat_near, sems.at[0]),
+        pltpu.make_async_copy(lat_hbm.at[tokens, columns(z + 2)], lat_far, sems.at[1]),
+        pltpu.make_async_copy(lat_hbm.at[:, columns(z)], lat_own, sems.at[2]),
+    )
+    for copy in copies:
+        copy.start()
+    for copy in copies:
         copy.wait()
 
 
 def attend_kernel(
-    place, lam, yown, yleft, yright, ytop, ybottom, zown, plus, minus, far,
-    q_left, q_right, q_far, q_plus, q_minus, q_zfar,
-    kv_left, kv_right, kv_far, v_plus, v_minus, v_zfar, own_q, own_k, own_v,
-    buf, stat, kpad, kturn, qpad, dq, dk, dv,
+    lam, yown, yleft, yright, ytop, ybottom, zown, plus, minus, far,
+    q_left, q_right, q_far, r_plus, r_minus, r_far,
+    kv_left, kv_right, kv_far, own_q, own_k, own_v,
+    buf, stat, kpad, kturn, qpad, dq, dk, dv, wide_w, tall_s,
 ):
-    z = place[0]
-    y = place[1]
+    z, y, _ = position()
     buf[0] = yown[...]
     buf[1] = yleft[...]
     buf[2] = yright[...]
@@ -196,9 +208,27 @@
 
     lax.fori_loop(0, 2 * SIDE, ready, 0)
 
-    def pair(zslot, yslot, kind, shift):
+    def slots_of(item):
+        own = item < SIDE + 1
+        rest = item - SIDE - 1
+        zslot = jnp.where(own, SIDE, SIDE + 1 + rest // SIDE)
+        yslot = jnp.where(own, jnp.maximum(item - 1, 0), lax.rem(jnp.maximum(rest, 0), SIDE))
+        offset = jnp.where(yslot == 1, SIDE - 1, jnp.where(yslot == 2, 1, yslot - 1))
+        behind = jnp.where(yslot == 0, item == 0, lax.rem(y + offset, SIDE) < y)
+        kind = jnp.where(
+            own,
+            1 - behind.astype(jnp.int32),
+            jnp.where(
+                zslot == SIDE + 1, keys_plus, jnp.where(zslot == SIDE + 2, keys_minus, keys_far)
+            ),
+        )
         qs = jnp.where(kind == 0, zslot, yslot)
         ks = jnp.where(kind == 0, yslot, zslot)
+        return qs, ks, kind
+
+    def front(item):
+        qs, ks, kind = slots_of(item)
+        shift = jnp.where(item < 2, 0, 2 * ROWS)
         factor = lam[kind]
         q = buf[qs, 0:ROWS]
         g = buf[qs, ROWS : 2 * ROWS]
@@ -216,55 +246,67 @@
         weights = (prob1 - prob2).astype(BF)
         score1 = (prob1 * (mixed - rows[2:3])).astype(BF)
         score2 = (prob2 * (rows[3:4] - mixed)).astype(BF)
-        dv[ks] += exact(weights, g)
-        dk[ks] += exact(jnp.concatenate([score1, score2], axis=1), qpad[qs])
-        dq[qs] += exact(kturn[ks], jnp.concatenate([score1, score2], axis=0))
+        return weights, score1, score2
+
+    def keep(values):
+        weights, score1, score2 = values
+        wide_w[...] = weights
+        tall_s[0:ROWS] = score1
+        tall_s[ROWS:] = score2
+
+    def back(item):
+        qs, ks, _ = slots_of(item)
+        weights = wide_w[...]
+        score1 = tall_s[0:ROWS]
+        score2 = tall_s[ROWS:]
+        g = buf[qs, ROWS : 2 * ROWS]
+        add_v = exact(weights, g)
+        add_k = exact(jnp.concatenate([score1, score2], axis=1), qpad[qs])
+        add_q = exact(kturn[ks], jnp.concatenate([score1, score2], axis=0))
+        return qs, ks, add_q, add_k, add_v
+
+    def add(sums):
+        qs, ks, add_q, add_k, add_v = sums
+        dv[ks] += add_v
+        dk[ks] += add_k
+        dq[qs] += add_q
+
+    items = SIDE * SIDE + 1
+    keep(front(0))
 
     def step(item, carry):
-        own = item < SIDE + 1
-        rest = item - SIDE - 1
-        zslot = jnp.where(own, SIDE, SIDE + 1 + rest // SIDE)
-        yslot = jnp.where(own, jnp.maximum(item - 1, 0), rest % SIDE)
-        offset = jnp.where(yslot == 1, SIDE - 1, jnp.where(yslot == 2, 1, yslot - 1))
-        behind = jnp.where(
-            yslot == 0, item == 0, (y + offset) % SIDE < y
-        )
-        kind = jnp.where(
-            own,
-            1 - behind.astype(jnp.int32),
-            jnp.where(
-                zslot == SIDE + 1, keys_plus, jnp.where(zslot == SIDE + 2, keys_minus, keys_far)
-            ),
-        )
-        shift = jnp.where(item < 2, 0, 2 * ROWS)
-        pair(zslot, yslot, kind, shift)
+        sums = back(item)
+        values = front(item + 1)
+        add(sums)
+        keep(values)
         return carry
 
-    lax.fori_loop(0, SIDE * SIDE + 1, step, 0)
+    lax.fori_loop(0, items - 1, step, 0)
+    add(back(items - 1))
 
     scale = DH ** (-0.5)
 
     def put_q(ref, slot):
         value = (dq[slot] * scale).astype(BF)
         ref[0:HALF] = value[:, 0:128]
-        ref[HALF:] = value[:, 128:]
+        ref[HALF:ROWS] = value[:, 128:]
 
     for slot, (ref, kv) in enumerate(((q_left, kv_left), (q_right, kv_right), (q_far, kv_far))):
         put_q(ref, slot + 1)
         kv[0:ROWS] = (dk[slot + 1] * scale).astype(BF)
         kv[ROWS:] = dv[slot + 1].astype(BF)
-    for slot, (ref, ref_v, keys) in enumerate(
-        ((q_plus, v_plus, keys_plus), (q_minus, v_minus, keys_minus), (q_zfar, v_zfar, keys_far))
+    for slot, (ref, keys) in enumerate(
+        ((r_plus, keys_plus), (r_minus, keys_minus), (r_far, keys_far))
     ):
         @pl.when(keys == 1)
         def _():
-            ref[...] = (dk[SIDE + 1 + slot] * scale).astype(BF)
+            ref[0:ROWS] = (dk[SIDE + 1 + slot] * scale).astype(BF)
+            ref[ROWS:] = dv[SIDE + 1 + slot].astype(BF)
 
         @pl.when(keys == 0)
         def _():
             put_q(ref, SIDE + 1 + slot)
-
-        ref_v[...] = dv[SIDE + 1 + slot].astype(BF)
+            ref[ROWS:] = jnp.zeros((ROWS, 128), BF)
 
     own_q[0] = dq[SIDE] * scale
     own_q[1] = dq[0] * scale
@@ -274,11 +316,11 @@
     own_v[1] = dv[SIDE]
 
 
-def queries_kernel(place, own_q, y1, y2, y3, z1, z2, z3, turned_out, rows_out, acc):
-    z = place[0]
+def queries_kernel(own_q, y1, y2, y3, z1, z2, z3, turned_out, acc):
+    z, _, _ = position()
 
     def lanes(ref):
-        return jnp.concatenate([ref[0:HALF].astype(F32), ref[HALF:].astype(F32)], axis=1)
+        return jnp.concatenate([ref[0:HALF].astype(F32), ref[HALF:ROWS].astype(F32)], axis=1)
 
     acc[...] = own_q[0]
     for ref, keys in ((z1, z < SIDE - 1), (z2, z == 0), (z3, z < SIDE // 2)):
@@ -286,32 +328,21 @@
         def _():
             acc[...] += lanes(ref)
 
-    first = acc[...].astype(BF)
-    second = (own_q[1] + lanes(y1) + lanes(y2) + lanes(y3)).astype(BF)
-    turned_out[0:128] = first
-    turned_out[128:256] = second
-    row = iota((ROWS, ROWS), 0)
-    col = iota((ROWS, ROWS), 1)
-    weave = one_hot(col == row % 2 * HALF + row // 2)
-    for half in range(2):
-        keep = slice(half * HALF, (half + 1) * HALF)
-        both = jnp.concatenate([first[:, keep], second[:, keep]], axis=1)
-        rows_out[half * ROWS : (half + 1) * ROWS] = turned(weave, both).astype(BF)
+    turned_out[0:128] = acc[...].astype(BF)
+    turned_out[128:256] = (own_q[1] + lanes(y1) + lanes(y2) + lanes(y3)).astype(BF)
 
 
 def keys_kernel(
-    place, own_k, own_v, y1, y2, y3, a1, a2, a3, b1, b2, b3, k_out, v_out, acc_k, acc_v
+    own_k, own_v, y1, y2, y3, z1, z2, z3, turned_in, q_out, k_out, v_out, acc_k, acc_v
 ):
-    z = place[0]
+    z, _, _ = position()
     acc_k[...] = own_k[1]
     acc_v[...] = own_v[1]
-    for ref, ref_v, keys in (
-        (a1, b1, z < SIDE - 1), (a2, b2, z == 0), (a3, b3, z < SIDE // 2)
-    ):
+    for ref, keys in ((z1, z < SIDE - 1), (z2, z == 0), (z3, z < SIDE // 2)):
         @pl.when(keys)
         def _():
-            acc_k[...] += ref[...].astype(F32)
-            acc_v[...] += ref_v[...].astype(F32)
+            acc_k[...] += ref[0:ROWS].astype(F32)
+            acc_v[...] += ref[ROWS:].astype(F32)
 
     row = iota((ROWS, ROWS), 0)
     col = iota((ROWS, ROWS), 1)
@@ -321,39 +352,45 @@
     for ref in (y1, y2, y3):
         k0 += ref[0:ROWS].astype(F32)
         v0 += ref[ROWS:].astype(F32)
-    k1 = acc_k[...].astype(BF)
-    v1 = acc_v[...].astype(BF)
     zero = jnp.concatenate([k0.astype(BF), v0.astype(BF)], axis=1)
-    one = jnp.concatenate([k1, v1], axis=1)
+    one = jnp.concatenate([acc_k[...].astype(BF), acc_v[...].astype(BF)], axis=1)
     for half in range(2):
         keep = slice(half * HALF, (half + 1) * HALF)
+        rows = slice(half * ROWS, (half + 1) * ROWS)
         woven = exact(weave, jnp.concatenate([zero[keep], one[keep]], axis=0)).astype(BF)
-        k_out[half * ROWS : (half + 1) * ROWS] = woven[:, 0:128]
-        v_out[half * ROWS : (half + 1) * ROWS] = woven[:, 128:256]
+        k_out[rows] = woven[:, 0:128]
+        v_out[rows] = woven[:, 128:256]
+        both = jnp.concatenate([turned_in[0:128, keep], turned_in[128:256, keep]], axis=1)
+        q_out[rows] = turned(weave, both).astype(BF)
 
 
 def project_kernel(
-    place, g0, g1, g2, g3, lat0, m1, m2, m3, s1, s2, s3, own, to_plus, to_minus, to_far, lat
+    g0, g1, g2, g3, lat0, near, near_swap, far, far_swap, own, to_plus, to_minus, to_far, lat
 ):
-    y = place[1]
-    core = place[2]
+    _, y, core = position()
     lat[0:ROWS] = lat0[...]
-    for n, (mine, swap) in enumerate(((m1, s1), (m2, s2), (m3, s3))):
-        base = (n + 1) * ROWS
-        for part in range(2):
-            rows = slice(base + part * HALF, base + (part + 1) * HALF)
-
-            @pl.when(core == part)
-            def _():
-                lat[rows] = mine[...]
-
-            @pl.when(core != part)
-            def _():
-                lat[rows] = swap[...]
+    first = slice(ROWS, 2 * ROWS)
+    second = slice(2 * ROWS, 3 * ROWS)
+    third = slice(3 * ROWS, 3 * ROWS + HALF)
+    fourth = slice(3 * ROWS + HALF, 4 * ROWS)
+
+    @pl.when(core == 0)
+    def _():
+        lat[first] = near[...]
+        lat[second] = near_swap[...]
+        lat[third] = far[...]
+        lat[fourth] = far_swap[...]
+
+    @pl.when(core == 1)
+    def _():
+        lat[first] = near_swap[...]
+        lat[second] = near[...]
+        lat[third] = far_swap[...]
+        lat[fourth] = far[...]
 
     grads = jnp.concatenate([g0[...], g1[...], g2[...], g3[...]], axis=1)
     for ref, step in ((to_plus, 1), (to_minus, SIDE - 1), (to_far, 2), (own, 0)):
-        columns = pl.ds(pl.multiple_of((y + step) % SIDE * ROWS, ROWS), ROWS)
+        columns = pl.ds(pl.multiple_of(lax.rem(y + step, SIDE) * ROWS, ROWS), ROWS)
         ref[...] = exact(grads, lat[:, columns]).astype(ref.dtype)
 
 
@@ -370,6 +407,17 @@
     return lax.ppermute(x, "sp", pairs)
 
 
+def moved_apart(x):
+    heads = lax.axis_size("tp")
+    pairs = []
+    for z in range(SIDE):
+        for y in range(SIDE):
+            for t in range(heads):
+                there = (z + (1 if t % 2 == 0 else SIDE - 1)) % SIDE * SIDE + y
+                pairs.append(((z * SIDE + y) * heads + t, there * heads + t))
+    return lax.ppermute(x, ("sp", "tp"), pairs)
+
+
 def partner(x):
     return lax.ppermute(x, "tp", [(t, t ^ 1) for t in range(lax.axis_size("tp"))])
 
@@ -379,7 +427,7 @@
 
 
 def call(kernel, outs, scalars, hbm, vmem, scratch, flops, mib=16):
-    return pl.pallas_call(
+    calling = pl.pallas_call(
         kernel,
         out_shape=outs,
         in_specs=[pl.BlockSpec(memory_space=pltpu.SMEM)] * scalars
@@ -390,6 +438,15 @@
         compiler_params=pltpu.CompilerParams(vmem_limit_bytes=mib * 2**20),
         cost_estimate=pl.CostEstimate(flops=flops, bytes_accessed=10**6, transcendentals=0),
     )
+
+    def run(*arrays):
+        held = [
+            pltpu.with_memory_space_constraint(x, pltpu.HBM)
+            for x in arrays[scalars : scalars + hbm]
+        ]
+        return calling(*arrays[:scalars], *held, *arrays[scalars + hbm :])
+
+    return run
 
 
 def body(
@@ -403,14 +460,11 @@
     mix_lambda,
     norm_gain,
 ):
-    index = lax.axis_index("sp")
-    place = jnp.stack([index // SIDE, index % SIDE, lax.axis_index("tp") % 2]).astype(jnp.int32)
-    part = shape(HALF, WIDE)
-    yown, zown, plus, minus, far, lat_own, lat_plus, lat_minus, lat_far = call(
+    yown, zown, plus, minus, far = call(
         prepare_kernel,
-        (shape(SLOT, 128),) * 2 + (shape(QG, 128),) * 3 + (shape(ROWS, WIDE), part, part, part),
-        2,
-        8,
+        (shape(SLOT, 128),) * 2 + (shape(QG, 128),) * 3,
+        1,
+        7,
         0,
         [pltpu.VMEM((2 * ROWS, 128), BF)] * 3
         + [
@@ -418,12 +472,10 @@
             pltpu.VMEM((2, 2, ROWS), F32),
             pltpu.VMEM((2 * ROWS, 128), BF),
             pltpu.VMEM((1, 128), F32),
-            pltpu.SemaphoreType.DMA((11,)),
+            pltpu.SemaphoreType.DMA((7,)),
         ],
         10**8,
-        54,
     )(
-        place,
         mix_lambda,
         query_heads.reshape(2 * ROWS, 128),
         key_heads.reshape(2 * ROWS, 128),
@@ -432,7 +484,6 @@
         jnp.transpose(log_sums, (1, 2, 0)),
         out_grad.reshape(2 * ROWS, 128),
         norm_gain.reshape(1, 128),
-        latents,
     )
     yleft = moved(yown, 0, 1)
     yright = moved(yown, 0, -1)
@@ -441,20 +492,31 @@
     zfar = moved(far, 2, 0)
     ytop = moved(yleft[0 : SLOT // 2], 0, 1)
     ybottom = moved(yright[SLOT // 2 :], 0, -1)
-    mine = (moved(lat_plus, 1, 0), moved(lat_minus, -1, 0), moved(lat_far, 2, 0))
-    swap = tuple(partner(x) for x in mine)
+    lat_own, lat_near, lat_far = call(
+        fetch_kernel,
+        (shape(ROWS, WIDE), shape(ROWS, WIDE), shape(HALF, WIDE)),
+        0,
+        1,
+        0,
+        [pltpu.SemaphoreType.DMA((3,))],
+        10**7,
+        1,
+    )(latents)
+    near = moved_apart(lat_near)
+    apart = moved(lat_far, 2, 0)
+    near_swap = partner(near)
+    apart_swap = partner(apart)
 
     slots = 2 * SIDE
     small = shape(ROWS, 128)
     both = shape(2 * ROWS, 128)
     results = call(
         attend_kernel,
-        (small,) * 6
-        + (both,) * 3
-        + (small,) * 3
+        (small,) * 3
+        + (both,) * 6
         + (shape(2, 128, ROWS, dtype=F32),)
         + (shape(2, ROWS, 128, dtype=F32),) * 2,
-        2,
+        1,
         0,
         9,
         [
@@ -466,54 +528,36 @@
             pltpu.VMEM((slots, 128, ROWS), F32),
             pltpu.VMEM((slots, ROWS, 128), F32),
             pltpu.VMEM((slots, ROWS, 128), F32),
+            pltpu.VMEM((ROWS, ROWS), BF),
+            pltpu.VMEM((2 * ROWS, ROWS), BF),
         ],
         17 * 10 * ROWS * ROWS * 128,
         24,
-    )(place, mix_lambda, yown, yleft, yright, ytop, ybottom, zown, zplus, zminus, zfar)
-    q_left, q_right, q_far, q_plus, q_minus, q_zfar = results[0:6]
-    kv_left, kv_right, kv_far, v_plus, v_minus, v_zfar = results[6:12]
-    own_q, own_k, own_v = results[12:15]
-    q_back = (
-        moved(q_left, 0, -1),
-        moved(q_right, 0, 1),
-        moved(q_far, 0, 2),
-        moved(q_plus, -1, 0),
-        moved(q_minus, 1, 0),
-        moved(q_zfar, 2, 0),
-    )
-    turned_grad, query_rows = call(
-        queries_kernel,
-        (shape(ROWS, ROWS), shape(2 * ROWS, 128)),
-        1,
-        0,
-        7,
-        [pltpu.VMEM((128, ROWS), F32)],
-        10**7,
-    )(place, own_q, *q_back)
+    )(mix_lambda, yown, yleft, yright, ytop, ybottom, zown, zplus, zminus, zfar)
+    q_left, q_right, q_far, r_plus, r_minus, r_far = results[0:6]
+    kv_left, kv_right, kv_far, own_q, own_k, own_v = results[6:12]
+    q_back = (moved(q_left, 0, -1), moved(q_right, 0, 1), moved(q_far, 0, 2))
+    z_back = (moved(r_plus, -1, 0), moved(r_minus, 1, 0), moved(r_far, 2, 0))
+    turned_grad = call(
+        queries_kernel, shape(ROWS, ROWS), 0, 0, 7, [pltpu.VMEM((128, ROWS), F32)], 10**7
+    )(own_q, *q_back, *z_back)
     grads = (
         turned_grad, moved(turned_grad, 1, 0), moved(turned_grad, -1, 0), moved(turned_grad, 2, 0)
     )
     kv_back = (moved(kv_left, 0, -1), moved(kv_right, 0, 1), moved(kv_far, 0, 2))
-    v_back = (moved(v_plus, -1, 0), moved(v_minus, 1, 0), moved(v_zfar, 2, 0))
-    key_rows, value_rows = call(
-        keys_kernel,
-        (shape(2 * ROWS, 128),) * 2,
-        1,
-        0,
-        11,
-        [pltpu.VMEM((ROWS, 128), F32)] * 2,
-        10**7,
-    )(place, own_k, own_v, *kv_back, *q_back[3:], *v_back)
     square = shape(ROWS, ROWS)
     own, to_plus, to_minus, to_far = call(
         project_kernel,
         (shape(ROWS, ROWS, dtype=F32), square, square, square),
-        1,
         0,
-        11,
+        0,
+        9,
         [pltpu.VMEM((WIDE, WIDE), BF)],
         2 * WIDE * WIDE * ROWS,
-    )(place, *grads, lat_own, *mine, *swap)
+    )(*grads, lat_own, near, near_swap, apart, apart_swap)
+    query_rows, key_rows, value_rows = call(
+        keys_kernel, (shape(2 * ROWS, 128),) * 3, 0, 0, 9, [pltpu.VMEM((ROWS, 128), F32)] * 2, 10**7
+    )(own_k, own_v, *kv_back, *z_back, turned_grad)
     weight_grad = call(total_kernel, shape(ROWS, ROWS, dtype=F32), 0, 0, 4, [], 10**6)(
         own, moved(to_plus, 0, 1), moved(to_minus, 0, -1), moved(to_far, 0, 2)
     )

time: 83.3 us -> 79.3 us (0.952)
  waiting for transfers between devices: 18.6 us -> 31.2 us
  starting transfers between devices: 39.6 us -> 29.6 us
  Pallas kernels: 21.6 us -> 17.7 us
  local copies, waits for them, and re-layouts: 1.93 us -> 0.03 us
    ppermute x28 -> x23, waiting for transfers between devices: 18.6 us -> 31.2 us  [moved(): return lax.ppermute(x, 'sp', pairs)]
    ppermute x28 -> x23, starting transfers between devices: 39.6 us -> 27.4 us  [moved(): return lax.ppermute(x, 'sp', pairs)]
    pallas_call x6 -> x7, Pallas kernels: 21.6 us -> 17.7 us  [run(): return calling(*arrays[:scalars], *held, *arrays[scalars + hbm:])]
    ppermute x0 -> x1, starting transfers between devices: none -> 2.1 us  [moved_apart(): return lax.ppermute(x, ('sp', 'tp'), pairs)]
    unnamed x10 -> x2, local copies, waits for them, and re-layouts: 1.91 us -> 0.01 us
  transfers between devices with their start and end apart: 31 -> 26, of which waited for: 12 -> 13; matrix products, arithmetic and copies ran while one was open for 0% -> 0% of each run, Pallas kernels for 20% -> 20%
where the time goes in v1:
time: 79.3 us; the launch traced here: 79.2 us
  waiting for transfers between devices  31.2 us (39%)
  starting transfers between devices  29.6 us (37%)
  Pallas kernels  17.7 us (22%)
    ppermute x23, waiting for transfers between devices, moved(): return lax.ppermute(x, 'sp', pairs)  31.2 us
    ppermute x23, starting transfers between devices, moved(): return lax.ppermute(x, 'sp', pairs)  27.4 us
    pallas_call x7, Pallas kernels, run(): return calling(*arrays[:scalars], *held, *arrays[scalars + hbm:])  17.7 us
    ppermute x1, starting transfers between devices, moved_apart(): return lax.ppermute(x, ('sp', 'tp'), pairs)  2.1 us
  transfers between devices with their start and end apart: 26, of which 13 were waited for; matrix products, arithmetic and copies ran while one was open for 0% of the time, Pallas kernels for 20%

profile of v1, /device:TPU:0, one launch (start us, length us, event | category | flops | bytes accessed | tf_op | source)
XLA Modules:
  0.0 79.2 jit_solution(260754976455981225)
XLA Ops:
  0.6 1.3 %shard_map.124 = (bf16[256,1024]{1,0:T(8,128)(2,1)S(1)}, bf16[256,1024]{1,0:T(8,128)(2,1)S(1)}, bf16[128,1024]{1,0:T(8,128)(2,1)S(1)}) custom-call(bf16[256,4096]{1,0:T(8,128)(2,1)} %lat_hbm.1), custom_call_target="tpu_custom_call" | custom-call | flops 10000000 | bytes 1000000 | tf_op jit(solution)/shard_map/pallas_call | solution.py:447
  2.0 2.1 %collective-permute-start.19 = (bf16[256,1024]{1,0:T(8,128)(2,1)S(1)}, bf16[256,1024]{1,0:T(8,128)(2,1)S(1)}, u32[]{:S(2)}, u32[]{:S(2)}) collective-permute-start(bf16[256,1024]{1,0:T(8,128)(2,1)S(1)} %get-tuple-element.52), channel_id=1, source_target_pairs={{0,32},{1,97},{2,34},{3,99},{4,36},{5,101},{6,38},{7,103},{8,40},{... | collective-permute-start | bytes 1572872 | tf_op jit(solution)/shard_map/ppermute | solution.py:418
  4.1 2.5 %shard_map.120 = (bf16[1056,128]{1,0:T(8,128)(2,1)S(1)}, bf16[1056,128]{1,0:T(8,128)(2,1)S(1)}, bf16[544,128]{1,0:T(8,128)(2,1)S(1)}, bf16[544,128]{1,0:T(8,128)(2,1)S(1)}, bf16[544,128]{1,0:T(8,128)(2,1)S(1)}) custom-call(f32[2]{0:T(128)S(1)} %copy-done, bf16[512,128]{1,0:T(8,128)(2,1)} %bitcast.11, bf16[512,128]{1,0:T(8,128)(2,1)} %bitcast.12, ...), custom_call_target="tpu_custom_call" | custom-call | flops 100000000 | bytes 1000000 | tf_op jit(solution)/shard_map/pallas_call | solution.py:447
  6.6 3.1 %collective-permute-start.1 = (bf16[1056,128]{1,0:T(8,128)(2,1)S(1)}, bf16[1056,128]{1,0:T(8,128)(2,1)S(1)}, u32[]{:S(2)}, u32[]{:S(2)}) collective-permute-start(bf16[1056,128]{1,0:T(8,128)(2,1)S(1)} %get-tuple-element.31.yown), channel_id=1, source_target_pairs={{0,24},{8,0},{16,8},{24,16},{32,56},{40,32},{48,40},{56,48},{64,88... | collective-permute-start | bytes 811016 | tf_op jit(solution)/shard_map/ppermute | solution.py:407
  9.7 1.9 %collective-permute-start.4 = (bf16[544,128]{1,0:T(8,128)(2,1)S(1)}, bf16[544,128]{1,0:T(8,128)(2,1)S(1)}, u32[]{:S(2)}, u32[]{:S(2)}) collective-permute-start(bf16[544,128]{1,0:T(8,128)(2,1)S(1)} %get-tuple-element.33), channel_id=1, source_target_pairs={{0,32},{8,40},{16,48},{24,56},{32,64},{40,72},{48,80},{56,88},{64,... | collective-permute-start | bytes 417800 | tf_op jit(solution)/shard_map/ppermute | solution.py:407
  11.6 1.3 %collective-permute-start.5 = (bf16[544,128]{1,0:T(8,128)(2,1)S(1)}, bf16[544,128]{1,0:T(8,128)(2,1)S(1)}, u32[]{:S(2)}, u32[]{:S(2)}) collective-permute-start(bf16[544,128]{1,0:T(8,128)(2,1)S(1)} %get-tuple-element.34), channel_id=1, source_target_pairs={{0,96},{8,104},{16,112},{24,120},{32,0},{40,8},{48,16},{56,24},{64... | collective-permute-start | bytes 417800 | tf_op jit(solution)/shard_map/ppermute | solution.py:407
  12.9 2.9 %collective-permute-done.1.yright = bf16[1056,128]{1,0:T(8,128)(2,1)S(1)} collective-permute-done((bf16[1056,128]{1,0:T(8,128)(2,1)S(1)}, bf16[1056,128]{1,0:T(8,128)(2,1)S(1)}, u32[]{:S(2)}, u32[]{:S(2)}) %collective-permute-start.1) | collective-permute-done | bytes 270368 | tf_op jit(solution)/shard_map/ppermute | solution.py:407
  15.9 1.6 %collective-permute-start.21 = (bf16[128,1024]{1,0:T(8,128)(2,1)S(1)}, bf16[128,1024]{1,0:T(8,128)(2,1)S(1)}, u32[]{:S(2)}, u32[]{:S(2)}) collective-permute-start(bf16[128,1024]{1,0:T(8,128)(2,1)S(1)} %get-tuple-element.53), channel_id=1, source_target_pairs={{0,64},{8,72},{16,80},{24,88},{32,96},{40,104},{48,112},{56,120},{... | collective-permute-start | bytes 786440 | tf_op jit(solution)/shard_map/ppermute | solution.py:407
  17.4 2.4 %collective-permute-done.yleft = bf16[1056,128]{1,0:T(8,128)(2,1)S(1)} collective-permute-done((bf16[1056,128]{1,0:T(8,128)(2,1)S(1)}, bf16[1056,128]{1,0:T(8,128)(2,1)S(1)}, u32[]{:S(2)}, u32[]{:S(2)}) %collective-permute-start) | collective-permute-done | bytes 270368 | tf_op jit(solution)/shard_map/ppermute | solution.py:407
  19.8 1.1 %collective-permute-start.6 = (bf16[544,128]{1,0:T(8,128)(2,1)S(1)}, bf16[544,128]{1,0:T(8,128)(2,1)S(1)}, u32[]{:S(2)}, u32[]{:S(2)}) collective-permute-start(bf16[544,128]{1,0:T(8,128)(2,1)S(1)} %get-tuple-element.35), channel_id=1, source_target_pairs={{0,64},{8,72},{16,80},{24,88},{32,96},{40,104},{48,112},{56,120},{... | collective-permute-start | bytes 417800 | tf_op jit(solution)/shard_map/ppermute | solution.py:407
  21.0 0.0 collective-permute-done.4.plus
  21.0 2.2 %collective-permute-start.3 = (bf16[528,128]{1,0:T(8,128)(2,1)S(1)}, bf16[528,128]{1,0:T(8,128)(2,1)S(1)}, u32[]{:S(2)}, u32[]{:S(2)}) collective-permute-start(bf16[528,128]{1,0:T(8,128)(2,1)S(1)} %slice.9), channel_id=1, source_target_pairs={{0,24},{8,0},{16,8},{24,16},{32,56},{40,32},{48,40},{56,48},{64,88... | collective-permute-start | bytes 405512 | tf_op jit(solution)/shard_map/ppermute | solution.py:407
  23.2 0.0 collective-permute-start.2
  23.2 0.0 collective-permute-done.19.near
  23.2 0.1 collective-permute-start.20
  23.3 3.2 %collective-permute-done.21.far = bf16[128,1024]{1,0:T(8,128)(2,1)S(1)} collective-permute-done((bf16[128,1024]{1,0:T(8,128)(2,1)S(1)}, bf16[128,1024]{1,0:T(8,128)(2,1)S(1)}, u32[]{:S(2)}, u32[]{:S(2)}) %collective-permute-start.21) | collective-permute-done | bytes 262176 | tf_op jit(solution)/shard_map/ppermute | solution.py:407
  26.5 0.0 collective-permute-start.22
  26.5 2.8 %collective-permute-done.6.far = bf16[544,128]{1,0:T(8,128)(2,1)S(1)} collective-permute-done((bf16[544,128]{1,0:T(8,128)(2,1)S(1)}, bf16[544,128]{1,0:T(8,128)(2,1)S(1)}, u32[]{:S(2)}, u32[]{:S(2)}) %collective-permute-start.6) | collective-permute-done | bytes 139296 | tf_op jit(solution)/shard_map/ppermute | solution.py:407
  29.4 0.0 collective-permute-done.3.ybottom
  29.4 0.5 collective-permute-done.2.ytop
  29.9 10.9 %shard_map.121 = (bf16[256,128]{1,0:T(8,128)(2,1)S(1)}, bf16[256,128]{1,0:T(8,128)(2,1)S(1)}, bf16[256,128]{1,0:T(8,128)(2,1)S(1)}, bf16[512,128]{1,0:T(8,128)(2...) custom-call(f32[2]{0:T(128)S(1)} %copy-done, ...), custom_call_target="tpu_custom_call" | custom-call | flops 1426063360 | bytes 1000000 | tf_op jit(solution)/shard_map/pallas_call | solution.py:447
  40.8 3.3 %collective-permute-start.13 = (bf16[256,128]{1,0:T(8,128)(2,1)S(1)}, bf16[256,128]{1,0:T(8,128)(2,1)S(1)}, u32[]{:S(2)}, u32[]{:S(2)}) collective-permute-start(bf16[256,128]{1,0:T(8,128)(2,1)S(1)} %get-tuple-element.45), channel_id=1, source_target_pairs={{0,24},{8,0},{16,8},{24,16},{32,56},{40,32},{48,40},{56,48},{64,88... | collective-permute-start | bytes 196616 | tf_op jit(solution)/shard_map/ppermute | solution.py:407
  44.1 0.0 collective-permute-start.14
  44.1 1.5 %collective-permute-start.15 = (bf16[256,128]{1,0:T(8,128)(2,1)S(1)}, bf16[256,128]{1,0:T(8,128)(2,1)S(1)}, u32[]{:S(2)}, u32[]{:S(2)}) collective-permute-start(bf16[256,128]{1,0:T(8,128)(2,1)S(1)} %get-tuple-element.47), channel_id=1, source_target_pairs={{0,16},{8,24},{16,0},{24,8},{32,48},{40,56},{48,32},{56,40},{64,80... | collective-permute-start | bytes 196616 | tf_op jit(solution)/shard_map/ppermute | solution.py:407
  45.6 0.4 collective-permute-done.13.y1
  46.0 0.5 collective-permute-start.10
  46.4 3.9 %collective-permute-done.14.y2 = bf16[256,128]{1,0:T(8,128)(2,1)S(1)} collective-permute-done((bf16[256,128]{1,0:T(8,128)(2,1)S(1)}, bf16[256,128]{1,0:T(8,128)(2,1)S(1)}, u32[]{:S(2)}, u32[]{:S(2)}) %collective-permute-start.14) | collective-permute-done | bytes 65568 | tf_op jit(solution)/shard_map/ppermute | solution.py:407
  50.4 0.0 collective-permute-done.15.y3
  50.4 1.4 %collective-permute-start.12 = (bf16[512,128]{1,0:T(8,128)(2,1)S(1)}, bf16[512,128]{1,0:T(8,128)(2,1)S(1)}, u32[]{:S(2)}, u32[]{:S(2)}) collective-permute-start(bf16[512,128]{1,0:T(8,128)(2,1)S(1)} %get-tuple-element.43), channel_id=1, source_target_pairs={{0,64},{8,72},{16,80},{24,88},{32,96},{40,104},{48,112},{56,120},{... | collective-permute-start | bytes 393224 | tf_op jit(solution)/shard_map/ppermute | solution.py:407
  51.7 6.9 %collective-permute-done.11.z2 = bf16[512,128]{1,0:T(8,128)(2,1)S(1)} collective-permute-done((bf16[512,128]{1,0:T(8,128)(2,1)S(1)}, bf16[512,128]{1,0:T(8,128)(2,1)S(1)}, u32[]{:S(2)}, u32[]{:S(2)}) %collective-permute-start.11) | collective-permute-done | bytes 131104 | tf_op jit(solution)/shard_map/ppermute | solution.py:407
  58.6 0.1 shard_map.122.turned_in.g0
  58.7 0.7 collective-permute-start.18
  59.3 1.0 %collective-permute-start.17 = (bf16[256,256]{1,0:T(8,128)(2,1)S(1)}, bf16[256,256]{1,0:T(8,128)(2,1)S(1)}, u32[]{:S(2)}, u32[]{:S(2)}) collective-permute-start(bf16[256,256]{1,0:T(8,128)(2,1)S(1)} %shard_map.122.turned_in.g0), channel_id=1, source_target_pairs={{0,96},{8,104},{16,112},{24,120},{32,0},{40,8},{48,16},{56,24},{64... | collective-permute-start | bytes 393224 | tf_op jit(solution)/shard_map/ppermute | solution.py:407
  60.3 1.0 %collective-permute-start.16 = (bf16[256,256]{1,0:T(8,128)(2,1)S(1)}, bf16[256,256]{1,0:T(8,128)(2,1)S(1)}, u32[]{:S(2)}, u32[]{:S(2)}) collective-permute-start(bf16[256,256]{1,0:T(8,128)(2,1)S(1)} %shard_map.122.turned_in.g0), channel_id=1, source_target_pairs={{0,32},{8,40},{16,48},{24,56},{32,64},{40,72},{48,80},{56,88},{64,... | collective-permute-start | bytes 393224 | tf_op jit(solution)/shard_map/ppermute | solution.py:407
  61.4 0.8 collective-permute-start.7
  62.1 3.1 %collective-permute-done.18.g3 = bf16[256,256]{1,0:T(8,128)(2,1)S(1)} collective-permute-done((bf16[256,256]{1,0:T(8,128)(2,1)S(1)}, bf16[256,256]{1,0:T(8,128)(2,1)S(1)}, u32[]{:S(2)}, u32[]{:S(2)}) %collective-permute-start.18) | collective-permute-done | bytes 131104 | tf_op jit(solution)/shard_map/ppermute | solution.py:407
  65.2 0.2 collective-permute-done.17.g2
  65.5 2.2 %collective-permute-start.9 = (bf16[512,128]{1,0:T(8,128)(2,1)S(1)}, bf16[512,128]{1,0:T(8,128)(2,1)S(1)}, u32[]{:S(2)}, u32[]{:S(2)}) collective-permute-start(bf16[512,128]{1,0:T(8,128)(2,1)S(1)} %get-tuple-element.40), channel_id=1, source_target_pairs={{0,16},{8,24},{16,0},{24,8},{32,48},{40,56},{48,32},{56,40},{64,80... | collective-permute-start | bytes 393224 | tf_op jit(solution)/shard_map/ppermute | solution.py:407
  67.7 0.9 %shard_map.125 = (f32[256,256]{1,0:T(8,128)S(1)}, bf16[256,256]{1,0:T(8,128)(2,1)S(1)}, bf16[256,256]{1,0:T(8,128)(2,1)S(1)}, bf16[256,256]{1,0:T(8,128)(2,1)S(1)}) custom-call(bf16[256,256]{1,0:T(8,128)(2,1)S(1)} %shard_map.122.turned_in.g0, bf16[256,256]{1,0:T(8,128)(2,1)S(1)} %collective-permute-done.16.g1, ...), custom_call_target="tpu_custom_call" | custom-call | flops 536870912 | bytes 1000000 | tf_op jit(solution)/shard_map/pallas_call | solution.py:447
  68.5 1.7 %collective-permute-start.23 = (bf16[256,256]{1,0:T(8,128)(2,1)S(1)}, bf16[256,256]{1,0:T(8,128)(2,1)S(1)}, u32[]{:S(2)}, u32[]{:S(2)}) collective-permute-start(bf16[256,256]{1,0:T(8,128)(2,1)S(1)} %get-tuple-element.55), channel_id=1, source_target_pairs={{0,8},{8,16},{16,24},{24,0},{32,40},{40,48},{48,56},{56,32},{64,72... | collective-permute-start | bytes 393224 | tf_op jit(solution)/shard_map/ppermute | solution.py:407
  70.3 1.6 %collective-permute-start.24 = (bf16[256,256]{1,0:T(8,128)(2,1)S(1)}, bf16[256,256]{1,0:T(8,128)(2,1)S(1)}, u32[]{:S(2)}, u32[]{:S(2)}) collective-permute-start(bf16[256,256]{1,0:T(8,128)(2,1)S(1)} %get-tuple-element.56), channel_id=1, source_target_pairs={{0,24},{8,0},{16,8},{24,16},{32,56},{40,32},{48,40},{56,48},{64,88... | collective-permute-start | bytes 393224 | tf_op jit(solution)/shard_map/ppermute | solution.py:407
  71.9 0.6 collective-permute-start.25
  72.4 1.8 %collective-permute-done.8.y2 = bf16[512,128]{1,0:T(8,128)(2,1)S(1)} collective-permute-done((bf16[512,128]{1,0:T(8,128)(2,1)S(1)}, bf16[512,128]{1,0:T(8,128)(2,1)S(1)}, u32[]{:S(2)}, u32[]{:S(2)}) %collective-permute-start.8) | collective-permute-done | bytes 131104 | tf_op jit(solution)/shard_map/ppermute | solution.py:407
  74.2 1.1 %shard_map.123 = (bf16[512,128]{1,0:T(8,128)(2,1)}, bf16[512,128]{1,0:T(8,128)(2,1)}, bf16[512,128]{1,0:T(8,128)(2,1)}) custom-call(f32[2,256,128]{2,1,0:T(8,128)S(1)} %get-tuple-element.36.own_k, f32[2,256,128]{2,1,0:T(8,128)S(1)} %get-tuple-element.37.own_v, bf16[512,128]{1,0:T(8,128)(2,1)S(1)} %collective-permute-done.7.y1, ...), custom_call_target="tpu_custom_call" | custom-call | flops 10000000 | bytes 1000000 | tf_op jit(solution)/shard_map/pallas_call | solution.py:447
  75.4 0.3 collective-permute-done.23.t1
  75.6 0.0 collective-permute-done.24.t2
  75.6 2.7 %collective-permute-done.25.t3 = bf16[256,256]{1,0:T(8,128)(2,1)S(1)} collective-permute-done((bf16[256,256]{1,0:T(8,128)(2,1)S(1)}, bf16[256,256]{1,0:T(8,128)(2,1)S(1)}, u32[]{:S(2)}, u32[]{:S(2)}) %collective-permute-start.25) | collective-permute-done | bytes 131104 | tf_op jit(solution)/shard_map/ppermute | solution.py:407
  78.3 0.8 %shard_map.126 = f32[256,256]{1,0:T(8,128)} custom-call(f32[256,256]{1,0:T(8,128)S(1)} %get-tuple-element.54.own, bf16[256,256]{1,0:T(8,128)(2,1)S(1)} %collective-permute-done.23.t1, bf16[256,256]{1,0:T(8,128)(2,1)S(1)} %collective-permute-done.24.t2, bf16[256,256]{1,0:T(8,128)(2,1)S(1)} %collective-permute-done.25.t3), custom_call_target="tpu_custom_call" | custom-call | flops 1000000 | bytes 1000000 | tf_op jit(solution)/shard_map/pallas_call | solution.py:447
  (15 shorter events, 0.1 us)
Async XLA Ops:
  0.6 3.4 %copy-start = (f32[2]{0:T(128)S(1)}, f32[2]{0:T(128)}, u32[]{:S(2)}) copy-start(f32[2]{0:T(128)} %lam.3) | copy-start | bytes 28
  2.0 21.2 %collective-permute-start.19 = (bf16[256,1024]{1,0:T(8,128)(2,1)S(1)}, bf16[256,1024]{1,0:T(8,128)(2,1)S(1)}, u32[]{:S(2)}, u32[]{:S(2)}) collective-permute-start(bf16[256,1024]{1,0:T(8,128)(2,1)S(1)} %get-tuple-element.52), channel_id=1, source_target_pairs={{0,32},{1,97},{2,34},{3,99},{4,36},{5,101},{6,38},{7,103},{8,40},{... | collective-permute-start | bytes 1572872 | tf_op jit(solution)/shard_map/ppermute | solution.py:418
  6.6 9.3 %collective-permute-start.1 = (bf16[1056,128]{1,0:T(8,128)(2,1)S(1)}, bf16[1056,128]{1,0:T(8,128)(2,1)S(1)}, u32[]{:S(2)}, u32[]{:S(2)}) collective-permute-start(bf16[1056,128]{1,0:T(8,128)(2,1)S(1)} %get-tuple-element.31.yown), channel_id=1, source_target_pairs={{0,24},{8,0},{16,8},{24,16},{32,56},{40,32},{48,40},{56,48},{64,88... | collective-permute-start | bytes 811016 | tf_op jit(solution)/shard_map/ppermute | solution.py:407
  9.7 10.1 %collective-permute-start = (bf16[1056,128]{1,0:T(8,128)(2,1)S(1)}, bf16[1056,128]{1,0:T(8,128)(2,1)S(1)}, u32[]{:S(2)}, u32[]{:S(2)}) collective-permute-start(bf16[1056,128]{1,0:T(8,128)(2,1)S(1)} %get-tuple-element.31.yown), channel_id=1, source_target_pairs={{0,8},{8,16},{16,24},{24,0},{32,40},{40,48},{48,56},{56,32},{64,72... | collective-permute-start | bytes 811016 | tf_op jit(solution)/shard_map/ppermute | solution.py:407
  9.7 11.3 %collective-permute-start.4 = (bf16[544,128]{1,0:T(8,128)(2,1)S(1)}, bf16[544,128]{1,0:T(8,128)(2,1)S(1)}, u32[]{:S(2)}, u32[]{:S(2)}) collective-permute-start(bf16[544,128]{1,0:T(8,128)(2,1)S(1)} %get-tuple-element.33), channel_id=1, source_target_pairs={{0,32},{8,40},{16,48},{24,56},{32,64},{40,72},{48,80},{56,88},{64,... | collective-permute-start | bytes 417800 | tf_op jit(solution)/shard_map/ppermute | solution.py:407
  11.6 11.6 %collective-permute-start.5 = (bf16[544,128]{1,0:T(8,128)(2,1)S(1)}, bf16[544,128]{1,0:T(8,128)(2,1)S(1)}, u32[]{:S(2)}, u32[]{:S(2)}) collective-permute-start(bf16[544,128]{1,0:T(8,128)(2,1)S(1)} %get-tuple-element.34), channel_id=1, source_target_pairs={{0,96},{8,104},{16,112},{24,120},{32,0},{40,8},{48,16},{56,24},{64... | collective-permute-start | bytes 417800 | tf_op jit(solution)/shard_map/ppermute | solution.py:407
  15.9 10.7 %collective-permute-start.21 = (bf16[128,1024]{1,0:T(8,128)(2,1)S(1)}, bf16[128,1024]{1,0:T(8,128)(2,1)S(1)}, u32[]{:S(2)}, u32[]{:S(2)}) collective-permute-start(bf16[128,1024]{1,0:T(8,128)(2,1)S(1)} %get-tuple-element.53), channel_id=1, source_target_pairs={{0,64},{8,72},{16,80},{24,88},{32,96},{40,104},{48,112},{56,120},{... | collective-permute-start | bytes 786440 | tf_op jit(solution)/shard_map/ppermute | solution.py:407
  19.8 9.6 %collective-permute-start.6 = (bf16[544,128]{1,0:T(8,128)(2,1)S(1)}, bf16[544,128]{1,0:T(8,128)(2,1)S(1)}, u32[]{:S(2)}, u32[]{:S(2)}) collective-permute-start(bf16[544,128]{1,0:T(8,128)(2,1)S(1)} %get-tuple-element.35), channel_id=1, source_target_pairs={{0,64},{8,72},{16,80},{24,88},{32,96},{40,104},{48,112},{56,120},{... | collective-permute-start | bytes 417800 | tf_op jit(solution)/shard_map/ppermute | solution.py:407
  21.0 8.4 %collective-permute-start.3 = (bf16[528,128]{1,0:T(8,128)(2,1)S(1)}, bf16[528,128]{1,0:T(8,128)(2,1)S(1)}, u32[]{:S(2)}, u32[]{:S(2)}) collective-permute-start(bf16[528,128]{1,0:T(8,128)(2,1)S(1)} %slice.9), channel_id=1, source_target_pairs={{0,24},{8,0},{16,8},{24,16},{32,56},{40,32},{48,40},{56,48},{64,88... | collective-permute-start | bytes 405512 | tf_op jit(solution)/shard_map/ppermute | solution.py:407
  23.2 6.7 %collective-permute-start.2 = (bf16[528,128]{1,0:T(8,128)(2,1)S(1)}, bf16[528,128]{1,0:T(8,128)(2,1)S(1)}, u32[]{:S(2)}, u32[]{:S(2)}) collective-permute-start(bf16[528,128]{1,0:T(8,128)(2,1)S(1)} %slice.8), channel_id=1, source_target_pairs={{0,8},{8,16},{16,24},{24,0},{32,40},{40,48},{48,56},{56,32},{64,72... | collective-permute-start | bytes 405512 | tf_op jit(solution)/shard_map/ppermute | solution.py:407
  23.2 44.5 %collective-permute-start.20 = (bf16[256,1024]{1,0:T(8,128)(2,1)S(1)}, bf16[256,1024]{1,0:T(8,128)(2,1)S(1)}, u32[]{:S(2)}, u32[]{:S(2)}) collective-permute-start(bf16[256,1024]{1,0:T(8,128)(2,1)S(1)} %collective-permute-done.19.near), channel_id=1, source_target_pairs={{0,1},{1,0},{2,3},{3,2},{4,5},{5,4},{6,7},{7,6},{8,9},{9,8},{10,11... | collective-permute-start | bytes 1572872 | tf_op jit(solution)/shard_map/ppermute | solution.py:422
  26.5 34.8 %collective-permute-start.22 = (bf16[128,1024]{1,0:T(8,128)(2,1)S(1)}, bf16[128,1024]{1,0:T(8,128)(2,1)S(1)}, u32[]{:S(2)}, u32[]{:S(2)}) collective-permute-start(bf16[128,1024]{1,0:T(8,128)(2,1)S(1)} %collective-permute-done.21.far), channel_id=1, source_target_pairs={{0,1},{1,0},{2,3},{3,2},{4,5},{5,4},{6,7},{7,6},{8,9},{9,8},{10,11... | collective-permute-start | bytes 786440 | tf_op jit(solution)/shard_map/ppermute | solution.py:422
  40.8 5.2 %collective-permute-start.13 = (bf16[256,128]{1,0:T(8,128)(2,1)S(1)}, bf16[256,128]{1,0:T(8,128)(2,1)S(1)}, u32[]{:S(2)}, u32[]{:S(2)}) collective-permute-start(bf16[256,128]{1,0:T(8,128)(2,1)S(1)} %get-tuple-element.45), channel_id=1, source_target_pairs={{0,24},{8,0},{16,8},{24,16},{32,56},{40,32},{48,40},{56,48},{64,88... | collective-permute-start | bytes 196616 | tf_op jit(solution)/shard_map/ppermute | solution.py:407
  44.1 6.3 %collective-permute-start.14 = (bf16[256,128]{1,0:T(8,128)(2,1)S(1)}, bf16[256,128]{1,0:T(8,128)(2,1)S(1)}, u32[]{:S(2)}, u32[]{:S(2)}) collective-permute-start(bf16[256,128]{1,0:T(8,128)(2,1)S(1)} %get-tuple-element.46), channel_id=1, source_target_pairs={{0,8},{8,16},{16,24},{24,0},{32,40},{40,48},{48,56},{56,32},{64,72... | collective-permute-start | bytes 196616 | tf_op jit(solution)/shard_map/ppermute | solution.py:407
  44.1 6.3 %collective-permute-start.15 = (bf16[256,128]{1,0:T(8,128)(2,1)S(1)}, bf16[256,128]{1,0:T(8,128)(2,1)S(1)}, u32[]{:S(2)}, u32[]{:S(2)}) collective-permute-start(bf16[256,128]{1,0:T(8,128)(2,1)S(1)} %get-tuple-element.47), channel_id=1, source_target_pairs={{0,16},{8,24},{16,0},{24,8},{32,48},{40,56},{48,32},{56,40},{64,80... | collective-permute-start | bytes 196616 | tf_op jit(solution)/shard_map/ppermute | solution.py:407
  46.0 5.8 %collective-permute-start.10 = (bf16[512,128]{1,0:T(8,128)(2,1)S(1)}, bf16[512,128]{1,0:T(8,128)(2,1)S(1)}, u32[]{:S(2)}, u32[]{:S(2)}) collective-permute-start(bf16[512,128]{1,0:T(8,128)(2,1)S(1)} %get-tuple-element.41), channel_id=1, source_target_pairs={{0,96},{8,104},{16,112},{24,120},{32,0},{40,8},{48,16},{56,24},{64... | collective-permute-start | bytes 393224 | tf_op jit(solution)/shard_map/ppermute | solution.py:407
  50.3 8.2 %collective-permute-start.11 = (bf16[512,128]{1,0:T(8,128)(2,1)S(1)}, bf16[512,128]{1,0:T(8,128)(2,1)S(1)}, u32[]{:S(2)}, u32[]{:S(2)}) collective-permute-start(bf16[512,128]{1,0:T(8,128)(2,1)S(1)} %get-tuple-element.42), channel_id=1, source_target_pairs={{0,32},{8,40},{16,48},{24,56},{32,64},{40,72},{48,80},{56,88},{64,... | collective-permute-start | bytes 393224 | tf_op jit(solution)/shard_map/ppermute | solution.py:407
  50.4 8.2 %collective-permute-start.12 = (bf16[512,128]{1,0:T(8,128)(2,1)S(1)}, bf16[512,128]{1,0:T(8,128)(2,1)S(1)}, u32[]{:S(2)}, u32[]{:S(2)}) collective-permute-start(bf16[512,128]{1,0:T(8,128)(2,1)S(1)} %get-tuple-element.43), channel_id=1, source_target_pairs={{0,64},{8,72},{16,80},{24,88},{32,96},{40,104},{48,112},{56,120},{... | collective-permute-start | bytes 393224 | tf_op jit(solution)/shard_map/ppermute | solution.py:407
  58.7 6.6 %collective-permute-start.18 = (bf16[256,256]{1,0:T(8,128)(2,1)S(1)}, bf16[256,256]{1,0:T(8,128)(2,1)S(1)}, u32[]{:S(2)}, u32[]{:S(2)}) collective-permute-start(bf16[256,256]{1,0:T(8,128)(2,1)S(1)} %shard_map.122.turned_in.g0), channel_id=1, source_target_pairs={{0,64},{8,72},{16,80},{24,88},{32,96},{40,104},{48,112},{56,120},{... | collective-permute-start | bytes 393224 | tf_op jit(solution)/shard_map/ppermute | solution.py:407
  59.3 6.1 %collective-permute-start.17 = (bf16[256,256]{1,0:T(8,128)(2,1)S(1)}, bf16[256,256]{1,0:T(8,128)(2,1)S(1)}, u32[]{:S(2)}, u32[]{:S(2)}) collective-permute-start(bf16[256,256]{1,0:T(8,128)(2,1)S(1)} %shard_map.122.turned_in.g0), channel_id=1, source_target_pairs={{0,96},{8,104},{16,112},{24,120},{32,0},{40,8},{48,16},{56,24},{64... | collective-permute-start | bytes 393224 | tf_op jit(solution)/shard_map/ppermute | solution.py:407
  60.3 7.3 %collective-permute-start.16 = (bf16[256,256]{1,0:T(8,128)(2,1)S(1)}, bf16[256,256]{1,0:T(8,128)(2,1)S(1)}, u32[]{:S(2)}, u32[]{:S(2)}) collective-permute-start(bf16[256,256]{1,0:T(8,128)(2,1)S(1)} %shard_map.122.turned_in.g0), channel_id=1, source_target_pairs={{0,32},{8,40},{16,48},{24,56},{32,64},{40,72},{48,80},{56,88},{64,... | collective-permute-start | bytes 393224 | tf_op jit(solution)/shard_map/ppermute | solution.py:407
  61.4 10.5 %collective-permute-start.7 = (bf16[512,128]{1,0:T(8,128)(2,1)S(1)}, bf16[512,128]{1,0:T(8,128)(2,1)S(1)}, u32[]{:S(2)}, u32[]{:S(2)}) collective-permute-start(bf16[512,128]{1,0:T(8,128)(2,1)S(1)} %get-tuple-element.38), channel_id=1, source_target_pairs={{0,24},{8,0},{16,8},{24,16},{32,56},{40,32},{48,40},{56,48},{64,88... | collective-permute-start | bytes 393224 | tf_op jit(solution)/shard_map/ppermute | solution.py:407
  65.2 9.0 %collective-permute-start.8 = (bf16[512,128]{1,0:T(8,128)(2,1)S(1)}, bf16[512,128]{1,0:T(8,128)(2,1)S(1)}, u32[]{:S(2)}, u32[]{:S(2)}) collective-permute-start(bf16[512,128]{1,0:T(8,128)(2,1)S(1)} %get-tuple-element.39), channel_id=1, source_target_pairs={{0,8},{8,16},{16,24},{24,0},{32,40},{40,48},{48,56},{56,32},{64,72... | collective-permute-start | bytes 393224 | tf_op jit(solution)/shard_map/ppermute | solution.py:407
  65.5 8.7 %collective-permute-start.9 = (bf16[512,128]{1,0:T(8,128)(2,1)S(1)}, bf16[512,128]{1,0:T(8,128)(2,1)S(1)}, u32[]{:S(2)}, u32[]{:S(2)}) collective-permute-start(bf16[512,128]{1,0:T(8,128)(2,1)S(1)} %get-tuple-element.40), channel_id=1, source_target_pairs={{0,16},{8,24},{16,0},{24,8},{32,48},{40,56},{48,32},{56,40},{64,80... | collective-permute-start | bytes 393224 | tf_op jit(solution)/shard_map/ppermute | solution.py:407
  68.5 7.1 %collective-permute-start.23 = (bf16[256,256]{1,0:T(8,128)(2,1)S(1)}, bf16[256,256]{1,0:T(8,128)(2,1)S(1)}, u32[]{:S(2)}, u32[]{:S(2)}) collective-permute-start(bf16[256,256]{1,0:T(8,128)(2,1)S(1)} %get-tuple-element.55), channel_id=1, source_target_pairs={{0,8},{8,16},{16,24},{24,0},{32,40},{40,48},{48,56},{56,32},{64,72... | collective-permute-start | bytes 393224 | tf_op jit(solution)/shard_map/ppermute | solution.py:407
  70.3 5.3 %collective-permute-start.24 = (bf16[256,256]{1,0:T(8,128)(2,1)S(1)}, bf16[256,256]{1,0:T(8,128)(2,1)S(1)}, u32[]{:S(2)}, u32[]{:S(2)}) collective-permute-start(bf16[256,256]{1,0:T(8,128)(2,1)S(1)} %get-tuple-element.56), channel_id=1, source_target_pairs={{0,24},{8,0},{16,8},{24,16},{32,56},{40,32},{48,40},{56,48},{64,88... | collective-permute-start | bytes 393224 | tf_op jit(solution)/shard_map/ppermute | solution.py:407
  71.9 6.5 %collective-permute-start.25 = (bf16[256,256]{1,0:T(8,128)(2,1)S(1)}, bf16[256,256]{1,0:T(8,128)(2,1)S(1)}, u32[]{:S(2)}, u32[]{:S(2)}) collective-permute-start(bf16[256,256]{1,0:T(8,128)(2,1)S(1)} %get-tuple-element.57), channel_id=1, source_target_pairs={{0,16},{8,24},{16,0},{24,8},{32,48},{40,56},{48,32},{56,40},{64,80... | collective-permute-start | bytes 393224 | tf_op jit(solution)/shard_map/ppermute | solution.py:407

commit v2 on v1

--- a/solution.py
+++ b/solution.py
@@ -56,14 +56,14 @@
 
 
 def prepare_kernel(
-    lam, q_hbm, k_hbm, v_hbm, maps_hbm, lse_hbm, out_hbm, gain_hbm,
-    yown, zown, plus, minus, far,
-    q_in, k_in, v_in, maps_in, lse_in, out_in, gain_in, sems,
+    q_hbm, k_hbm, v_hbm, maps_hbm, lse_hbm, out_hbm, gain_hbm, lam_hbm,
+    yown, zown, send1, send2, send3,
+    q_in, k_in, v_in, maps_in, lse_in, out_in, gain_in, lam, sems,
 ):
     z, _, _ = position()
     pairs = [
         (maps_hbm, maps_in), (out_hbm, out_in), (gain_hbm, gain_in), (lse_hbm, lse_in),
-        (q_hbm, q_in), (k_hbm, k_in), (v_hbm, v_in),
+        (lam_hbm, lam), (q_hbm, q_in), (k_hbm, k_in), (v_hbm, v_in),
     ]
     copies = [pltpu.make_async_copy(a, b, sems.at[n]) for n, (a, b) in enumerate(pairs)]
     for copy in copies:
@@ -72,7 +72,7 @@
     col = iota((ROWS, ROWS), 1)
     spread = one_hot(col == 2 * (row % HALF) + row // HALF)
     deal = one_hot(col == 4 * (row % DH) + row // DH)
-    for copy in copies[:4]:
+    for copy in copies[:5]:
         copy.wait()
     left = exact(deal, jnp.concatenate([maps_in[0:256], maps_in[256:512]], axis=1))
     right = exact(deal, jnp.concatenate([maps_in[512:768], maps_in[768:1024]], axis=1))
@@ -109,7 +109,7 @@
         ref[ROWS : 2 * ROWS] = grad
         ref[2 * ROWS : 2 * ROWS + 16] = packed[:, 0:128]
         ref[2 * ROWS + 16 : QG] = packed[:, 128:256]
-    for copy in copies[4:7]:
+    for copy in copies[5:]:
         copy.wait()
     q0, q1, k0, k1 = two_heads(spread, q_in, k_in)
     v0, v1, _, _ = two_heads(spread, v_in, v_in)
@@ -130,22 +130,21 @@
         def _():
             ref[...] = zown[0:QG]
 
-    send(plus, z < SIDE - 1)
-    send(minus, z == 0)
-    send(far, z < SIDE // 2)
+    for n, ref in enumerate((send1, send2, send3)):
+        send(ref, z < jnp.bitwise_xor(z, n + 1))
 
 
 def fetch_kernel(lat_hbm, lat_own, lat_near, lat_far, sems):
     z, _, core = position()
 
     def columns(block):
-        return pl.ds(pl.multiple_of(lax.rem(block, SIDE) * WIDE, WIDE), WIDE)
+        return pl.ds(pl.multiple_of(block * WIDE, WIDE), WIDE)
 
     tokens = pl.ds(pl.multiple_of(core * HALF, HALF), HALF)
-    near = jnp.where(core == 0, z + 1, z + SIDE - 1)
+    near = jnp.bitwise_xor(z, jnp.where(core == 0, 1, 3))
     copies = (
         pltpu.make_async_copy(lat_hbm.at[:, columns(near)], lat_near, sems.at[0]),
-        pltpu.make_async_copy(lat_hbm.at[tokens, columns(z + 2)], lat_far, sems.at[1]),
+        pltpu.make_async_copy(lat_hbm.at[tokens, columns(jnp.bitwise_xor(z, 2))], lat_far, sems.at[1]),
         pltpu.make_async_copy(lat_hbm.at[:, columns(z)], lat_own, sems.at[2]),
     )
     for copy in copies:
@@ -155,22 +154,15 @@
 
 
 def attend_kernel(
-    lam, yown, yleft, yright, ytop, ybottom, zown, plus, minus, far,
-    q_left, q_right, q_far, r_plus, r_minus, r_far,
-    kv_left, kv_right, kv_far, own_q, own_k, own_v,
+    lam, yown, y1, y2, y3, zown, z1, z2, z3,
+    q1, q2, q3, r1, r2, r3, kv1, kv2, kv3, own_q, own_k, own_v,
     buf, stat, kpad, kturn, qpad, dq, dk, dv, wide_w, tall_s,
 ):
     z, y, _ = position()
-    buf[0] = yown[...]
-    buf[1] = yleft[...]
-    buf[2] = yright[...]
-    buf[3, 0 : SLOT // 2] = ytop[...]
-    buf[3, SLOT // 2 :] = ybottom[...]
-    buf[SIDE] = zown[...]
-    keys_plus = (z > 0).astype(jnp.int32)
-    keys_minus = (z == SIDE - 1).astype(jnp.int32)
-    keys_far = (z >= SIDE // 2).astype(jnp.int32)
-    for slot, (ref, keys) in enumerate(((plus, keys_plus), (minus, keys_minus), (far, keys_far))):
+    for slot, ref in enumerate((yown, y1, y2, y3, zown)):
+        buf[slot] = ref[...]
+    keys_of = [(jnp.bitwise_xor(z, n) < z).astype(jnp.int32) for n in range(1, SIDE)]
+    for slot, (ref, keys) in enumerate(zip((z1, z2, z3), keys_of)):
         @pl.when(keys == 1)
         def _():
             buf[SIDE + 1 + slot, QG:SLOT] = ref[0 : 2 * ROWS]
@@ -213,15 +205,9 @@
         rest = item - SIDE - 1
         zslot = jnp.where(own, SIDE, SIDE + 1 + rest // SIDE)
         yslot = jnp.where(own, jnp.maximum(item - 1, 0), lax.rem(jnp.maximum(rest, 0), SIDE))
-        offset = jnp.where(yslot == 1, SIDE - 1, jnp.where(yslot == 2, 1, yslot - 1))
-        behind = jnp.where(yslot == 0, item == 0, lax.rem(y + offset, SIDE) < y)
-        kind = jnp.where(
-            own,
-            1 - behind.astype(jnp.int32),
-            jnp.where(
-                zslot == SIDE + 1, keys_plus, jnp.where(zslot == SIDE + 2, keys_minus, keys_far)
-            ),
-        )
+        behind = jnp.where(yslot == 0, item == 0, jnp.bitwise_xor(y, yslot) < y)
+        other = (jnp.bitwise_xor(z, zslot - SIDE) < z).astype(jnp.int32)
+        kind = jnp.where(own, 1 - behind.astype(jnp.int32), other)
         qs = jnp.where(kind == 0, zslot, yslot)
         ks = jnp.where(kind == 0, yslot, zslot)
         return qs, ks, kind
@@ -291,13 +277,11 @@
         ref[0:HALF] = value[:, 0:128]
         ref[HALF:ROWS] = value[:, 128:]
 
-    for slot, (ref, kv) in enumerate(((q_left, kv_left), (q_right, kv_right), (q_far, kv_far))):
+    for slot, (ref, kv) in enumerate(((q1, kv1), (q2, kv2), (q3, kv3))):
         put_q(ref, slot + 1)
         kv[0:ROWS] = (dk[slot + 1] * scale).astype(BF)
         kv[ROWS:] = dv[slot + 1].astype(BF)
-    for slot, (ref, keys) in enumerate(
-        ((r_plus, keys_plus), (r_minus, keys_minus), (r_far, keys_far))
-    ):
+    for slot, (ref, keys) in enumerate(zip((r1, r2, r3), keys_of)):
         @pl.when(keys == 1)
         def _():
             ref[0:ROWS] = (dk[SIDE + 1 + slot] * scale).astype(BF)
@@ -323,7 +307,9 @@
         return jnp.concatenate([ref[0:HALF].astype(F32), ref[HALF:ROWS].astype(F32)], axis=1)
 
     acc[...] = own_q[0]
-    for ref, keys in ((z1, z < SIDE - 1), (z2, z == 0), (z3, z < SIDE // 2)):
+    for n, ref in enumerate((z1, z2, z3)):
+        keys = z < jnp.bitwise_xor(z, n + 1)
+
         @pl.when(jnp.logical_not(keys))
         def _():
             acc[...] += lanes(ref)
@@ -338,7 +324,9 @@
     z, _, _ = position()
     acc_k[...] = own_k[1]
     acc_v[...] = own_v[1]
-    for ref, keys in ((z1, z < SIDE - 1), (z2, z == 0), (z3, z < SIDE // 2)):
+    for n, ref in enumerate((z1, z2, z3)):
+        keys = z < jnp.bitwise_xor(z, n + 1)
+
         @pl.when(keys)
         def _():
             acc_k[...] += ref[0:ROWS].astype(F32)
@@ -365,32 +353,32 @@
 
 
 def project_kernel(
-    g0, g1, g2, g3, lat0, near, near_swap, far, far_swap, own, to_plus, to_minus, to_far, lat
+    g0, g1, g2, g3, lat0, near, near_swap, far, far_swap, own, to1, to2, to3, lat
 ):
     _, y, core = position()
     lat[0:ROWS] = lat0[...]
     first = slice(ROWS, 2 * ROWS)
-    second = slice(2 * ROWS, 3 * ROWS)
-    third = slice(3 * ROWS, 3 * ROWS + HALF)
-    fourth = slice(3 * ROWS + HALF, 4 * ROWS)
+    second = slice(2 * ROWS, 2 * ROWS + HALF)
+    third = slice(2 * ROWS + HALF, 3 * ROWS)
+    fourth = slice(3 * ROWS, 4 * ROWS)
 
     @pl.when(core == 0)
     def _():
         lat[first] = near[...]
-        lat[second] = near_swap[...]
-        lat[third] = far[...]
-        lat[fourth] = far_swap[...]
+        lat[second] = far[...]
+        lat[third] = far_swap[...]
+        lat[fourth] = near_swap[...]
 
     @pl.when(core == 1)
     def _():
         lat[first] = near_swap[...]
-        lat[second] = near[...]
-        lat[third] = far_swap[...]
-        lat[fourth] = far[...]
+        lat[second] = far_swap[...]
+        lat[third] = far[...]
+        lat[fourth] = near[...]
 
     grads = jnp.concatenate([g0[...], g1[...], g2[...], g3[...]], axis=1)
-    for ref, step in ((to_plus, 1), (to_minus, SIDE - 1), (to_far, 2), (own, 0)):
-        columns = pl.ds(pl.multiple_of(lax.rem(y + step, SIDE) * ROWS, ROWS), ROWS)
+    for n, ref in ((1, to1), (2, to2), (3, to3), (0, own)):
+        columns = pl.ds(pl.multiple_of(jnp.bitwise_xor(y, n) * ROWS, ROWS), ROWS)
         ref[...] = exact(grads, lat[:, columns]).astype(ref.dtype)
 
 
@@ -399,22 +387,18 @@
     out[...] = whole.T
 
 
-def moved(x, dz, dy):
-    pairs = []
-    for z in range(SIDE):
-        for y in range(SIDE):
-            pairs.append((z * SIDE + y, (z + dz) % SIDE * SIDE + (y + dy) % SIDE))
-    return lax.ppermute(x, "sp", pairs)
-
-
-def moved_apart(x):
+def traded(x, axis, n):
+    step = n * (SIDE if axis == "z" else 1)
+    return lax.ppermute(x, "sp", [(s, s ^ step) for s in range(SIDE * SIDE)])
+
+
+def traded_apart(x):
     heads = lax.axis_size("tp")
     pairs = []
-    for z in range(SIDE):
-        for y in range(SIDE):
-            for t in range(heads):
-                there = (z + (1 if t % 2 == 0 else SIDE - 1)) % SIDE * SIDE + y
-                pairs.append(((z * SIDE + y) * heads + t, there * heads + t))
+    for s in range(SIDE * SIDE):
+        for t in range(heads):
+            there = s ^ (SIDE * (1 if t % 2 == 0 else 3))
+            pairs.append((s * heads + t, there * heads + t))
     return lax.ppermute(x, ("sp", "tp"), pairs)
 
 
@@ -460,11 +444,11 @@
     mix_lambda,
     norm_gain,
 ):
-    yown, zown, plus, minus, far = call(
+    yown, zown, *sends = call(
         prepare_kernel,
         (shape(SLOT, 128),) * 2 + (shape(QG, 128),) * 3,
-        1,
-        7,
+        0,
+        8,
         0,
         [pltpu.VMEM((2 * ROWS, 128), BF)] * 3
         + [
@@ -472,11 +456,11 @@
             pltpu.VMEM((2, 2, ROWS), F32),
             pltpu.VMEM((2 * ROWS, 128), BF),
             pltpu.VMEM((1, 128), F32),
-            pltpu.SemaphoreType.DMA((7,)),
+            pltpu.SMEM((2,), F32),
+            pltpu.SemaphoreType.DMA((8,)),
         ],
         10**8,
     )(
-        mix_lambda,
         query_heads.reshape(2 * ROWS, 128),
         key_heads.reshape(2 * ROWS, 128),
         value_heads.reshape(2 * ROWS, 128),
@@ -484,14 +468,10 @@
         jnp.transpose(log_sums, (1, 2, 0)),
         out_grad.reshape(2 * ROWS, 128),
         norm_gain.reshape(1, 128),
+        mix_lambda,
     )
-    yleft = moved(yown, 0, 1)
-    yright = moved(yown, 0, -1)
-    zplus = moved(plus, 1, 0)
-    zminus = moved(minus, -1, 0)
-    zfar = moved(far, 2, 0)
-    ytop = moved(yleft[0 : SLOT // 2], 0, 1)
-    ybottom = moved(yright[SLOT // 2 :], 0, -1)
+    ys = [traded(yown, "y", n) for n in range(1, SIDE)]
+    zs = [traded(x, "z", n) for n, x in enumerate(sends, 1)]
     lat_own, lat_near, lat_far = call(
         fetch_kernel,
         (shape(ROWS, WIDE), shape(ROWS, WIDE), shape(HALF, WIDE)),
@@ -502,8 +482,8 @@
         10**7,
         1,
     )(latents)
-    near = moved_apart(lat_near)
-    apart = moved(lat_far, 2, 0)
+    near = traded_apart(lat_near)
+    apart = traded(lat_far, "z", 2)
     near_swap = partner(near)
     apart_swap = partner(apart)
 
@@ -518,7 +498,7 @@
         + (shape(2, ROWS, 128, dtype=F32),) * 2,
         1,
         0,
-        9,
+        8,
         [
             pltpu.VMEM((slots, SLOT, 128), BF),
             pltpu.VMEM((slots, 8, ROWS), F32),
@@ -533,20 +513,17 @@
         ],
         17 * 10 * ROWS * ROWS * 128,
         24,
-    )(mix_lambda, yown, yleft, yright, ytop, ybottom, zown, zplus, zminus, zfar)
-    q_left, q_right, q_far, r_plus, r_minus, r_far = results[0:6]
-    kv_left, kv_right, kv_far, own_q, own_k, own_v = results[6:12]
-    q_back = (moved(q_left, 0, -1), moved(q_right, 0, 1), moved(q_far, 0, 2))
-    z_back = (moved(r_plus, -1, 0), moved(r_minus, 1, 0), moved(r_far, 2, 0))
+    )(mix_lambda, yown, *ys, zown, *zs)
+    own_q, own_k, own_v = results[9:12]
+    q_back = [traded(x, "y", n) for n, x in enumerate(results[0:3], 1)]
+    z_back = [traded(x, "z", n) for n, x in enumerate(results[3:6], 1)]
     turned_grad = call(
         queries_kernel, shape(ROWS, ROWS), 0, 0, 7, [pltpu.VMEM((128, ROWS), F32)], 10**7
     )(own_q, *q_back, *z_back)
-    grads = (
-        turned_grad, moved(turned_grad, 1, 0), moved(turned_grad, -1, 0), moved(turned_grad, 2, 0)
-    )
-    kv_back = (moved(kv_left, 0, -1), moved(kv_right, 0, 1), moved(kv_far, 0, 2))
+    grads = [traded(turned_grad, "z", n) for n in range(1, SIDE)]
+    kv_back = [traded(x, "y", n) for n, x in enumerate(results[6:9], 1)]
     square = shape(ROWS, ROWS)
-    own, to_plus, to_minus, to_far = call(
+    own, *parts = call(
         project_kernel,
         (shape(ROWS, ROWS, dtype=F32), square, square, square),
         0,
@@ -554,13 +531,13 @@
         9,
         [pltpu.VMEM((WIDE, WIDE), BF)],
         2 * WIDE * WIDE * ROWS,
-    )(*grads, lat_own, near, near_swap, apart, apart_swap)
+    )(turned_grad, *grads, lat_own, near, near_swap, apart, apart_swap)
     query_rows, key_rows, value_rows = call(
         keys_kernel, (shape(2 * ROWS, 128),) * 3, 0, 0, 9, [pltpu.VMEM((ROWS, 128), F32)] * 2, 10**7
     )(own_k, own_v, *kv_back, *z_back, turned_grad)
-    weight_grad = call(total_kernel, shape(ROWS, ROWS, dtype=F32), 0, 0, 4, [], 10**6)(
-        own, moved(to_plus, 0, 1), moved(to_minus, 0, -1), moved(to_far, 0, 2)
-    )
+    weight_grad = call(
+        total_kernel, shape(ROWS, ROWS, dtype=F32), 0, 0, 4, [], 10**6
+    )(own, *[traded(x, "y", n) for n, x in enumerate(parts, 1)])
     whole = (ROWS, 2, 128)
     return (
         query_rows.reshape(whole),

time: 79.3 us -> 82 us (1.034)
  starting transfers between devices: 29.6 us -> 36.9 us
  waiting for transfers between devices: 31.2 us -> 27.2 us
    ppermute x24 -> x23, starting transfers between devices: 29.5 us -> 36.9 us  [the longest x22 34.8 us: traded(): return lax.ppermute(x, 'sp', [(s, s ^ step) for s in range(SIDE * SIDE)])]
    ppermute x24 -> x23, waiting for transfers between devices: 31.2 us -> 27.2 us  [the longest x22 27.2 us: traded(): return lax.ppermute(x, 'sp', [(s, s ^ step) for s in range(SIDE * SIDE)])]
  transfers between devices with their start and end apart: 26 -> 25, of which waited for: 13 -> 12; matrix products, arithmetic and copies ran while one was open for 0% -> 0% of each run, Pallas kernels for 20% -> 18%
where the time goes in v2:
time: 82 us; the launch traced here: 81.9 us
  starting transfers between devices  36.9 us (45%)
  waiting for transfers between devices  27.2 us (33%)
  Pallas kernels  17.1 us (21%)
    ppermute x22, starting transfers between devices, traded(): return lax.ppermute(x, 'sp', [(s, s ^ step) for s in range(SIDE * SIDE)])  34.8 us
    ppermute x22, waiting for transfers between devices, traded(): return lax.ppermute(x, 'sp', [(s, s ^ step) for s in range(SIDE * SIDE)])  27.2 us
    pallas_call x7, Pallas kernels, run(): return calling(*arrays[:scalars], *held, *arrays[scalars + hbm:])  17.1 us
    ppermute x1, starting transfers between devices, traded_apart(): return lax.ppermute(x, ('sp', 'tp'), pairs)  2.11 us
  transfers between devices with their start and end apart: 25, of which 12 were waited for; matrix products, arithmetic and copies ran while one was open for 0% of the time, Pallas kernels for 18%

profile of v2, /device:TPU:0, one launch (start us, length us, event | category | flops | bytes accessed | tf_op | source)
XLA Modules:
  0.0 81.9 jit_solution(9614257745284026783)
XLA Ops:
  0.6 0.0 copy-start
  0.6 1.3 %shard_map.124 = (bf16[256,1024]{1,0:T(8,128)(2,1)S(1)}, bf16[256,1024]{1,0:T(8,128)(2,1)S(1)}, bf16[128,1024]{1,0:T(8,128)(2,1)S(1)}) custom-call(bf16[256,4096]{1,0:T(8,128)(2,1)} %lat_hbm.1), custom_call_target="tpu_custom_call" | custom-call | flops 10000000 | bytes 1000000 | tf_op jit(solution)/shard_map/pallas_call | solution.py:431
  2.0 2.1 %collective-permute-start.18 = (bf16[256,1024]{1,0:T(8,128)(2,1)S(1)}, bf16[256,1024]{1,0:T(8,128)(2,1)S(1)}, u32[]{:S(2)}, u32[]{:S(2)}) collective-permute-start(bf16[256,1024]{1,0:T(8,128)(2,1)S(1)} %get-tuple-element.52), channel_id=1, source_target_pairs={{0,32},{1,97},{2,34},{3,99},{4,36},{5,101},{6,38},{7,103},{8,40},{... | collective-permute-start | bytes 1572872 | tf_op jit(solution)/shard_map/ppermute | solution.py:402
  4.1 2.0 %shard_map.120 = (bf16[1056,128]{1,0:T(8,128)(2,1)S(1)}, bf16[1056,128]{1,0:T(8,128)(2,1)S(1)}, bf16[544,128]{1,0:T(8,128)(2,1)S(1)}, bf16[544,128]{1,0:T(8,128)(2,1)S(1)}, bf16[544,128]{1,0:T(8,128)(2,1)S(1)}) custom-call(bf16[512,128]{1,0:T(8,128)(2,1)} %bitcast.11, bf16[512,128]{1,0:T(8,128)(2,1)} %bitcast.12, bf16[512,128]{1,0:T(8,128)(2,1)} %bitcast.13, ...), custom_call_target="tpu_custom_call" | custom-call | flops 100000000 | bytes 1000000 | tf_op jit(solution)/shard_map/pallas_call | solution.py:431
  6.1 0.1 collective-permute-start.3
  6.2 4.0 %collective-permute-start.4 = (bf16[544,128]{1,0:T(8,128)(2,1)S(1)}, bf16[544,128]{1,0:T(8,128)(2,1)S(1)}, u32[]{:S(2)}, u32[]{:S(2)}) collective-permute-start(bf16[544,128]{1,0:T(8,128)(2,1)S(1)} %get-tuple-element.34), channel_id=1, source_target_pairs={{0,64},{8,72},{16,80},{24,88},{32,96},{40,104},{48,112},{56,120},{... | collective-permute-start | bytes 417800 | tf_op jit(solution)/shard_map/ppermute | solution.py:392
  10.2 0.7 collective-permute-start.5
  10.9 3.0 %collective-permute-start.2 = (bf16[1056,128]{1,0:T(8,128)(2,1)S(1)}, bf16[1056,128]{1,0:T(8,128)(2,1)S(1)}, u32[]{:S(2)}, u32[]{:S(2)}) collective-permute-start(bf16[1056,128]{1,0:T(8,128)(2,1)S(1)} %get-tuple-element.31.yown), channel_id=1, source_target_pairs={{0,24},{8,16},{16,8},{24,0},{32,56},{40,48},{48,40},{56,32},{64,88... | collective-permute-start | bytes 811016 | tf_op jit(solution)/shard_map/ppermute | solution.py:392
  13.9 1.4 %collective-permute-done.3.z1 = bf16[544,128]{1,0:T(8,128)(2,1)S(1)} collective-permute-done((bf16[544,128]{1,0:T(8,128)(2,1)S(1)}, bf16[544,128]{1,0:T(8,128)(2,1)S(1)}, u32[]{:S(2)}, u32[]{:S(2)}) %collective-permute-start.3) | collective-permute-done | bytes 139296 | tf_op jit(solution)/shard_map/ppermute | solution.py:392
  15.3 3.2 %collective-permute-start.1 = (bf16[1056,128]{1,0:T(8,128)(2,1)S(1)}, bf16[1056,128]{1,0:T(8,128)(2,1)S(1)}, u32[]{:S(2)}, u32[]{:S(2)}) collective-permute-start(bf16[1056,128]{1,0:T(8,128)(2,1)S(1)} %get-tuple-element.31.yown), channel_id=1, source_target_pairs={{0,16},{8,24},{16,0},{24,8},{32,48},{40,56},{48,32},{56,40},{64,80... | collective-permute-start | bytes 811016 | tf_op jit(solution)/shard_map/ppermute | solution.py:392
  18.5 2.3 %collective-permute-done.4.z2 = bf16[544,128]{1,0:T(8,128)(2,1)S(1)} collective-permute-done((bf16[544,128]{1,0:T(8,128)(2,1)S(1)}, bf16[544,128]{1,0:T(8,128)(2,1)S(1)}, u32[]{:S(2)}, u32[]{:S(2)}) %collective-permute-start.4) | collective-permute-done | bytes 139296 | tf_op jit(solution)/shard_map/ppermute | solution.py:392
  20.8 1.6 %collective-permute-start = (bf16[1056,128]{1,0:T(8,128)(2,1)S(1)}, bf16[1056,128]{1,0:T(8,128)(2,1)S(1)}, u32[]{:S(2)}, u32[]{:S(2)}) collective-permute-start(bf16[1056,128]{1,0:T(8,128)(2,1)S(1)} %get-tuple-element.31.yown), channel_id=1, source_target_pairs={{0,8},{8,0},{16,24},{24,16},{32,40},{40,32},{48,56},{56,48},{64,72... | collective-permute-start | bytes 811016 | tf_op jit(solution)/shard_map/ppermute | solution.py:392
  22.4 0.0 collective-permute-done.5.z3
  22.4 1.2 %collective-permute-start.20 = (bf16[128,1024]{1,0:T(8,128)(2,1)S(1)}, bf16[128,1024]{1,0:T(8,128)(2,1)S(1)}, u32[]{:S(2)}, u32[]{:S(2)}) collective-permute-start(bf16[128,1024]{1,0:T(8,128)(2,1)S(1)} %get-tuple-element.53), channel_id=1, source_target_pairs={{0,64},{8,72},{16,80},{24,88},{32,96},{40,104},{48,112},{56,120},{... | collective-permute-start | bytes 786440 | tf_op jit(solution)/shard_map/ppermute | solution.py:392
  23.6 6.7 %collective-permute-done.20.far = bf16[128,1024]{1,0:T(8,128)(2,1)S(1)} collective-permute-done((bf16[128,1024]{1,0:T(8,128)(2,1)S(1)}, bf16[128,1024]{1,0:T(8,128)(2,1)S(1)}, u32[]{:S(2)}, u32[]{:S(2)}) %collective-permute-start.20) | collective-permute-done | bytes 262176 | tf_op jit(solution)/shard_map/ppermute | solution.py:392
  30.3 0.0 collective-permute-done.2.y3
  30.3 0.0 collective-permute-done.1.y2
  30.3 0.0 collective-permute-done.y1
  30.3 10.8 %shard_map.121 = (bf16[256,128]{1,0:T(8,128)(2,1)S(1)}, bf16[256,128]{1,0:T(8,128)(2,1)S(1)}, bf16[256,128]{1,0:T(8,128)(2,1)S(1)}, bf16[512,128]{1,0:T(8,128)(2...) custom-call(f32[2]{0:T(128)S(1)} %copy-done, ...), custom_call_target="tpu_custom_call" | custom-call | flops 1426063360 | bytes 1000000 | tf_op jit(solution)/shard_map/pallas_call | solution.py:431
  41.1 0.7 collective-permute-start.12
  41.8 3.0 %collective-permute-start.13 = (bf16[256,128]{1,0:T(8,128)(2,1)S(1)}, bf16[256,128]{1,0:T(8,128)(2,1)S(1)}, u32[]{:S(2)}, u32[]{:S(2)}) collective-permute-start(bf16[256,128]{1,0:T(8,128)(2,1)S(1)} %get-tuple-element.46), channel_id=1, source_target_pairs={{0,16},{8,24},{16,0},{24,8},{32,48},{40,56},{48,32},{56,40},{64,80... | collective-permute-start | bytes 196616 | tf_op jit(solution)/shard_map/ppermute | solution.py:392
  44.8 1.1 %collective-permute-start.14 = (bf16[256,128]{1,0:T(8,128)(2,1)S(1)}, bf16[256,128]{1,0:T(8,128)(2,1)S(1)}, u32[]{:S(2)}, u32[]{:S(2)}) collective-permute-start(bf16[256,128]{1,0:T(8,128)(2,1)S(1)} %get-tuple-element.47), channel_id=1, source_target_pairs={{0,24},{8,16},{16,8},{24,0},{32,56},{40,48},{48,40},{56,32},{64,88... | collective-permute-start | bytes 196616 | tf_op jit(solution)/shard_map/ppermute | solution.py:392
  45.9 0.0 collective-permute-start.9
  45.9 2.8 %collective-permute-done.13.y2 = bf16[256,128]{1,0:T(8,128)(2,1)S(1)} collective-permute-done((bf16[256,128]{1,0:T(8,128)(2,1)S(1)}, bf16[256,128]{1,0:T(8,128)(2,1)S(1)}, u32[]{:S(2)}, u32[]{:S(2)}) %collective-permute-start.13) | collective-permute-done | bytes 65568 | tf_op jit(solution)/shard_map/ppermute | solution.py:392
  48.7 0.8 %collective-permute-start.10 = (bf16[512,128]{1,0:T(8,128)(2,1)S(1)}, bf16[512,128]{1,0:T(8,128)(2,1)S(1)}, u32[]{:S(2)}, u32[]{:S(2)}) collective-permute-start(bf16[512,128]{1,0:T(8,128)(2,1)S(1)} %get-tuple-element.42), channel_id=1, source_target_pairs={{0,64},{8,72},{16,80},{24,88},{32,96},{40,104},{48,112},{56,120},{... | collective-permute-start | bytes 393224 | tf_op jit(solution)/shard_map/ppermute | solution.py:392
  49.6 0.8 collective-permute-done.14.y3
  50.3 2.0 %collective-permute-start.11 = (bf16[512,128]{1,0:T(8,128)(2,1)S(1)}, bf16[512,128]{1,0:T(8,128)(2,1)S(1)}, u32[]{:S(2)}, u32[]{:S(2)}) collective-permute-start(bf16[512,128]{1,0:T(8,128)(2,1)S(1)} %get-tuple-element.43), channel_id=1, source_target_pairs={{0,96},{8,104},{16,112},{24,120},{32,64},{40,72},{48,80},{56,88},{... | collective-permute-start | bytes 393224 | tf_op jit(solution)/shard_map/ppermute | solution.py:392
  52.3 3.0 %collective-permute-done.10.z2 = bf16[512,128]{1,0:T(8,128)(2,1)S(1)} collective-permute-done((bf16[512,128]{1,0:T(8,128)(2,1)S(1)}, bf16[512,128]{1,0:T(8,128)(2,1)S(1)}, u32[]{:S(2)}, u32[]{:S(2)}) %collective-permute-start.10) | collective-permute-done | bytes 131104 | tf_op jit(solution)/shard_map/ppermute | solution.py:392
  55.4 2.7 %collective-permute-done.11.z3 = bf16[512,128]{1,0:T(8,128)(2,1)S(1)} collective-permute-done((bf16[512,128]{1,0:T(8,128)(2,1)S(1)}, bf16[512,128]{1,0:T(8,128)(2,1)S(1)}, u32[]{:S(2)}, u32[]{:S(2)}) %collective-permute-start.11) | collective-permute-done | bytes 131104 | tf_op jit(solution)/shard_map/ppermute | solution.py:392
  58.1 0.1 shard_map.122.turned_in.g0
  58.2 2.1 %collective-permute-start.17 = (bf16[256,256]{1,0:T(8,128)(2,1)S(1)}, bf16[256,256]{1,0:T(8,128)(2,1)S(1)}, u32[]{:S(2)}, u32[]{:S(2)}) collective-permute-start(bf16[256,256]{1,0:T(8,128)(2,1)S(1)} %shard_map.122.turned_in.g0), channel_id=1, source_target_pairs={{0,96},{8,104},{16,112},{24,120},{32,64},{40,72},{48,80},{56,88},{... | collective-permute-start | bytes 393224 | tf_op jit(solution)/shard_map/ppermute | solution.py:392
  60.3 2.1 %collective-permute-start.15 = (bf16[256,256]{1,0:T(8,128)(2,1)S(1)}, bf16[256,256]{1,0:T(8,128)(2,1)S(1)}, u32[]{:S(2)}, u32[]{:S(2)}) collective-permute-start(bf16[256,256]{1,0:T(8,128)(2,1)S(1)} %shard_map.122.turned_in.g0), channel_id=1, source_target_pairs={{0,32},{8,40},{16,48},{24,56},{32,0},{40,8},{48,16},{56,24},{64,96... | collective-permute-start | bytes 393224 | tf_op jit(solution)/shard_map/ppermute | solution.py:392
  62.3 0.0 collective-permute-done.21.far_swap
  62.3 0.7 collective-permute-start.6
  63.0 4.2 %collective-permute-done.17.g3 = bf16[256,256]{1,0:T(8,128)(2,1)S(1)} collective-permute-done((bf16[256,256]{1,0:T(8,128)(2,1)S(1)}, bf16[256,256]{1,0:T(8,128)(2,1)S(1)}, u32[]{:S(2)}, u32[]{:S(2)}) %collective-permute-start.17) | collective-permute-done | bytes 131104 | tf_op jit(solution)/shard_map/ppermute | solution.py:392
  67.2 0.8 collective-permute-start.7
  68.0 0.1 collective-permute-done.16.g2
  68.1 2.9 %collective-permute-start.8 = (bf16[512,128]{1,0:T(8,128)(2,1)S(1)}, bf16[512,128]{1,0:T(8,128)(2,1)S(1)}, u32[]{:S(2)}, u32[]{:S(2)}) collective-permute-start(bf16[512,128]{1,0:T(8,128)(2,1)S(1)} %get-tuple-element.40), channel_id=1, source_target_pairs={{0,24},{8,16},{16,8},{24,0},{32,56},{40,48},{48,40},{56,32},{64,88... | collective-permute-start | bytes 393224 | tf_op jit(solution)/shard_map/ppermute | solution.py:392
  71.1 0.9 %shard_map.125 = (f32[256,256]{1,0:T(8,128)S(1)}, bf16[256,256]{1,0:T(8,128)(2,1)S(1)}, bf16[256,256]{1,0:T(8,128)(2,1)S(1)}, bf16[256,256]{1,0:T(8,128)(2,1)S(1)}) custom-call(bf16[256,256]{1,0:T(8,128)(2,1)S(1)} %shard_map.122.turned_in.g0, bf16[256,256]{1,0:T(8,128)(2,1)S(1)} %collective-permute-done.15.g1, ...), custom_call_target="tpu_custom_call" | custom-call | flops 536870912 | bytes 1000000 | tf_op jit(solution)/shard_map/pallas_call | solution.py:431
  71.9 0.1 collective-permute-start.22
  72.0 1.8 %collective-permute-start.23 = (bf16[256,256]{1,0:T(8,128)(2,1)S(1)}, bf16[256,256]{1,0:T(8,128)(2,1)S(1)}, u32[]{:S(2)}, u32[]{:S(2)}) collective-permute-start(bf16[256,256]{1,0:T(8,128)(2,1)S(1)} %get-tuple-element.56), channel_id=1, source_target_pairs={{0,16},{8,24},{16,0},{24,8},{32,48},{40,56},{48,32},{56,40},{64,80... | collective-permute-start | bytes 393224 | tf_op jit(solution)/shard_map/ppermute | solution.py:392
  73.8 2.9 %collective-permute-start.24 = (bf16[256,256]{1,0:T(8,128)(2,1)S(1)}, bf16[256,256]{1,0:T(8,128)(2,1)S(1)}, u32[]{:S(2)}, u32[]{:S(2)}) collective-permute-start(bf16[256,256]{1,0:T(8,128)(2,1)S(1)} %get-tuple-element.57), channel_id=1, source_target_pairs={{0,24},{8,16},{16,8},{24,0},{32,56},{40,48},{48,40},{56,32},{64,88... | collective-permute-start | bytes 393224 | tf_op jit(solution)/shard_map/ppermute | solution.py:392
  76.7 0.0 collective-permute-done.7.y2
  76.7 0.2 collective-permute-done.8.y3
  76.9 1.1 %shard_map.123 = (bf16[512,128]{1,0:T(8,128)(2,1)}, bf16[512,128]{1,0:T(8,128)(2,1)}, bf16[512,128]{1,0:T(8,128)(2,1)}) custom-call(f32[2,256,128]{2,1,0:T(8,128)S(1)} %get-tuple-element.36.own_k, f32[2,256,128]{2,1,0:T(8,128)S(1)} %get-tuple-element.37.own_v, bf16[512,128]{1,0:T(8,128)(2,1)S(1)} %collective-permute-done.6.y1, ...), custom_call_target="tpu_custom_call" | custom-call | flops 10000000 | bytes 1000000 | tf_op jit(solution)/shard_map/pallas_call | solution.py:431
  78.1 1.1 %collective-permute-done.23.t2 = bf16[256,256]{1,0:T(8,128)(2,1)S(1)} collective-permute-done((bf16[256,256]{1,0:T(8,128)(2,1)S(1)}, bf16[256,256]{1,0:T(8,128)(2,1)S(1)}, u32[]{:S(2)}, u32[]{:S(2)}) %collective-permute-start.23) | collective-permute-done | bytes 131104 | tf_op jit(solution)/shard_map/ppermute | solution.py:392
  79.2 1.8 %collective-permute-done.24.t3 = bf16[256,256]{1,0:T(8,128)(2,1)S(1)} collective-permute-done((bf16[256,256]{1,0:T(8,128)(2,1)S(1)}, bf16[256,256]{1,0:T(8,128)(2,1)S(1)}, u32[]{:S(2)}, u32[]{:S(2)}) %collective-permute-start.24) | collective-permute-done | bytes 131104 | tf_op jit(solution)/shard_map/ppermute | solution.py:392
  81.0 0.8 %shard_map.126 = f32[256,256]{1,0:T(8,128)} custom-call(f32[256,256]{1,0:T(8,128)S(1)} %get-tuple-element.54.own, bf16[256,256]{1,0:T(8,128)(2,1)S(1)} %collective-permute-done.22.t1, bf16[256,256]{1,0:T(8,128)(2,1)S(1)} %collective-permute-done.23.t2, bf16[256,256]{1,0:T(8,128)(2,1)S(1)} %collective-permute-done.24.t3), custom_call_target="tpu_custom_call" | custom-call | flops 1000000 | bytes 1000000 | tf_op jit(solution)/shard_map/pallas_call | solution.py:431
  (11 shorter events, 0.0 us)
Async XLA Ops:
  0.6 29.6 %copy-start = (f32[2]{0:T(128)S(1)}, f32[2]{0:T(128)}, u32[]{:S(2)}) copy-start(f32[2]{0:T(128)} %lam.1) | copy-start | bytes 28
  2.0 21.6 %collective-permute-start.18 = (bf16[256,1024]{1,0:T(8,128)(2,1)S(1)}, bf16[256,1024]{1,0:T(8,128)(2,1)S(1)}, u32[]{:S(2)}, u32[]{:S(2)}) collective-permute-start(bf16[256,1024]{1,0:T(8,128)(2,1)S(1)} %get-tuple-element.52), channel_id=1, source_target_pairs={{0,32},{1,97},{2,34},{3,99},{4,36},{5,101},{6,38},{7,103},{8,40},{... | collective-permute-start | bytes 1572872 | tf_op jit(solution)/shard_map/ppermute | solution.py:402
  6.1 9.2 %collective-permute-start.3 = (bf16[544,128]{1,0:T(8,128)(2,1)S(1)}, bf16[544,128]{1,0:T(8,128)(2,1)S(1)}, u32[]{:S(2)}, u32[]{:S(2)}) collective-permute-start(bf16[544,128]{1,0:T(8,128)(2,1)S(1)} %get-tuple-element.33), channel_id=1, source_target_pairs={{0,32},{8,40},{16,48},{24,56},{32,0},{40,8},{48,16},{56,24},{64,96... | collective-permute-start | bytes 417800 | tf_op jit(solution)/shard_map/ppermute | solution.py:392
  6.2 14.6 %collective-permute-start.4 = (bf16[544,128]{1,0:T(8,128)(2,1)S(1)}, bf16[544,128]{1,0:T(8,128)(2,1)S(1)}, u32[]{:S(2)}, u32[]{:S(2)}) collective-permute-start(bf16[544,128]{1,0:T(8,128)(2,1)S(1)} %get-tuple-element.34), channel_id=1, source_target_pairs={{0,64},{8,72},{16,80},{24,88},{32,96},{40,104},{48,112},{56,120},{... | collective-permute-start | bytes 417800 | tf_op jit(solution)/shard_map/ppermute | solution.py:392
  10.2 12.2 %collective-permute-start.5 = (bf16[544,128]{1,0:T(8,128)(2,1)S(1)}, bf16[544,128]{1,0:T(8,128)(2,1)S(1)}, u32[]{:S(2)}, u32[]{:S(2)}) collective-permute-start(bf16[544,128]{1,0:T(8,128)(2,1)S(1)} %get-tuple-element.35), channel_id=1, source_target_pairs={{0,96},{8,104},{16,112},{24,120},{32,64},{40,72},{48,80},{56,88},{... | collective-permute-start | bytes 417800 | tf_op jit(solution)/shard_map/ppermute | solution.py:392
  10.9 19.4 %collective-permute-start.2 = (bf16[1056,128]{1,0:T(8,128)(2,1)S(1)}, bf16[1056,128]{1,0:T(8,128)(2,1)S(1)}, u32[]{:S(2)}, u32[]{:S(2)}) collective-permute-start(bf16[1056,128]{1,0:T(8,128)(2,1)S(1)} %get-tuple-element.31.yown), channel_id=1, source_target_pairs={{0,24},{8,16},{16,8},{24,0},{32,56},{40,48},{48,40},{56,32},{64,88... | collective-permute-start | bytes 811016 | tf_op jit(solution)/shard_map/ppermute | solution.py:392
  15.3 15.0 %collective-permute-start.1 = (bf16[1056,128]{1,0:T(8,128)(2,1)S(1)}, bf16[1056,128]{1,0:T(8,128)(2,1)S(1)}, u32[]{:S(2)}, u32[]{:S(2)}) collective-permute-start(bf16[1056,128]{1,0:T(8,128)(2,1)S(1)} %get-tuple-element.31.yown), channel_id=1, source_target_pairs={{0,16},{8,24},{16,0},{24,8},{32,48},{40,56},{48,32},{56,40},{64,80... | collective-permute-start | bytes 811016 | tf_op jit(solution)/shard_map/ppermute | solution.py:392
  20.8 9.5 %collective-permute-start = (bf16[1056,128]{1,0:T(8,128)(2,1)S(1)}, bf16[1056,128]{1,0:T(8,128)(2,1)S(1)}, u32[]{:S(2)}, u32[]{:S(2)}) collective-permute-start(bf16[1056,128]{1,0:T(8,128)(2,1)S(1)} %get-tuple-element.31.yown), channel_id=1, source_target_pairs={{0,8},{8,0},{16,24},{24,16},{32,40},{40,32},{48,56},{56,48},{64,72... | collective-permute-start | bytes 811016 | tf_op jit(solution)/shard_map/ppermute | solution.py:392
  22.4 7.9 %collective-permute-start.20 = (bf16[128,1024]{1,0:T(8,128)(2,1)S(1)}, bf16[128,1024]{1,0:T(8,128)(2,1)S(1)}, u32[]{:S(2)}, u32[]{:S(2)}) collective-permute-start(bf16[128,1024]{1,0:T(8,128)(2,1)S(1)} %get-tuple-element.53), channel_id=1, source_target_pairs={{0,64},{8,72},{16,80},{24,88},{32,96},{40,104},{48,112},{56,120},{... | collective-permute-start | bytes 786440 | tf_op jit(solution)/shard_map/ppermute | solution.py:392
  23.6 47.5 %collective-permute-start.19 = (bf16[256,1024]{1,0:T(8,128)(2,1)S(1)}, bf16[256,1024]{1,0:T(8,128)(2,1)S(1)}, u32[]{:S(2)}, u32[]{:S(2)}) collective-permute-start(bf16[256,1024]{1,0:T(8,128)(2,1)S(1)} %collective-permute-done.18.near), channel_id=1, source_target_pairs={{0,1},{1,0},{2,3},{3,2},{4,5},{5,4},{6,7},{7,6},{8,9},{9,8},{10,11... | collective-permute-start | bytes 1572872 | tf_op jit(solution)/shard_map/ppermute | solution.py:406
  30.2 32.1 %collective-permute-start.21 = (bf16[128,1024]{1,0:T(8,128)(2,1)S(1)}, bf16[128,1024]{1,0:T(8,128)(2,1)S(1)}, u32[]{:S(2)}, u32[]{:S(2)}) collective-permute-start(bf16[128,1024]{1,0:T(8,128)(2,1)S(1)} %collective-permute-done.20.far), channel_id=1, source_target_pairs={{0,1},{1,0},{2,3},{3,2},{4,5},{5,4},{6,7},{7,6},{8,9},{9,8},{10,11... | collective-permute-start | bytes 786440 | tf_op jit(solution)/shard_map/ppermute | solution.py:406
  41.1 4.8 %collective-permute-start.12 = (bf16[256,128]{1,0:T(8,128)(2,1)S(1)}, bf16[256,128]{1,0:T(8,128)(2,1)S(1)}, u32[]{:S(2)}, u32[]{:S(2)}) collective-permute-start(bf16[256,128]{1,0:T(8,128)(2,1)S(1)} %get-tuple-element.45), channel_id=1, source_target_pairs={{0,8},{8,0},{16,24},{24,16},{32,40},{40,32},{48,56},{56,48},{64,72... | collective-permute-start | bytes 196616 | tf_op jit(solution)/shard_map/ppermute | solution.py:392
  41.8 6.9 %collective-permute-start.13 = (bf16[256,128]{1,0:T(8,128)(2,1)S(1)}, bf16[256,128]{1,0:T(8,128)(2,1)S(1)}, u32[]{:S(2)}, u32[]{:S(2)}) collective-permute-start(bf16[256,128]{1,0:T(8,128)(2,1)S(1)} %get-tuple-element.46), channel_id=1, source_target_pairs={{0,16},{8,24},{16,0},{24,8},{32,48},{40,56},{48,32},{56,40},{64,80... | collective-permute-start | bytes 196616 | tf_op jit(solution)/shard_map/ppermute | solution.py:392
  44.8 5.5 %collective-permute-start.14 = (bf16[256,128]{1,0:T(8,128)(2,1)S(1)}, bf16[256,128]{1,0:T(8,128)(2,1)S(1)}, u32[]{:S(2)}, u32[]{:S(2)}) collective-permute-start(bf16[256,128]{1,0:T(8,128)(2,1)S(1)} %get-tuple-element.47), channel_id=1, source_target_pairs={{0,24},{8,16},{16,8},{24,0},{32,56},{40,48},{48,40},{56,32},{64,88... | collective-permute-start | bytes 196616 | tf_op jit(solution)/shard_map/ppermute | solution.py:392
  45.9 6.4 %collective-permute-start.9 = (bf16[512,128]{1,0:T(8,128)(2,1)S(1)}, bf16[512,128]{1,0:T(8,128)(2,1)S(1)}, u32[]{:S(2)}, u32[]{:S(2)}) collective-permute-start(bf16[512,128]{1,0:T(8,128)(2,1)S(1)} %get-tuple-element.41), channel_id=1, source_target_pairs={{0,32},{8,40},{16,48},{24,56},{32,0},{40,8},{48,16},{56,24},{64,96... | collective-permute-start | bytes 393224 | tf_op jit(solution)/shard_map/ppermute | solution.py:392
  48.7 6.6 %collective-permute-start.10 = (bf16[512,128]{1,0:T(8,128)(2,1)S(1)}, bf16[512,128]{1,0:T(8,128)(2,1)S(1)}, u32[]{:S(2)}, u32[]{:S(2)}) collective-permute-start(bf16[512,128]{1,0:T(8,128)(2,1)S(1)} %get-tuple-element.42), channel_id=1, source_target_pairs={{0,64},{8,72},{16,80},{24,88},{32,96},{40,104},{48,112},{56,120},{... | collective-permute-start | bytes 393224 | tf_op jit(solution)/shard_map/ppermute | solution.py:392
  50.3 7.8 %collective-permute-start.11 = (bf16[512,128]{1,0:T(8,128)(2,1)S(1)}, bf16[512,128]{1,0:T(8,128)(2,1)S(1)}, u32[]{:S(2)}, u32[]{:S(2)}) collective-permute-start(bf16[512,128]{1,0:T(8,128)(2,1)S(1)} %get-tuple-element.43), channel_id=1, source_target_pairs={{0,96},{8,104},{16,112},{24,120},{32,64},{40,72},{48,80},{56,88},{... | collective-permute-start | bytes 393224 | tf_op jit(solution)/shard_map/ppermute | solution.py:392
  58.2 9.0 %collective-permute-start.17 = (bf16[256,256]{1,0:T(8,128)(2,1)S(1)}, bf16[256,256]{1,0:T(8,128)(2,1)S(1)}, u32[]{:S(2)}, u32[]{:S(2)}) collective-permute-start(bf16[256,256]{1,0:T(8,128)(2,1)S(1)} %shard_map.122.turned_in.g0), channel_id=1, source_target_pairs={{0,96},{8,104},{16,112},{24,120},{32,64},{40,72},{48,80},{56,88},{... | collective-permute-start | bytes 393224 | tf_op jit(solution)/shard_map/ppermute | solution.py:392
  60.3 7.9 %collective-permute-start.16 = (bf16[256,256]{1,0:T(8,128)(2,1)S(1)}, bf16[256,256]{1,0:T(8,128)(2,1)S(1)}, u32[]{:S(2)}, u32[]{:S(2)}) collective-permute-start(bf16[256,256]{1,0:T(8,128)(2,1)S(1)} %shard_map.122.turned_in.g0), channel_id=1, source_target_pairs={{0,64},{8,72},{16,80},{24,88},{32,96},{40,104},{48,112},{56,120},{... | collective-permute-start | bytes 393224 | tf_op jit(solution)/shard_map/ppermute | solution.py:392
  60.3 10.8 %collective-permute-start.15 = (bf16[256,256]{1,0:T(8,128)(2,1)S(1)}, bf16[256,256]{1,0:T(8,128)(2,1)S(1)}, u32[]{:S(2)}, u32[]{:S(2)}) collective-permute-start(bf16[256,256]{1,0:T(8,128)(2,1)S(1)} %shard_map.122.turned_in.g0), channel_id=1, source_target_pairs={{0,32},{8,40},{16,48},{24,56},{32,0},{40,8},{48,16},{56,24},{64,96... | collective-permute-start | bytes 393224 | tf_op jit(solution)/shard_map/ppermute | solution.py:392
  62.3 11.5 %collective-permute-start.6 = (bf16[512,128]{1,0:T(8,128)(2,1)S(1)}, bf16[512,128]{1,0:T(8,128)(2,1)S(1)}, u32[]{:S(2)}, u32[]{:S(2)}) collective-permute-start(bf16[512,128]{1,0:T(8,128)(2,1)S(1)} %get-tuple-element.38), channel_id=1, source_target_pairs={{0,8},{8,0},{16,24},{24,16},{32,40},{40,32},{48,56},{56,48},{64,72... | collective-permute-start | bytes 393224 | tf_op jit(solution)/shard_map/ppermute | solution.py:392
  67.2 9.5 %collective-permute-start.7 = (bf16[512,128]{1,0:T(8,128)(2,1)S(1)}, bf16[512,128]{1,0:T(8,128)(2,1)S(1)}, u32[]{:S(2)}, u32[]{:S(2)}) collective-permute-start(bf16[512,128]{1,0:T(8,128)(2,1)S(1)} %get-tuple-element.39), channel_id=1, source_target_pairs={{0,16},{8,24},{16,0},{24,8},{32,48},{40,56},{48,32},{56,40},{64,80... | collective-permute-start | bytes 393224 | tf_op jit(solution)/shard_map/ppermute | solution.py:392
  68.1 8.8 %collective-permute-start.8 = (bf16[512,128]{1,0:T(8,128)(2,1)S(1)}, bf16[512,128]{1,0:T(8,128)(2,1)S(1)}, u32[]{:S(2)}, u32[]{:S(2)}) collective-permute-start(bf16[512,128]{1,0:T(8,128)(2,1)S(1)} %get-tuple-element.40), channel_id=1, source_target_pairs={{0,24},{8,16},{16,8},{24,0},{32,56},{40,48},{48,40},{56,32},{64,88... | collective-permute-start | bytes 393224 | tf_op jit(solution)/shard_map/ppermute | solution.py:392
  71.9 6.2 %collective-permute-start.22 = (bf16[256,256]{1,0:T(8,128)(2,1)S(1)}, bf16[256,256]{1,0:T(8,128)(2,1)S(1)}, u32[]{:S(2)}, u32[]{:S(2)}) collective-permute-start(bf16[256,256]{1,0:T(8,128)(2,1)S(1)} %get-tuple-element.55), channel_id=1, source_target_pairs={{0,8},{8,0},{16,24},{24,16},{32,40},{40,32},{48,56},{56,48},{64,72... | collective-permute-start | bytes 393224 | tf_op jit(solution)/shard_map/ppermute | solution.py:392
  72.0 7.2 %collective-permute-start.23 = (bf16[256,256]{1,0:T(8,128)(2,1)S(1)}, bf16[256,256]{1,0:T(8,128)(2,1)S(1)}, u32[]{:S(2)}, u32[]{:S(2)}) collective-permute-start(bf16[256,256]{1,0:T(8,128)(2,1)S(1)} %get-tuple-element.56), channel_id=1, source_target_pairs={{0,16},{8,24},{16,0},{24,8},{32,48},{40,56},{48,32},{56,40},{64,80... | collective-permute-start | bytes 393224 | tf_op jit(solution)/shard_map/ppermute | solution.py:392
  73.8 7.2 %collective-permute-start.24 = (bf16[256,256]{1,0:T(8,128)(2,1)S(1)}, bf16[256,256]{1,0:T(8,128)(2,1)S(1)}, u32[]{:S(2)}, u32[]{:S(2)}) collective-permute-start(bf16[256,256]{1,0:T(8,128)(2,1)S(1)} %get-tuple-element.57), channel_id=1, source_target_pairs={{0,24},{8,16},{16,8},{24,0},{32,56},{40,48},{48,40},{56,32},{64,88... | collective-permute-start | bytes 393224 | tf_op jit(solution)/shard_map/ppermute | solution.py:392

commit v3 on v2

--- a/solution.py
+++ b/solution.py
@@ -153,123 +153,147 @@
         copy.wait()
 
 
-def attend_kernel(
-    lam, yown, y1, y2, y3, zown, z1, z2, z3,
+def ready(slot, buf, stat, kpad, kturn, qpad, dq, dk, dv):
+    row = iota((128, 128), 0)
+    col = iota((128, 128), 1)
+    lane = iota((ROWS, 128), 1)
+    q = buf[slot, 0:ROWS]
+    k = buf[slot, QG : QG + ROWS]
+    zero = jnp.zeros_like(q)
+    qpad[slot, 0:ROWS] = jnp.where(lane < DH, q, zero)
+    qpad[slot, ROWS:] = jnp.where(lane < DH, zero, q)
+    kpad[slot, 0:ROWS] = jnp.where(lane < DH, k, zero)
+    kpad[slot, ROWS:] = jnp.where(lane < DH, zero, k)
+    eye_first = one_hot(jnp.logical_and(row == col, row < DH))
+    eye_second = one_hot(jnp.logical_and(row == col, row >= DH))
+    kturn[slot, :, 0:ROWS] = turned(eye_first, k).astype(BF)
+    kturn[slot, :, ROWS:] = turned(eye_second, k).astype(BF)
+    left = buf[slot, 2 * ROWS : 2 * ROWS + 16].astype(F32)
+    right = buf[slot, 2 * ROWS + 16 : QG].astype(F32)
+    pieces = jnp.concatenate([left, right], axis=1)
+    rows = pieces[0:4] + pieces[4:8] + pieces[8:12]
+    stat[slot, 0:2] = rows[0:2] * LOG2E
+    stat[slot, 2:4] = rows[2:4]
+    dq[slot] = jnp.zeros((128, ROWS), F32)
+    dk[slot] = jnp.zeros((ROWS, 128), F32)
+    dv[slot] = jnp.zeros((ROWS, 128), F32)
+
+
+def take(z, n, ref, buf):
+    keys = jnp.bitwise_xor(z, n) < z
+
+    @pl.when(keys)
+    def _():
+        buf[SIDE + n, QG:SLOT] = ref[0 : 2 * ROWS]
+
+    @pl.when(jnp.logical_not(keys))
+    def _():
+        buf[SIDE + n, 0:QG] = ref[...]
+
+
+def run_pairs(items, z, y, lam, state, wide_w, tall_s):
+    buf, stat, kpad, kturn, qpad, dq, dk, dv = state
+
+    def slots_of(item):
+        zslot, yslot, kind = item
+        if kind is None:
+            if zslot == SIDE:
+                kind = 1 - (jnp.bitwise_xor(y, yslot) < y).astype(jnp.int32)
+            else:
+                kind = (jnp.bitwise_xor(z, zslot - SIDE) < z).astype(jnp.int32)
+            qs = jnp.where(kind == 0, zslot, yslot)
+            return qs, zslot + yslot - qs, kind
+        return (zslot, yslot, kind) if kind == 0 else (yslot, zslot, kind)
+
+    slots = [slots_of(item) for item in items]
+
+    def dots(n):
+        qs, ks, _ = slots[n]
+        q = buf[qs, 0:ROWS]
+        g = buf[qs, ROWS : 2 * ROWS]
+        v = buf[ks, QG + ROWS : SLOT]
+        scores = lax.dot_general(kpad[ks], q, NT, preferred_element_type=F32)
+        mixed = lax.dot_general(v, g, NT, preferred_element_type=F32)
+        return scores, mixed
+
+    def front(n, started):
+        scores, mixed = started
+        qs, _, kind = slots[n]
+        factor = lam[kind]
+        rows = stat[qs]
+        scale = DH ** (-0.5) * LOG2E
+        power1 = scores[0:ROWS] * scale - rows[0:1]
+        power2 = scores[ROWS:] * scale - rows[1:2]
+        if items[n][2] is not None:
+            seen = iota((ROWS, ROWS), 0) <= iota((ROWS, ROWS), 1)
+            gone = jnp.full((ROWS, ROWS), -1e30, F32)
+            power1 = jnp.where(seen, power1, gone)
+            power2 = jnp.where(seen, power2, gone)
+        prob1 = jnp.exp2(power1)
+        prob2 = factor * jnp.exp2(power2)
+        hold = n % 2
+        wide_w[hold] = (prob1 - prob2).astype(BF)
+        tall_s[hold, 0:ROWS] = (prob1 * (mixed - rows[2:3])).astype(BF)
+        tall_s[hold, ROWS:] = (prob2 * (rows[3:4] - mixed)).astype(BF)
+
+    def back(n):
+        qs, ks, _ = slots[n]
+        hold = n % 2
+        weights = wide_w[hold]
+        score1 = tall_s[hold, 0:ROWS]
+        score2 = tall_s[hold, ROWS:]
+        g = buf[qs, ROWS : 2 * ROWS]
+        add_v = exact(weights, g)
+        add_k = exact(jnp.concatenate([score1, score2], axis=1), qpad[qs])
+        add_q = exact(kturn[ks], tall_s[hold])
+        return add_q, add_k, add_v
+
+    front(0, dots(0))
+    for n in range(len(items)):
+        more = n + 1 < len(items)
+        if more:
+            started = dots(n + 1)
+        add_q, add_k, add_v = back(n)
+        if more:
+            front(n + 1, started)
+        qs, ks, _ = slots[n]
+        dv[ks] += add_v
+        dk[ks] += add_k
+        dq[qs] += add_q
+
+
+def attend_near_kernel(
+    lam, yown, y1, y3, zown, z1, z3,
+    buf, stat, kpad, kturn, qpad, dq, dk, dv, wide_w, tall_s,
+):
+    z, y, _ = position()
+    state = (buf, stat, kpad, kturn, qpad, dq, dk, dv)
+    for slot, ref in ((0, yown), (1, y1), (3, y3), (SIDE, zown)):
+        buf[slot] = ref[...]
+    take(z, 1, z1, buf)
+    take(z, 3, z3, buf)
+    for slot in (0, 1, 3, 4, 5, 7):
+        ready(slot, *state)
+    items = [(4, 0, 0), (4, 0, 1)]
+    items += [(4, 1, None), (4, 3, None)]
+    items += [(zslot, yslot, None) for zslot in (5, 7) for yslot in (0, 1, 3)]
+    run_pairs(items, z, y, lam, state, wide_w, tall_s)
+
+
+def attend_far_kernel(
+    lam, y2, z2, buf_in, stat_in, kpad_in, kturn_in, qpad_in, dq_in, dk_in, dv_in,
     q1, q2, q3, r1, r2, r3, kv1, kv2, kv3, own_q, own_k, own_v,
     buf, stat, kpad, kturn, qpad, dq, dk, dv, wide_w, tall_s,
 ):
     z, y, _ = position()
-    for slot, ref in enumerate((yown, y1, y2, y3, zown)):
-        buf[slot] = ref[...]
-    keys_of = [(jnp.bitwise_xor(z, n) < z).astype(jnp.int32) for n in range(1, SIDE)]
-    for slot, (ref, keys) in enumerate(zip((z1, z2, z3), keys_of)):
-        @pl.when(keys == 1)
-        def _():
-            buf[SIDE + 1 + slot, QG:SLOT] = ref[0 : 2 * ROWS]
-
-        @pl.when(keys == 0)
-        def _():
-            buf[SIDE + 1 + slot, 0:QG] = ref[...]
-
-    row = iota((128, 128), 0)
-    col = iota((128, 128), 1)
-    eye_first = one_hot(jnp.logical_and(row == col, row < DH))
-    eye_second = one_hot(jnp.logical_and(row == col, row >= DH))
-
-    def ready(slot, carry):
-        lane = iota((ROWS, 128), 1)
-        q = buf[slot, 0:ROWS]
-        k = buf[slot, QG : QG + ROWS]
-        zero = jnp.zeros_like(q)
-        qpad[slot, 0:ROWS] = jnp.where(lane < DH, q, zero)
-        qpad[slot, ROWS:] = jnp.where(lane < DH, zero, q)
-        kpad[slot, 0:ROWS] = jnp.where(lane < DH, k, zero)
-        kpad[slot, ROWS:] = jnp.where(lane < DH, zero, k)
-        kturn[slot, :, 0:ROWS] = turned(eye_first, k).astype(BF)
-        kturn[slot, :, ROWS:] = turned(eye_second, k).astype(BF)
-        left = buf[slot, 2 * ROWS : 2 * ROWS + 16].astype(F32)
-        right = buf[slot, 2 * ROWS + 16 : QG].astype(F32)
-        pieces = jnp.concatenate([left, right], axis=1)
-        rows = pieces[0:4] + pieces[4:8] + pieces[8:12]
-        stat[slot, 0:2] = rows[0:2] * LOG2E
-        stat[slot, 2:4] = rows[2:4]
-        dq[slot] = jnp.zeros((128, ROWS), F32)
-        dk[slot] = jnp.zeros((ROWS, 128), F32)
-        dv[slot] = jnp.zeros((ROWS, 128), F32)
-        return carry
-
-    lax.fori_loop(0, 2 * SIDE, ready, 0)
-
-    def slots_of(item):
-        own = item < SIDE + 1
-        rest = item - SIDE - 1
-        zslot = jnp.where(own, SIDE, SIDE + 1 + rest // SIDE)
-        yslot = jnp.where(own, jnp.maximum(item - 1, 0), lax.rem(jnp.maximum(rest, 0), SIDE))
-        behind = jnp.where(yslot == 0, item == 0, jnp.bitwise_xor(y, yslot) < y)
-        other = (jnp.bitwise_xor(z, zslot - SIDE) < z).astype(jnp.int32)
-        kind = jnp.where(own, 1 - behind.astype(jnp.int32), other)
-        qs = jnp.where(kind == 0, zslot, yslot)
-        ks = jnp.where(kind == 0, yslot, zslot)
-        return qs, ks, kind
-
-    def front(item):
-        qs, ks, kind = slots_of(item)
-        shift = jnp.where(item < 2, 0, 2 * ROWS)
-        factor = lam[kind]
-        q = buf[qs, 0:ROWS]
-        g = buf[qs, ROWS : 2 * ROWS]
-        v = buf[ks, QG + ROWS : SLOT]
-        rows = stat[qs]
-        scores = lax.dot_general(kpad[ks], q, NT, preferred_element_type=F32)
-        mixed = lax.dot_general(v, g, NT, preferred_element_type=F32)
-        scale = DH ** (-0.5) * LOG2E
-        power1 = scores[0:ROWS] * scale - rows[0:1]
-        power2 = scores[ROWS:] * scale - rows[1:2]
-        seen = iota((ROWS, ROWS), 0) <= iota((ROWS, ROWS), 1) + shift
-        gone = jnp.full((ROWS, ROWS), -1e30, F32)
-        prob1 = jnp.exp2(jnp.where(seen, power1, gone))
-        prob2 = factor * jnp.exp2(jnp.where(seen, power2, gone))
-        weights = (prob1 - prob2).astype(BF)
-        score1 = (prob1 * (mixed - rows[2:3])).astype(BF)
-        score2 = (prob2 * (rows[3:4] - mixed)).astype(BF)
-        return weights, score1, score2
-
-    def keep(values):
-        weights, score1, score2 = values
-        wide_w[...] = weights
-        tall_s[0:ROWS] = score1
-        tall_s[ROWS:] = score2
-
-    def back(item):
-        qs, ks, _ = slots_of(item)
-        weights = wide_w[...]
-        score1 = tall_s[0:ROWS]
-        score2 = tall_s[ROWS:]
-        g = buf[qs, ROWS : 2 * ROWS]
-        add_v = exact(weights, g)
-        add_k = exact(jnp.concatenate([score1, score2], axis=1), qpad[qs])
-        add_q = exact(kturn[ks], jnp.concatenate([score1, score2], axis=0))
-        return qs, ks, add_q, add_k, add_v
-
-    def add(sums):
-        qs, ks, add_q, add_k, add_v = sums
-        dv[ks] += add_v
-        dk[ks] += add_k
-        dq[qs] += add_q
-
-    items = SIDE * SIDE + 1
-    keep(front(0))
-
-    def step(item, carry):
-        sums = back(item)
-        values = front(item + 1)
-        add(sums)
-        keep(values)
-        return carry
-
-    lax.fori_loop(0, items - 1, step, 0)
-    add(back(items - 1))
-
+    state = (buf, stat, kpad, kturn, qpad, dq, dk, dv)
+    buf[2] = y2[...]
+    take(z, 2, z2, buf)
+    for slot in (2, 6):
+        ready(slot, *state)
+    items = [(zslot, 2, None) for zslot in (4, 5, 7)]
+    items += [(6, yslot, None) for yslot in range(SIDE)]
+    run_pairs(items, z, y, lam, state, wide_w, tall_s)
     scale = DH ** (-0.5)
 
     def put_q(ref, slot):
@@ -281,15 +305,17 @@
         put_q(ref, slot + 1)
         kv[0:ROWS] = (dk[slot + 1] * scale).astype(BF)
         kv[ROWS:] = dv[slot + 1].astype(BF)
-    for slot, (ref, keys) in enumerate(zip((r1, r2, r3), keys_of)):
-        @pl.when(keys == 1)
+    for n, ref in enumerate((r1, r2, r3), 1):
+        keys = jnp.bitwise_xor(z, n) < z
+
+        @pl.when(keys)
         def _():
-            ref[0:ROWS] = (dk[SIDE + 1 + slot] * scale).astype(BF)
-            ref[ROWS:] = dv[SIDE + 1 + slot].astype(BF)
-
-        @pl.when(keys == 0)
+            ref[0:ROWS] = (dk[SIDE + n] * scale).astype(BF)
+            ref[ROWS:] = dv[SIDE + n].astype(BF)
+
+        @pl.when(jnp.logical_not(keys))
         def _():
-            put_q(ref, SIDE + 1 + slot)
+            put_q(ref, SIDE + n)
             ref[ROWS:] = jnp.zeros((ROWS, 128), BF)
 
     own_q[0] = dq[SIDE] * scale
@@ -410,7 +436,7 @@
     return jax.ShapeDtypeStruct(dims, dtype)
 
 
-def call(kernel, outs, scalars, hbm, vmem, scratch, flops, mib=16):
+def call(kernel, outs, scalars, hbm, vmem, scratch, flops, mib=16, aliases=None):
     calling = pl.pallas_call(
         kernel,
         out_shape=outs,
@@ -419,6 +445,7 @@
         + [pl.BlockSpec(memory_space=pltpu.VMEM)] * vmem,
         out_specs=jax.tree.map(lambda _: pl.BlockSpec(memory_space=pltpu.VMEM), outs),
         scratch_shapes=scratch,
+        input_output_aliases=aliases or {},
         compiler_params=pltpu.CompilerParams(vmem_limit_bytes=mib * 2**20),
         cost_estimate=pl.CostEstimate(flops=flops, bytes_accessed=10**6, transcendentals=0),
     )
@@ -428,7 +455,10 @@
             pltpu.with_memory_space_constraint(x, pltpu.HBM)
             for x in arrays[scalars : scalars + hbm]
         ]
-        return calling(*arrays[:scalars], *held, *arrays[scalars + hbm :])
+        rest = arrays[scalars + hbm :]
+        if aliases:
+            rest = [pltpu.with_memory_space_constraint(x, pltpu.VMEM) for x in rest]
+        return calling(*arrays[:scalars], *held, *rest)
 
     return run
 
@@ -490,35 +520,48 @@
     slots = 2 * SIDE
     small = shape(ROWS, 128)
     both = shape(2 * ROWS, 128)
-    results = call(
-        attend_kernel,
+    state_shapes = (
+        shape(slots, SLOT, 128),
+        shape(slots, 8, ROWS, dtype=F32),
+        shape(slots, 2 * ROWS, 128),
+        shape(slots, 128, 2 * ROWS),
+        shape(slots, 2 * ROWS, 128),
+        shape(slots, 128, ROWS, dtype=F32),
+        shape(slots, ROWS, 128, dtype=F32),
+        shape(slots, ROWS, 128, dtype=F32),
+    )
+    holds = [pltpu.VMEM((2, ROWS, ROWS), BF), pltpu.VMEM((2, 2 * ROWS, ROWS), BF)]
+    pair_flops = 10 * ROWS * ROWS * 128
+    state = call(
+        attend_near_kernel, state_shapes, 1, 0, 6, holds, 10 * pair_flops
+    )(mix_lambda, yown, ys[0], ys[2], zown, zs[0], zs[2])
+    result_shapes = (
         (small,) * 3
         + (both,) * 6
         + (shape(2, 128, ROWS, dtype=F32),)
-        + (shape(2, ROWS, 128, dtype=F32),) * 2,
+        + (shape(2, ROWS, 128, dtype=F32),) * 2
+    )
+    results = call(
+        attend_far_kernel,
+        result_shapes + state_shapes,
         1,
         0,
-        8,
-        [
-            pltpu.VMEM((slots, SLOT, 128), BF),
-            pltpu.VMEM((slots, 8, ROWS), F32),
-            pltpu.VMEM((slots, 2 * ROWS, 128), BF),
-            pltpu.VMEM((slots, 128, 2 * ROWS), BF),
-            pltpu.VMEM((slots, 2 * ROWS, 128), BF),
-            pltpu.VMEM((slots, 128, ROWS), F32),
-            pltpu.VMEM((slots, ROWS, 128), F32),
-            pltpu.VMEM((slots, ROWS, 128), F32),
-            pltpu.VMEM((ROWS, ROWS), BF),
-            pltpu.VMEM((2 * ROWS, ROWS), BF),
-        ],
-        17 * 10 * ROWS * ROWS * 128,
-        24,
-    )(mix_lambda, yown, *ys, zown, *zs)
+        10,
+        holds,
+        7 * pair_flops,
+        aliases={3 + n: len(result_shapes) + n for n in range(len(state_shapes))},
+    )(mix_lambda, ys[1], zs[1], *state)
     own_q, own_k, own_v = results[9:12]
     q_back = [traded(x, "y", n) for n, x in enumerate(results[0:3], 1)]
     z_back = [traded(x, "z", n) for n, x in enumerate(results[3:6], 1)]
     turned_grad = call(
-        queries_kernel, shape(ROWS, ROWS), 0, 0, 7, [pltpu.VMEM((128, ROWS), F32)], 10**7
+        queries_kernel,
+        shape(ROWS, ROWS),
+        0,
+        0,
+        7,
+        [pltpu.VMEM((128, ROWS), F32)],
+        10**7,
     )(own_q, *q_back, *z_back)
     grads = [traded(turned_grad, "z", n) for n in range(1, SIDE)]
     kv_back = [traded(x, "y", n) for n, x in enumerate(results[6:9], 1)]
@@ -533,7 +576,13 @@
         2 * WIDE * WIDE * ROWS,
     )(turned_grad, *grads, lat_own, near, near_swap, apart, apart_swap)
     query_rows, key_rows, value_rows = call(
-        keys_kernel, (shape(2 * ROWS, 128),) * 3, 0, 0, 9, [pltpu.VMEM((ROWS, 128), F32)] * 2, 10**7
+        keys_kernel,
+        (shape(2 * ROWS, 128),) * 3,
+        0,
+        0,
+        9,
+        [pltpu.VMEM((ROWS, 128), F32)] * 2,
+        10**7,
     )(own_k, own_v, *kv_back, *z_back, turned_grad)
     weight_grad = call(
         total_kernel, shape(ROWS, ROWS, dtype=F32), 0, 0, 4, [], 10**6

time: 82 us -> 77.7 us (0.948)
  waiting for transfers between devices: 27.2 us -> 16.1 us
  starting transfers between devices: 36.9 us -> 47.6 us
  Pallas kernels: 17.1 us -> 13.1 us
    ppermute x22, waiting for transfers between devices: 27.2 us -> 16.1 us  [traded(): return lax.ppermute(x, 'sp', [(s, s ^ step) for s in range(SIDE * SIDE)])]
    ppermute x22, starting transfers between devices: 34.8 us -> 45 us  [traded(): return lax.ppermute(x, 'sp', [(s, s ^ step) for s in range(SIDE * SIDE)])]
    pallas_call x7 -> x8, Pallas kernels: 17.1 us -> 13.1 us  [run(): return calling(*arrays[:scalars], *held, *rest)]
  transfers between devices with their start and end apart: 25 -> 25, of which waited for: 12 -> 9; matrix products, arithmetic and copies ran while one was open for 0% -> 0% of each run, Pallas kernels for 18% -> 14%
where the time goes in v3:
time: 77.7 us; the launch traced here: 77.5 us
  starting transfers between devices  47.6 us (61%)
  waiting for transfers between devices  16.1 us (21%)
  Pallas kernels  13.1 us (17%)
    ppermute x22, starting transfers between devices, traded(): return lax.ppermute(x, 'sp', [(s, s ^ step) for s in range(SIDE * SIDE)])  45 us
    ppermute x22, waiting for transfers between devices, traded(): return lax.ppermute(x, 'sp', [(s, s ^ step) for s in range(SIDE * SIDE)])  16.1 us
    pallas_call x8, Pallas kernels, run(): return calling(*arrays[:scalars], *held, *rest)  13.1 us
    ppermute x1, starting transfers between devices, traded_apart(): return lax.ppermute(x, ('sp', 'tp'), pairs)  2.11 us
  transfers between devices with their start and end apart: 25, of which 9 were waited for; matrix products, arithmetic and copies ran while one was open for 0% of the time, Pallas kernels for 14%

profile of v3, /device:TPU:0, one launch (start us, length us, event | category | flops | bytes accessed | tf_op | source)
XLA Modules:
  0.0 77.5 jit_solution(12253965675253851414)
XLA Ops:
  0.6 0.0 copy-start
  0.6 1.3 %shard_map.125 = (bf16[256,1024]{1,0:T(8,128)(2,1)S(1)}, bf16[256,1024]{1,0:T(8,128)(2,1)S(1)}, bf16[128,1024]{1,0:T(8,128)(2,1)S(1)}) custom-call(bf16[256,4096]{1,0:T(8,128)(2,1)} %lat_hbm.1), custom_call_target="tpu_custom_call" | custom-call | flops 10000000 | bytes 1000000 | tf_op jit(solution)/shard_map/pallas_call | solution.py:461
  2.0 2.1 %collective-permute-start.18 = (bf16[256,1024]{1,0:T(8,128)(2,1)S(1)}, bf16[256,1024]{1,0:T(8,128)(2,1)S(1)}, u32[]{:S(2)}, u32[]{:S(2)}) collective-permute-start(bf16[256,1024]{1,0:T(8,128)(2,1)S(1)} %get-tuple-element.68), channel_id=1, source_target_pairs={{0,32},{1,97},{2,34},{3,99},{4,36},{5,101},{6,38},{7,103},{8,40},{... | collective-permute-start | bytes 1572872 | tf_op jit(solution)/shard_map/ppermute | solution.py:428
  4.1 2.0 %shard_map.120 = (bf16[1056,128]{1,0:T(8,128)(2,1)S(1)}, bf16[1056,128]{1,0:T(8,128)(2,1)S(1)}, bf16[544,128]{1,0:T(8,128)(2,1)S(1)}, bf16[544,128]{1,0:T(8,128)(2,1)S(1)}, bf16[544,128]{1,0:T(8,128)(2,1)S(1)}) custom-call(bf16[512,128]{1,0:T(8,128)(2,1)} %bitcast.11, bf16[512,128]{1,0:T(8,128)(2,1)} %bitcast.12, bf16[512,128]{1,0:T(8,128)(2,1)} %bitcast.13, ...), custom_call_target="tpu_custom_call" | custom-call | flops 100000000 | bytes 1000000 | tf_op jit(solution)/shard_map/pallas_call | solution.py:461
  6.1 0.1 collective-permute-start.4
  6.2 4.1 %collective-permute-start.5 = (bf16[544,128]{1,0:T(8,128)(2,1)S(1)}, bf16[544,128]{1,0:T(8,128)(2,1)S(1)}, u32[]{:S(2)}, u32[]{:S(2)}) collective-permute-start(bf16[544,128]{1,0:T(8,128)(2,1)S(1)} %get-tuple-element.43), channel_id=1, source_target_pairs={{0,96},{8,104},{16,112},{24,120},{32,64},{40,72},{48,80},{56,88},{... | collective-permute-start | bytes 417800 | tf_op jit(solution)/shard_map/ppermute | solution.py:418
  10.3 0.0 collective-permute-start.20
  10.3 1.6 %collective-permute-start.2 = (bf16[1056,128]{1,0:T(8,128)(2,1)S(1)}, bf16[1056,128]{1,0:T(8,128)(2,1)S(1)}, u32[]{:S(2)}, u32[]{:S(2)}) collective-permute-start(bf16[1056,128]{1,0:T(8,128)(2,1)S(1)} %get-tuple-element.39.yown), channel_id=1, source_target_pairs={{0,8},{8,0},{16,24},{24,16},{32,40},{40,32},{48,56},{56,48},{64,72... | collective-permute-start | bytes 811016 | tf_op jit(solution)/shard_map/ppermute | solution.py:418
  11.9 4.1 %collective-permute-done.4.z1 = bf16[544,128]{1,0:T(8,128)(2,1)S(1)} collective-permute-done((bf16[544,128]{1,0:T(8,128)(2,1)S(1)}, bf16[544,128]{1,0:T(8,128)(2,1)S(1)}, u32[]{:S(2)}, u32[]{:S(2)}) %collective-permute-start.4) | collective-permute-done | bytes 139296 | tf_op jit(solution)/shard_map/ppermute | solution.py:418
  16.0 3.0 %collective-permute-start.3 = (bf16[1056,128]{1,0:T(8,128)(2,1)S(1)}, bf16[1056,128]{1,0:T(8,128)(2,1)S(1)}, u32[]{:S(2)}, u32[]{:S(2)}) collective-permute-start(bf16[1056,128]{1,0:T(8,128)(2,1)S(1)} %get-tuple-element.39.yown), channel_id=1, source_target_pairs={{0,24},{8,16},{16,8},{24,0},{32,56},{40,48},{48,40},{56,32},{64,88... | collective-permute-start | bytes 811016 | tf_op jit(solution)/shard_map/ppermute | solution.py:418
  19.1 0.8 %collective-permute-done.5.z3 = bf16[544,128]{1,0:T(8,128)(2,1)S(1)} collective-permute-done((bf16[544,128]{1,0:T(8,128)(2,1)S(1)}, bf16[544,128]{1,0:T(8,128)(2,1)S(1)}, u32[]{:S(2)}, u32[]{:S(2)}) %collective-permute-start.5) | collective-permute-done | bytes 139296 | tf_op jit(solution)/shard_map/ppermute | solution.py:418
  19.9 3.2 %collective-permute-start = (bf16[1056,128]{1,0:T(8,128)(2,1)S(1)}, bf16[1056,128]{1,0:T(8,128)(2,1)S(1)}, u32[]{:S(2)}, u32[]{:S(2)}) collective-permute-start(bf16[1056,128]{1,0:T(8,128)(2,1)S(1)} %get-tuple-element.39.yown), channel_id=1, source_target_pairs={{0,16},{8,24},{16,0},{24,8},{32,48},{40,56},{48,32},{56,40},{64,80... | collective-permute-start | bytes 811016 | tf_op jit(solution)/shard_map/ppermute | solution.py:418
  23.0 0.4 collective-permute-done.20.far
  23.4 1.2 %collective-permute-start.1 = (bf16[544,128]{1,0:T(8,128)(2,1)S(1)}, bf16[544,128]{1,0:T(8,128)(2,1)S(1)}, u32[]{:S(2)}, u32[]{:S(2)}) collective-permute-start(bf16[544,128]{1,0:T(8,128)(2,1)S(1)} %get-tuple-element.40), channel_id=1, source_target_pairs={{0,64},{8,72},{16,80},{24,88},{32,96},{40,104},{48,112},{56,120},{... | collective-permute-start | bytes 417800 | tf_op jit(solution)/shard_map/ppermute | solution.py:418
  24.7 0.0 collective-permute-done.18.near
  24.7 0.0 collective-permute-start.19
  24.7 0.0 collective-permute-done.2.y1
  24.7 0.5 collective-permute-start.21
  25.2 3.9 %shard_map.121 = (bf16[8,1056,128]{2,1,0:T(8,128)(2,1)S(1)}, f32[8,8,256]{2,1,0:T(8,128)S(1)}, bf16[8,512,128]{2,1,0:T(8,128)(2,1)S(1)}, bf16[8,128,512]{2,1,0:T...) custom-call(f32[2]{0:T(128)S(1)} %copy-done, ...), custom_call_target="tpu_custom_call" | custom-call | flops 838860800 | bytes 1000000 | tf_op jit(solution)/shard_map/pallas_call | solution.py:461
  29.1 1.4 %collective-permute-done.1.z2 = bf16[544,128]{1,0:T(8,128)(2,1)S(1)} collective-permute-done((bf16[544,128]{1,0:T(8,128)(2,1)S(1)}, bf16[544,128]{1,0:T(8,128)(2,1)S(1)}, u32[]{:S(2)}, u32[]{:S(2)}) %collective-permute-start.1) | collective-permute-done | bytes 139296 | tf_op jit(solution)/shard_map/ppermute | solution.py:418
  30.5 0.0 collective-permute-done.y2
  30.5 2.9 %shard_map.122 = (bf16[256,128]{1,0:T(8,128)(2,1)S(1)}, bf16[256,128]{1,0:T(8,128)(2,1)S(1)}, bf16[256,128]{1,0:T(8,128)(2,1)S(1)}, bf16[512,128]{1,0:T(8,128)(2...) custom-call(f32[2]{0:T(128)S(1)} %copy-done, ...), custom_call_target="tpu_custom_call", output_to_operand_aliasing={{12}: (3, {}), {13}: (4, {}), {14}: (5, {}), {15}: (6, {}),... | custom-call | flops 587202560 | bytes 1000000 | tf_op jit(solution)/shard_map/pallas_call | solution.py:461
  33.4 1.5 %collective-permute-start.12 = (bf16[256,128]{1,0:T(8,128)(2,1)S(1)}, bf16[256,128]{1,0:T(8,128)(2,1)S(1)}, u32[]{:S(2)}, u32[]{:S(2)}) collective-permute-start(bf16[256,128]{1,0:T(8,128)(2,1)S(1)} %get-tuple-element.61), channel_id=1, source_target_pairs={{0,8},{8,0},{16,24},{24,16},{32,40},{40,32},{48,56},{56,48},{64,72... | collective-permute-start | bytes 196616 | tf_op jit(solution)/shard_map/ppermute | solution.py:418
  35.0 2.9 %collective-permute-start.13 = (bf16[256,128]{1,0:T(8,128)(2,1)S(1)}, bf16[256,128]{1,0:T(8,128)(2,1)S(1)}, u32[]{:S(2)}, u32[]{:S(2)}) collective-permute-start(bf16[256,128]{1,0:T(8,128)(2,1)S(1)} %get-tuple-element.62), channel_id=1, source_target_pairs={{0,16},{8,24},{16,0},{24,8},{32,48},{40,56},{48,32},{56,40},{64,80... | collective-permute-start | bytes 196616 | tf_op jit(solution)/shard_map/ppermute | solution.py:418
  37.9 0.3 collective-permute-start.14
  38.2 4.8 %collective-permute-start.10 = (bf16[512,128]{1,0:T(8,128)(2,1)S(1)}, bf16[512,128]{1,0:T(8,128)(2,1)S(1)}, u32[]{:S(2)}, u32[]{:S(2)}) collective-permute-start(bf16[512,128]{1,0:T(8,128)(2,1)S(1)} %get-tuple-element.58), channel_id=1, source_target_pairs={{0,64},{8,72},{16,80},{24,88},{32,96},{40,104},{48,112},{56,120},{... | collective-permute-start | bytes 393224 | tf_op jit(solution)/shard_map/ppermute | solution.py:418
  43.0 6.0 %collective-permute-start.11 = (bf16[512,128]{1,0:T(8,128)(2,1)S(1)}, bf16[512,128]{1,0:T(8,128)(2,1)S(1)}, u32[]{:S(2)}, u32[]{:S(2)}) collective-permute-start(bf16[512,128]{1,0:T(8,128)(2,1)S(1)} %get-tuple-element.59), channel_id=1, source_target_pairs={{0,96},{8,104},{16,112},{24,120},{32,64},{40,72},{48,80},{56,88},{... | collective-permute-start | bytes 393224 | tf_op jit(solution)/shard_map/ppermute | solution.py:418
  49.0 0.0 collective-permute-done.14.y3
  49.0 0.0 collective-permute-start.9
  49.0 5.0 %collective-permute-done.11.z3 = bf16[512,128]{1,0:T(8,128)(2,1)S(1)} collective-permute-done((bf16[512,128]{1,0:T(8,128)(2,1)S(1)}, bf16[512,128]{1,0:T(8,128)(2,1)S(1)}, u32[]{:S(2)}, u32[]{:S(2)}) %collective-permute-start.11) | collective-permute-done | bytes 131104 | tf_op jit(solution)/shard_map/ppermute | solution.py:418
  54.1 0.3 collective-permute-done.9.z1
  54.4 0.1 shard_map.123.turned_in.g0
  54.4 1.0 %collective-permute-start.15 = (bf16[256,256]{1,0:T(8,128)(2,1)S(1)}, bf16[256,256]{1,0:T(8,128)(2,1)S(1)}, u32[]{:S(2)}, u32[]{:S(2)}) collective-permute-start(bf16[256,256]{1,0:T(8,128)(2,1)S(1)} %shard_map.123.turned_in.g0), channel_id=1, source_target_pairs={{0,32},{8,40},{16,48},{24,56},{32,0},{40,8},{48,16},{56,24},{64,96... | collective-permute-start | bytes 393224 | tf_op jit(solution)/shard_map/ppermute | solution.py:418
  55.5 3.9 %collective-permute-start.16 = (bf16[256,256]{1,0:T(8,128)(2,1)S(1)}, bf16[256,256]{1,0:T(8,128)(2,1)S(1)}, u32[]{:S(2)}, u32[]{:S(2)}) collective-permute-start(bf16[256,256]{1,0:T(8,128)(2,1)S(1)} %shard_map.123.turned_in.g0), channel_id=1, source_target_pairs={{0,64},{8,72},{16,80},{24,88},{32,96},{40,104},{48,112},{56,120},{... | collective-permute-start | bytes 393224 | tf_op jit(solution)/shard_map/ppermute | solution.py:418
  59.4 0.0 collective-permute-start.17
  59.4 0.3 collective-permute-start.6
  59.8 0.0 collective-permute-done.15.g1
  59.8 3.6 %collective-permute-start.7 = (bf16[512,128]{1,0:T(8,128)(2,1)S(1)}, bf16[512,128]{1,0:T(8,128)(2,1)S(1)}, u32[]{:S(2)}, u32[]{:S(2)}) collective-permute-start(bf16[512,128]{1,0:T(8,128)(2,1)S(1)} %get-tuple-element.55), channel_id=1, source_target_pairs={{0,16},{8,24},{16,0},{24,8},{32,48},{40,56},{48,32},{56,40},{64,80... | collective-permute-start | bytes 393224 | tf_op jit(solution)/shard_map/ppermute | solution.py:418
  63.4 0.4 collective-permute-done.16.g2
  63.8 2.5 %collective-permute-start.8 = (bf16[512,128]{1,0:T(8,128)(2,1)S(1)}, bf16[512,128]{1,0:T(8,128)(2,1)S(1)}, u32[]{:S(2)}, u32[]{:S(2)}) collective-permute-start(bf16[512,128]{1,0:T(8,128)(2,1)S(1)} %get-tuple-element.56), channel_id=1, source_target_pairs={{0,24},{8,16},{16,8},{24,0},{32,56},{40,48},{48,40},{56,32},{64,88... | collective-permute-start | bytes 393224 | tf_op jit(solution)/shard_map/ppermute | solution.py:418
  66.2 0.9 %shard_map.126 = (f32[256,256]{1,0:T(8,128)S(1)}, bf16[256,256]{1,0:T(8,128)(2,1)S(1)}, bf16[256,256]{1,0:T(8,128)(2,1)S(1)}, bf16[256,256]{1,0:T(8,128)(2,1)S(1)}) custom-call(bf16[256,256]{1,0:T(8,128)(2,1)S(1)} %shard_map.123.turned_in.g0, bf16[256,256]{1,0:T(8,128)(2,1)S(1)} %collective-permute-done.15.g1, ...), custom_call_target="tpu_custom_call" | custom-call | flops 536870912 | bytes 1000000 | tf_op jit(solution)/shard_map/pallas_call | solution.py:461
  67.1 0.2 collective-permute-start.22
  67.3 3.2 %collective-permute-start.23 = (bf16[256,256]{1,0:T(8,128)(2,1)S(1)}, bf16[256,256]{1,0:T(8,128)(2,1)S(1)}, u32[]{:S(2)}, u32[]{:S(2)}) collective-permute-start(bf16[256,256]{1,0:T(8,128)(2,1)S(1)} %get-tuple-element.72), channel_id=1, source_target_pairs={{0,16},{8,24},{16,0},{24,8},{32,48},{40,56},{48,32},{56,40},{64,80... | collective-permute-start | bytes 393224 | tf_op jit(solution)/shard_map/ppermute | solution.py:418
  70.5 1.4 %collective-permute-start.24 = (bf16[256,256]{1,0:T(8,128)(2,1)S(1)}, bf16[256,256]{1,0:T(8,128)(2,1)S(1)}, u32[]{:S(2)}, u32[]{:S(2)}) collective-permute-start(bf16[256,256]{1,0:T(8,128)(2,1)S(1)} %get-tuple-element.73), channel_id=1, source_target_pairs={{0,24},{8,16},{16,8},{24,0},{32,56},{40,48},{48,40},{56,32},{64,88... | collective-permute-start | bytes 393224 | tf_op jit(solution)/shard_map/ppermute | solution.py:418
  71.9 1.1 %shard_map.124 = (bf16[512,128]{1,0:T(8,128)(2,1)}, bf16[512,128]{1,0:T(8,128)(2,1)}, bf16[512,128]{1,0:T(8,128)(2,1)}) custom-call(f32[2,256,128]{2,1,0:T(8,128)S(1)} %get-tuple-element.52.own_k, f32[2,256,128]{2,1,0:T(8,128)S(1)} %get-tuple-element.53.own_v, bf16[512,128]{1,0:T(8,128)(2,1)S(1)} %collective-permute-done.6.y1, ...), custom_call_target="tpu_custom_call" | custom-call | flops 10000000 | bytes 1000000 | tf_op jit(solution)/shard_map/pallas_call | solution.py:461
  73.1 1.8 %collective-permute-done.23.t2 = bf16[256,256]{1,0:T(8,128)(2,1)S(1)} collective-permute-done((bf16[256,256]{1,0:T(8,128)(2,1)S(1)}, bf16[256,256]{1,0:T(8,128)(2,1)S(1)}, u32[]{:S(2)}, u32[]{:S(2)}) %collective-permute-start.23) | collective-permute-done | bytes 131104 | tf_op jit(solution)/shard_map/ppermute | solution.py:418
  74.9 1.8 %collective-permute-done.24.t3 = bf16[256,256]{1,0:T(8,128)(2,1)S(1)} collective-permute-done((bf16[256,256]{1,0:T(8,128)(2,1)S(1)}, bf16[256,256]{1,0:T(8,128)(2,1)S(1)}, u32[]{:S(2)}, u32[]{:S(2)}) %collective-permute-start.24) | collective-permute-done | bytes 131104 | tf_op jit(solution)/shard_map/ppermute | solution.py:418
  76.7 0.8 %shard_map.127 = f32[256,256]{1,0:T(8,128)} custom-call(f32[256,256]{1,0:T(8,128)S(1)} %get-tuple-element.70.own, bf16[256,256]{1,0:T(8,128)(2,1)S(1)} %collective-permute-done.22.t1, bf16[256,256]{1,0:T(8,128)(2,1)S(1)} %collective-permute-done.23.t2, bf16[256,256]{1,0:T(8,128)(2,1)S(1)} %collective-permute-done.24.t3), custom_call_target="tpu_custom_call" | custom-call | flops 1000000 | bytes 1000000 | tf_op jit(solution)/shard_map/pallas_call | solution.py:461
  (12 shorter events, 0.0 us)
Async XLA Ops:
  0.6 24.6 %copy-start = (f32[2]{0:T(128)S(1)}, f32[2]{0:T(128)}, u32[]{:S(2)}) copy-start(f32[2]{0:T(128)} %lam.3) | copy-start | bytes 28
  2.0 22.7 %collective-permute-start.18 = (bf16[256,1024]{1,0:T(8,128)(2,1)S(1)}, bf16[256,1024]{1,0:T(8,128)(2,1)S(1)}, u32[]{:S(2)}, u32[]{:S(2)}) collective-permute-start(bf16[256,1024]{1,0:T(8,128)(2,1)S(1)} %get-tuple-element.68), channel_id=1, source_target_pairs={{0,32},{1,97},{2,34},{3,99},{4,36},{5,101},{6,38},{7,103},{8,40},{... | collective-permute-start | bytes 1572872 | tf_op jit(solution)/shard_map/ppermute | solution.py:428
  6.1 10.0 %collective-permute-start.4 = (bf16[544,128]{1,0:T(8,128)(2,1)S(1)}, bf16[544,128]{1,0:T(8,128)(2,1)S(1)}, u32[]{:S(2)}, u32[]{:S(2)}) collective-permute-start(bf16[544,128]{1,0:T(8,128)(2,1)S(1)} %get-tuple-element.42), channel_id=1, source_target_pairs={{0,32},{8,40},{16,48},{24,56},{32,0},{40,8},{48,16},{56,24},{64,96... | collective-permute-start | bytes 417800 | tf_op jit(solution)/shard_map/ppermute | solution.py:418
  6.2 13.7 %collective-permute-start.5 = (bf16[544,128]{1,0:T(8,128)(2,1)S(1)}, bf16[544,128]{1,0:T(8,128)(2,1)S(1)}, u32[]{:S(2)}, u32[]{:S(2)}) collective-permute-start(bf16[544,128]{1,0:T(8,128)(2,1)S(1)} %get-tuple-element.43), channel_id=1, source_target_pairs={{0,96},{8,104},{16,112},{24,120},{32,64},{40,72},{48,80},{56,88},{... | collective-permute-start | bytes 417800 | tf_op jit(solution)/shard_map/ppermute | solution.py:418
  10.3 13.1 %collective-permute-start.20 = (bf16[128,1024]{1,0:T(8,128)(2,1)S(1)}, bf16[128,1024]{1,0:T(8,128)(2,1)S(1)}, u32[]{:S(2)}, u32[]{:S(2)}) collective-permute-start(bf16[128,1024]{1,0:T(8,128)(2,1)S(1)} %get-tuple-element.69), channel_id=1, source_target_pairs={{0,64},{8,72},{16,80},{24,88},{32,96},{40,104},{48,112},{56,120},{... | collective-permute-start | bytes 786440 | tf_op jit(solution)/shard_map/ppermute | solution.py:418
  10.3 14.4 %collective-permute-start.2 = (bf16[1056,128]{1,0:T(8,128)(2,1)S(1)}, bf16[1056,128]{1,0:T(8,128)(2,1)S(1)}, u32[]{:S(2)}, u32[]{:S(2)}) collective-permute-start(bf16[1056,128]{1,0:T(8,128)(2,1)S(1)} %get-tuple-element.39.yown), channel_id=1, source_target_pairs={{0,8},{8,0},{16,24},{24,16},{32,40},{40,32},{48,56},{56,48},{64,72... | collective-permute-start | bytes 811016 | tf_op jit(solution)/shard_map/ppermute | solution.py:418
  16.0 9.2 %collective-permute-start.3 = (bf16[1056,128]{1,0:T(8,128)(2,1)S(1)}, bf16[1056,128]{1,0:T(8,128)(2,1)S(1)}, u32[]{:S(2)}, u32[]{:S(2)}) collective-permute-start(bf16[1056,128]{1,0:T(8,128)(2,1)S(1)} %get-tuple-element.39.yown), channel_id=1, source_target_pairs={{0,24},{8,16},{16,8},{24,0},{32,56},{40,48},{48,40},{56,32},{64,88... | collective-permute-start | bytes 811016 | tf_op jit(solution)/shard_map/ppermute | solution.py:418
  19.9 10.6 %collective-permute-start = (bf16[1056,128]{1,0:T(8,128)(2,1)S(1)}, bf16[1056,128]{1,0:T(8,128)(2,1)S(1)}, u32[]{:S(2)}, u32[]{:S(2)}) collective-permute-start(bf16[1056,128]{1,0:T(8,128)(2,1)S(1)} %get-tuple-element.39.yown), channel_id=1, source_target_pairs={{0,16},{8,24},{16,0},{24,8},{32,48},{40,56},{48,32},{56,40},{64,80... | collective-permute-start | bytes 811016 | tf_op jit(solution)/shard_map/ppermute | solution.py:418
  23.4 7.1 %collective-permute-start.1 = (bf16[544,128]{1,0:T(8,128)(2,1)S(1)}, bf16[544,128]{1,0:T(8,128)(2,1)S(1)}, u32[]{:S(2)}, u32[]{:S(2)}) collective-permute-start(bf16[544,128]{1,0:T(8,128)(2,1)S(1)} %get-tuple-element.40), channel_id=1, source_target_pairs={{0,64},{8,72},{16,80},{24,88},{32,96},{40,104},{48,112},{56,120},{... | collective-permute-start | bytes 417800 | tf_op jit(solution)/shard_map/ppermute | solution.py:418
  24.7 41.6 %collective-permute-start.19 = (bf16[256,1024]{1,0:T(8,128)(2,1)S(1)}, bf16[256,1024]{1,0:T(8,128)(2,1)S(1)}, u32[]{:S(2)}, u32[]{:S(2)}) collective-permute-start(bf16[256,1024]{1,0:T(8,128)(2,1)S(1)} %collective-permute-done.18.near), channel_id=1, source_target_pairs={{0,1},{1,0},{2,3},{3,2},{4,5},{5,4},{6,7},{7,6},{8,9},{9,8},{10,11... | collective-permute-start | bytes 1572872 | tf_op jit(solution)/shard_map/ppermute | solution.py:432
  24.7 34.7 %collective-permute-start.21 = (bf16[128,1024]{1,0:T(8,128)(2,1)S(1)}, bf16[128,1024]{1,0:T(8,128)(2,1)S(1)}, u32[]{:S(2)}, u32[]{:S(2)}) collective-permute-start(bf16[128,1024]{1,0:T(8,128)(2,1)S(1)} %collective-permute-done.20.far), channel_id=1, source_target_pairs={{0,1},{1,0},{2,3},{3,2},{4,5},{5,4},{6,7},{7,6},{8,9},{9,8},{10,11... | collective-permute-start | bytes 786440 | tf_op jit(solution)/shard_map/ppermute | solution.py:432
  33.4 4.8 %collective-permute-start.12 = (bf16[256,128]{1,0:T(8,128)(2,1)S(1)}, bf16[256,128]{1,0:T(8,128)(2,1)S(1)}, u32[]{:S(2)}, u32[]{:S(2)}) collective-permute-start(bf16[256,128]{1,0:T(8,128)(2,1)S(1)} %get-tuple-element.61), channel_id=1, source_target_pairs={{0,8},{8,0},{16,24},{24,16},{32,40},{40,32},{48,56},{56,48},{64,72... | collective-permute-start | bytes 196616 | tf_op jit(solution)/shard_map/ppermute | solution.py:418
  35.0 8.0 %collective-permute-start.13 = (bf16[256,128]{1,0:T(8,128)(2,1)S(1)}, bf16[256,128]{1,0:T(8,128)(2,1)S(1)}, u32[]{:S(2)}, u32[]{:S(2)}) collective-permute-start(bf16[256,128]{1,0:T(8,128)(2,1)S(1)} %get-tuple-element.62), channel_id=1, source_target_pairs={{0,16},{8,24},{16,0},{24,8},{32,48},{40,56},{48,32},{56,40},{64,80... | collective-permute-start | bytes 196616 | tf_op jit(solution)/shard_map/ppermute | solution.py:418
  37.9 11.1 %collective-permute-start.14 = (bf16[256,128]{1,0:T(8,128)(2,1)S(1)}, bf16[256,128]{1,0:T(8,128)(2,1)S(1)}, u32[]{:S(2)}, u32[]{:S(2)}) collective-permute-start(bf16[256,128]{1,0:T(8,128)(2,1)S(1)} %get-tuple-element.63), channel_id=1, source_target_pairs={{0,24},{8,16},{16,8},{24,0},{32,56},{40,48},{48,40},{56,32},{64,88... | collective-permute-start | bytes 196616 | tf_op jit(solution)/shard_map/ppermute | solution.py:418
  38.2 10.8 %collective-permute-start.10 = (bf16[512,128]{1,0:T(8,128)(2,1)S(1)}, bf16[512,128]{1,0:T(8,128)(2,1)S(1)}, u32[]{:S(2)}, u32[]{:S(2)}) collective-permute-start(bf16[512,128]{1,0:T(8,128)(2,1)S(1)} %get-tuple-element.58), channel_id=1, source_target_pairs={{0,64},{8,72},{16,80},{24,88},{32,96},{40,104},{48,112},{56,120},{... | collective-permute-start | bytes 393224 | tf_op jit(solution)/shard_map/ppermute | solution.py:418
  43.0 11.0 %collective-permute-start.11 = (bf16[512,128]{1,0:T(8,128)(2,1)S(1)}, bf16[512,128]{1,0:T(8,128)(2,1)S(1)}, u32[]{:S(2)}, u32[]{:S(2)}) collective-permute-start(bf16[512,128]{1,0:T(8,128)(2,1)S(1)} %get-tuple-element.59), channel_id=1, source_target_pairs={{0,96},{8,104},{16,112},{24,120},{32,64},{40,72},{48,80},{56,88},{... | collective-permute-start | bytes 393224 | tf_op jit(solution)/shard_map/ppermute | solution.py:418
  49.0 5.3 %collective-permute-start.9 = (bf16[512,128]{1,0:T(8,128)(2,1)S(1)}, bf16[512,128]{1,0:T(8,128)(2,1)S(1)}, u32[]{:S(2)}, u32[]{:S(2)}) collective-permute-start(bf16[512,128]{1,0:T(8,128)(2,1)S(1)} %get-tuple-element.57), channel_id=1, source_target_pairs={{0,32},{8,40},{16,48},{24,56},{32,0},{40,8},{48,16},{56,24},{64,96... | collective-permute-start | bytes 393224 | tf_op jit(solution)/shard_map/ppermute | solution.py:418
  54.4 5.3 %collective-permute-start.15 = (bf16[256,256]{1,0:T(8,128)(2,1)S(1)}, bf16[256,256]{1,0:T(8,128)(2,1)S(1)}, u32[]{:S(2)}, u32[]{:S(2)}) collective-permute-start(bf16[256,256]{1,0:T(8,128)(2,1)S(1)} %shard_map.123.turned_in.g0), channel_id=1, source_target_pairs={{0,32},{8,40},{16,48},{24,56},{32,0},{40,8},{48,16},{56,24},{64,96... | collective-permute-start | bytes 393224 | tf_op jit(solution)/shard_map/ppermute | solution.py:418
  55.5 8.3 %collective-permute-start.16 = (bf16[256,256]{1,0:T(8,128)(2,1)S(1)}, bf16[256,256]{1,0:T(8,128)(2,1)S(1)}, u32[]{:S(2)}, u32[]{:S(2)}) collective-permute-start(bf16[256,256]{1,0:T(8,128)(2,1)S(1)} %shard_map.123.turned_in.g0), channel_id=1, source_target_pairs={{0,64},{8,72},{16,80},{24,88},{32,96},{40,104},{48,112},{56,120},{... | collective-permute-start | bytes 393224 | tf_op jit(solution)/shard_map/ppermute | solution.py:418
  59.4 6.8 %collective-permute-start.17 = (bf16[256,256]{1,0:T(8,128)(2,1)S(1)}, bf16[256,256]{1,0:T(8,128)(2,1)S(1)}, u32[]{:S(2)}, u32[]{:S(2)}) collective-permute-start(bf16[256,256]{1,0:T(8,128)(2,1)S(1)} %shard_map.123.turned_in.g0), channel_id=1, source_target_pairs={{0,96},{8,104},{16,112},{24,120},{32,64},{40,72},{48,80},{56,88},{... | collective-permute-start | bytes 393224 | tf_op jit(solution)/shard_map/ppermute | solution.py:418
  59.4 11.1 %collective-permute-start.6 = (bf16[512,128]{1,0:T(8,128)(2,1)S(1)}, bf16[512,128]{1,0:T(8,128)(2,1)S(1)}, u32[]{:S(2)}, u32[]{:S(2)}) collective-permute-start(bf16[512,128]{1,0:T(8,128)(2,1)S(1)} %get-tuple-element.54), channel_id=1, source_target_pairs={{0,8},{8,0},{16,24},{24,16},{32,40},{40,32},{48,56},{56,48},{64,72... | collective-permute-start | bytes 393224 | tf_op jit(solution)/shard_map/ppermute | solution.py:418
  59.8 12.1 %collective-permute-start.7 = (bf16[512,128]{1,0:T(8,128)(2,1)S(1)}, bf16[512,128]{1,0:T(8,128)(2,1)S(1)}, u32[]{:S(2)}, u32[]{:S(2)}) collective-permute-start(bf16[512,128]{1,0:T(8,128)(2,1)S(1)} %get-tuple-element.55), channel_id=1, source_target_pairs={{0,16},{8,24},{16,0},{24,8},{32,48},{40,56},{48,32},{56,40},{64,80... | collective-permute-start | bytes 393224 | tf_op jit(solution)/shard_map/ppermute | solution.py:418
  63.8 8.2 %collective-permute-start.8 = (bf16[512,128]{1,0:T(8,128)(2,1)S(1)}, bf16[512,128]{1,0:T(8,128)(2,1)S(1)}, u32[]{:S(2)}, u32[]{:S(2)}) collective-permute-start(bf16[512,128]{1,0:T(8,128)(2,1)S(1)} %get-tuple-element.56), channel_id=1, source_target_pairs={{0,24},{8,16},{16,8},{24,0},{32,56},{40,48},{48,40},{56,32},{64,88... | collective-permute-start | bytes 393224 | tf_op jit(solution)/shard_map/ppermute | solution.py:418
  67.1 5.9 %collective-permute-start.22 = (bf16[256,256]{1,0:T(8,128)(2,1)S(1)}, bf16[256,256]{1,0:T(8,128)(2,1)S(1)}, u32[]{:S(2)}, u32[]{:S(2)}) collective-permute-start(bf16[256,256]{1,0:T(8,128)(2,1)S(1)} %get-tuple-element.71), channel_id=1, source_target_pairs={{0,8},{8,0},{16,24},{24,16},{32,40},{40,32},{48,56},{56,48},{64,72... | collective-permute-start | bytes 393224 | tf_op jit(solution)/shard_map/ppermute | solution.py:418
  67.3 7.5 %collective-permute-start.23 = (bf16[256,256]{1,0:T(8,128)(2,1)S(1)}, bf16[256,256]{1,0:T(8,128)(2,1)S(1)}, u32[]{:S(2)}, u32[]{:S(2)}) collective-permute-start(bf16[256,256]{1,0:T(8,128)(2,1)S(1)} %get-tuple-element.72), channel_id=1, source_target_pairs={{0,16},{8,24},{16,0},{24,8},{32,48},{40,56},{48,32},{56,40},{64,80... | collective-permute-start | bytes 393224 | tf_op jit(solution)/shard_map/ppermute | solution.py:418
  70.5 6.2 %collective-permute-start.24 = (bf16[256,256]{1,0:T(8,128)(2,1)S(1)}, bf16[256,256]{1,0:T(8,128)(2,1)S(1)}, u32[]{:S(2)}, u32[]{:S(2)}) collective-permute-start(bf16[256,256]{1,0:T(8,128)(2,1)S(1)} %get-tuple-element.73), channel_id=1, source_target_pairs={{0,24},{8,16},{16,8},{24,0},{32,56},{40,48},{48,40},{56,32},{64,88... | collective-permute-start | bytes 393224 | tf_op jit(solution)/shard_map/ppermute | solution.py:418

commit v4 on v3

--- a/solution.py
+++ b/solution.py
@@ -56,15 +56,21 @@
 
 
 def prepare_kernel(
-    q_hbm, k_hbm, v_hbm, maps_hbm, lse_hbm, out_hbm, gain_hbm, lam_hbm,
-    yown, zown, send1, send2, send3,
+    q_hbm, k_hbm, v_hbm, maps_hbm, lse_hbm, out_hbm, gain_hbm, lam_hbm, lat_hbm,
+    yown, zown, send1, send2, send3, lat_near, lat_far,
     q_in, k_in, v_in, maps_in, lse_in, out_in, gain_in, lam, sems,
 ):
-    z, _, _ = position()
+    z, _, core = position()
     pairs = [
         (maps_hbm, maps_in), (out_hbm, out_in), (gain_hbm, gain_in), (lse_hbm, lse_in),
         (lam_hbm, lam), (q_hbm, q_in), (k_hbm, k_in), (v_hbm, v_in),
     ]
+    near = jnp.bitwise_xor(z, jnp.where(core == 0, 1, 3))
+    columns = pl.ds(pl.multiple_of(near * WIDE, WIDE), WIDE)
+    pairs.append((lat_hbm.at[:, columns], lat_near))
+    tokens = pl.ds(pl.multiple_of(core * HALF, HALF), HALF)
+    columns = pl.ds(pl.multiple_of(jnp.bitwise_xor(z, 2) * WIDE, WIDE), WIDE)
+    pairs.append((lat_hbm.at[tokens, columns], lat_far))
     copies = [pltpu.make_async_copy(a, b, sems.at[n]) for n, (a, b) in enumerate(pairs)]
     for copy in copies:
         copy.start()
@@ -109,7 +115,7 @@
         ref[ROWS : 2 * ROWS] = grad
         ref[2 * ROWS : 2 * ROWS + 16] = packed[:, 0:128]
         ref[2 * ROWS + 16 : QG] = packed[:, 128:256]
-    for copy in copies[5:]:
+    for copy in copies[5:8]:
         copy.wait()
     q0, q1, k0, k1 = two_heads(spread, q_in, k_in)
     v0, v1, _, _ = two_heads(spread, v_in, v_in)
@@ -132,24 +138,7 @@
 
     for n, ref in enumerate((send1, send2, send3)):
         send(ref, z < jnp.bitwise_xor(z, n + 1))
-
-
-def fetch_kernel(lat_hbm, lat_own, lat_near, lat_far, sems):
-    z, _, core = position()
-
-    def columns(block):
-        return pl.ds(pl.multiple_of(block * WIDE, WIDE), WIDE)
-
-    tokens = pl.ds(pl.multiple_of(core * HALF, HALF), HALF)
-    near = jnp.bitwise_xor(z, jnp.where(core == 0, 1, 3))
-    copies = (
-        pltpu.make_async_copy(lat_hbm.at[:, columns(near)], lat_near, sems.at[0]),
-        pltpu.make_async_copy(lat_hbm.at[tokens, columns(jnp.bitwise_xor(z, 2))], lat_far, sems.at[1]),
-        pltpu.make_async_copy(lat_hbm.at[:, columns(z)], lat_own, sems.at[2]),
-    )
-    for copy in copies:
-        copy.start()
-    for copy in copies:
+    for copy in copies[8:]:
         copy.wait()
 
 
@@ -263,10 +252,13 @@
 
 
 def attend_near_kernel(
-    lam, yown, y1, y3, zown, z1, z3,
-    buf, stat, kpad, kturn, qpad, dq, dk, dv, wide_w, tall_s,
+    lam, lat_hbm, yown, y1, y3, zown, z1, z3,
+    buf, stat, kpad, kturn, qpad, dq, dk, dv, lat_own, wide_w, tall_s, sem,
 ):
     z, y, _ = position()
+    columns = pl.ds(pl.multiple_of(z * WIDE, WIDE), WIDE)
+    fetch = pltpu.make_async_copy(lat_hbm.at[:, columns], lat_own, sem)
+    fetch.start()
     state = (buf, stat, kpad, kturn, qpad, dq, dk, dv)
     for slot, ref in ((0, yown), (1, y1), (3, y3), (SIDE, zown)):
         buf[slot] = ref[...]
@@ -278,11 +270,12 @@
     items += [(4, 1, None), (4, 3, None)]
     items += [(zslot, yslot, None) for zslot in (5, 7) for yslot in (0, 1, 3)]
     run_pairs(items, z, y, lam, state, wide_w, tall_s)
+    fetch.wait()
 
 
 def attend_far_kernel(
     lam, y2, z2, buf_in, stat_in, kpad_in, kturn_in, qpad_in, dq_in, dk_in, dv_in,
-    q1, q2, q3, r1, r2, r3, kv1, kv2, kv3, own_q, own_k, own_v,
+    g1, g2, g3, r1, r2, r3, own_q, own_k, own_v,
     buf, stat, kpad, kturn, qpad, dq, dk, dv, wide_w, tall_s,
 ):
     z, y, _ = position()
@@ -301,10 +294,10 @@
         ref[0:HALF] = value[:, 0:128]
         ref[HALF:ROWS] = value[:, 128:]
 
-    for slot, (ref, kv) in enumerate(((q1, kv1), (q2, kv2), (q3, kv3))):
-        put_q(ref, slot + 1)
-        kv[0:ROWS] = (dk[slot + 1] * scale).astype(BF)
-        kv[ROWS:] = dv[slot + 1].astype(BF)
+    for slot, ref in enumerate((g1, g2, g3), 1):
+        put_q(ref, slot)
+        ref[ROWS : 2 * ROWS] = (dk[slot] * scale).astype(BF)
+        ref[2 * ROWS :] = dv[slot].astype(BF)
     for n, ref in enumerate((r1, r2, r3), 1):
         keys = jnp.bitwise_xor(z, n) < z
 
@@ -364,8 +357,8 @@
     k0 = own_k[0]
     v0 = own_v[0]
     for ref in (y1, y2, y3):
-        k0 += ref[0:ROWS].astype(F32)
-        v0 += ref[ROWS:].astype(F32)
+        k0 += ref[ROWS : 2 * ROWS].astype(F32)
+        v0 += ref[2 * ROWS :].astype(F32)
     zero = jnp.concatenate([k0.astype(BF), v0.astype(BF)], axis=1)
     one = jnp.concatenate([acc_k[...].astype(BF), acc_v[...].astype(BF)], axis=1)
     for half in range(2):
@@ -474,11 +467,13 @@
     mix_lambda,
     norm_gain,
 ):
-    yown, zown, *sends = call(
+    yown, zown, *sends, lat_near, lat_far = call(
         prepare_kernel,
-        (shape(SLOT, 128),) * 2 + (shape(QG, 128),) * 3,
-        0,
-        8,
+        (shape(SLOT, 128),) * 2
+        + (shape(QG, 128),) * 3
+        + (shape(ROWS, WIDE), shape(HALF, WIDE)),
+        0,
+        9,
         0,
         [pltpu.VMEM((2 * ROWS, 128), BF)] * 3
         + [
@@ -487,7 +482,7 @@
             pltpu.VMEM((2 * ROWS, 128), BF),
             pltpu.VMEM((1, 128), F32),
             pltpu.SMEM((2,), F32),
-            pltpu.SemaphoreType.DMA((8,)),
+            pltpu.SemaphoreType.DMA((10,)),
         ],
         10**8,
     )(
@@ -499,27 +494,16 @@
         out_grad.reshape(2 * ROWS, 128),
         norm_gain.reshape(1, 128),
         mix_lambda,
+        latents,
     )
     ys = [traded(yown, "y", n) for n in range(1, SIDE)]
     zs = [traded(x, "z", n) for n, x in enumerate(sends, 1)]
-    lat_own, lat_near, lat_far = call(
-        fetch_kernel,
-        (shape(ROWS, WIDE), shape(ROWS, WIDE), shape(HALF, WIDE)),
-        0,
-        1,
-        0,
-        [pltpu.SemaphoreType.DMA((3,))],
-        10**7,
-        1,
-    )(latents)
     near = traded_apart(lat_near)
     apart = traded(lat_far, "z", 2)
     near_swap = partner(near)
     apart_swap = partner(apart)
 
     slots = 2 * SIDE
-    small = shape(ROWS, 128)
-    both = shape(2 * ROWS, 128)
     state_shapes = (
         shape(slots, SLOT, 128),
         shape(slots, 8, ROWS, dtype=F32),
@@ -532,12 +516,18 @@
     )
     holds = [pltpu.VMEM((2, ROWS, ROWS), BF), pltpu.VMEM((2, 2 * ROWS, ROWS), BF)]
     pair_flops = 10 * ROWS * ROWS * 128
-    state = call(
-        attend_near_kernel, state_shapes, 1, 0, 6, holds, 10 * pair_flops
-    )(mix_lambda, yown, ys[0], ys[2], zown, zs[0], zs[2])
+    *state, lat_own = call(
+        attend_near_kernel,
+        state_shapes + (shape(ROWS, WIDE),),
+        1,
+        1,
+        6,
+        holds + [pltpu.SemaphoreType.DMA],
+        10 * pair_flops,
+    )(mix_lambda, latents, yown, ys[0], ys[2], zown, zs[0], zs[2])
     result_shapes = (
-        (small,) * 3
-        + (both,) * 6
+        (shape(3 * ROWS, 128),) * 3
+        + (shape(2 * ROWS, 128),) * 3
         + (shape(2, 128, ROWS, dtype=F32),)
         + (shape(2, ROWS, 128, dtype=F32),) * 2
     )
@@ -551,8 +541,8 @@
         7 * pair_flops,
         aliases={3 + n: len(result_shapes) + n for n in range(len(state_shapes))},
     )(mix_lambda, ys[1], zs[1], *state)
-    own_q, own_k, own_v = results[9:12]
-    q_back = [traded(x, "y", n) for n, x in enumerate(results[0:3], 1)]
+    own_q, own_k, own_v = results[6:9]
+    y_back = [traded(x, "y", n) for n, x in enumerate(results[0:3], 1)]
     z_back = [traded(x, "z", n) for n, x in enumerate(results[3:6], 1)]
     turned_grad = call(
         queries_kernel,
@@ -562,9 +552,8 @@
         7,
         [pltpu.VMEM((128, ROWS), F32)],
         10**7,
-    )(own_q, *q_back, *z_back)
+    )(own_q, *y_back, *z_back)
     grads = [traded(turned_grad, "z", n) for n in range(1, SIDE)]
-    kv_back = [traded(x, "y", n) for n, x in enumerate(results[6:9], 1)]
     square = shape(ROWS, ROWS)
     own, *parts = call(
         project_kernel,
@@ -583,7 +572,7 @@
         9,
         [pltpu.VMEM((ROWS, 128), F32)] * 2,
         10**7,
-    )(own_k, own_v, *kv_back, *z_back, turned_grad)
+    )(own_k, own_v, *y_back, *z_back, turned_grad)
     weight_grad = call(
         total_kernel, shape(ROWS, ROWS, dtype=F32), 0, 0, 4, [], 10**6
     )(own, *[traded(x, "y", n) for n, x in enumerate(parts, 1)])

time: 77.7 us -> 74.3 us (0.956)
  starting transfers between devices: 47.6 us -> 33.5 us
  waiting for transfers between devices: 16.1 us -> 27.7 us
  Pallas kernels: 13.1 us -> 12 us
    ppermute x22 -> x19, starting transfers between devices: 45 us -> 31.4 us  [traded(): return lax.ppermute(x, 'sp', [(s, s ^ step) for s in range(SIDE * SIDE)])]
    ppermute x22 -> x19, waiting for transfers between devices: 16.1 us -> 27.7 us  [traded(): return lax.ppermute(x, 'sp', [(s, s ^ step) for s in range(SIDE * SIDE)])]
    pallas_call x8 -> x7, Pallas kernels: 13.1 us -> 12 us  [run(): return calling(*arrays[:scalars], *held, *rest)]
  transfers between devices with their start and end apart: 25 -> 22, of which waited for: 9 -> 12; matrix products, arithmetic and copies ran while one was open for 0% -> 0% of each run, Pallas kernels for 14% -> 11%
where the time goes in v4:
time: 74.3 us; the launch traced here: 74.1 us
  starting transfers between devices  33.5 us (45%)
  waiting for transfers between devices  27.7 us (37%)
  Pallas kernels  12 us (16%)
    ppermute x19, starting transfers between devices, traded(): return lax.ppermute(x, 'sp', [(s, s ^ step) for s in range(SIDE * SIDE)])  31.4 us
    ppermute x19, waiting for transfers between devices, traded(): return lax.ppermute(x, 'sp', [(s, s ^ step) for s in range(SIDE * SIDE)])  27.7 us
    pallas_call x7, Pallas kernels, run(): return calling(*arrays[:scalars], *held, *rest)  12 us
    ppermute x1, starting transfers between devices, traded_apart(): return lax.ppermute(x, ('sp', 'tp'), pairs)  2.11 us
  transfers between devices with their start and end apart: 22, of which 12 were waited for; matrix products, arithmetic and copies ran while one was open for 0% of the time, Pallas kernels for 11%

profile of v4, /device:TPU:0, one launch (start us, length us, event | category | flops | bytes accessed | tf_op | source)
XLA Modules:
  0.0 74.1 jit_solution(14486445869300486008)
XLA Ops:
  0.6 2.0 %shard_map.120 = (bf16[1056,128]{1,0:T(8,128)(2,1)S(1)}, bf16[1056,128]{1,0:T(8,128)(2,1)S(1)}, bf16[544,128]{1,0:T(8,128)(2,1)S(1)}, bf16[544,128]{1,0:T(8,128)...) custom-call(bf16[512,128]{1,0:T(8,128)(2,1)} %bitcast.11, ...), custom_call_target="tpu_custom_call" | custom-call | flops 100000000 | bytes 1000000 | tf_op jit(solution)/shard_map/pallas_call | solution.py:454
  2.7 2.1 %collective-permute-start.15 = (bf16[256,1024]{1,0:T(8,128)(2,1)S(1)}, bf16[256,1024]{1,0:T(8,128)(2,1)S(1)}, u32[]{:S(2)}, u32[]{:S(2)}) collective-permute-start(bf16[256,1024]{1,0:T(8,128)(2,1)S(1)} %get-tuple-element.62), channel_id=1, source_target_pairs={{0,32},{1,97},{2,34},{3,99},{4,36},{5,101},{6,38},{7,103},{8,40},{... | collective-permute-start | bytes 1572872 | tf_op jit(solution)/shard_map/ppermute | solution.py:421
  4.8 0.1 collective-permute-start.4
  4.9 1.6 %collective-permute-start.2 = (bf16[1056,128]{1,0:T(8,128)(2,1)S(1)}, bf16[1056,128]{1,0:T(8,128)(2,1)S(1)}, u32[]{:S(2)}, u32[]{:S(2)}) collective-permute-start(bf16[1056,128]{1,0:T(8,128)(2,1)S(1)} %get-tuple-element.36.yown), channel_id=1, source_target_pairs={{0,8},{8,0},{16,24},{24,16},{32,40},{40,32},{48,56},{56,48},{64,72... | collective-permute-start | bytes 811016 | tf_op jit(solution)/shard_map/ppermute | solution.py:411
  6.5 2.2 %collective-permute-start.3 = (bf16[1056,128]{1,0:T(8,128)(2,1)S(1)}, bf16[1056,128]{1,0:T(8,128)(2,1)S(1)}, u32[]{:S(2)}, u32[]{:S(2)}) collective-permute-start(bf16[1056,128]{1,0:T(8,128)(2,1)S(1)} %get-tuple-element.36.yown), channel_id=1, source_target_pairs={{0,24},{8,16},{16,8},{24,0},{32,56},{40,48},{48,40},{56,32},{64,88... | collective-permute-start | bytes 811016 | tf_op jit(solution)/shard_map/ppermute | solution.py:411
  8.7 4.0 %collective-permute-start.5 = (bf16[544,128]{1,0:T(8,128)(2,1)S(1)}, bf16[544,128]{1,0:T(8,128)(2,1)S(1)}, u32[]{:S(2)}, u32[]{:S(2)}) collective-permute-start(bf16[544,128]{1,0:T(8,128)(2,1)S(1)} %get-tuple-element.40), channel_id=1, source_target_pairs={{0,96},{8,104},{16,112},{24,120},{32,64},{40,72},{48,80},{56,88},{... | collective-permute-start | bytes 417800 | tf_op jit(solution)/shard_map/ppermute | solution.py:411
  12.7 2.2 %collective-permute-done.4.z1 = bf16[544,128]{1,0:T(8,128)(2,1)S(1)} collective-permute-done((bf16[544,128]{1,0:T(8,128)(2,1)S(1)}, bf16[544,128]{1,0:T(8,128)(2,1)S(1)}, u32[]{:S(2)}, u32[]{:S(2)}) %collective-permute-start.4) | collective-permute-done | bytes 139296 | tf_op jit(solution)/shard_map/ppermute | solution.py:411
  14.9 3.3 %collective-permute-start = (bf16[1056,128]{1,0:T(8,128)(2,1)S(1)}, bf16[1056,128]{1,0:T(8,128)(2,1)S(1)}, u32[]{:S(2)}, u32[]{:S(2)}) collective-permute-start(bf16[1056,128]{1,0:T(8,128)(2,1)S(1)} %get-tuple-element.36.yown), channel_id=1, source_target_pairs={{0,16},{8,24},{16,0},{24,8},{32,48},{40,56},{48,32},{56,40},{64,80... | collective-permute-start | bytes 811016 | tf_op jit(solution)/shard_map/ppermute | solution.py:411
  18.2 0.0 collective-permute-done.5.z3
  18.2 2.8 %collective-permute-start.1 = (bf16[544,128]{1,0:T(8,128)(2,1)S(1)}, bf16[544,128]{1,0:T(8,128)(2,1)S(1)}, u32[]{:S(2)}, u32[]{:S(2)}) collective-permute-start(bf16[544,128]{1,0:T(8,128)(2,1)S(1)} %get-tuple-element.37), channel_id=1, source_target_pairs={{0,64},{8,72},{16,80},{24,88},{32,96},{40,104},{48,112},{56,120},{... | collective-permute-start | bytes 417800 | tf_op jit(solution)/shard_map/ppermute | solution.py:411
  21.1 0.0 collective-permute-done.2.y1
  21.1 0.7 collective-permute-start.17
  21.8 0.0 collective-permute-done.15.near
  21.8 0.0 collective-permute-start.16
  21.8 0.0 collective-permute-done.3.y3
  21.8 3.9 %shard_map.121 = (bf16[8,1056,128]{2,1,0:T(8,128)(2,1)S(1)}, f32[8,8,256]{2,1,0:T(8,128)S(1)}, bf16[8,512,128]{2,1,0:T(8,128)(2,1)S(1)}, bf16[8,128,512]{2,1,0:T...) custom-call(f32[2]{0:T(128)S(1)} %copy-done, ...), custom_call_target="tpu_custom_call" | custom-call | flops 838860800 | bytes 1000000 | tf_op jit(solution)/shard_map/pallas_call | solution.py:454
  25.7 0.0 collective-permute-done.1.z2
  25.7 3.2 %shard_map.122 = (bf16[768,128]{1,0:T(8,128)(2,1)S(1)}, bf16[768,128]{1,0:T(8,128)(2,1)S(1)}, bf16[768,128]{1,0:T(8,128)(2,1)S(1)}, bf16[512,128]{1,0:T(8,128)(2...) custom-call(f32[2]{0:T(128)S(1)} %copy-done, ...), custom_call_target="tpu_custom_call", output_to_operand_aliasing={{9}: (3, {}), {10}: (4, {}), {11}: (5, {}), {12}: (6, {}), ... | custom-call | flops 587202560 | bytes 1000000 | tf_op jit(solution)/shard_map/pallas_call | solution.py:454
  28.9 2.9 %collective-permute-start.10 = (bf16[512,128]{1,0:T(8,128)(2,1)S(1)}, bf16[512,128]{1,0:T(8,128)(2,1)S(1)}, u32[]{:S(2)}, u32[]{:S(2)}) collective-permute-start(bf16[512,128]{1,0:T(8,128)(2,1)S(1)} %get-tuple-element.55), channel_id=1, source_target_pairs={{0,64},{8,72},{16,80},{24,88},{32,96},{40,104},{48,112},{56,120},{... | collective-permute-start | bytes 393224 | tf_op jit(solution)/shard_map/ppermute | solution.py:411
  31.8 1.8 %collective-permute-start.11 = (bf16[512,128]{1,0:T(8,128)(2,1)S(1)}, bf16[512,128]{1,0:T(8,128)(2,1)S(1)}, u32[]{:S(2)}, u32[]{:S(2)}) collective-permute-start(bf16[512,128]{1,0:T(8,128)(2,1)S(1)} %get-tuple-element.56), channel_id=1, source_target_pairs={{0,96},{8,104},{16,112},{24,120},{32,64},{40,72},{48,80},{56,88},{... | collective-permute-start | bytes 393224 | tf_op jit(solution)/shard_map/ppermute | solution.py:411
  33.6 0.0 collective-permute-start.9
  33.6 0.0 collective-permute-done.17.far
  33.6 1.2 %collective-permute-start.6 = (bf16[768,128]{1,0:T(8,128)(2,1)S(1)}, bf16[768,128]{1,0:T(8,128)(2,1)S(1)}, u32[]{:S(2)}, u32[]{:S(2)}) collective-permute-start(bf16[768,128]{1,0:T(8,128)(2,1)S(1)} %get-tuple-element.51), channel_id=1, source_target_pairs={{0,8},{8,0},{16,24},{24,16},{32,40},{40,32},{48,56},{56,48},{64,72... | collective-permute-start | bytes 589832 | tf_op jit(solution)/shard_map/ppermute | solution.py:411
  34.8 1.6 %collective-permute-done.10.z2 = bf16[512,128]{1,0:T(8,128)(2,1)S(1)} collective-permute-done((bf16[512,128]{1,0:T(8,128)(2,1)S(1)}, bf16[512,128]{1,0:T(8,128)(2,1)S(1)}, u32[]{:S(2)}, u32[]{:S(2)}) %collective-permute-start.10) | collective-permute-done | bytes 131104 | tf_op jit(solution)/shard_map/ppermute | solution.py:411
  36.4 0.2 collective-permute-start.7
  36.7 2.5 %collective-permute-done.11.z3 = bf16[512,128]{1,0:T(8,128)(2,1)S(1)} collective-permute-done((bf16[512,128]{1,0:T(8,128)(2,1)S(1)}, bf16[512,128]{1,0:T(8,128)(2,1)S(1)}, u32[]{:S(2)}, u32[]{:S(2)}) %collective-permute-start.11) | collective-permute-done | bytes 131104 | tf_op jit(solution)/shard_map/ppermute | solution.py:411
  39.2 1.1 %collective-permute-start.8 = (bf16[768,128]{1,0:T(8,128)(2,1)S(1)}, bf16[768,128]{1,0:T(8,128)(2,1)S(1)}, u32[]{:S(2)}, u32[]{:S(2)}) collective-permute-start(bf16[768,128]{1,0:T(8,128)(2,1)S(1)} %get-tuple-element.53), channel_id=1, source_target_pairs={{0,24},{8,16},{16,8},{24,0},{32,56},{40,48},{48,40},{56,32},{64,88... | collective-permute-start | bytes 589832 | tf_op jit(solution)/shard_map/ppermute | solution.py:411
  40.2 0.0 collective-permute-done.9.z1
  40.2 0.0 collective-permute-start.18
  40.3 1.1 %collective-permute-done.6.y1 = bf16[768,128]{1,0:T(8,128)(2,1)S(1)} collective-permute-done((bf16[768,128]{1,0:T(8,128)(2,1)S(1)}, bf16[768,128]{1,0:T(8,128)(2,1)S(1)}, u32[]{:S(2)}, u32[]{:S(2)}) %collective-permute-start.6) | collective-permute-done | bytes 196640 | tf_op jit(solution)/shard_map/ppermute | solution.py:411
  41.4 3.8 %collective-permute-done.7.y2 = bf16[768,128]{1,0:T(8,128)(2,1)S(1)} collective-permute-done((bf16[768,128]{1,0:T(8,128)(2,1)S(1)}, bf16[768,128]{1,0:T(8,128)(2,1)S(1)}, u32[]{:S(2)}, u32[]{:S(2)}) %collective-permute-start.7) | collective-permute-done | bytes 196640 | tf_op jit(solution)/shard_map/ppermute | solution.py:411
  45.1 4.1 %collective-permute-done.8.y3 = bf16[768,128]{1,0:T(8,128)(2,1)S(1)} collective-permute-done((bf16[768,128]{1,0:T(8,128)(2,1)S(1)}, bf16[768,128]{1,0:T(8,128)(2,1)S(1)}, u32[]{:S(2)}, u32[]{:S(2)}) %collective-permute-start.8) | collective-permute-done | bytes 196640 | tf_op jit(solution)/shard_map/ppermute | solution.py:411
  49.2 0.1 shard_map.123.turned_in.g0
  49.3 1.8 %collective-permute-start.12 = (bf16[256,256]{1,0:T(8,128)(2,1)S(1)}, bf16[256,256]{1,0:T(8,128)(2,1)S(1)}, u32[]{:S(2)}, u32[]{:S(2)}) collective-permute-start(bf16[256,256]{1,0:T(8,128)(2,1)S(1)} %shard_map.123.turned_in.g0), channel_id=1, source_target_pairs={{0,32},{8,40},{16,48},{24,56},{32,0},{40,8},{48,16},{56,24},{64,96... | collective-permute-start | bytes 393224 | tf_op jit(solution)/shard_map/ppermute | solution.py:411
  51.1 2.0 %collective-permute-start.13 = (bf16[256,256]{1,0:T(8,128)(2,1)S(1)}, bf16[256,256]{1,0:T(8,128)(2,1)S(1)}, u32[]{:S(2)}, u32[]{:S(2)}) collective-permute-start(bf16[256,256]{1,0:T(8,128)(2,1)S(1)} %shard_map.123.turned_in.g0), channel_id=1, source_target_pairs={{0,64},{8,72},{16,80},{24,88},{32,96},{40,104},{48,112},{56,120},{... | collective-permute-start | bytes 393224 | tf_op jit(solution)/shard_map/ppermute | solution.py:411
  53.1 1.0 %collective-permute-start.14 = (bf16[256,256]{1,0:T(8,128)(2,1)S(1)}, bf16[256,256]{1,0:T(8,128)(2,1)S(1)}, u32[]{:S(2)}, u32[]{:S(2)}) collective-permute-start(bf16[256,256]{1,0:T(8,128)(2,1)S(1)} %shard_map.123.turned_in.g0), channel_id=1, source_target_pairs={{0,96},{8,104},{16,112},{24,120},{32,64},{40,72},{48,80},{56,88},{... | collective-permute-start | bytes 393224 | tf_op jit(solution)/shard_map/ppermute | solution.py:411
  54.1 1.7 %collective-permute-done.12.g1 = bf16[256,256]{1,0:T(8,128)(2,1)S(1)} collective-permute-done((bf16[256,256]{1,0:T(8,128)(2,1)S(1)}, bf16[256,256]{1,0:T(8,128)(2,1)S(1)}, u32[]{:S(2)}, u32[]{:S(2)}) %collective-permute-start.12) | collective-permute-done | bytes 131104 | tf_op jit(solution)/shard_map/ppermute | solution.py:411
  55.8 3.7 %collective-permute-done.13.g2 = bf16[256,256]{1,0:T(8,128)(2,1)S(1)} collective-permute-done((bf16[256,256]{1,0:T(8,128)(2,1)S(1)}, bf16[256,256]{1,0:T(8,128)(2,1)S(1)}, u32[]{:S(2)}, u32[]{:S(2)}) %collective-permute-start.13) | collective-permute-done | bytes 131104 | tf_op jit(solution)/shard_map/ppermute | solution.py:411
  59.4 2.2 %collective-permute-done.14.g3 = bf16[256,256]{1,0:T(8,128)(2,1)S(1)} collective-permute-done((bf16[256,256]{1,0:T(8,128)(2,1)S(1)}, bf16[256,256]{1,0:T(8,128)(2,1)S(1)}, u32[]{:S(2)}, u32[]{:S(2)}) %collective-permute-start.14) | collective-permute-done | bytes 131104 | tf_op jit(solution)/shard_map/ppermute | solution.py:411
  61.6 0.9 %shard_map.125 = (f32[256,256]{1,0:T(8,128)S(1)}, bf16[256,256]{1,0:T(8,128)(2,1)S(1)}, bf16[256,256]{1,0:T(8,128)(2,1)S(1)}, bf16[256,256]{1,0:T(8,128)(2,1)S(1)}) custom-call(bf16[256,256]{1,0:T(8,128)(2,1)S(1)} %shard_map.123.turned_in.g0, bf16[256,256]{1,0:T(8,128)(2,1)S(1)} %collective-permute-done.12.g1, ...), custom_call_target="tpu_custom_call" | custom-call | flops 536870912 | bytes 1000000 | tf_op jit(solution)/shard_map/pallas_call | solution.py:454
  62.5 0.1 collective-permute-start.19
  62.6 2.9 %collective-permute-start.20 = (bf16[256,256]{1,0:T(8,128)(2,1)S(1)}, bf16[256,256]{1,0:T(8,128)(2,1)S(1)}, u32[]{:S(2)}, u32[]{:S(2)}) collective-permute-start(bf16[256,256]{1,0:T(8,128)(2,1)S(1)} %get-tuple-element.66), channel_id=1, source_target_pairs={{0,16},{8,24},{16,0},{24,8},{32,48},{40,56},{48,32},{56,40},{64,80... | collective-permute-start | bytes 393224 | tf_op jit(solution)/shard_map/ppermute | solution.py:411
  65.5 1.7 %collective-permute-start.21 = (bf16[256,256]{1,0:T(8,128)(2,1)S(1)}, bf16[256,256]{1,0:T(8,128)(2,1)S(1)}, u32[]{:S(2)}, u32[]{:S(2)}) collective-permute-start(bf16[256,256]{1,0:T(8,128)(2,1)S(1)} %get-tuple-element.67), channel_id=1, source_target_pairs={{0,24},{8,16},{16,8},{24,0},{32,56},{40,48},{48,40},{56,32},{64,88... | collective-permute-start | bytes 393224 | tf_op jit(solution)/shard_map/ppermute | solution.py:411
  67.3 1.1 %shard_map.124 = (bf16[512,128]{1,0:T(8,128)(2,1)}, bf16[512,128]{1,0:T(8,128)(2,1)}, bf16[512,128]{1,0:T(8,128)(2,1)}) custom-call(f32[2,256,128]{2,1,0:T(8,128)S(1)} %get-tuple-element.49.own_k, f32[2,256,128]{2,1,0:T(8,128)S(1)} %get-tuple-element.50.own_v, bf16[768,128]{1,0:T(8,128)(2,1)S(1)} %collective-permute-done.6.y1, ...), custom_call_target="tpu_custom_call" | custom-call | flops 10000000 | bytes 1000000 | tf_op jit(solution)/shard_map/pallas_call | solution.py:454
  68.4 0.4 collective-permute-done.19.t1
  68.9 2.4 %collective-permute-done.20.t2 = bf16[256,256]{1,0:T(8,128)(2,1)S(1)} collective-permute-done((bf16[256,256]{1,0:T(8,128)(2,1)S(1)}, bf16[256,256]{1,0:T(8,128)(2,1)S(1)}, u32[]{:S(2)}, u32[]{:S(2)}) %collective-permute-start.20) | collective-permute-done | bytes 131104 | tf_op jit(solution)/shard_map/ppermute | solution.py:411
  71.3 1.9 %collective-permute-done.21.t3 = bf16[256,256]{1,0:T(8,128)(2,1)S(1)} collective-permute-done((bf16[256,256]{1,0:T(8,128)(2,1)S(1)}, bf16[256,256]{1,0:T(8,128)(2,1)S(1)}, u32[]{:S(2)}, u32[]{:S(2)}) %collective-permute-start.21) | collective-permute-done | bytes 131104 | tf_op jit(solution)/shard_map/ppermute | solution.py:411
  73.2 0.8 %shard_map.126 = f32[256,256]{1,0:T(8,128)} custom-call(f32[256,256]{1,0:T(8,128)S(1)} %get-tuple-element.64.own, bf16[256,256]{1,0:T(8,128)(2,1)S(1)} %collective-permute-done.19.t1, bf16[256,256]{1,0:T(8,128)(2,1)S(1)} %collective-permute-done.20.t2, bf16[256,256]{1,0:T(8,128)(2,1)S(1)} %collective-permute-done.21.t3), custom_call_target="tpu_custom_call" | custom-call | flops 1000000 | bytes 1000000 | tf_op jit(solution)/shard_map/pallas_call | solution.py:454
  (5 shorter events, 0.0 us)
Async XLA Ops:
  0.6 21.1 %copy-start = (f32[2]{0:T(128)S(1)}, f32[2]{0:T(128)}, u32[]{:S(2)}) copy-start(f32[2]{0:T(128)} %lam.3) | copy-start | bytes 28
  2.7 19.1 %collective-permute-start.15 = (bf16[256,1024]{1,0:T(8,128)(2,1)S(1)}, bf16[256,1024]{1,0:T(8,128)(2,1)S(1)}, u32[]{:S(2)}, u32[]{:S(2)}) collective-permute-start(bf16[256,1024]{1,0:T(8,128)(2,1)S(1)} %get-tuple-element.62), channel_id=1, source_target_pairs={{0,32},{1,97},{2,34},{3,99},{4,36},{5,101},{6,38},{7,103},{8,40},{... | collective-permute-start | bytes 1572872 | tf_op jit(solution)/shard_map/ppermute | solution.py:421
  4.8 10.1 %collective-permute-start.4 = (bf16[544,128]{1,0:T(8,128)(2,1)S(1)}, bf16[544,128]{1,0:T(8,128)(2,1)S(1)}, u32[]{:S(2)}, u32[]{:S(2)}) collective-permute-start(bf16[544,128]{1,0:T(8,128)(2,1)S(1)} %get-tuple-element.39), channel_id=1, source_target_pairs={{0,32},{8,40},{16,48},{24,56},{32,0},{40,8},{48,16},{56,24},{64,96... | collective-permute-start | bytes 417800 | tf_op jit(solution)/shard_map/ppermute | solution.py:411
  4.9 16.2 %collective-permute-start.2 = (bf16[1056,128]{1,0:T(8,128)(2,1)S(1)}, bf16[1056,128]{1,0:T(8,128)(2,1)S(1)}, u32[]{:S(2)}, u32[]{:S(2)}) collective-permute-start(bf16[1056,128]{1,0:T(8,128)(2,1)S(1)} %get-tuple-element.36.yown), channel_id=1, source_target_pairs={{0,8},{8,0},{16,24},{24,16},{32,40},{40,32},{48,56},{56,48},{64,72... | collective-permute-start | bytes 811016 | tf_op jit(solution)/shard_map/ppermute | solution.py:411
  6.5 15.3 %collective-permute-start.3 = (bf16[1056,128]{1,0:T(8,128)(2,1)S(1)}, bf16[1056,128]{1,0:T(8,128)(2,1)S(1)}, u32[]{:S(2)}, u32[]{:S(2)}) collective-permute-start(bf16[1056,128]{1,0:T(8,128)(2,1)S(1)} %get-tuple-element.36.yown), channel_id=1, source_target_pairs={{0,24},{8,16},{16,8},{24,0},{32,56},{40,48},{48,40},{56,32},{64,88... | collective-permute-start | bytes 811016 | tf_op jit(solution)/shard_map/ppermute | solution.py:411
  8.7 9.6 %collective-permute-start.5 = (bf16[544,128]{1,0:T(8,128)(2,1)S(1)}, bf16[544,128]{1,0:T(8,128)(2,1)S(1)}, u32[]{:S(2)}, u32[]{:S(2)}) collective-permute-start(bf16[544,128]{1,0:T(8,128)(2,1)S(1)} %get-tuple-element.40), channel_id=1, source_target_pairs={{0,96},{8,104},{16,112},{24,120},{32,64},{40,72},{48,80},{56,88},{... | collective-permute-start | bytes 417800 | tf_op jit(solution)/shard_map/ppermute | solution.py:411
  14.9 10.8 %collective-permute-start = (bf16[1056,128]{1,0:T(8,128)(2,1)S(1)}, bf16[1056,128]{1,0:T(8,128)(2,1)S(1)}, u32[]{:S(2)}, u32[]{:S(2)}) collective-permute-start(bf16[1056,128]{1,0:T(8,128)(2,1)S(1)} %get-tuple-element.36.yown), channel_id=1, source_target_pairs={{0,16},{8,24},{16,0},{24,8},{32,48},{40,56},{48,32},{56,40},{64,80... | collective-permute-start | bytes 811016 | tf_op jit(solution)/shard_map/ppermute | solution.py:411
  18.2 7.5 %collective-permute-start.1 = (bf16[544,128]{1,0:T(8,128)(2,1)S(1)}, bf16[544,128]{1,0:T(8,128)(2,1)S(1)}, u32[]{:S(2)}, u32[]{:S(2)}) collective-permute-start(bf16[544,128]{1,0:T(8,128)(2,1)S(1)} %get-tuple-element.37), channel_id=1, source_target_pairs={{0,64},{8,72},{16,80},{24,88},{32,96},{40,104},{48,112},{56,120},{... | collective-permute-start | bytes 417800 | tf_op jit(solution)/shard_map/ppermute | solution.py:411
  21.1 12.5 %collective-permute-start.17 = (bf16[128,1024]{1,0:T(8,128)(2,1)S(1)}, bf16[128,1024]{1,0:T(8,128)(2,1)S(1)}, u32[]{:S(2)}, u32[]{:S(2)}) collective-permute-start(bf16[128,1024]{1,0:T(8,128)(2,1)S(1)} %get-tuple-element.63), channel_id=1, source_target_pairs={{0,64},{8,72},{16,80},{24,88},{32,96},{40,104},{48,112},{56,120},{... | collective-permute-start | bytes 786440 | tf_op jit(solution)/shard_map/ppermute | solution.py:411
  21.8 39.9 %collective-permute-start.16 = (bf16[256,1024]{1,0:T(8,128)(2,1)S(1)}, bf16[256,1024]{1,0:T(8,128)(2,1)S(1)}, u32[]{:S(2)}, u32[]{:S(2)}) collective-permute-start(bf16[256,1024]{1,0:T(8,128)(2,1)S(1)} %collective-permute-done.15.near), channel_id=1, source_target_pairs={{0,1},{1,0},{2,3},{3,2},{4,5},{5,4},{6,7},{7,6},{8,9},{9,8},{10,11... | collective-permute-start | bytes 1572872 | tf_op jit(solution)/shard_map/ppermute | solution.py:425
  28.9 7.5 %collective-permute-start.10 = (bf16[512,128]{1,0:T(8,128)(2,1)S(1)}, bf16[512,128]{1,0:T(8,128)(2,1)S(1)}, u32[]{:S(2)}, u32[]{:S(2)}) collective-permute-start(bf16[512,128]{1,0:T(8,128)(2,1)S(1)} %get-tuple-element.55), channel_id=1, source_target_pairs={{0,64},{8,72},{16,80},{24,88},{32,96},{40,104},{48,112},{56,120},{... | collective-permute-start | bytes 393224 | tf_op jit(solution)/shard_map/ppermute | solution.py:411
  31.8 7.4 %collective-permute-start.11 = (bf16[512,128]{1,0:T(8,128)(2,1)S(1)}, bf16[512,128]{1,0:T(8,128)(2,1)S(1)}, u32[]{:S(2)}, u32[]{:S(2)}) collective-permute-start(bf16[512,128]{1,0:T(8,128)(2,1)S(1)} %get-tuple-element.56), channel_id=1, source_target_pairs={{0,96},{8,104},{16,112},{24,120},{32,64},{40,72},{48,80},{56,88},{... | collective-permute-start | bytes 393224 | tf_op jit(solution)/shard_map/ppermute | solution.py:411
  33.6 6.7 %collective-permute-start.9 = (bf16[512,128]{1,0:T(8,128)(2,1)S(1)}, bf16[512,128]{1,0:T(8,128)(2,1)S(1)}, u32[]{:S(2)}, u32[]{:S(2)}) collective-permute-start(bf16[512,128]{1,0:T(8,128)(2,1)S(1)} %get-tuple-element.54), channel_id=1, source_target_pairs={{0,32},{8,40},{16,48},{24,56},{32,0},{40,8},{48,16},{56,24},{64,96... | collective-permute-start | bytes 393224 | tf_op jit(solution)/shard_map/ppermute | solution.py:411
  33.6 7.8 %collective-permute-start.6 = (bf16[768,128]{1,0:T(8,128)(2,1)S(1)}, bf16[768,128]{1,0:T(8,128)(2,1)S(1)}, u32[]{:S(2)}, u32[]{:S(2)}) collective-permute-start(bf16[768,128]{1,0:T(8,128)(2,1)S(1)} %get-tuple-element.51), channel_id=1, source_target_pairs={{0,8},{8,0},{16,24},{24,16},{32,40},{40,32},{48,56},{56,48},{64,72... | collective-permute-start | bytes 589832 | tf_op jit(solution)/shard_map/ppermute | solution.py:411
  36.4 8.7 %collective-permute-start.7 = (bf16[768,128]{1,0:T(8,128)(2,1)S(1)}, bf16[768,128]{1,0:T(8,128)(2,1)S(1)}, u32[]{:S(2)}, u32[]{:S(2)}) collective-permute-start(bf16[768,128]{1,0:T(8,128)(2,1)S(1)} %get-tuple-element.52), channel_id=1, source_target_pairs={{0,16},{8,24},{16,0},{24,8},{32,48},{40,56},{48,32},{56,40},{64,80... | collective-permute-start | bytes 589832 | tf_op jit(solution)/shard_map/ppermute | solution.py:411
  39.2 10.0 %collective-permute-start.8 = (bf16[768,128]{1,0:T(8,128)(2,1)S(1)}, bf16[768,128]{1,0:T(8,128)(2,1)S(1)}, u32[]{:S(2)}, u32[]{:S(2)}) collective-permute-start(bf16[768,128]{1,0:T(8,128)(2,1)S(1)} %get-tuple-element.53), channel_id=1, source_target_pairs={{0,24},{8,16},{16,8},{24,0},{32,56},{40,48},{48,40},{56,32},{64,88... | collective-permute-start | bytes 589832 | tf_op jit(solution)/shard_map/ppermute | solution.py:411
  40.2 13.8 %collective-permute-start.18 = (bf16[128,1024]{1,0:T(8,128)(2,1)S(1)}, bf16[128,1024]{1,0:T(8,128)(2,1)S(1)}, u32[]{:S(2)}, u32[]{:S(2)}) collective-permute-start(bf16[128,1024]{1,0:T(8,128)(2,1)S(1)} %collective-permute-done.17.far), channel_id=1, source_target_pairs={{0,1},{1,0},{2,3},{3,2},{4,5},{5,4},{6,7},{7,6},{8,9},{9,8},{10,11... | collective-permute-start | bytes 786440 | tf_op jit(solution)/shard_map/ppermute | solution.py:425
  49.3 6.4 %collective-permute-start.12 = (bf16[256,256]{1,0:T(8,128)(2,1)S(1)}, bf16[256,256]{1,0:T(8,128)(2,1)S(1)}, u32[]{:S(2)}, u32[]{:S(2)}) collective-permute-start(bf16[256,256]{1,0:T(8,128)(2,1)S(1)} %shard_map.123.turned_in.g0), channel_id=1, source_target_pairs={{0,32},{8,40},{16,48},{24,56},{32,0},{40,8},{48,16},{56,24},{64,96... | collective-permute-start | bytes 393224 | tf_op jit(solution)/shard_map/ppermute | solution.py:411
  51.1 8.3 %collective-permute-start.13 = (bf16[256,256]{1,0:T(8,128)(2,1)S(1)}, bf16[256,256]{1,0:T(8,128)(2,1)S(1)}, u32[]{:S(2)}, u32[]{:S(2)}) collective-permute-start(bf16[256,256]{1,0:T(8,128)(2,1)S(1)} %shard_map.123.turned_in.g0), channel_id=1, source_target_pairs={{0,64},{8,72},{16,80},{24,88},{32,96},{40,104},{48,112},{56,120},{... | collective-permute-start | bytes 393224 | tf_op jit(solution)/shard_map/ppermute | solution.py:411
  53.1 8.5 %collective-permute-start.14 = (bf16[256,256]{1,0:T(8,128)(2,1)S(1)}, bf16[256,256]{1,0:T(8,128)(2,1)S(1)}, u32[]{:S(2)}, u32[]{:S(2)}) collective-permute-start(bf16[256,256]{1,0:T(8,128)(2,1)S(1)} %shard_map.123.turned_in.g0), channel_id=1, source_target_pairs={{0,96},{8,104},{16,112},{24,120},{32,64},{40,72},{48,80},{56,88},{... | collective-permute-start | bytes 393224 | tf_op jit(solution)/shard_map/ppermute | solution.py:411
  62.5 6.4 %collective-permute-start.19 = (bf16[256,256]{1,0:T(8,128)(2,1)S(1)}, bf16[256,256]{1,0:T(8,128)(2,1)S(1)}, u32[]{:S(2)}, u32[]{:S(2)}) collective-permute-start(bf16[256,256]{1,0:T(8,128)(2,1)S(1)} %get-tuple-element.65), channel_id=1, source_target_pairs={{0,8},{8,0},{16,24},{24,16},{32,40},{40,32},{48,56},{56,48},{64,72... | collective-permute-start | bytes 393224 | tf_op jit(solution)/shard_map/ppermute | solution.py:411
  62.6 8.7 %collective-permute-start.20 = (bf16[256,256]{1,0:T(8,128)(2,1)S(1)}, bf16[256,256]{1,0:T(8,128)(2,1)S(1)}, u32[]{:S(2)}, u32[]{:S(2)}) collective-permute-start(bf16[256,256]{1,0:T(8,128)(2,1)S(1)} %get-tuple-element.66), channel_id=1, source_target_pairs={{0,16},{8,24},{16,0},{24,8},{32,48},{40,56},{48,32},{56,40},{64,80... | collective-permute-start | bytes 393224 | tf_op jit(solution)/shard_map/ppermute | solution.py:411
  65.5 7.7 %collective-permute-start.21 = (bf16[256,256]{1,0:T(8,128)(2,1)S(1)}, bf16[256,256]{1,0:T(8,128)(2,1)S(1)}, u32[]{:S(2)}, u32[]{:S(2)}) collective-permute-start(bf16[256,256]{1,0:T(8,128)(2,1)S(1)} %get-tuple-element.67), channel_id=1, source_target_pairs={{0,24},{8,16},{16,8},{24,0},{32,56},{40,48},{48,40},{56,32},{64,88... | collective-permute-start | bytes 393224 | tf_op jit(solution)/shard_map/ppermute | solution.py:411

commit v5 on v4

--- a/solution.py
+++ b/solution.py
@@ -55,6 +55,10 @@
     return index // SIDE, lax.rem(index, SIDE), lax.rem(lax.axis_index("tp"), 2)
 
 
+def side():
+    return lax.rem(lax.axis_index("tp") // 2, 2)
+
+
 def prepare_kernel(
     q_hbm, k_hbm, v_hbm, maps_hbm, lse_hbm, out_hbm, gain_hbm, lam_hbm, lat_hbm,
     yown, zown, send1, send2, send3, lat_near, lat_far,
@@ -67,9 +71,10 @@
     ]
     near = jnp.bitwise_xor(z, jnp.where(core == 0, 1, 3))
     columns = pl.ds(pl.multiple_of(near * WIDE, WIDE), WIDE)
-    pairs.append((lat_hbm.at[:, columns], lat_near))
-    tokens = pl.ds(pl.multiple_of(core * HALF, HALF), HALF)
+    tokens = pl.ds(pl.multiple_of(side() * HALF, HALF), HALF)
+    pairs.append((lat_hbm.at[tokens, columns], lat_near))
     columns = pl.ds(pl.multiple_of(jnp.bitwise_xor(z, 2) * WIDE, WIDE), WIDE)
+    tokens = pl.ds(pl.multiple_of(core * HALF + side() * DH, DH), DH)
     pairs.append((lat_hbm.at[tokens, columns], lat_far))
     copies = [pltpu.make_async_copy(a, b, sems.at[n]) for n, (a, b) in enumerate(pairs)]
     for copy in copies:
@@ -372,28 +377,25 @@
 
 
 def project_kernel(
-    g0, g1, g2, g3, lat0, near, near_swap, far, far_swap, own, to1, to2, to3, lat
+    g0, g1, g2, g3, lat0, n0, n1, m0, m1, f0, f1, e0, e1, own, to1, to2, to3, lat
 ):
     _, y, core = position()
     lat[0:ROWS] = lat0[...]
-    first = slice(ROWS, 2 * ROWS)
-    second = slice(2 * ROWS, 2 * ROWS + HALF)
-    third = slice(2 * ROWS + HALF, 3 * ROWS)
-    fourth = slice(3 * ROWS, 4 * ROWS)
-
-    @pl.when(core == 0)
-    def _():
-        lat[first] = near[...]
-        lat[second] = far[...]
-        lat[third] = far_swap[...]
-        lat[fourth] = near_swap[...]
-
-    @pl.when(core == 1)
-    def _():
-        lat[first] = near_swap[...]
-        lat[second] = far_swap[...]
-        lat[third] = far[...]
-        lat[fourth] = near[...]
+    other = side()
+    for c in range(2):
+        for x in range(2):
+            @pl.when(jnp.logical_and(core == c, other == x))
+            def _():
+                for half in range(2):
+                    mine = (n0, n1, f0, f1) if half == c else (m0, m1, e0, e1)
+                    block = ROWS * (1 if half == 0 else 3)
+                    far = 2 * ROWS + half * HALF
+                    for step in range(2):
+                        which = step ^ x
+                        rows = block + step * HALF
+                        lat[rows : rows + HALF] = mine[which][...]
+                        rows = far + step * DH
+                        lat[rows : rows + DH] = mine[2 + which][...]
 
     grads = jnp.concatenate([g0[...], g1[...], g2[...], g3[...]], axis=1)
     for n, ref in ((1, to1), (2, to2), (3, to3), (0, own)):
@@ -419,6 +421,10 @@
             there = s ^ (SIDE * (1 if t % 2 == 0 else 3))
             pairs.append((s * heads + t, there * heads + t))
     return lax.ppermute(x, ("sp", "tp"), pairs)
+
+
+def across(x):
+    return lax.ppermute(x, "tp", [(t, t ^ 2) for t in range(lax.axis_size("tp"))])
 
 
 def partner(x):
@@ -471,7 +477,7 @@
         prepare_kernel,
         (shape(SLOT, 128),) * 2
         + (shape(QG, 128),) * 3
-        + (shape(ROWS, WIDE), shape(HALF, WIDE)),
+        + (shape(HALF, WIDE), shape(DH, WIDE)),
         0,
         9,
         0,
@@ -500,8 +506,18 @@
     zs = [traded(x, "z", n) for n, x in enumerate(sends, 1)]
     near = traded_apart(lat_near)
     apart = traded(lat_far, "z", 2)
-    near_swap = partner(near)
-    apart_swap = partner(apart)
+    near_side = across(near)
+    apart_side = across(apart)
+    lats = (
+        near,
+        near_side,
+        partner(near),
+        partner(near_side),
+        apart,
+        apart_side,
+        partner(apart),
+        partner(apart_side),
+    )
 
     slots = 2 * SIDE
     state_shapes = (
@@ -560,10 +576,10 @@
         (shape(ROWS, ROWS, dtype=F32), square, square, square),
         0,
         0,
-        9,
+        13,
         [pltpu.VMEM((WIDE, WIDE), BF)],
         2 * WIDE * WIDE * ROWS,
-    )(turned_grad, *grads, lat_own, near, near_swap, apart, apart_swap)
+    )(turned_grad, *grads, lat_own, *lats)
     query_rows, key_rows, value_rows = call(
         keys_kernel,
         (shape(2 * ROWS, 128),) * 3,

time: 74.3 us -> 68.8 us (0.926)
  waiting for transfers between devices: 27.7 us -> 17.2 us
  starting transfers between devices: 33.5 us -> 38 us
    ppermute x19, waiting for transfers between devices: 27.7 us -> 17.2 us  [traded(): return lax.ppermute(x, 'sp', [(s, s ^ step) for s in range(SIDE * SIDE)])]
    ppermute x0 -> x2, starting transfers between devices: none -> 2.4 us  [across(): lax.ppermute(x, 'tp', [(t, t ^ 2) for t in range(lax.axis_size('tp'))])]
    ppermute x19, starting transfers between devices: 31.4 us -> 33.5 us  [traded(): return lax.ppermute(x, 'sp', [(s, s ^ step) for s in range(SIDE * SIDE)])]
    ppermute x1, starting transfers between devices: 2.11 us -> 1.02 us  [traded_apart(): return lax.ppermute(x, ('sp', 'tp'), pairs)]
    ppermute x2 -> x4, starting transfers between devices: 0.01 us -> 1.02 us  [partner(): lax.ppermute(x, 'tp', [(t, t ^ 1) for t in range(lax.axis_size('tp'))])]
  transfers between devices with their start and end apart: 22 -> 26, of which waited for: 12 -> 12; matrix products, arithmetic and copies ran while one was open for 0% -> 0% of each run, Pallas kernels for 11% -> 12%
where the time goes in v5:
time: 68.8 us; the launch traced here: 67.9 us
  starting transfers between devices  38 us (55%)
  waiting for transfers between devices  17.2 us (25%)
  Pallas kernels  12 us (17%)
  between operations  0.71 us (1%)
    ppermute x19, starting transfers between devices, traded(): return lax.ppermute(x, 'sp', [(s, s ^ step) for s in range(SIDE * SIDE)])  33.5 us
    ppermute x19, waiting for transfers between devices, traded(): return lax.ppermute(x, 'sp', [(s, s ^ step) for s in range(SIDE * SIDE)])  17.2 us
    pallas_call x7, Pallas kernels, run(): return calling(*arrays[:scalars], *held, *rest)  12 us
    ppermute x2, starting transfers between devices, across(): lax.ppermute(x, 'tp', [(t, t ^ 2) for t in range(lax.axis_size('tp'))])  2.4 us
  transfers between devices with their start and end apart: 26, of which 12 were waited for; matrix products, arithmetic and copies ran while one was open for 0% of the time, Pallas kernels for 12%

profile of v5, /device:TPU:0, one launch (start us, length us, event | category | flops | bytes accessed | tf_op | source)
XLA Modules:
  0.0 67.9 jit_solution(12888589298320021343)
XLA Ops:
  0.6 2.0 %shard_map.120 = (bf16[1056,128]{1,0:T(8,128)(2,1)S(1)}, bf16[1056,128]{1,0:T(8,128)(2,1)S(1)}, bf16[544,128]{1,0:T(8,128)(2,1)S(1)}, bf16[544,128]{1,0:T(8,128)...) custom-call(bf16[512,128]{1,0:T(8,128)(2,1)} %bitcast.11, ...), custom_call_target="tpu_custom_call" | custom-call | flops 100000000 | bytes 1000000 | tf_op jit(solution)/shard_map/pallas_call | solution.py:460
  2.7 4.1 %collective-permute-start.19 = (bf16[64,1024]{1,0:T(8,128)(2,1)S(1)}, bf16[64,1024]{1,0:T(8,128)(2,1)S(1)}, u32[]{:S(2)}, u32[]{:S(2)}) collective-permute-start(bf16[64,1024]{1,0:T(8,128)(2,1)S(1)} %get-tuple-element.63), channel_id=1, source_target_pairs={{0,64},{8,72},{16,80},{24,88},{32,96},{40,104},{48,112},{56,120},{... | collective-permute-start | bytes 393224 | tf_op jit(solution)/shard_map/ppermute | solution.py:413
  6.7 1.6 %collective-permute-start.2 = (bf16[1056,128]{1,0:T(8,128)(2,1)S(1)}, bf16[1056,128]{1,0:T(8,128)(2,1)S(1)}, u32[]{:S(2)}, u32[]{:S(2)}) collective-permute-start(bf16[1056,128]{1,0:T(8,128)(2,1)S(1)} %get-tuple-element.36.yown), channel_id=1, source_target_pairs={{0,8},{8,0},{16,24},{24,16},{32,40},{40,32},{48,56},{56,48},{64,72... | collective-permute-start | bytes 811016 | tf_op jit(solution)/shard_map/ppermute | solution.py:413
  8.3 2.2 %collective-permute-start.3 = (bf16[1056,128]{1,0:T(8,128)(2,1)S(1)}, bf16[1056,128]{1,0:T(8,128)(2,1)S(1)}, u32[]{:S(2)}, u32[]{:S(2)}) collective-permute-start(bf16[1056,128]{1,0:T(8,128)(2,1)S(1)} %get-tuple-element.36.yown), channel_id=1, source_target_pairs={{0,24},{8,16},{16,8},{24,0},{32,56},{40,48},{48,40},{56,32},{64,88... | collective-permute-start | bytes 811016 | tf_op jit(solution)/shard_map/ppermute | solution.py:413
  10.5 1.0 %collective-permute-start.4 = (bf16[544,128]{1,0:T(8,128)(2,1)S(1)}, bf16[544,128]{1,0:T(8,128)(2,1)S(1)}, u32[]{:S(2)}, u32[]{:S(2)}) collective-permute-start(bf16[544,128]{1,0:T(8,128)(2,1)S(1)} %get-tuple-element.39), channel_id=1, source_target_pairs={{0,32},{8,40},{16,48},{24,56},{32,0},{40,8},{48,16},{56,24},{64,96... | collective-permute-start | bytes 417800 | tf_op jit(solution)/shard_map/ppermute | solution.py:413
  11.5 0.0 collective-permute-start.5
  11.5 0.0 collective-permute-done.19.f0
  11.5 2.2 %collective-permute-start = (bf16[1056,128]{1,0:T(8,128)(2,1)S(1)}, bf16[1056,128]{1,0:T(8,128)(2,1)S(1)}, u32[]{:S(2)}, u32[]{:S(2)}) collective-permute-start(bf16[1056,128]{1,0:T(8,128)(2,1)S(1)} %get-tuple-element.36.yown), channel_id=1, source_target_pairs={{0,16},{8,24},{16,0},{24,8},{32,48},{40,56},{48,32},{56,40},{64,80... | collective-permute-start | bytes 811016 | tf_op jit(solution)/shard_map/ppermute | solution.py:413
  13.8 1.8 %collective-permute-done.4.z1 = bf16[544,128]{1,0:T(8,128)(2,1)S(1)} collective-permute-done((bf16[544,128]{1,0:T(8,128)(2,1)S(1)}, bf16[544,128]{1,0:T(8,128)(2,1)S(1)}, u32[]{:S(2)}, u32[]{:S(2)}) %collective-permute-start.4) | collective-permute-done | bytes 139296 | tf_op jit(solution)/shard_map/ppermute | solution.py:413
  15.6 1.0 %collective-permute-start.15 = (bf16[128,1024]{1,0:T(8,128)(2,1)S(1)}, bf16[128,1024]{1,0:T(8,128)(2,1)S(1)}, u32[]{:S(2)}, u32[]{:S(2)}) collective-permute-start(bf16[128,1024]{1,0:T(8,128)(2,1)S(1)} %get-tuple-element.62), channel_id=1, source_target_pairs={{0,32},{1,97},{2,34},{3,99},{4,36},{5,101},{6,38},{7,103},{8,40},{... | collective-permute-start | bytes 786440 | tf_op jit(solution)/shard_map/ppermute | solution.py:423
  16.6 1.5 %collective-permute-done.5.z3 = bf16[544,128]{1,0:T(8,128)(2,1)S(1)} collective-permute-done((bf16[544,128]{1,0:T(8,128)(2,1)S(1)}, bf16[544,128]{1,0:T(8,128)(2,1)S(1)}, u32[]{:S(2)}, u32[]{:S(2)}) %collective-permute-start.5) | collective-permute-done | bytes 139296 | tf_op jit(solution)/shard_map/ppermute | solution.py:413
  18.1 1.3 %collective-permute-start.1 = (bf16[544,128]{1,0:T(8,128)(2,1)S(1)}, bf16[544,128]{1,0:T(8,128)(2,1)S(1)}, u32[]{:S(2)}, u32[]{:S(2)}) collective-permute-start(bf16[544,128]{1,0:T(8,128)(2,1)S(1)} %get-tuple-element.37), channel_id=1, source_target_pairs={{0,64},{8,72},{16,80},{24,88},{32,96},{40,104},{48,112},{56,120},{... | collective-permute-start | bytes 417800 | tf_op jit(solution)/shard_map/ppermute | solution.py:413
  19.4 1.5 %collective-permute-start.20 = (bf16[64,1024]{1,0:T(8,128)(2,1)S(1)}, bf16[64,1024]{1,0:T(8,128)(2,1)S(1)}, u32[]{:S(2)}, u32[]{:S(2)}) collective-permute-start(bf16[64,1024]{1,0:T(8,128)(2,1)S(1)} %collective-permute-done.19.f0), channel_id=1, source_target_pairs={{0,2},{1,3},{2,0},{3,1},{4,6},{5,7},{6,4},{7,5},{8,10},{9,11},{10,... | collective-permute-start | bytes 393224 | tf_op jit(solution)/shard_map/ppermute | solution.py:427
  20.9 0.6 collective-permute-done.3.y3
  21.5 3.9 %shard_map.121 = (bf16[8,1056,128]{2,1,0:T(8,128)(2,1)S(1)}, f32[8,8,256]{2,1,0:T(8,128)S(1)}, bf16[8,512,128]{2,1,0:T(8,128)(2,1)S(1)}, bf16[8,128,512]{2,1,0:T...) custom-call(f32[2]{0:T(128)S(1)} %copy-done, ...), custom_call_target="tpu_custom_call" | custom-call | flops 838860800 | bytes 1000000 | tf_op jit(solution)/shard_map/pallas_call | solution.py:460
  25.4 0.2 collective-permute-done.1.z2
  25.6 0.0 collective-permute-done.y2
  25.6 3.2 %shard_map.122 = (bf16[768,128]{1,0:T(8,128)(2,1)S(1)}, bf16[768,128]{1,0:T(8,128)(2,1)S(1)}, bf16[768,128]{1,0:T(8,128)(2,1)S(1)}, bf16[512,128]{1,0:T(8,128)(2...) custom-call(f32[2]{0:T(128)S(1)} %copy-done, ...), custom_call_target="tpu_custom_call", output_to_operand_aliasing={{9}: (3, {}), {10}: (4, {}), {11}: (5, {}), {12}: (6, {}), ... | custom-call | flops 587202560 | bytes 1000000 | tf_op jit(solution)/shard_map/pallas_call | solution.py:460
  28.8 1.5 %collective-permute-start.10 = (bf16[512,128]{1,0:T(8,128)(2,1)S(1)}, bf16[512,128]{1,0:T(8,128)(2,1)S(1)}, u32[]{:S(2)}, u32[]{:S(2)}) collective-permute-start(bf16[512,128]{1,0:T(8,128)(2,1)S(1)} %get-tuple-element.55), channel_id=1, source_target_pairs={{0,64},{8,72},{16,80},{24,88},{32,96},{40,104},{48,112},{56,120},{... | collective-permute-start | bytes 393224 | tf_op jit(solution)/shard_map/ppermute | solution.py:413
  30.3 0.9 %collective-permute-start.16 = (bf16[128,1024]{1,0:T(8,128)(2,1)S(1)}, bf16[128,1024]{1,0:T(8,128)(2,1)S(1)}, u32[]{:S(2)}, u32[]{:S(2)}) collective-permute-start(bf16[128,1024]{1,0:T(8,128)(2,1)S(1)} %collective-permute-done.15.n0), channel_id=1, source_target_pairs={{0,2},{1,3},{2,0},{3,1},{4,6},{5,7},{6,4},{7,5},{8,10},{9,11},{10,... | collective-permute-start | bytes 786440 | tf_op jit(solution)/shard_map/ppermute | solution.py:427
  31.2 2.7 %collective-permute-start.11 = (bf16[512,128]{1,0:T(8,128)(2,1)S(1)}, bf16[512,128]{1,0:T(8,128)(2,1)S(1)}, u32[]{:S(2)}, u32[]{:S(2)}) collective-permute-start(bf16[512,128]{1,0:T(8,128)(2,1)S(1)} %get-tuple-element.56), channel_id=1, source_target_pairs={{0,96},{8,104},{16,112},{24,120},{32,64},{40,72},{48,80},{56,88},{... | collective-permute-start | bytes 393224 | tf_op jit(solution)/shard_map/ppermute | solution.py:413
  33.9 0.7 collective-permute-start.6
  34.5 4.5 %collective-permute-start.7 = (bf16[768,128]{1,0:T(8,128)(2,1)S(1)}, bf16[768,128]{1,0:T(8,128)(2,1)S(1)}, u32[]{:S(2)}, u32[]{:S(2)}) collective-permute-start(bf16[768,128]{1,0:T(8,128)(2,1)S(1)} %get-tuple-element.52), channel_id=1, source_target_pairs={{0,16},{8,24},{16,0},{24,8},{32,48},{40,56},{48,32},{56,40},{64,80... | collective-permute-start | bytes 589832 | tf_op jit(solution)/shard_map/ppermute | solution.py:413
  39.0 0.0 collective-permute-start.9
  39.0 0.0 collective-permute-done.11.z3
  39.0 2.3 %collective-permute-start.8 = (bf16[768,128]{1,0:T(8,128)(2,1)S(1)}, bf16[768,128]{1,0:T(8,128)(2,1)S(1)}, u32[]{:S(2)}, u32[]{:S(2)}) collective-permute-start(bf16[768,128]{1,0:T(8,128)(2,1)S(1)} %get-tuple-element.53), channel_id=1, source_target_pairs={{0,24},{8,16},{16,8},{24,0},{32,56},{40,48},{48,40},{56,32},{64,88... | collective-permute-start | bytes 589832 | tf_op jit(solution)/shard_map/ppermute | solution.py:413
  41.3 2.7 %collective-permute-done.9.z1 = bf16[512,128]{1,0:T(8,128)(2,1)S(1)} collective-permute-done((bf16[512,128]{1,0:T(8,128)(2,1)S(1)}, bf16[512,128]{1,0:T(8,128)(2,1)S(1)}, u32[]{:S(2)}, u32[]{:S(2)}) %collective-permute-start.9) | collective-permute-done | bytes 131104 | tf_op jit(solution)/shard_map/ppermute | solution.py:413
  44.0 0.5 collective-permute-start.17
  44.5 1.2 %collective-permute-done.7.y2 = bf16[768,128]{1,0:T(8,128)(2,1)S(1)} collective-permute-done((bf16[768,128]{1,0:T(8,128)(2,1)S(1)}, bf16[768,128]{1,0:T(8,128)(2,1)S(1)}, u32[]{:S(2)}, u32[]{:S(2)}) %collective-permute-start.7) | collective-permute-done | bytes 196640 | tf_op jit(solution)/shard_map/ppermute | solution.py:413
  45.7 0.0 collective-permute-start.22
  45.7 0.0 collective-permute-done.16.n1
  45.7 0.5 collective-permute-start.18
  46.2 1.5 %collective-permute-done.8.y3 = bf16[768,128]{1,0:T(8,128)(2,1)S(1)} collective-permute-done((bf16[768,128]{1,0:T(8,128)(2,1)S(1)}, bf16[768,128]{1,0:T(8,128)(2,1)S(1)}, u32[]{:S(2)}, u32[]{:S(2)}) %collective-permute-start.8) | collective-permute-done | bytes 196640 | tf_op jit(solution)/shard_map/ppermute | solution.py:413
  47.7 0.1 shard_map.123.turned_in.g0
  47.8 0.5 collective-permute-start.12
  48.3 1.9 %collective-permute-start.13 = (bf16[256,256]{1,0:T(8,128)(2,1)S(1)}, bf16[256,256]{1,0:T(8,128)(2,1)S(1)}, u32[]{:S(2)}, u32[]{:S(2)}) collective-permute-start(bf16[256,256]{1,0:T(8,128)(2,1)S(1)} %shard_map.123.turned_in.g0), channel_id=1, source_target_pairs={{0,64},{8,72},{16,80},{24,88},{32,96},{40,104},{48,112},{56,120},{... | collective-permute-start | bytes 393224 | tf_op jit(solution)/shard_map/ppermute | solution.py:413
  50.1 2.4 %collective-permute-start.14 = (bf16[256,256]{1,0:T(8,128)(2,1)S(1)}, bf16[256,256]{1,0:T(8,128)(2,1)S(1)}, u32[]{:S(2)}, u32[]{:S(2)}) collective-permute-start(bf16[256,256]{1,0:T(8,128)(2,1)S(1)} %shard_map.123.turned_in.g0), channel_id=1, source_target_pairs={{0,96},{8,104},{16,112},{24,120},{32,64},{40,72},{48,80},{56,88},{... | collective-permute-start | bytes 393224 | tf_op jit(solution)/shard_map/ppermute | solution.py:413
  52.5 0.6 collective-permute-done.12.g1
  53.2 1.7 %collective-permute-done.13.g2 = bf16[256,256]{1,0:T(8,128)(2,1)S(1)} collective-permute-done((bf16[256,256]{1,0:T(8,128)(2,1)S(1)}, bf16[256,256]{1,0:T(8,128)(2,1)S(1)}, u32[]{:S(2)}, u32[]{:S(2)}) %collective-permute-start.13) | collective-permute-done | bytes 131104 | tf_op jit(solution)/shard_map/ppermute | solution.py:413
  54.8 1.5 %collective-permute-done.14.g3 = bf16[256,256]{1,0:T(8,128)(2,1)S(1)} collective-permute-done((bf16[256,256]{1,0:T(8,128)(2,1)S(1)}, bf16[256,256]{1,0:T(8,128)(2,1)S(1)}, u32[]{:S(2)}, u32[]{:S(2)}) %collective-permute-start.14) | collective-permute-done | bytes 131104 | tf_op jit(solution)/shard_map/ppermute | solution.py:413
  56.3 0.9 %shard_map.125 = (f32[256,256]{1,0:T(8,128)S(1)}, bf16[256,256]{1,0:T(8,128)(2,1)S(1)}, bf16[256,256]{1,0:T(8,128)(2,1)S(1)}, bf16[256,256]{1,0:T(8,128)(2,1)S(1)}) custom-call(bf16[256,256]{1,0:T(8,128)(2,1)S(1)} %shard_map.123.turned_in.g0, bf16[256,256]{1,0:T(8,128)(2,1)S(1)} %collective-permute-done.12.g1, ...), custom_call_target="tpu_custom_call" | custom-call | flops 536870912 | bytes 1000000 | tf_op jit(solution)/shard_map/pallas_call | solution.py:460
  57.2 0.1 collective-permute-start.23
  57.3 3.6 %collective-permute-start.24 = (bf16[256,256]{1,0:T(8,128)(2,1)S(1)}, bf16[256,256]{1,0:T(8,128)(2,1)S(1)}, u32[]{:S(2)}, u32[]{:S(2)}) collective-permute-start(bf16[256,256]{1,0:T(8,128)(2,1)S(1)} %get-tuple-element.66), channel_id=1, source_target_pairs={{0,16},{8,24},{16,0},{24,8},{32,48},{40,56},{48,32},{56,40},{64,80... | collective-permute-start | bytes 393224 | tf_op jit(solution)/shard_map/ppermute | solution.py:413
  60.9 1.1 %collective-permute-start.25 = (bf16[256,256]{1,0:T(8,128)(2,1)S(1)}, bf16[256,256]{1,0:T(8,128)(2,1)S(1)}, u32[]{:S(2)}, u32[]{:S(2)}) collective-permute-start(bf16[256,256]{1,0:T(8,128)(2,1)S(1)} %get-tuple-element.67), channel_id=1, source_target_pairs={{0,24},{8,16},{16,8},{24,0},{32,56},{40,48},{48,40},{56,32},{64,88... | collective-permute-start | bytes 393224 | tf_op jit(solution)/shard_map/ppermute | solution.py:413
  62.0 1.1 %shard_map.124 = (bf16[512,128]{1,0:T(8,128)(2,1)}, bf16[512,128]{1,0:T(8,128)(2,1)}, bf16[512,128]{1,0:T(8,128)(2,1)}) custom-call(f32[2,256,128]{2,1,0:T(8,128)S(1)} %get-tuple-element.49.own_k, f32[2,256,128]{2,1,0:T(8,128)S(1)} %get-tuple-element.50.own_v, bf16[768,128]{1,0:T(8,128)(2,1)S(1)} %collective-permute-done.6.y1, ...), custom_call_target="tpu_custom_call" | custom-call | flops 10000000 | bytes 1000000 | tf_op jit(solution)/shard_map/pallas_call | solution.py:460
  63.1 2.1 %collective-permute-done.24.t2 = bf16[256,256]{1,0:T(8,128)(2,1)S(1)} collective-permute-done((bf16[256,256]{1,0:T(8,128)(2,1)S(1)}, bf16[256,256]{1,0:T(8,128)(2,1)S(1)}, u32[]{:S(2)}, u32[]{:S(2)}) %collective-permute-start.24) | collective-permute-done | bytes 131104 | tf_op jit(solution)/shard_map/ppermute | solution.py:413
  65.2 1.8 %collective-permute-done.25.t3 = bf16[256,256]{1,0:T(8,128)(2,1)S(1)} collective-permute-done((bf16[256,256]{1,0:T(8,128)(2,1)S(1)}, bf16[256,256]{1,0:T(8,128)(2,1)S(1)}, u32[]{:S(2)}, u32[]{:S(2)}) %collective-permute-start.25) | collective-permute-done | bytes 131104 | tf_op jit(solution)/shard_map/ppermute | solution.py:413
  67.1 0.8 %shard_map.126 = f32[256,256]{1,0:T(8,128)} custom-call(f32[256,256]{1,0:T(8,128)S(1)} %get-tuple-element.64.own, bf16[256,256]{1,0:T(8,128)(2,1)S(1)} %collective-permute-done.23.t1, bf16[256,256]{1,0:T(8,128)(2,1)S(1)} %collective-permute-done.24.t2, bf16[256,256]{1,0:T(8,128)(2,1)S(1)} %collective-permute-done.25.t3), custom_call_target="tpu_custom_call" | custom-call | flops 1000000 | bytes 1000000 | tf_op jit(solution)/shard_map/pallas_call | solution.py:460
  (13 shorter events, 0.0 us)
Async XLA Ops:
  0.6 20.8 %copy-start = (f32[2]{0:T(128)S(1)}, f32[2]{0:T(128)}, u32[]{:S(2)}) copy-start(f32[2]{0:T(128)} %lam.3) | copy-start | bytes 28
  2.7 8.9 %collective-permute-start.19 = (bf16[64,1024]{1,0:T(8,128)(2,1)S(1)}, bf16[64,1024]{1,0:T(8,128)(2,1)S(1)}, u32[]{:S(2)}, u32[]{:S(2)}) collective-permute-start(bf16[64,1024]{1,0:T(8,128)(2,1)S(1)} %get-tuple-element.63), channel_id=1, source_target_pairs={{0,64},{8,72},{16,80},{24,88},{32,96},{40,104},{48,112},{56,120},{... | collective-permute-start | bytes 393224 | tf_op jit(solution)/shard_map/ppermute | solution.py:413
  6.7 12.6 %collective-permute-start.2 = (bf16[1056,128]{1,0:T(8,128)(2,1)S(1)}, bf16[1056,128]{1,0:T(8,128)(2,1)S(1)}, u32[]{:S(2)}, u32[]{:S(2)}) collective-permute-start(bf16[1056,128]{1,0:T(8,128)(2,1)S(1)} %get-tuple-element.36.yown), channel_id=1, source_target_pairs={{0,8},{8,0},{16,24},{24,16},{32,40},{40,32},{48,56},{56,48},{64,72... | collective-permute-start | bytes 811016 | tf_op jit(solution)/shard_map/ppermute | solution.py:413
  8.3 13.2 %collective-permute-start.3 = (bf16[1056,128]{1,0:T(8,128)(2,1)S(1)}, bf16[1056,128]{1,0:T(8,128)(2,1)S(1)}, u32[]{:S(2)}, u32[]{:S(2)}) collective-permute-start(bf16[1056,128]{1,0:T(8,128)(2,1)S(1)} %get-tuple-element.36.yown), channel_id=1, source_target_pairs={{0,24},{8,16},{16,8},{24,0},{32,56},{40,48},{48,40},{56,32},{64,88... | collective-permute-start | bytes 811016 | tf_op jit(solution)/shard_map/ppermute | solution.py:413
  10.5 5.1 %collective-permute-start.4 = (bf16[544,128]{1,0:T(8,128)(2,1)S(1)}, bf16[544,128]{1,0:T(8,128)(2,1)S(1)}, u32[]{:S(2)}, u32[]{:S(2)}) collective-permute-start(bf16[544,128]{1,0:T(8,128)(2,1)S(1)} %get-tuple-element.39), channel_id=1, source_target_pairs={{0,32},{8,40},{16,48},{24,56},{32,0},{40,8},{48,16},{56,24},{64,96... | collective-permute-start | bytes 417800 | tf_op jit(solution)/shard_map/ppermute | solution.py:413
  11.5 6.6 %collective-permute-start.5 = (bf16[544,128]{1,0:T(8,128)(2,1)S(1)}, bf16[544,128]{1,0:T(8,128)(2,1)S(1)}, u32[]{:S(2)}, u32[]{:S(2)}) collective-permute-start(bf16[544,128]{1,0:T(8,128)(2,1)S(1)} %get-tuple-element.40), channel_id=1, source_target_pairs={{0,96},{8,104},{16,112},{24,120},{32,64},{40,72},{48,80},{56,88},{... | collective-permute-start | bytes 417800 | tf_op jit(solution)/shard_map/ppermute | solution.py:413
  11.5 14.1 %collective-permute-start = (bf16[1056,128]{1,0:T(8,128)(2,1)S(1)}, bf16[1056,128]{1,0:T(8,128)(2,1)S(1)}, u32[]{:S(2)}, u32[]{:S(2)}) collective-permute-start(bf16[1056,128]{1,0:T(8,128)(2,1)S(1)} %get-tuple-element.36.yown), channel_id=1, source_target_pairs={{0,16},{8,24},{16,0},{24,8},{32,48},{40,56},{48,32},{56,40},{64,80... | collective-permute-start | bytes 811016 | tf_op jit(solution)/shard_map/ppermute | solution.py:413
  15.6 14.7 %collective-permute-start.15 = (bf16[128,1024]{1,0:T(8,128)(2,1)S(1)}, bf16[128,1024]{1,0:T(8,128)(2,1)S(1)}, u32[]{:S(2)}, u32[]{:S(2)}) collective-permute-start(bf16[128,1024]{1,0:T(8,128)(2,1)S(1)} %get-tuple-element.62), channel_id=1, source_target_pairs={{0,32},{1,97},{2,34},{3,99},{4,36},{5,101},{6,38},{7,103},{8,40},{... | collective-permute-start | bytes 786440 | tf_op jit(solution)/shard_map/ppermute | solution.py:423
  18.1 7.5 %collective-permute-start.1 = (bf16[544,128]{1,0:T(8,128)(2,1)S(1)}, bf16[544,128]{1,0:T(8,128)(2,1)S(1)}, u32[]{:S(2)}, u32[]{:S(2)}) collective-permute-start(bf16[544,128]{1,0:T(8,128)(2,1)S(1)} %get-tuple-element.37), channel_id=1, source_target_pairs={{0,64},{8,72},{16,80},{24,88},{32,96},{40,104},{48,112},{56,120},{... | collective-permute-start | bytes 417800 | tf_op jit(solution)/shard_map/ppermute | solution.py:413
  19.4 15.2 %collective-permute-start.20 = (bf16[64,1024]{1,0:T(8,128)(2,1)S(1)}, bf16[64,1024]{1,0:T(8,128)(2,1)S(1)}, u32[]{:S(2)}, u32[]{:S(2)}) collective-permute-start(bf16[64,1024]{1,0:T(8,128)(2,1)S(1)} %collective-permute-done.19.f0), channel_id=1, source_target_pairs={{0,2},{1,3},{2,0},{3,1},{4,6},{5,7},{6,4},{7,5},{8,10},{9,11},{10,... | collective-permute-start | bytes 393224 | tf_op jit(solution)/shard_map/ppermute | solution.py:427
  28.8 10.3 %collective-permute-start.10 = (bf16[512,128]{1,0:T(8,128)(2,1)S(1)}, bf16[512,128]{1,0:T(8,128)(2,1)S(1)}, u32[]{:S(2)}, u32[]{:S(2)}) collective-permute-start(bf16[512,128]{1,0:T(8,128)(2,1)S(1)} %get-tuple-element.55), channel_id=1, source_target_pairs={{0,64},{8,72},{16,80},{24,88},{32,96},{40,104},{48,112},{56,120},{... | collective-permute-start | bytes 393224 | tf_op jit(solution)/shard_map/ppermute | solution.py:413
  30.3 15.4 %collective-permute-start.16 = (bf16[128,1024]{1,0:T(8,128)(2,1)S(1)}, bf16[128,1024]{1,0:T(8,128)(2,1)S(1)}, u32[]{:S(2)}, u32[]{:S(2)}) collective-permute-start(bf16[128,1024]{1,0:T(8,128)(2,1)S(1)} %collective-permute-done.15.n0), channel_id=1, source_target_pairs={{0,2},{1,3},{2,0},{3,1},{4,6},{5,7},{6,4},{7,5},{8,10},{9,11},{10,... | collective-permute-start | bytes 786440 | tf_op jit(solution)/shard_map/ppermute | solution.py:427
  31.2 7.8 %collective-permute-start.11 = (bf16[512,128]{1,0:T(8,128)(2,1)S(1)}, bf16[512,128]{1,0:T(8,128)(2,1)S(1)}, u32[]{:S(2)}, u32[]{:S(2)}) collective-permute-start(bf16[512,128]{1,0:T(8,128)(2,1)S(1)} %get-tuple-element.56), channel_id=1, source_target_pairs={{0,96},{8,104},{16,112},{24,120},{32,64},{40,72},{48,80},{56,88},{... | collective-permute-start | bytes 393224 | tf_op jit(solution)/shard_map/ppermute | solution.py:413
  33.9 10.1 %collective-permute-start.6 = (bf16[768,128]{1,0:T(8,128)(2,1)S(1)}, bf16[768,128]{1,0:T(8,128)(2,1)S(1)}, u32[]{:S(2)}, u32[]{:S(2)}) collective-permute-start(bf16[768,128]{1,0:T(8,128)(2,1)S(1)} %get-tuple-element.51), channel_id=1, source_target_pairs={{0,8},{8,0},{16,24},{24,16},{32,40},{40,32},{48,56},{56,48},{64,72... | collective-permute-start | bytes 589832 | tf_op jit(solution)/shard_map/ppermute | solution.py:413
  34.5 11.1 %collective-permute-start.7 = (bf16[768,128]{1,0:T(8,128)(2,1)S(1)}, bf16[768,128]{1,0:T(8,128)(2,1)S(1)}, u32[]{:S(2)}, u32[]{:S(2)}) collective-permute-start(bf16[768,128]{1,0:T(8,128)(2,1)S(1)} %get-tuple-element.52), channel_id=1, source_target_pairs={{0,16},{8,24},{16,0},{24,8},{32,48},{40,56},{48,32},{56,40},{64,80... | collective-permute-start | bytes 589832 | tf_op jit(solution)/shard_map/ppermute | solution.py:413
  39.0 5.0 %collective-permute-start.9 = (bf16[512,128]{1,0:T(8,128)(2,1)S(1)}, bf16[512,128]{1,0:T(8,128)(2,1)S(1)}, u32[]{:S(2)}, u32[]{:S(2)}) collective-permute-start(bf16[512,128]{1,0:T(8,128)(2,1)S(1)} %get-tuple-element.54), channel_id=1, source_target_pairs={{0,32},{8,40},{16,48},{24,56},{32,0},{40,8},{48,16},{56,24},{64,96... | collective-permute-start | bytes 393224 | tf_op jit(solution)/shard_map/ppermute | solution.py:413
  39.0 8.7 %collective-permute-start.8 = (bf16[768,128]{1,0:T(8,128)(2,1)S(1)}, bf16[768,128]{1,0:T(8,128)(2,1)S(1)}, u32[]{:S(2)}, u32[]{:S(2)}) collective-permute-start(bf16[768,128]{1,0:T(8,128)(2,1)S(1)} %get-tuple-element.53), channel_id=1, source_target_pairs={{0,24},{8,16},{16,8},{24,0},{32,56},{40,48},{48,40},{56,32},{64,88... | collective-permute-start | bytes 589832 | tf_op jit(solution)/shard_map/ppermute | solution.py:413
  44.0 4.3 %collective-permute-start.21 = (bf16[64,1024]{1,0:T(8,128)(2,1)S(1)}, bf16[64,1024]{1,0:T(8,128)(2,1)S(1)}, u32[]{:S(2)}, u32[]{:S(2)}) collective-permute-start(bf16[64,1024]{1,0:T(8,128)(2,1)S(1)} %collective-permute-done.19.f0), channel_id=1, source_target_pairs={{0,1},{1,0},{2,3},{3,2},{4,5},{5,4},{6,7},{7,6},{8,9},{9,8},{10,11... | collective-permute-start | bytes 393224 | tf_op jit(solution)/shard_map/ppermute | solution.py:431
  44.0 8.6 %collective-permute-start.17 = (bf16[128,1024]{1,0:T(8,128)(2,1)S(1)}, bf16[128,1024]{1,0:T(8,128)(2,1)S(1)}, u32[]{:S(2)}, u32[]{:S(2)}) collective-permute-start(bf16[128,1024]{1,0:T(8,128)(2,1)S(1)} %collective-permute-done.15.n0), channel_id=1, source_target_pairs={{0,1},{1,0},{2,3},{3,2},{4,5},{5,4},{6,7},{7,6},{8,9},{9,8},{10,11... | collective-permute-start | bytes 786440 | tf_op jit(solution)/shard_map/ppermute | solution.py:431
  45.7 4.5 %collective-permute-start.22 = (bf16[64,1024]{1,0:T(8,128)(2,1)S(1)}, bf16[64,1024]{1,0:T(8,128)(2,1)S(1)}, u32[]{:S(2)}, u32[]{:S(2)}) collective-permute-start(bf16[64,1024]{1,0:T(8,128)(2,1)S(1)} %collective-permute-done.20.f1), channel_id=1, source_target_pairs={{0,1},{1,0},{2,3},{3,2},{4,5},{5,4},{6,7},{7,6},{8,9},{9,8},{10,11... | collective-permute-start | bytes 393224 | tf_op jit(solution)/shard_map/ppermute | solution.py:431
  45.7 10.6 %collective-permute-start.18 = (bf16[128,1024]{1,0:T(8,128)(2,1)S(1)}, bf16[128,1024]{1,0:T(8,128)(2,1)S(1)}, u32[]{:S(2)}, u32[]{:S(2)}) collective-permute-start(bf16[128,1024]{1,0:T(8,128)(2,1)S(1)} %collective-permute-done.16.n1), channel_id=1, source_target_pairs={{0,1},{1,0},{2,3},{3,2},{4,5},{5,4},{6,7},{7,6},{8,9},{9,8},{10,11... | collective-permute-start | bytes 786440 | tf_op jit(solution)/shard_map/ppermute | solution.py:431
  47.8 5.4 %collective-permute-start.12 = (bf16[256,256]{1,0:T(8,128)(2,1)S(1)}, bf16[256,256]{1,0:T(8,128)(2,1)S(1)}, u32[]{:S(2)}, u32[]{:S(2)}) collective-permute-start(bf16[256,256]{1,0:T(8,128)(2,1)S(1)} %shard_map.123.turned_in.g0), channel_id=1, source_target_pairs={{0,32},{8,40},{16,48},{24,56},{32,0},{40,8},{48,16},{56,24},{64,96... | collective-permute-start | bytes 393224 | tf_op jit(solution)/shard_map/ppermute | solution.py:413
  48.3 6.6 %collective-permute-start.13 = (bf16[256,256]{1,0:T(8,128)(2,1)S(1)}, bf16[256,256]{1,0:T(8,128)(2,1)S(1)}, u32[]{:S(2)}, u32[]{:S(2)}) collective-permute-start(bf16[256,256]{1,0:T(8,128)(2,1)S(1)} %shard_map.123.turned_in.g0), channel_id=1, source_target_pairs={{0,64},{8,72},{16,80},{24,88},{32,96},{40,104},{48,112},{56,120},{... | collective-permute-start | bytes 393224 | tf_op jit(solution)/shard_map/ppermute | solution.py:413
  50.1 6.2 %collective-permute-start.14 = (bf16[256,256]{1,0:T(8,128)(2,1)S(1)}, bf16[256,256]{1,0:T(8,128)(2,1)S(1)}, u32[]{:S(2)}, u32[]{:S(2)}) collective-permute-start(bf16[256,256]{1,0:T(8,128)(2,1)S(1)} %shard_map.123.turned_in.g0), channel_id=1, source_target_pairs={{0,96},{8,104},{16,112},{24,120},{32,64},{40,72},{48,80},{56,88},{... | collective-permute-start | bytes 393224 | tf_op jit(solution)/shard_map/ppermute | solution.py:413
  57.2 5.9 %collective-permute-start.23 = (bf16[256,256]{1,0:T(8,128)(2,1)S(1)}, bf16[256,256]{1,0:T(8,128)(2,1)S(1)}, u32[]{:S(2)}, u32[]{:S(2)}) collective-permute-start(bf16[256,256]{1,0:T(8,128)(2,1)S(1)} %get-tuple-element.65), channel_id=1, source_target_pairs={{0,8},{8,0},{16,24},{24,16},{32,40},{40,32},{48,56},{56,48},{64,72... | collective-permute-start | bytes 393224 | tf_op jit(solution)/shard_map/ppermute | solution.py:413
  57.3 7.9 %collective-permute-start.24 = (bf16[256,256]{1,0:T(8,128)(2,1)S(1)}, bf16[256,256]{1,0:T(8,128)(2,1)S(1)}, u32[]{:S(2)}, u32[]{:S(2)}) collective-permute-start(bf16[256,256]{1,0:T(8,128)(2,1)S(1)} %get-tuple-element.66), channel_id=1, source_target_pairs={{0,16},{8,24},{16,0},{24,8},{32,48},{40,56},{48,32},{56,40},{64,80... | collective-permute-start | bytes 393224 | tf_op jit(solution)/shard_map/ppermute | solution.py:413
  60.9 6.2 %collective-permute-start.25 = (bf16[256,256]{1,0:T(8,128)(2,1)S(1)}, bf16[256,256]{1,0:T(8,128)(2,1)S(1)}, u32[]{:S(2)}, u32[]{:S(2)}) collective-permute-start(bf16[256,256]{1,0:T(8,128)(2,1)S(1)} %get-tuple-element.67), channel_id=1, source_target_pairs={{0,24},{8,16},{16,8},{24,0},{32,56},{40,48},{48,40},{56,32},{64,88... | collective-permute-start | bytes 393224 | tf_op jit(solution)/shard_map/ppermute | solution.py:413

commit v6 on v5

--- a/solution.py
+++ b/solution.py
@@ -61,7 +61,7 @@
 
 def prepare_kernel(
     q_hbm, k_hbm, v_hbm, maps_hbm, lse_hbm, out_hbm, gain_hbm, lam_hbm, lat_hbm,
-    yown, zown, send1, send2, send3, lat_near, lat_far,
+    yown, zown, send1, send2, send3,
     q_in, k_in, v_in, maps_in, lse_in, out_in, gain_in, lam, sems,
 ):
     z, _, core = position()
@@ -69,13 +69,13 @@
         (maps_hbm, maps_in), (out_hbm, out_in), (gain_hbm, gain_in), (lse_hbm, lse_in),
         (lam_hbm, lam), (q_hbm, q_in), (k_hbm, k_in), (v_hbm, v_in),
     ]
-    near = jnp.bitwise_xor(z, jnp.where(core == 0, 1, 3))
-    columns = pl.ds(pl.multiple_of(near * WIDE, WIDE), WIDE)
-    tokens = pl.ds(pl.multiple_of(side() * HALF, HALF), HALF)
-    pairs.append((lat_hbm.at[tokens, columns], lat_near))
-    columns = pl.ds(pl.multiple_of(jnp.bitwise_xor(z, 2) * WIDE, WIDE), WIDE)
     tokens = pl.ds(pl.multiple_of(core * HALF + side() * DH, DH), DH)
-    pairs.append((lat_hbm.at[tokens, columns], lat_far))
+    for n, ref in enumerate((send1, send2, send3), 1):
+        for tile in range(WIDE // 128):
+            first = jnp.bitwise_xor(z, n) * WIDE + tile * 128
+            columns = pl.ds(pl.multiple_of(first, 128), 128)
+            rows = pl.ds(QG + tile * DH, DH)
+            pairs.append((lat_hbm.at[tokens, columns], ref.at[rows]))
     copies = [pltpu.make_async_copy(a, b, sems.at[n]) for n, (a, b) in enumerate(pairs)]
     for copy in copies:
         copy.start()
@@ -139,7 +139,7 @@
 
         @pl.when(jnp.logical_not(keys))
         def _():
-            ref[...] = zown[0:QG]
+            ref[0:QG] = zown[0:QG]
 
     for n, ref in enumerate((send1, send2, send3)):
         send(ref, z < jnp.bitwise_xor(z, n + 1))
@@ -182,7 +182,7 @@
 
     @pl.when(jnp.logical_not(keys))
     def _():
-        buf[SIDE + n, 0:QG] = ref[...]
+        buf[SIDE + n, 0:QG] = ref[0:QG]
 
 
 def run_pairs(items, z, y, lam, state, wide_w, tall_s):
@@ -279,12 +279,14 @@
 
 
 def attend_far_kernel(
-    lam, y2, z2, buf_in, stat_in, kpad_in, kturn_in, qpad_in, dq_in, dk_in, dv_in,
-    g1, g2, g3, r1, r2, r3, own_q, own_k, own_v,
+    lam, y2, z2, z1, z3, buf_in, stat_in, kpad_in, kturn_in, qpad_in, dq_in, dk_in, dv_in,
+    g1, g2, g3, r1, r2, r3, own_q, own_k, own_v, lat_mine,
     buf, stat, kpad, kturn, qpad, dq, dk, dv, wide_w, tall_s,
 ):
     z, y, _ = position()
     state = (buf, stat, kpad, kturn, qpad, dq, dk, dv)
+    for n, ref in enumerate((z1, z2, z3)):
+        lat_mine[n * 2 * ROWS : (n + 1) * 2 * ROWS] = ref[QG:SLOT]
     buf[2] = y2[...]
     take(z, 2, z2, buf)
     for slot in (2, 6):
@@ -376,9 +378,7 @@
         q_out[rows] = turned(weave, both).astype(BF)
 
 
-def project_kernel(
-    g0, g1, g2, g3, lat0, n0, n1, m0, m1, f0, f1, e0, e1, own, to1, to2, to3, lat
-):
+def project_kernel(g0, g1, g2, g3, lat0, a0, a1, b0, b1, own, to1, to2, to3, lat):
     _, y, core = position()
     lat[0:ROWS] = lat0[...]
     other = side()
@@ -387,15 +387,15 @@
             @pl.when(jnp.logical_and(core == c, other == x))
             def _():
                 for half in range(2):
-                    mine = (n0, n1, f0, f1) if half == c else (m0, m1, e0, e1)
-                    block = ROWS * (1 if half == 0 else 3)
-                    far = 2 * ROWS + half * HALF
-                    for step in range(2):
-                        which = step ^ x
-                        rows = block + step * HALF
-                        lat[rows : rows + HALF] = mine[which][...]
-                        rows = far + step * DH
-                        lat[rows : rows + DH] = mine[2 + which][...]
+                    for part in range(2):
+                        ref = ((a0, a1) if half == c else (b0, b1))[part ^ x]
+                        for n in range(SIDE - 1):
+                            first = (n + 1) * ROWS + half * HALF + part * DH
+                            for tile in range(WIDE // 128):
+                                rows = n * 2 * ROWS + tile * DH
+                                lat[first : first + DH, tile * 128 : (tile + 1) * 128] = ref[
+                                    rows : rows + DH
+                                ]
 
     grads = jnp.concatenate([g0[...], g1[...], g2[...], g3[...]], axis=1)
     for n, ref in ((1, to1), (2, to2), (3, to3), (0, own)):
@@ -411,16 +411,6 @@
 def traded(x, axis, n):
     step = n * (SIDE if axis == "z" else 1)
     return lax.ppermute(x, "sp", [(s, s ^ step) for s in range(SIDE * SIDE)])
-
-
-def traded_apart(x):
-    heads = lax.axis_size("tp")
-    pairs = []
-    for s in range(SIDE * SIDE):
-        for t in range(heads):
-            there = s ^ (SIDE * (1 if t % 2 == 0 else 3))
-            pairs.append((s * heads + t, there * heads + t))
-    return lax.ppermute(x, ("sp", "tp"), pairs)
 
 
 def across(x):
@@ -473,11 +463,9 @@
     mix_lambda,
     norm_gain,
 ):
-    yown, zown, *sends, lat_near, lat_far = call(
+    yown, zown, *sends = call(
         prepare_kernel,
-        (shape(SLOT, 128),) * 2
-        + (shape(QG, 128),) * 3
-        + (shape(HALF, WIDE), shape(DH, WIDE)),
+        (shape(SLOT, 128),) * 5,
         0,
         9,
         0,
@@ -488,7 +476,7 @@
             pltpu.VMEM((2 * ROWS, 128), BF),
             pltpu.VMEM((1, 128), F32),
             pltpu.SMEM((2,), F32),
-            pltpu.SemaphoreType.DMA((10,)),
+            pltpu.SemaphoreType.DMA((32,)),
         ],
         10**8,
     )(
@@ -504,21 +492,6 @@
     )
     ys = [traded(yown, "y", n) for n in range(1, SIDE)]
     zs = [traded(x, "z", n) for n, x in enumerate(sends, 1)]
-    near = traded_apart(lat_near)
-    apart = traded(lat_far, "z", 2)
-    near_side = across(near)
-    apart_side = across(apart)
-    lats = (
-        near,
-        near_side,
-        partner(near),
-        partner(near_side),
-        apart,
-        apart_side,
-        partner(apart),
-        partner(apart_side),
-    )
-
     slots = 2 * SIDE
     state_shapes = (
         shape(slots, SLOT, 128),
@@ -546,28 +519,25 @@
         + (shape(2 * ROWS, 128),) * 3
         + (shape(2, 128, ROWS, dtype=F32),)
         + (shape(2, ROWS, 128, dtype=F32),) * 2
+        + (shape(6 * ROWS, 128),)
     )
     results = call(
         attend_far_kernel,
         result_shapes + state_shapes,
         1,
         0,
-        10,
+        12,
         holds,
         7 * pair_flops,
-        aliases={3 + n: len(result_shapes) + n for n in range(len(state_shapes))},
-    )(mix_lambda, ys[1], zs[1], *state)
-    own_q, own_k, own_v = results[6:9]
+        aliases={5 + n: len(result_shapes) + n for n in range(len(state_shapes))},
+    )(mix_lambda, ys[1], zs[1], zs[0], zs[2], *state)
+    own_q, own_k, own_v, lat_mine = results[6:10]
+    lat_side = across(lat_mine)
+    lats = (lat_mine, lat_side, partner(lat_mine), partner(lat_side))
     y_back = [traded(x, "y", n) for n, x in enumerate(results[0:3], 1)]
     z_back = [traded(x, "z", n) for n, x in enumerate(results[3:6], 1)]
     turned_grad = call(
-        queries_kernel,
-        shape(ROWS, ROWS),
-        0,
-        0,
-        7,
-        [pltpu.VMEM((128, ROWS), F32)],
-        10**7,
+        queries_kernel, shape(ROWS, ROWS), 0, 0, 7, [pltpu.VMEM((128, ROWS), F32)], 10**7
     )(own_q, *y_back, *z_back)
     grads = [traded(turned_grad, "z", n) for n in range(1, SIDE)]
     square = shape(ROWS, ROWS)
@@ -576,18 +546,12 @@
         (shape(ROWS, ROWS, dtype=F32), square, square, square),
         0,
         0,
-        13,
+        9,
         [pltpu.VMEM((WIDE, WIDE), BF)],
         2 * WIDE * WIDE * ROWS,
     )(turned_grad, *grads, lat_own, *lats)
     query_rows, key_rows, value_rows = call(
-        keys_kernel,
-        (shape(2 * ROWS, 128),) * 3,
-        0,
-        0,
-        9,
-        [pltpu.VMEM((ROWS, 128), F32)] * 2,
-        10**7,
+        keys_kernel, (shape(2 * ROWS, 128),) * 3, 0, 0, 9, [pltpu.VMEM((ROWS, 128), F32)] * 2, 10**7
     )(own_k, own_v, *y_back, *z_back, turned_grad)
     weight_grad = call(
         total_kernel, shape(ROWS, ROWS, dtype=F32), 0, 0, 4, [], 10**6

time: 68.8 us -> 73.6 us (1.070); the launches traced: 67.9 us -> 73.4 us
  waiting for transfers between devices: 17.2 us -> 26 us
  starting transfers between devices: 38 us -> 34.2 us
    ppermute x19 -> x18, waiting for transfers between devices: 17.2 us -> 23.4 us  [traded(): return lax.ppermute(x, 'sp', [(s, s ^ step) for s in range(SIDE * SIDE)])]
    ppermute x2 -> x1, waiting for transfers between devices: 0.01 us -> 2.61 us  [across(): lax.ppermute(x, 'tp', [(t, t ^ 2) for t in range(lax.axis_size('tp'))])]
    ppermute x1 -> x0, starting transfers between devices: 1.02 us -> none  [traded_apart(): return lax.ppermute(x, ('sp', 'tp'), pairs)]
    ppermute x4 -> x2, starting transfers between devices: 1.02 us -> 0.01 us  [partner(): lax.ppermute(x, 'tp', [(t, t ^ 1) for t in range(lax.axis_size('tp'))])]
    ppermute x19 -> x18, starting transfers between devices: 33.5 us -> 32.7 us  [traded(): return lax.ppermute(x, 'sp', [(s, s ^ step) for s in range(SIDE * SIDE)])]
    ppermute x2 -> x1, starting transfers between devices: 2.4 us -> 1.58 us  [across(): lax.ppermute(x, 'tp', [(t, t ^ 2) for t in range(lax.axis_size('tp'))])]
  transfers between devices with their start and end apart: 26 -> 21, of which waited for: 12 -> 11; matrix products, arithmetic and copies ran while one was open for 0% -> 0% of each run, Pallas kernels for 12% -> 7%
where the time goes in v6:
time: 73.6 us; the launch traced here: 73.4 us
  starting transfers between devices  34.2 us (46%)
  waiting for transfers between devices  26 us (35%)
  Pallas kernels  12.5 us (17%)
    ppermute x18, starting transfers between devices, traded(): return lax.ppermute(x, 'sp', [(s, s ^ step) for s in range(SIDE * SIDE)])  32.7 us
    ppermute x18, waiting for transfers between devices, traded(): return lax.ppermute(x, 'sp', [(s, s ^ step) for s in range(SIDE * SIDE)])  23.4 us
    pallas_call x7, Pallas kernels, run(): return calling(*arrays[:scalars], *held, *rest)  12.5 us
    ppermute x1, waiting for transfers between devices, across(): lax.ppermute(x, 'tp', [(t, t ^ 2) for t in range(lax.axis_size('tp'))])  2.61 us
    ppermute x1, starting transfers between devices, across(): lax.ppermute(x, 'tp', [(t, t ^ 2) for t in range(lax.axis_size('tp'))])  1.58 us
  transfers between devices with their start and end apart: 21, of which 11 were waited for; matrix products, arithmetic and copies ran while one was open for 0% of the time, Pallas kernels for 7%

profile of v6, /device:TPU:0, one launch (start us, length us, event | category | flops | bytes accessed | tf_op | source)
XLA Modules:
  0.0 73.4 jit_solution(15381442660409006981)
XLA Ops:
  0.6 2.3 %shard_map.120 = (bf16[1056,128]{1,0:T(8,128)(2,1)S(1)}, bf16[1056,128]{1,0:T(8,128)(2,1)S(1)}, bf16[1056,128]{1,0:T(8,128)(2,1)S(1)}, bf16[1056,128]{1,0:T(8,128)(2,1)S(1)}, bf16[1056,128]{1,0:T(8,128)(2,1)S(1)}) custom-call(bf16[512,128]{1,0:T(8,128)(2,1)} %bitcast.11, bf16[512,128]{1,0:T(8,128)(2,1)} %bitcast.12, bf16[512,128]{1,0:T(8,128)(2,1)} %bitcast.13, ...), custom_call_target="tpu_custom_call" | custom-call | flops 100000000 | bytes 1000000 | tf_op jit(solution)/shard_map/pallas_call | solution.py:450
  2.9 2.1 %collective-permute-start.2 = (bf16[1056,128]{1,0:T(8,128)(2,1)S(1)}, bf16[1056,128]{1,0:T(8,128)(2,1)S(1)}, u32[]{:S(2)}, u32[]{:S(2)}) collective-permute-start(bf16[1056,128]{1,0:T(8,128)(2,1)S(1)} %get-tuple-element.37), channel_id=1, source_target_pairs={{0,32},{8,40},{16,48},{24,56},{32,0},{40,8},{48,16},{56,24},{64,96... | collective-permute-start | bytes 811016 | tf_op jit(solution)/shard_map/ppermute | solution.py:413
  5.0 2.5 %collective-permute-start.3 = (bf16[1056,128]{1,0:T(8,128)(2,1)S(1)}, bf16[1056,128]{1,0:T(8,128)(2,1)S(1)}, u32[]{:S(2)}, u32[]{:S(2)}) collective-permute-start(bf16[1056,128]{1,0:T(8,128)(2,1)S(1)} %get-tuple-element.38), channel_id=1, source_target_pairs={{0,96},{8,104},{16,112},{24,120},{32,64},{40,72},{48,80},{56,88},{... | collective-permute-start | bytes 811016 | tf_op jit(solution)/shard_map/ppermute | solution.py:413
  7.5 3.0 %collective-permute-start.5 = (bf16[1056,128]{1,0:T(8,128)(2,1)S(1)}, bf16[1056,128]{1,0:T(8,128)(2,1)S(1)}, u32[]{:S(2)}, u32[]{:S(2)}) collective-permute-start(bf16[1056,128]{1,0:T(8,128)(2,1)S(1)} %get-tuple-element.35.yown), channel_id=1, source_target_pairs={{0,24},{8,16},{16,8},{24,0},{32,56},{40,48},{48,40},{56,32},{64,88... | collective-permute-start | bytes 811016 | tf_op jit(solution)/shard_map/ppermute | solution.py:413
  10.6 0.1 collective-permute-start.4
  10.7 1.1 %collective-permute-start.1 = (bf16[1056,128]{1,0:T(8,128)(2,1)S(1)}, bf16[1056,128]{1,0:T(8,128)(2,1)S(1)}, u32[]{:S(2)}, u32[]{:S(2)}) collective-permute-start(bf16[1056,128]{1,0:T(8,128)(2,1)S(1)} %get-tuple-element.36), channel_id=1, source_target_pairs={{0,64},{8,72},{16,80},{24,88},{32,96},{40,104},{48,112},{56,120},{... | collective-permute-start | bytes 811016 | tf_op jit(solution)/shard_map/ppermute | solution.py:413
  11.8 0.0 collective-permute-done.2.z1
  11.8 3.9 %collective-permute-start = (bf16[1056,128]{1,0:T(8,128)(2,1)S(1)}, bf16[1056,128]{1,0:T(8,128)(2,1)S(1)}, u32[]{:S(2)}, u32[]{:S(2)}) collective-permute-start(bf16[1056,128]{1,0:T(8,128)(2,1)S(1)} %get-tuple-element.35.yown), channel_id=1, source_target_pairs={{0,16},{8,24},{16,0},{24,8},{32,48},{40,56},{48,32},{56,40},{64,80... | collective-permute-start | bytes 811016 | tf_op jit(solution)/shard_map/ppermute | solution.py:413
  15.7 3.1 %collective-permute-done.3.z3 = bf16[1056,128]{1,0:T(8,128)(2,1)S(1)} collective-permute-done((bf16[1056,128]{1,0:T(8,128)(2,1)S(1)}, bf16[1056,128]{1,0:T(8,128)(2,1)S(1)}, u32[]{:S(2)}, u32[]{:S(2)}) %collective-permute-start.3) | collective-permute-done | bytes 270368 | tf_op jit(solution)/shard_map/ppermute | solution.py:413
  18.8 0.0 collective-permute-done.5.y3
  18.8 1.1 %collective-permute-done.4.y1 = bf16[1056,128]{1,0:T(8,128)(2,1)S(1)} collective-permute-done((bf16[1056,128]{1,0:T(8,128)(2,1)S(1)}, bf16[1056,128]{1,0:T(8,128)(2,1)S(1)}, u32[]{:S(2)}, u32[]{:S(2)}) %collective-permute-start.4) | collective-permute-done | bytes 270368 | tf_op jit(solution)/shard_map/ppermute | solution.py:413
  19.9 3.9 %shard_map.121 = (bf16[8,1056,128]{2,1,0:T(8,128)(2,1)S(1)}, f32[8,8,256]{2,1,0:T(8,128)S(1)}, bf16[8,512,128]{2,1,0:T(8,128)(2,1)S(1)}, bf16[8,128,512]{2,1,0:T...) custom-call(f32[2]{0:T(128)S(1)} %copy-done, ...), custom_call_target="tpu_custom_call" | custom-call | flops 838860800 | bytes 1000000 | tf_op jit(solution)/shard_map/pallas_call | solution.py:450
  23.8 0.0 collective-permute-done.1.z2
  23.8 0.0 collective-permute-done.y2
  23.8 3.0 %shard_map.122 = (bf16[768,128]{1,0:T(8,128)(2,1)S(1)}, bf16[768,128]{1,0:T(8,128)(2,1)S(1)}, bf16[768,128]{1,0:T(8,128)(2,1)S(1)}, bf16[512,128]{1,0:T(8,128)(2...) custom-call(f32[2]{0:T(128)S(1)} %copy-done, ...), custom_call_target="tpu_custom_call", output_to_operand_aliasing={{10}: (5, {}), {11}: (6, {}), {12}: (7, {}), {13}: (8, {}),... | custom-call | flops 587202560 | bytes 1000000 | tf_op jit(solution)/shard_map/pallas_call | solution.py:450
  26.9 1.6 %collective-permute-start.15 = (bf16[1536,128]{1,0:T(8,128)(2,1)S(1)}, bf16[1536,128]{1,0:T(8,128)(2,1)S(1)}, u32[]{:S(2)}, u32[]{:S(2)}) collective-permute-start(bf16[1536,128]{1,0:T(8,128)(2,1)S(1)} %get-tuple-element.61.a0), channel_id=1, source_target_pairs={{0,2},{1,3},{2,0},{3,1},{4,6},{5,7},{6,4},{7,5},{8,10},{9,11},{10,... | collective-permute-start | bytes 1179656 | tf_op jit(solution)/shard_map/ppermute | solution.py:417
  28.5 1.0 %collective-permute-start.9 = (bf16[512,128]{1,0:T(8,128)(2,1)S(1)}, bf16[512,128]{1,0:T(8,128)(2,1)S(1)}, u32[]{:S(2)}, u32[]{:S(2)}) collective-permute-start(bf16[512,128]{1,0:T(8,128)(2,1)S(1)} %get-tuple-element.53), channel_id=1, source_target_pairs={{0,32},{8,40},{16,48},{24,56},{32,0},{40,8},{48,16},{56,24},{64,96... | collective-permute-start | bytes 393224 | tf_op jit(solution)/shard_map/ppermute | solution.py:413
  29.5 3.0 %collective-permute-start.10 = (bf16[512,128]{1,0:T(8,128)(2,1)S(1)}, bf16[512,128]{1,0:T(8,128)(2,1)S(1)}, u32[]{:S(2)}, u32[]{:S(2)}) collective-permute-start(bf16[512,128]{1,0:T(8,128)(2,1)S(1)} %get-tuple-element.54), channel_id=1, source_target_pairs={{0,64},{8,72},{16,80},{24,88},{32,96},{40,104},{48,112},{56,120},{... | collective-permute-start | bytes 393224 | tf_op jit(solution)/shard_map/ppermute | solution.py:413
  32.5 0.6 collective-permute-start.11
  33.2 0.0 collective-permute-start.16
  33.2 2.6 %collective-permute-done.15.a1 = bf16[1536,128]{1,0:T(8,128)(2,1)S(1)} collective-permute-done((bf16[1536,128]{1,0:T(8,128)(2,1)S(1)}, bf16[1536,128]{1,0:T(8,128)(2,1)S(1)}, u32[]{:S(2)}, u32[]{:S(2)}) %collective-permute-start.15) | collective-permute-done | bytes 393248 | tf_op jit(solution)/shard_map/ppermute | solution.py:417
  35.8 0.0 collective-permute-start.17
  35.8 0.0 collective-permute-done.9.z1
  35.8 1.2 %collective-permute-start.6 = (bf16[768,128]{1,0:T(8,128)(2,1)S(1)}, bf16[768,128]{1,0:T(8,128)(2,1)S(1)}, u32[]{:S(2)}, u32[]{:S(2)}) collective-permute-start(bf16[768,128]{1,0:T(8,128)(2,1)S(1)} %get-tuple-element.50), channel_id=1, source_target_pairs={{0,8},{8,0},{16,24},{24,16},{32,40},{40,32},{48,56},{56,48},{64,72... | collective-permute-start | bytes 589832 | tf_op jit(solution)/shard_map/ppermute | solution.py:413
  37.0 0.1 collective-permute-done.10.z2
  37.2 3.2 %collective-permute-start.7 = (bf16[768,128]{1,0:T(8,128)(2,1)S(1)}, bf16[768,128]{1,0:T(8,128)(2,1)S(1)}, u32[]{:S(2)}, u32[]{:S(2)}) collective-permute-start(bf16[768,128]{1,0:T(8,128)(2,1)S(1)} %get-tuple-element.51), channel_id=1, source_target_pairs={{0,16},{8,24},{16,0},{24,8},{32,48},{40,56},{48,32},{56,40},{64,80... | collective-permute-start | bytes 589832 | tf_op jit(solution)/shard_map/ppermute | solution.py:413
  40.4 0.0 collective-permute-done.11.z3
  40.4 1.3 %collective-permute-start.8 = (bf16[768,128]{1,0:T(8,128)(2,1)S(1)}, bf16[768,128]{1,0:T(8,128)(2,1)S(1)}, u32[]{:S(2)}, u32[]{:S(2)}) collective-permute-start(bf16[768,128]{1,0:T(8,128)(2,1)S(1)} %get-tuple-element.52), channel_id=1, source_target_pairs={{0,24},{8,16},{16,8},{24,0},{32,56},{40,48},{48,40},{56,32},{64,88... | collective-permute-start | bytes 589832 | tf_op jit(solution)/shard_map/ppermute | solution.py:413
  41.7 1.9 %collective-permute-done.6.y1 = bf16[768,128]{1,0:T(8,128)(2,1)S(1)} collective-permute-done((bf16[768,128]{1,0:T(8,128)(2,1)S(1)}, bf16[768,128]{1,0:T(8,128)(2,1)S(1)}, u32[]{:S(2)}, u32[]{:S(2)}) %collective-permute-start.6) | collective-permute-done | bytes 196640 | tf_op jit(solution)/shard_map/ppermute | solution.py:413
  43.6 6.2 %collective-permute-done.7.y2 = bf16[768,128]{1,0:T(8,128)(2,1)S(1)} collective-permute-done((bf16[768,128]{1,0:T(8,128)(2,1)S(1)}, bf16[768,128]{1,0:T(8,128)(2,1)S(1)}, u32[]{:S(2)}, u32[]{:S(2)}) %collective-permute-start.7) | collective-permute-done | bytes 196640 | tf_op jit(solution)/shard_map/ppermute | solution.py:413
  49.7 2.6 %collective-permute-done.8.y3 = bf16[768,128]{1,0:T(8,128)(2,1)S(1)} collective-permute-done((bf16[768,128]{1,0:T(8,128)(2,1)S(1)}, bf16[768,128]{1,0:T(8,128)(2,1)S(1)}, u32[]{:S(2)}, u32[]{:S(2)}) %collective-permute-start.8) | collective-permute-done | bytes 196640 | tf_op jit(solution)/shard_map/ppermute | solution.py:413
  52.3 0.1 shard_map.123.turned_in.g0
  52.4 3.7 %collective-permute-start.14 = (bf16[256,256]{1,0:T(8,128)(2,1)S(1)}, bf16[256,256]{1,0:T(8,128)(2,1)S(1)}, u32[]{:S(2)}, u32[]{:S(2)}) collective-permute-start(bf16[256,256]{1,0:T(8,128)(2,1)S(1)} %shard_map.123.turned_in.g0), channel_id=1, source_target_pairs={{0,96},{8,104},{16,112},{24,120},{32,64},{40,72},{48,80},{56,88},{... | collective-permute-start | bytes 393224 | tf_op jit(solution)/shard_map/ppermute | solution.py:413
  56.1 0.0 collective-permute-start.13
  56.1 0.9 %collective-permute-start.12 = (bf16[256,256]{1,0:T(8,128)(2,1)S(1)}, bf16[256,256]{1,0:T(8,128)(2,1)S(1)}, u32[]{:S(2)}, u32[]{:S(2)}) collective-permute-start(bf16[256,256]{1,0:T(8,128)(2,1)S(1)} %shard_map.123.turned_in.g0), channel_id=1, source_target_pairs={{0,32},{8,40},{16,48},{24,56},{32,0},{40,8},{48,16},{56,24},{64,96... | collective-permute-start | bytes 393224 | tf_op jit(solution)/shard_map/ppermute | solution.py:413
  57.1 3.9 %collective-permute-done.14.g3 = bf16[256,256]{1,0:T(8,128)(2,1)S(1)} collective-permute-done((bf16[256,256]{1,0:T(8,128)(2,1)S(1)}, bf16[256,256]{1,0:T(8,128)(2,1)S(1)}, u32[]{:S(2)}, u32[]{:S(2)}) %collective-permute-start.14) | collective-permute-done | bytes 131104 | tf_op jit(solution)/shard_map/ppermute | solution.py:413
  61.0 2.3 %collective-permute-done.13.g2 = bf16[256,256]{1,0:T(8,128)(2,1)S(1)} collective-permute-done((bf16[256,256]{1,0:T(8,128)(2,1)S(1)}, bf16[256,256]{1,0:T(8,128)(2,1)S(1)}, u32[]{:S(2)}, u32[]{:S(2)}) %collective-permute-start.13) | collective-permute-done | bytes 131104 | tf_op jit(solution)/shard_map/ppermute | solution.py:413
  63.2 0.0 collective-permute-done.12.g1
  63.3 0.0 collective-permute-done.16.b0
  63.3 0.0 collective-permute-done.17.b1
  63.3 1.3 %shard_map.125 = (f32[256,256]{1,0:T(8,128)S(1)}, bf16[256,256]{1,0:T(8,128)(2,1)S(1)}, bf16[256,256]{1,0:T(8,128)(2,1)S(1)}, bf16[256,256]{1,0:T(8,128)(2,1)S(1)}) custom-call(bf16[256,256]{1,0:T(8,128)(2,1)S(1)} %shard_map.123.turned_in.g0, bf16[256,256]{1,0:T(8,128)(2,1)S(1)} %collective-permute-done.12.g1, ...), custom_call_target="tpu_custom_call" | custom-call | flops 536870912 | bytes 1000000 | tf_op jit(solution)/shard_map/pallas_call | solution.py:450
  64.5 0.1 collective-permute-start.18
  64.6 1.8 %collective-permute-start.19 = (bf16[256,256]{1,0:T(8,128)(2,1)S(1)}, bf16[256,256]{1,0:T(8,128)(2,1)S(1)}, u32[]{:S(2)}, u32[]{:S(2)}) collective-permute-start(bf16[256,256]{1,0:T(8,128)(2,1)S(1)} %get-tuple-element.64), channel_id=1, source_target_pairs={{0,16},{8,24},{16,0},{24,8},{32,48},{40,56},{48,32},{56,40},{64,80... | collective-permute-start | bytes 393224 | tf_op jit(solution)/shard_map/ppermute | solution.py:413
  66.4 2.9 %collective-permute-start.20 = (bf16[256,256]{1,0:T(8,128)(2,1)S(1)}, bf16[256,256]{1,0:T(8,128)(2,1)S(1)}, u32[]{:S(2)}, u32[]{:S(2)}) collective-permute-start(bf16[256,256]{1,0:T(8,128)(2,1)S(1)} %get-tuple-element.65), channel_id=1, source_target_pairs={{0,24},{8,16},{16,8},{24,0},{32,56},{40,48},{48,40},{56,32},{64,88... | collective-permute-start | bytes 393224 | tf_op jit(solution)/shard_map/ppermute | solution.py:413
  69.3 1.1 %shard_map.124 = (bf16[512,128]{1,0:T(8,128)(2,1)}, bf16[512,128]{1,0:T(8,128)(2,1)}, bf16[512,128]{1,0:T(8,128)(2,1)}) custom-call(f32[2,256,128]{2,1,0:T(8,128)S(1)} %get-tuple-element.48.own_k, f32[2,256,128]{2,1,0:T(8,128)S(1)} %get-tuple-element.49.own_v, bf16[768,128]{1,0:T(8,128)(2,1)S(1)} %collective-permute-done.6.y1, ...), custom_call_target="tpu_custom_call" | custom-call | flops 10000000 | bytes 1000000 | tf_op jit(solution)/shard_map/pallas_call | solution.py:450
  70.4 0.7 collective-permute-done.19.t2
  71.2 1.4 %collective-permute-done.20.t3 = bf16[256,256]{1,0:T(8,128)(2,1)S(1)} collective-permute-done((bf16[256,256]{1,0:T(8,128)(2,1)S(1)}, bf16[256,256]{1,0:T(8,128)(2,1)S(1)}, u32[]{:S(2)}, u32[]{:S(2)}) %collective-permute-start.20) | collective-permute-done | bytes 131104 | tf_op jit(solution)/shard_map/ppermute | solution.py:413
  72.6 0.8 %shard_map.126 = f32[256,256]{1,0:T(8,128)} custom-call(f32[256,256]{1,0:T(8,128)S(1)} %get-tuple-element.62.own, bf16[256,256]{1,0:T(8,128)(2,1)S(1)} %collective-permute-done.18.t1, bf16[256,256]{1,0:T(8,128)(2,1)S(1)} %collective-permute-done.19.t2, bf16[256,256]{1,0:T(8,128)(2,1)S(1)} %collective-permute-done.20.t3), custom_call_target="tpu_custom_call" | custom-call | flops 1000000 | bytes 1000000 | tf_op jit(solution)/shard_map/pallas_call | solution.py:450
  (3 shorter events, 0.0 us)
Async XLA Ops:
  0.6 19.3 %copy-start = (f32[2]{0:T(128)S(1)}, f32[2]{0:T(128)}, u32[]{:S(2)}) copy-start(f32[2]{0:T(128)} %lam.3) | copy-start | bytes 28
  2.9 8.9 %collective-permute-start.2 = (bf16[1056,128]{1,0:T(8,128)(2,1)S(1)}, bf16[1056,128]{1,0:T(8,128)(2,1)S(1)}, u32[]{:S(2)}, u32[]{:S(2)}) collective-permute-start(bf16[1056,128]{1,0:T(8,128)(2,1)S(1)} %get-tuple-element.37), channel_id=1, source_target_pairs={{0,32},{8,40},{16,48},{24,56},{32,0},{40,8},{48,16},{56,24},{64,96... | collective-permute-start | bytes 811016 | tf_op jit(solution)/shard_map/ppermute | solution.py:413
  5.0 13.8 %collective-permute-start.3 = (bf16[1056,128]{1,0:T(8,128)(2,1)S(1)}, bf16[1056,128]{1,0:T(8,128)(2,1)S(1)}, u32[]{:S(2)}, u32[]{:S(2)}) collective-permute-start(bf16[1056,128]{1,0:T(8,128)(2,1)S(1)} %get-tuple-element.38), channel_id=1, source_target_pairs={{0,96},{8,104},{16,112},{24,120},{32,64},{40,72},{48,80},{56,88},{... | collective-permute-start | bytes 811016 | tf_op jit(solution)/shard_map/ppermute | solution.py:413
  7.5 11.3 %collective-permute-start.5 = (bf16[1056,128]{1,0:T(8,128)(2,1)S(1)}, bf16[1056,128]{1,0:T(8,128)(2,1)S(1)}, u32[]{:S(2)}, u32[]{:S(2)}) collective-permute-start(bf16[1056,128]{1,0:T(8,128)(2,1)S(1)} %get-tuple-element.35.yown), channel_id=1, source_target_pairs={{0,24},{8,16},{16,8},{24,0},{32,56},{40,48},{48,40},{56,32},{64,88... | collective-permute-start | bytes 811016 | tf_op jit(solution)/shard_map/ppermute | solution.py:413
  10.6 9.4 %collective-permute-start.4 = (bf16[1056,128]{1,0:T(8,128)(2,1)S(1)}, bf16[1056,128]{1,0:T(8,128)(2,1)S(1)}, u32[]{:S(2)}, u32[]{:S(2)}) collective-permute-start(bf16[1056,128]{1,0:T(8,128)(2,1)S(1)} %get-tuple-element.35.yown), channel_id=1, source_target_pairs={{0,8},{8,0},{16,24},{24,16},{32,40},{40,32},{48,56},{56,48},{64,72... | collective-permute-start | bytes 811016 | tf_op jit(solution)/shard_map/ppermute | solution.py:413
  10.7 13.1 %collective-permute-start.1 = (bf16[1056,128]{1,0:T(8,128)(2,1)S(1)}, bf16[1056,128]{1,0:T(8,128)(2,1)S(1)}, u32[]{:S(2)}, u32[]{:S(2)}) collective-permute-start(bf16[1056,128]{1,0:T(8,128)(2,1)S(1)} %get-tuple-element.36), channel_id=1, source_target_pairs={{0,64},{8,72},{16,80},{24,88},{32,96},{40,104},{48,112},{56,120},{... | collective-permute-start | bytes 811016 | tf_op jit(solution)/shard_map/ppermute | solution.py:413
  11.8 12.1 %collective-permute-start = (bf16[1056,128]{1,0:T(8,128)(2,1)S(1)}, bf16[1056,128]{1,0:T(8,128)(2,1)S(1)}, u32[]{:S(2)}, u32[]{:S(2)}) collective-permute-start(bf16[1056,128]{1,0:T(8,128)(2,1)S(1)} %get-tuple-element.35.yown), channel_id=1, source_target_pairs={{0,16},{8,24},{16,0},{24,8},{32,48},{40,56},{48,32},{56,40},{64,80... | collective-permute-start | bytes 811016 | tf_op jit(solution)/shard_map/ppermute | solution.py:413
  26.9 8.9 %collective-permute-start.15 = (bf16[1536,128]{1,0:T(8,128)(2,1)S(1)}, bf16[1536,128]{1,0:T(8,128)(2,1)S(1)}, u32[]{:S(2)}, u32[]{:S(2)}) collective-permute-start(bf16[1536,128]{1,0:T(8,128)(2,1)S(1)} %get-tuple-element.61.a0), channel_id=1, source_target_pairs={{0,2},{1,3},{2,0},{3,1},{4,6},{5,7},{6,4},{7,5},{8,10},{9,11},{10,... | collective-permute-start | bytes 1179656 | tf_op jit(solution)/shard_map/ppermute | solution.py:417
  28.5 7.3 %collective-permute-start.9 = (bf16[512,128]{1,0:T(8,128)(2,1)S(1)}, bf16[512,128]{1,0:T(8,128)(2,1)S(1)}, u32[]{:S(2)}, u32[]{:S(2)}) collective-permute-start(bf16[512,128]{1,0:T(8,128)(2,1)S(1)} %get-tuple-element.53), channel_id=1, source_target_pairs={{0,32},{8,40},{16,48},{24,56},{32,0},{40,8},{48,16},{56,24},{64,96... | collective-permute-start | bytes 393224 | tf_op jit(solution)/shard_map/ppermute | solution.py:413
  29.5 7.7 %collective-permute-start.10 = (bf16[512,128]{1,0:T(8,128)(2,1)S(1)}, bf16[512,128]{1,0:T(8,128)(2,1)S(1)}, u32[]{:S(2)}, u32[]{:S(2)}) collective-permute-start(bf16[512,128]{1,0:T(8,128)(2,1)S(1)} %get-tuple-element.54), channel_id=1, source_target_pairs={{0,64},{8,72},{16,80},{24,88},{32,96},{40,104},{48,112},{56,120},{... | collective-permute-start | bytes 393224 | tf_op jit(solution)/shard_map/ppermute | solution.py:413
  32.5 7.9 %collective-permute-start.11 = (bf16[512,128]{1,0:T(8,128)(2,1)S(1)}, bf16[512,128]{1,0:T(8,128)(2,1)S(1)}, u32[]{:S(2)}, u32[]{:S(2)}) collective-permute-start(bf16[512,128]{1,0:T(8,128)(2,1)S(1)} %get-tuple-element.55), channel_id=1, source_target_pairs={{0,96},{8,104},{16,112},{24,120},{32,64},{40,72},{48,80},{56,88},{... | collective-permute-start | bytes 393224 | tf_op jit(solution)/shard_map/ppermute | solution.py:413
  33.2 30.1 %collective-permute-start.16 = (bf16[1536,128]{1,0:T(8,128)(2,1)S(1)}, bf16[1536,128]{1,0:T(8,128)(2,1)S(1)}, u32[]{:S(2)}, u32[]{:S(2)}) collective-permute-start(bf16[1536,128]{1,0:T(8,128)(2,1)S(1)} %get-tuple-element.61.a0), channel_id=1, source_target_pairs={{0,1},{1,0},{2,3},{3,2},{4,5},{5,4},{6,7},{7,6},{8,9},{9,8},{10,11... | collective-permute-start | bytes 1179656 | tf_op jit(solution)/shard_map/ppermute | solution.py:421
  35.8 27.5 %collective-permute-start.17 = (bf16[1536,128]{1,0:T(8,128)(2,1)S(1)}, bf16[1536,128]{1,0:T(8,128)(2,1)S(1)}, u32[]{:S(2)}, u32[]{:S(2)}) collective-permute-start(bf16[1536,128]{1,0:T(8,128)(2,1)S(1)} %collective-permute-done.15.a1), channel_id=1, source_target_pairs={{0,1},{1,0},{2,3},{3,2},{4,5},{5,4},{6,7},{7,6},{8,9},{9,8},{10,11... | collective-permute-start | bytes 1179656 | tf_op jit(solution)/shard_map/ppermute | solution.py:421
  35.8 7.8 %collective-permute-start.6 = (bf16[768,128]{1,0:T(8,128)(2,1)S(1)}, bf16[768,128]{1,0:T(8,128)(2,1)S(1)}, u32[]{:S(2)}, u32[]{:S(2)}) collective-permute-start(bf16[768,128]{1,0:T(8,128)(2,1)S(1)} %get-tuple-element.50), channel_id=1, source_target_pairs={{0,8},{8,0},{16,24},{24,16},{32,40},{40,32},{48,56},{56,48},{64,72... | collective-permute-start | bytes 589832 | tf_op jit(solution)/shard_map/ppermute | solution.py:413
  37.2 12.6 %collective-permute-start.7 = (bf16[768,128]{1,0:T(8,128)(2,1)S(1)}, bf16[768,128]{1,0:T(8,128)(2,1)S(1)}, u32[]{:S(2)}, u32[]{:S(2)}) collective-permute-start(bf16[768,128]{1,0:T(8,128)(2,1)S(1)} %get-tuple-element.51), channel_id=1, source_target_pairs={{0,16},{8,24},{16,0},{24,8},{32,48},{40,56},{48,32},{56,40},{64,80... | collective-permute-start | bytes 589832 | tf_op jit(solution)/shard_map/ppermute | solution.py:413
  40.4 11.9 %collective-permute-start.8 = (bf16[768,128]{1,0:T(8,128)(2,1)S(1)}, bf16[768,128]{1,0:T(8,128)(2,1)S(1)}, u32[]{:S(2)}, u32[]{:S(2)}) collective-permute-start(bf16[768,128]{1,0:T(8,128)(2,1)S(1)} %get-tuple-element.52), channel_id=1, source_target_pairs={{0,24},{8,16},{16,8},{24,0},{32,56},{40,48},{48,40},{56,32},{64,88... | collective-permute-start | bytes 589832 | tf_op jit(solution)/shard_map/ppermute | solution.py:413
  52.4 8.6 %collective-permute-start.14 = (bf16[256,256]{1,0:T(8,128)(2,1)S(1)}, bf16[256,256]{1,0:T(8,128)(2,1)S(1)}, u32[]{:S(2)}, u32[]{:S(2)}) collective-permute-start(bf16[256,256]{1,0:T(8,128)(2,1)S(1)} %shard_map.123.turned_in.g0), channel_id=1, source_target_pairs={{0,96},{8,104},{16,112},{24,120},{32,64},{40,72},{48,80},{56,88},{... | collective-permute-start | bytes 393224 | tf_op jit(solution)/shard_map/ppermute | solution.py:413
  56.1 7.1 %collective-permute-start.13 = (bf16[256,256]{1,0:T(8,128)(2,1)S(1)}, bf16[256,256]{1,0:T(8,128)(2,1)S(1)}, u32[]{:S(2)}, u32[]{:S(2)}) collective-permute-start(bf16[256,256]{1,0:T(8,128)(2,1)S(1)} %shard_map.123.turned_in.g0), channel_id=1, source_target_pairs={{0,64},{8,72},{16,80},{24,88},{32,96},{40,104},{48,112},{56,120},{... | collective-permute-start | bytes 393224 | tf_op jit(solution)/shard_map/ppermute | solution.py:413
  56.1 7.1 %collective-permute-start.12 = (bf16[256,256]{1,0:T(8,128)(2,1)S(1)}, bf16[256,256]{1,0:T(8,128)(2,1)S(1)}, u32[]{:S(2)}, u32[]{:S(2)}) collective-permute-start(bf16[256,256]{1,0:T(8,128)(2,1)S(1)} %shard_map.123.turned_in.g0), channel_id=1, source_target_pairs={{0,32},{8,40},{16,48},{24,56},{32,0},{40,8},{48,16},{56,24},{64,96... | collective-permute-start | bytes 393224 | tf_op jit(solution)/shard_map/ppermute | solution.py:413
  64.5 5.9 %collective-permute-start.18 = (bf16[256,256]{1,0:T(8,128)(2,1)S(1)}, bf16[256,256]{1,0:T(8,128)(2,1)S(1)}, u32[]{:S(2)}, u32[]{:S(2)}) collective-permute-start(bf16[256,256]{1,0:T(8,128)(2,1)S(1)} %get-tuple-element.63), channel_id=1, source_target_pairs={{0,8},{8,0},{16,24},{24,16},{32,40},{40,32},{48,56},{56,48},{64,72... | collective-permute-start | bytes 393224 | tf_op jit(solution)/shard_map/ppermute | solution.py:413
  64.6 6.6 %collective-permute-start.19 = (bf16[256,256]{1,0:T(8,128)(2,1)S(1)}, bf16[256,256]{1,0:T(8,128)(2,1)S(1)}, u32[]{:S(2)}, u32[]{:S(2)}) collective-permute-start(bf16[256,256]{1,0:T(8,128)(2,1)S(1)} %get-tuple-element.64), channel_id=1, source_target_pairs={{0,16},{8,24},{16,0},{24,8},{32,48},{40,56},{48,32},{56,40},{64,80... | collective-permute-start | bytes 393224 | tf_op jit(solution)/shard_map/ppermute | solution.py:413
  66.4 6.2 %collective-permute-start.20 = (bf16[256,256]{1,0:T(8,128)(2,1)S(1)}, bf16[256,256]{1,0:T(8,128)(2,1)S(1)}, u32[]{:S(2)}, u32[]{:S(2)}) collective-permute-start(bf16[256,256]{1,0:T(8,128)(2,1)S(1)} %get-tuple-element.65), channel_id=1, source_target_pairs={{0,24},{8,16},{16,8},{24,0},{32,56},{40,48},{48,40},{56,32},{64,88... | collective-permute-start | bytes 393224 | tf_op jit(solution)/shard_map/ppermute | solution.py:413

commit v7 on v4

--- a/solution.py
+++ b/solution.py
@@ -275,7 +275,7 @@
 
 def attend_far_kernel(
     lam, y2, z2, buf_in, stat_in, kpad_in, kturn_in, qpad_in, dq_in, dk_in, dv_in,
-    g1, g2, g3, r1, r2, r3, own_q, own_k, own_v,
+    g1, g2, g3, r1, r2, r3, v1, v2, v3, own_q, own_k, own_v,
     buf, stat, kpad, kturn, qpad, dq, dk, dv, wide_w, tall_s,
 ):
     z, y, _ = position()
@@ -298,18 +298,17 @@
         put_q(ref, slot)
         ref[ROWS : 2 * ROWS] = (dk[slot] * scale).astype(BF)
         ref[2 * ROWS :] = dv[slot].astype(BF)
-    for n, ref in enumerate((r1, r2, r3), 1):
+    for n, (ref, ref_v) in enumerate(((r1, v1), (r2, v2), (r3, v3)), 1):
         keys = jnp.bitwise_xor(z, n) < z
+        ref_v[...] = dv[SIDE + n].astype(BF)
 
         @pl.when(keys)
         def _():
-            ref[0:ROWS] = (dk[SIDE + n] * scale).astype(BF)
-            ref[ROWS:] = dv[SIDE + n].astype(BF)
+            ref[...] = (dk[SIDE + n] * scale).astype(BF)
 
         @pl.when(jnp.logical_not(keys))
         def _():
             put_q(ref, SIDE + n)
-            ref[ROWS:] = jnp.zeros((ROWS, 128), BF)
 
     own_q[0] = dq[SIDE] * scale
     own_q[1] = dq[0] * scale
@@ -338,18 +337,19 @@
 
 
 def keys_kernel(
-    own_k, own_v, y1, y2, y3, z1, z2, z3, turned_in, q_out, k_out, v_out, acc_k, acc_v
+    own_k, own_v, y1, y2, y3, z1, z2, z3, v1, v2, v3, turned_in,
+    q_out, k_out, v_out, acc_k, acc_v,
 ):
     z, _, _ = position()
     acc_k[...] = own_k[1]
     acc_v[...] = own_v[1]
-    for n, ref in enumerate((z1, z2, z3)):
-        keys = z < jnp.bitwise_xor(z, n + 1)
+    for n, (ref, ref_v) in enumerate(((z1, v1), (z2, v2), (z3, v3)), 1):
+        keys = z < jnp.bitwise_xor(z, n)
 
         @pl.when(keys)
         def _():
-            acc_k[...] += ref[0:ROWS].astype(F32)
-            acc_v[...] += ref[ROWS:].astype(F32)
+            acc_k[...] += ref[...].astype(F32)
+            acc_v[...] += ref_v[...].astype(F32)
 
     row = iota((ROWS, ROWS), 0)
     col = iota((ROWS, ROWS), 1)
@@ -527,7 +527,7 @@
     )(mix_lambda, latents, yown, ys[0], ys[2], zown, zs[0], zs[2])
     result_shapes = (
         (shape(3 * ROWS, 128),) * 3
-        + (shape(2 * ROWS, 128),) * 3
+        + (shape(ROWS, 128),) * 6
         + (shape(2, 128, ROWS, dtype=F32),)
         + (shape(2, ROWS, 128, dtype=F32),) * 2
     )
@@ -541,9 +541,10 @@
         7 * pair_flops,
         aliases={3 + n: len(result_shapes) + n for n in range(len(state_shapes))},
     )(mix_lambda, ys[1], zs[1], *state)
-    own_q, own_k, own_v = results[6:9]
+    own_q, own_k, own_v = results[9:12]
     y_back = [traded(x, "y", n) for n, x in enumerate(results[0:3], 1)]
     z_back = [traded(x, "z", n) for n, x in enumerate(results[3:6], 1)]
+    v_back = [traded(x, "z", n) for n, x in enumerate(results[6:9], 1)]
     turned_grad = call(
         queries_kernel,
         shape(ROWS, ROWS),
@@ -569,10 +570,10 @@
         (shape(2 * ROWS, 128),) * 3,
         0,
         0,
-        9,
+        12,
         [pltpu.VMEM((ROWS, 128), F32)] * 2,
         10**7,
-    )(own_k, own_v, *y_back, *z_back, turned_grad)
+    )(own_k, own_v, *y_back, *z_back, *v_back, turned_grad)
     weight_grad = call(
         total_kernel, shape(ROWS, ROWS, dtype=F32), 0, 0, 4, [], 10**6
     )(own, *[traded(x, "y", n) for n, x in enumerate(parts, 1)])

time: 74.3 us -> 73.6 us (level)
  waiting for transfers between devices: 27.7 us -> 21.2 us
  starting transfers between devices: 33.5 us -> 39.8 us
    ppermute x19 -> x22, waiting for transfers between devices: 27.7 us -> 21.1 us  [traded(): return lax.ppermute(x, 'sp', [(s, s ^ step) for s in range(SIDE * SIDE)])]
    ppermute x19 -> x22, starting transfers between devices: 31.4 us -> 37.7 us  [traded(): return lax.ppermute(x, 'sp', [(s, s ^ step) for s in range(SIDE * SIDE)])]
  transfers between devices with their start and end apart: 22 -> 25, of which waited for: 12 -> 10; matrix products, arithmetic and copies ran while one was open for 0% -> 0% of each run, Pallas kernels for 11% -> 12%
where the time goes in v7:
time: 73.6 us; the launch traced here: 73.5 us
  starting transfers between devices  39.8 us (54%)
  waiting for transfers between devices  21.2 us (29%)
  Pallas kernels  11.8 us (16%)
  between operations  0.74 us (1%)
    ppermute x22, starting transfers between devices, traded(): return lax.ppermute(x, 'sp', [(s, s ^ step) for s in range(SIDE * SIDE)])  37.7 us
    ppermute x22, waiting for transfers between devices, traded(): return lax.ppermute(x, 'sp', [(s, s ^ step) for s in range(SIDE * SIDE)])  21.1 us
    pallas_call x7, Pallas kernels, run(): return calling(*arrays[:scalars], *held, *rest)  11.8 us
    ppermute x1, starting transfers between devices, traded_apart(): return lax.ppermute(x, ('sp', 'tp'), pairs)  2.1 us
  transfers between devices with their start and end apart: 25, of which 10 were waited for; matrix products, arithmetic and copies ran while one was open for 0% of the time, Pallas kernels for 12%

profile of v7, /device:TPU:0, one launch (start us, length us, event | category | flops | bytes accessed | tf_op | source)
XLA Modules:
  0.0 73.5 jit_solution(17040791645569958278)
XLA Ops:
  0.6 2.0 %shard_map.120 = (bf16[1056,128]{1,0:T(8,128)(2,1)S(1)}, bf16[1056,128]{1,0:T(8,128)(2,1)S(1)}, bf16[544,128]{1,0:T(8,128)(2,1)S(1)}, bf16[544,128]{1,0:T(8,128)...) custom-call(bf16[512,128]{1,0:T(8,128)(2,1)} %bitcast.11, ...), custom_call_target="tpu_custom_call" | custom-call | flops 100000000 | bytes 1000000 | tf_op jit(solution)/shard_map/pallas_call | solution.py:454
  2.7 2.1 %collective-permute-start.18 = (bf16[256,1024]{1,0:T(8,128)(2,1)S(1)}, bf16[256,1024]{1,0:T(8,128)(2,1)S(1)}, u32[]{:S(2)}, u32[]{:S(2)}) collective-permute-start(bf16[256,1024]{1,0:T(8,128)(2,1)S(1)} %get-tuple-element.68), channel_id=1, source_target_pairs={{0,32},{1,97},{2,34},{3,99},{4,36},{5,101},{6,38},{7,103},{8,40},{... | collective-permute-start | bytes 1572872 | tf_op jit(solution)/shard_map/ppermute | solution.py:421
  4.8 1.6 %collective-permute-start.2 = (bf16[1056,128]{1,0:T(8,128)(2,1)S(1)}, bf16[1056,128]{1,0:T(8,128)(2,1)S(1)}, u32[]{:S(2)}, u32[]{:S(2)}) collective-permute-start(bf16[1056,128]{1,0:T(8,128)(2,1)S(1)} %get-tuple-element.39.yown), channel_id=1, source_target_pairs={{0,8},{8,0},{16,24},{24,16},{32,40},{40,32},{48,56},{56,48},{64,72... | collective-permute-start | bytes 811016 | tf_op jit(solution)/shard_map/ppermute | solution.py:411
  6.4 0.1 collective-permute-start.4
  6.5 2.2 %collective-permute-start.3 = (bf16[1056,128]{1,0:T(8,128)(2,1)S(1)}, bf16[1056,128]{1,0:T(8,128)(2,1)S(1)}, u32[]{:S(2)}, u32[]{:S(2)}) collective-permute-start(bf16[1056,128]{1,0:T(8,128)(2,1)S(1)} %get-tuple-element.39.yown), channel_id=1, source_target_pairs={{0,24},{8,16},{16,8},{24,0},{32,56},{40,48},{48,40},{56,32},{64,88... | collective-permute-start | bytes 811016 | tf_op jit(solution)/shard_map/ppermute | solution.py:411
  8.7 4.0 %collective-permute-start.5 = (bf16[544,128]{1,0:T(8,128)(2,1)S(1)}, bf16[544,128]{1,0:T(8,128)(2,1)S(1)}, u32[]{:S(2)}, u32[]{:S(2)}) collective-permute-start(bf16[544,128]{1,0:T(8,128)(2,1)S(1)} %get-tuple-element.43), channel_id=1, source_target_pairs={{0,96},{8,104},{16,112},{24,120},{32,64},{40,72},{48,80},{56,88},{... | collective-permute-start | bytes 417800 | tf_op jit(solution)/shard_map/ppermute | solution.py:411
  12.7 2.2 %collective-permute-done.4.z1 = bf16[544,128]{1,0:T(8,128)(2,1)S(1)} collective-permute-done((bf16[544,128]{1,0:T(8,128)(2,1)S(1)}, bf16[544,128]{1,0:T(8,128)(2,1)S(1)}, u32[]{:S(2)}, u32[]{:S(2)}) %collective-permute-start.4) | collective-permute-done | bytes 139296 | tf_op jit(solution)/shard_map/ppermute | solution.py:411
  14.9 3.3 %collective-permute-start = (bf16[1056,128]{1,0:T(8,128)(2,1)S(1)}, bf16[1056,128]{1,0:T(8,128)(2,1)S(1)}, u32[]{:S(2)}, u32[]{:S(2)}) collective-permute-start(bf16[1056,128]{1,0:T(8,128)(2,1)S(1)} %get-tuple-element.39.yown), channel_id=1, source_target_pairs={{0,16},{8,24},{16,0},{24,8},{32,48},{40,56},{48,32},{56,40},{64,80... | collective-permute-start | bytes 811016 | tf_op jit(solution)/shard_map/ppermute | solution.py:411
  18.2 3.8 %collective-permute-start.20 = (bf16[128,1024]{1,0:T(8,128)(2,1)S(1)}, bf16[128,1024]{1,0:T(8,128)(2,1)S(1)}, u32[]{:S(2)}, u32[]{:S(2)}) collective-permute-start(bf16[128,1024]{1,0:T(8,128)(2,1)S(1)} %get-tuple-element.69), channel_id=1, source_target_pairs={{0,64},{8,72},{16,80},{24,88},{32,96},{40,104},{48,112},{56,120},{... | collective-permute-start | bytes 786440 | tf_op jit(solution)/shard_map/ppermute | solution.py:411
  22.1 0.1 collective-permute-start.1
  22.2 0.0 collective-permute-start.19
  22.2 0.0 collective-permute-done.3.y3
  22.2 3.9 %shard_map.121 = (bf16[8,1056,128]{2,1,0:T(8,128)(2,1)S(1)}, f32[8,8,256]{2,1,0:T(8,128)S(1)}, bf16[8,512,128]{2,1,0:T(8,128)(2,1)S(1)}, bf16[8,128,512]{2,1,0:T...) custom-call(f32[2]{0:T(128)S(1)} %copy-done, ...), custom_call_target="tpu_custom_call" | custom-call | flops 838860800 | bytes 1000000 | tf_op jit(solution)/shard_map/pallas_call | solution.py:454
  26.1 2.7 %collective-permute-done.1.z2 = bf16[544,128]{1,0:T(8,128)(2,1)S(1)} collective-permute-done((bf16[544,128]{1,0:T(8,128)(2,1)S(1)}, bf16[544,128]{1,0:T(8,128)(2,1)S(1)}, u32[]{:S(2)}, u32[]{:S(2)}) %collective-permute-start.1) | collective-permute-done | bytes 139296 | tf_op jit(solution)/shard_map/ppermute | solution.py:411
  28.8 2.9 %shard_map.122 = (bf16[768,128]{1,0:T(8,128)(2,1)S(1)}, bf16[768,128]{1,0:T(8,128)(2,1)S(1)}, bf16[768,128]{1,0:T(8,128)(2,1)S(1)}, bf16[256,128]{1,0:T(8,128)(2...) custom-call(f32[2]{0:T(128)S(1)} %copy-done, ...), custom_call_target="tpu_custom_call", output_to_operand_aliasing={{12}: (3, {}), {13}: (4, {}), {14}: (5, {}), {15}: (6, {}),... | custom-call | flops 587202560 | bytes 1000000 | tf_op jit(solution)/shard_map/pallas_call | solution.py:454
  31.7 2.7 %collective-permute-start.10 = (bf16[256,128]{1,0:T(8,128)(2,1)S(1)}, bf16[256,128]{1,0:T(8,128)(2,1)S(1)}, u32[]{:S(2)}, u32[]{:S(2)}) collective-permute-start(bf16[256,128]{1,0:T(8,128)(2,1)S(1)} %get-tuple-element.58), channel_id=1, source_target_pairs={{0,64},{8,72},{16,80},{24,88},{32,96},{40,104},{48,112},{56,120},{... | collective-permute-start | bytes 196616 | tf_op jit(solution)/shard_map/ppermute | solution.py:411
  34.5 0.9 %collective-permute-start.11 = (bf16[256,128]{1,0:T(8,128)(2,1)S(1)}, bf16[256,128]{1,0:T(8,128)(2,1)S(1)}, u32[]{:S(2)}, u32[]{:S(2)}) collective-permute-start(bf16[256,128]{1,0:T(8,128)(2,1)S(1)} %get-tuple-element.59), channel_id=1, source_target_pairs={{0,96},{8,104},{16,112},{24,120},{32,64},{40,72},{48,80},{56,88},{... | collective-permute-start | bytes 196616 | tf_op jit(solution)/shard_map/ppermute | solution.py:411
  35.3 1.2 %collective-permute-start.6 = (bf16[768,128]{1,0:T(8,128)(2,1)S(1)}, bf16[768,128]{1,0:T(8,128)(2,1)S(1)}, u32[]{:S(2)}, u32[]{:S(2)}) collective-permute-start(bf16[768,128]{1,0:T(8,128)(2,1)S(1)} %get-tuple-element.54), channel_id=1, source_target_pairs={{0,8},{8,0},{16,24},{24,16},{32,40},{40,32},{48,56},{56,48},{64,72... | collective-permute-start | bytes 589832 | tf_op jit(solution)/shard_map/ppermute | solution.py:411
  36.6 0.0 collective-permute-done.20.far
  36.6 3.1 %collective-permute-start.7 = (bf16[768,128]{1,0:T(8,128)(2,1)S(1)}, bf16[768,128]{1,0:T(8,128)(2,1)S(1)}, u32[]{:S(2)}, u32[]{:S(2)}) collective-permute-start(bf16[768,128]{1,0:T(8,128)(2,1)S(1)} %get-tuple-element.55), channel_id=1, source_target_pairs={{0,16},{8,24},{16,0},{24,8},{32,48},{40,56},{48,32},{56,40},{64,80... | collective-permute-start | bytes 589832 | tf_op jit(solution)/shard_map/ppermute | solution.py:411
  39.7 0.8 %collective-permute-start.8 = (bf16[768,128]{1,0:T(8,128)(2,1)S(1)}, bf16[768,128]{1,0:T(8,128)(2,1)S(1)}, u32[]{:S(2)}, u32[]{:S(2)}) collective-permute-start(bf16[768,128]{1,0:T(8,128)(2,1)S(1)} %get-tuple-element.56), channel_id=1, source_target_pairs={{0,24},{8,16},{16,8},{24,0},{32,56},{40,48},{48,40},{56,32},{64,88... | collective-permute-start | bytes 589832 | tf_op jit(solution)/shard_map/ppermute | solution.py:411
  40.5 0.0 collective-permute-done.11.z3
  40.5 1.0 %collective-permute-start.9 = (bf16[256,128]{1,0:T(8,128)(2,1)S(1)}, bf16[256,128]{1,0:T(8,128)(2,1)S(1)}, u32[]{:S(2)}, u32[]{:S(2)}) collective-permute-start(bf16[256,128]{1,0:T(8,128)(2,1)S(1)} %get-tuple-element.57), channel_id=1, source_target_pairs={{0,32},{8,40},{16,48},{24,56},{32,0},{40,8},{48,16},{56,24},{64,96... | collective-permute-start | bytes 196616 | tf_op jit(solution)/shard_map/ppermute | solution.py:411
  41.5 3.3 %collective-permute-done.9.z1 = bf16[256,128]{1,0:T(8,128)(2,1)S(1)} collective-permute-done((bf16[256,128]{1,0:T(8,128)(2,1)S(1)}, bf16[256,128]{1,0:T(8,128)(2,1)S(1)}, u32[]{:S(2)}, u32[]{:S(2)}) %collective-permute-start.9) | collective-permute-done | bytes 65568 | tf_op jit(solution)/shard_map/ppermute | solution.py:411
  44.8 0.0 collective-permute-start.21
  44.8 0.0 collective-permute-done.6.y1
  44.8 2.5 %collective-permute-done.7.y2 = bf16[768,128]{1,0:T(8,128)(2,1)S(1)} collective-permute-done((bf16[768,128]{1,0:T(8,128)(2,1)S(1)}, bf16[768,128]{1,0:T(8,128)(2,1)S(1)}, u32[]{:S(2)}, u32[]{:S(2)}) %collective-permute-start.7) | collective-permute-done | bytes 196640 | tf_op jit(solution)/shard_map/ppermute | solution.py:411
  47.3 2.1 %collective-permute-done.8.y3 = bf16[768,128]{1,0:T(8,128)(2,1)S(1)} collective-permute-done((bf16[768,128]{1,0:T(8,128)(2,1)S(1)}, bf16[768,128]{1,0:T(8,128)(2,1)S(1)}, u32[]{:S(2)}, u32[]{:S(2)}) %collective-permute-start.8) | collective-permute-done | bytes 196640 | tf_op jit(solution)/shard_map/ppermute | solution.py:411
  49.4 0.1 shard_map.123.turned_in.g0
  49.5 1.0 %collective-permute-start.15 = (bf16[256,256]{1,0:T(8,128)(2,1)S(1)}, bf16[256,256]{1,0:T(8,128)(2,1)S(1)}, u32[]{:S(2)}, u32[]{:S(2)}) collective-permute-start(bf16[256,256]{1,0:T(8,128)(2,1)S(1)} %shard_map.123.turned_in.g0), channel_id=1, source_target_pairs={{0,32},{8,40},{16,48},{24,56},{32,0},{40,8},{48,16},{56,24},{64,96... | collective-permute-start | bytes 393224 | tf_op jit(solution)/shard_map/ppermute | solution.py:411
  50.5 1.7 %collective-permute-start.16 = (bf16[256,256]{1,0:T(8,128)(2,1)S(1)}, bf16[256,256]{1,0:T(8,128)(2,1)S(1)}, u32[]{:S(2)}, u32[]{:S(2)}) collective-permute-start(bf16[256,256]{1,0:T(8,128)(2,1)S(1)} %shard_map.123.turned_in.g0), channel_id=1, source_target_pairs={{0,64},{8,72},{16,80},{24,88},{32,96},{40,104},{48,112},{56,120},{... | collective-permute-start | bytes 393224 | tf_op jit(solution)/shard_map/ppermute | solution.py:411
  52.2 2.1 %collective-permute-start.17 = (bf16[256,256]{1,0:T(8,128)(2,1)S(1)}, bf16[256,256]{1,0:T(8,128)(2,1)S(1)}, u32[]{:S(2)}, u32[]{:S(2)}) collective-permute-start(bf16[256,256]{1,0:T(8,128)(2,1)S(1)} %shard_map.123.turned_in.g0), channel_id=1, source_target_pairs={{0,96},{8,104},{16,112},{24,120},{32,64},{40,72},{48,80},{56,88},{... | collective-permute-start | bytes 393224 | tf_op jit(solution)/shard_map/ppermute | solution.py:411
  54.3 0.0 collective-permute-start.12
  54.3 1.4 %collective-permute-done.15.g1 = bf16[256,256]{1,0:T(8,128)(2,1)S(1)} collective-permute-done((bf16[256,256]{1,0:T(8,128)(2,1)S(1)}, bf16[256,256]{1,0:T(8,128)(2,1)S(1)}, u32[]{:S(2)}, u32[]{:S(2)}) %collective-permute-start.15) | collective-permute-done | bytes 131104 | tf_op jit(solution)/shard_map/ppermute | solution.py:411
  55.7 2.3 %collective-permute-done.16.g2 = bf16[256,256]{1,0:T(8,128)(2,1)S(1)} collective-permute-done((bf16[256,256]{1,0:T(8,128)(2,1)S(1)}, bf16[256,256]{1,0:T(8,128)(2,1)S(1)}, u32[]{:S(2)}, u32[]{:S(2)}) %collective-permute-start.16) | collective-permute-done | bytes 131104 | tf_op jit(solution)/shard_map/ppermute | solution.py:411
  58.0 1.3 %collective-permute-done.17.g3 = bf16[256,256]{1,0:T(8,128)(2,1)S(1)} collective-permute-done((bf16[256,256]{1,0:T(8,128)(2,1)S(1)}, bf16[256,256]{1,0:T(8,128)(2,1)S(1)}, u32[]{:S(2)}, u32[]{:S(2)}) %collective-permute-start.17) | collective-permute-done | bytes 131104 | tf_op jit(solution)/shard_map/ppermute | solution.py:411
  59.3 0.0 collective-permute-done.19.near_swap
  59.3 0.9 %shard_map.125 = (f32[256,256]{1,0:T(8,128)S(1)}, bf16[256,256]{1,0:T(8,128)(2,1)S(1)}, bf16[256,256]{1,0:T(8,128)(2,1)S(1)}, bf16[256,256]{1,0:T(8,128)(2,1)S(1)}) custom-call(bf16[256,256]{1,0:T(8,128)(2,1)S(1)} %shard_map.123.turned_in.g0, bf16[256,256]{1,0:T(8,128)(2,1)S(1)} %collective-permute-done.15.g1, ...), custom_call_target="tpu_custom_call" | custom-call | flops 536870912 | bytes 1000000 | tf_op jit(solution)/shard_map/pallas_call | solution.py:454
  60.2 0.1 collective-permute-start.22
  60.3 3.1 %collective-permute-start.23 = (bf16[256,256]{1,0:T(8,128)(2,1)S(1)}, bf16[256,256]{1,0:T(8,128)(2,1)S(1)}, u32[]{:S(2)}, u32[]{:S(2)}) collective-permute-start(bf16[256,256]{1,0:T(8,128)(2,1)S(1)} %get-tuple-element.72), channel_id=1, source_target_pairs={{0,16},{8,24},{16,0},{24,8},{32,48},{40,56},{48,32},{56,40},{64,80... | collective-permute-start | bytes 393224 | tf_op jit(solution)/shard_map/ppermute | solution.py:411
  63.4 1.6 %collective-permute-start.24 = (bf16[256,256]{1,0:T(8,128)(2,1)S(1)}, bf16[256,256]{1,0:T(8,128)(2,1)S(1)}, u32[]{:S(2)}, u32[]{:S(2)}) collective-permute-start(bf16[256,256]{1,0:T(8,128)(2,1)S(1)} %get-tuple-element.73), channel_id=1, source_target_pairs={{0,24},{8,16},{16,8},{24,0},{32,56},{40,48},{48,40},{56,32},{64,88... | collective-permute-start | bytes 393224 | tf_op jit(solution)/shard_map/ppermute | solution.py:411
  65.0 1.1 %collective-permute-start.13 = (bf16[256,128]{1,0:T(8,128)(2,1)S(1)}, bf16[256,128]{1,0:T(8,128)(2,1)S(1)}, u32[]{:S(2)}, u32[]{:S(2)}) collective-permute-start(bf16[256,128]{1,0:T(8,128)(2,1)S(1)} %get-tuple-element.61), channel_id=1, source_target_pairs={{0,64},{8,72},{16,80},{24,88},{32,96},{40,104},{48,112},{56,120},{... | collective-permute-start | bytes 196616 | tf_op jit(solution)/shard_map/ppermute | solution.py:411
  66.0 0.0 collective-permute-done.12.v1
  66.0 2.2 %collective-permute-start.14 = (bf16[256,128]{1,0:T(8,128)(2,1)S(1)}, bf16[256,128]{1,0:T(8,128)(2,1)S(1)}, u32[]{:S(2)}, u32[]{:S(2)}) collective-permute-start(bf16[256,128]{1,0:T(8,128)(2,1)S(1)} %get-tuple-element.62), channel_id=1, source_target_pairs={{0,96},{8,104},{16,112},{24,120},{32,64},{40,72},{48,80},{56,88},{... | collective-permute-start | bytes 196616 | tf_op jit(solution)/shard_map/ppermute | solution.py:411
  68.2 2.5 %collective-permute-done.13.v2 = bf16[256,128]{1,0:T(8,128)(2,1)S(1)} collective-permute-done((bf16[256,128]{1,0:T(8,128)(2,1)S(1)}, bf16[256,128]{1,0:T(8,128)(2,1)S(1)}, u32[]{:S(2)}, u32[]{:S(2)}) %collective-permute-start.13) | collective-permute-done | bytes 65568 | tf_op jit(solution)/shard_map/ppermute | solution.py:411
  70.7 0.8 %collective-permute-done.14.v3 = bf16[256,128]{1,0:T(8,128)(2,1)S(1)} collective-permute-done((bf16[256,128]{1,0:T(8,128)(2,1)S(1)}, bf16[256,128]{1,0:T(8,128)(2,1)S(1)}, u32[]{:S(2)}, u32[]{:S(2)}) %collective-permute-start.14) | collective-permute-done | bytes 65568 | tf_op jit(solution)/shard_map/ppermute | solution.py:411
  71.5 1.1 %shard_map.124 = (bf16[512,128]{1,0:T(8,128)(2,1)}, bf16[512,128]{1,0:T(8,128)(2,1)}, bf16[512,128]{1,0:T(8,128)(2,1)}) custom-call(f32[2,256,128]{2,1,0:T(8,128)S(1)} %get-tuple-element.52.own_k, f32[2,256,128]{2,1,0:T(8,128)S(1)} %get-tuple-element.53.own_v, bf16[768,128]{1,0:T(8,128)(2,1)S(1)} %collective-permute-done.6.y1, ...), custom_call_target="tpu_custom_call" | custom-call | flops 10000000 | bytes 1000000 | tf_op jit(solution)/shard_map/pallas_call | solution.py:454
  72.7 0.8 %shard_map.126 = f32[256,256]{1,0:T(8,128)} custom-call(f32[256,256]{1,0:T(8,128)S(1)} %get-tuple-element.70.own, bf16[256,256]{1,0:T(8,128)(2,1)S(1)} %collective-permute-done.22.t1, bf16[256,256]{1,0:T(8,128)(2,1)S(1)} %collective-permute-done.23.t2, bf16[256,256]{1,0:T(8,128)(2,1)S(1)} %collective-permute-done.24.t3), custom_call_target="tpu_custom_call" | custom-call | flops 1000000 | bytes 1000000 | tf_op jit(solution)/shard_map/pallas_call | solution.py:454
  (11 shorter events, 0.0 us)
Async XLA Ops:
  0.6 21.6 %copy-start = (f32[2]{0:T(128)S(1)}, f32[2]{0:T(128)}, u32[]{:S(2)}) copy-start(f32[2]{0:T(128)} %lam.3) | copy-start | bytes 28
  2.7 19.5 %collective-permute-start.18 = (bf16[256,1024]{1,0:T(8,128)(2,1)S(1)}, bf16[256,1024]{1,0:T(8,128)(2,1)S(1)}, u32[]{:S(2)}, u32[]{:S(2)}) collective-permute-start(bf16[256,1024]{1,0:T(8,128)(2,1)S(1)} %get-tuple-element.68), channel_id=1, source_target_pairs={{0,32},{1,97},{2,34},{3,99},{4,36},{5,101},{6,38},{7,103},{8,40},{... | collective-permute-start | bytes 1572872 | tf_op jit(solution)/shard_map/ppermute | solution.py:421
  4.8 17.3 %collective-permute-start.2 = (bf16[1056,128]{1,0:T(8,128)(2,1)S(1)}, bf16[1056,128]{1,0:T(8,128)(2,1)S(1)}, u32[]{:S(2)}, u32[]{:S(2)}) collective-permute-start(bf16[1056,128]{1,0:T(8,128)(2,1)S(1)} %get-tuple-element.39.yown), channel_id=1, source_target_pairs={{0,8},{8,0},{16,24},{24,16},{32,40},{40,32},{48,56},{56,48},{64,72... | collective-permute-start | bytes 811016 | tf_op jit(solution)/shard_map/ppermute | solution.py:411
  6.4 8.6 %collective-permute-start.4 = (bf16[544,128]{1,0:T(8,128)(2,1)S(1)}, bf16[544,128]{1,0:T(8,128)(2,1)S(1)}, u32[]{:S(2)}, u32[]{:S(2)}) collective-permute-start(bf16[544,128]{1,0:T(8,128)(2,1)S(1)} %get-tuple-element.42), channel_id=1, source_target_pairs={{0,32},{8,40},{16,48},{24,56},{32,0},{40,8},{48,16},{56,24},{64,96... | collective-permute-start | bytes 417800 | tf_op jit(solution)/shard_map/ppermute | solution.py:411
  6.5 15.7 %collective-permute-start.3 = (bf16[1056,128]{1,0:T(8,128)(2,1)S(1)}, bf16[1056,128]{1,0:T(8,128)(2,1)S(1)}, u32[]{:S(2)}, u32[]{:S(2)}) collective-permute-start(bf16[1056,128]{1,0:T(8,128)(2,1)S(1)} %get-tuple-element.39.yown), channel_id=1, source_target_pairs={{0,24},{8,16},{16,8},{24,0},{32,56},{40,48},{48,40},{56,32},{64,88... | collective-permute-start | bytes 811016 | tf_op jit(solution)/shard_map/ppermute | solution.py:411
  8.7 9.6 %collective-permute-start.5 = (bf16[544,128]{1,0:T(8,128)(2,1)S(1)}, bf16[544,128]{1,0:T(8,128)(2,1)S(1)}, u32[]{:S(2)}, u32[]{:S(2)}) collective-permute-start(bf16[544,128]{1,0:T(8,128)(2,1)S(1)} %get-tuple-element.43), channel_id=1, source_target_pairs={{0,96},{8,104},{16,112},{24,120},{32,64},{40,72},{48,80},{56,88},{... | collective-permute-start | bytes 417800 | tf_op jit(solution)/shard_map/ppermute | solution.py:411
  14.9 13.8 %collective-permute-start = (bf16[1056,128]{1,0:T(8,128)(2,1)S(1)}, bf16[1056,128]{1,0:T(8,128)(2,1)S(1)}, u32[]{:S(2)}, u32[]{:S(2)}) collective-permute-start(bf16[1056,128]{1,0:T(8,128)(2,1)S(1)} %get-tuple-element.39.yown), channel_id=1, source_target_pairs={{0,16},{8,24},{16,0},{24,8},{32,48},{40,56},{48,32},{56,40},{64,80... | collective-permute-start | bytes 811016 | tf_op jit(solution)/shard_map/ppermute | solution.py:411
  18.2 18.4 %collective-permute-start.20 = (bf16[128,1024]{1,0:T(8,128)(2,1)S(1)}, bf16[128,1024]{1,0:T(8,128)(2,1)S(1)}, u32[]{:S(2)}, u32[]{:S(2)}) collective-permute-start(bf16[128,1024]{1,0:T(8,128)(2,1)S(1)} %get-tuple-element.69), channel_id=1, source_target_pairs={{0,64},{8,72},{16,80},{24,88},{32,96},{40,104},{48,112},{56,120},{... | collective-permute-start | bytes 786440 | tf_op jit(solution)/shard_map/ppermute | solution.py:411
  22.1 6.7 %collective-permute-start.1 = (bf16[544,128]{1,0:T(8,128)(2,1)S(1)}, bf16[544,128]{1,0:T(8,128)(2,1)S(1)}, u32[]{:S(2)}, u32[]{:S(2)}) collective-permute-start(bf16[544,128]{1,0:T(8,128)(2,1)S(1)} %get-tuple-element.40), channel_id=1, source_target_pairs={{0,64},{8,72},{16,80},{24,88},{32,96},{40,104},{48,112},{56,120},{... | collective-permute-start | bytes 417800 | tf_op jit(solution)/shard_map/ppermute | solution.py:411
  22.2 37.1 %collective-permute-start.19 = (bf16[256,1024]{1,0:T(8,128)(2,1)S(1)}, bf16[256,1024]{1,0:T(8,128)(2,1)S(1)}, u32[]{:S(2)}, u32[]{:S(2)}) collective-permute-start(bf16[256,1024]{1,0:T(8,128)(2,1)S(1)} %collective-permute-done.18.near), channel_id=1, source_target_pairs={{0,1},{1,0},{2,3},{3,2},{4,5},{5,4},{6,7},{7,6},{8,9},{9,8},{10,11... | collective-permute-start | bytes 1572872 | tf_op jit(solution)/shard_map/ppermute | solution.py:425
  31.7 8.0 %collective-permute-start.10 = (bf16[256,128]{1,0:T(8,128)(2,1)S(1)}, bf16[256,128]{1,0:T(8,128)(2,1)S(1)}, u32[]{:S(2)}, u32[]{:S(2)}) collective-permute-start(bf16[256,128]{1,0:T(8,128)(2,1)S(1)} %get-tuple-element.58), channel_id=1, source_target_pairs={{0,64},{8,72},{16,80},{24,88},{32,96},{40,104},{48,112},{56,120},{... | collective-permute-start | bytes 196616 | tf_op jit(solution)/shard_map/ppermute | solution.py:411
  34.5 6.1 %collective-permute-start.11 = (bf16[256,128]{1,0:T(8,128)(2,1)S(1)}, bf16[256,128]{1,0:T(8,128)(2,1)S(1)}, u32[]{:S(2)}, u32[]{:S(2)}) collective-permute-start(bf16[256,128]{1,0:T(8,128)(2,1)S(1)} %get-tuple-element.59), channel_id=1, source_target_pairs={{0,96},{8,104},{16,112},{24,120},{32,64},{40,72},{48,80},{56,88},{... | collective-permute-start | bytes 196616 | tf_op jit(solution)/shard_map/ppermute | solution.py:411
  35.3 9.4 %collective-permute-start.6 = (bf16[768,128]{1,0:T(8,128)(2,1)S(1)}, bf16[768,128]{1,0:T(8,128)(2,1)S(1)}, u32[]{:S(2)}, u32[]{:S(2)}) collective-permute-start(bf16[768,128]{1,0:T(8,128)(2,1)S(1)} %get-tuple-element.54), channel_id=1, source_target_pairs={{0,8},{8,0},{16,24},{24,16},{32,40},{40,32},{48,56},{56,48},{64,72... | collective-permute-start | bytes 589832 | tf_op jit(solution)/shard_map/ppermute | solution.py:411
  36.6 10.7 %collective-permute-start.7 = (bf16[768,128]{1,0:T(8,128)(2,1)S(1)}, bf16[768,128]{1,0:T(8,128)(2,1)S(1)}, u32[]{:S(2)}, u32[]{:S(2)}) collective-permute-start(bf16[768,128]{1,0:T(8,128)(2,1)S(1)} %get-tuple-element.55), channel_id=1, source_target_pairs={{0,16},{8,24},{16,0},{24,8},{32,48},{40,56},{48,32},{56,40},{64,80... | collective-permute-start | bytes 589832 | tf_op jit(solution)/shard_map/ppermute | solution.py:411
  39.7 9.7 %collective-permute-start.8 = (bf16[768,128]{1,0:T(8,128)(2,1)S(1)}, bf16[768,128]{1,0:T(8,128)(2,1)S(1)}, u32[]{:S(2)}, u32[]{:S(2)}) collective-permute-start(bf16[768,128]{1,0:T(8,128)(2,1)S(1)} %get-tuple-element.56), channel_id=1, source_target_pairs={{0,24},{8,16},{16,8},{24,0},{32,56},{40,48},{48,40},{56,32},{64,88... | collective-permute-start | bytes 589832 | tf_op jit(solution)/shard_map/ppermute | solution.py:411
  40.5 4.3 %collective-permute-start.9 = (bf16[256,128]{1,0:T(8,128)(2,1)S(1)}, bf16[256,128]{1,0:T(8,128)(2,1)S(1)}, u32[]{:S(2)}, u32[]{:S(2)}) collective-permute-start(bf16[256,128]{1,0:T(8,128)(2,1)S(1)} %get-tuple-element.57), channel_id=1, source_target_pairs={{0,32},{8,40},{16,48},{24,56},{32,0},{40,8},{48,16},{56,24},{64,96... | collective-permute-start | bytes 196616 | tf_op jit(solution)/shard_map/ppermute | solution.py:411
  44.8 9.5 %collective-permute-start.21 = (bf16[128,1024]{1,0:T(8,128)(2,1)S(1)}, bf16[128,1024]{1,0:T(8,128)(2,1)S(1)}, u32[]{:S(2)}, u32[]{:S(2)}) collective-permute-start(bf16[128,1024]{1,0:T(8,128)(2,1)S(1)} %collective-permute-done.20.far), channel_id=1, source_target_pairs={{0,1},{1,0},{2,3},{3,2},{4,5},{5,4},{6,7},{7,6},{8,9},{9,8},{10,11... | collective-permute-start | bytes 786440 | tf_op jit(solution)/shard_map/ppermute | solution.py:425
  49.5 6.2 %collective-permute-start.15 = (bf16[256,256]{1,0:T(8,128)(2,1)S(1)}, bf16[256,256]{1,0:T(8,128)(2,1)S(1)}, u32[]{:S(2)}, u32[]{:S(2)}) collective-permute-start(bf16[256,256]{1,0:T(8,128)(2,1)S(1)} %shard_map.123.turned_in.g0), channel_id=1, source_target_pairs={{0,32},{8,40},{16,48},{24,56},{32,0},{40,8},{48,16},{56,24},{64,96... | collective-permute-start | bytes 393224 | tf_op jit(solution)/shard_map/ppermute | solution.py:411
  50.5 7.5 %collective-permute-start.16 = (bf16[256,256]{1,0:T(8,128)(2,1)S(1)}, bf16[256,256]{1,0:T(8,128)(2,1)S(1)}, u32[]{:S(2)}, u32[]{:S(2)}) collective-permute-start(bf16[256,256]{1,0:T(8,128)(2,1)S(1)} %shard_map.123.turned_in.g0), channel_id=1, source_target_pairs={{0,64},{8,72},{16,80},{24,88},{32,96},{40,104},{48,112},{56,120},{... | collective-permute-start | bytes 393224 | tf_op jit(solution)/shard_map/ppermute | solution.py:411
  52.2 7.1 %collective-permute-start.17 = (bf16[256,256]{1,0:T(8,128)(2,1)S(1)}, bf16[256,256]{1,0:T(8,128)(2,1)S(1)}, u32[]{:S(2)}, u32[]{:S(2)}) collective-permute-start(bf16[256,256]{1,0:T(8,128)(2,1)S(1)} %shard_map.123.turned_in.g0), channel_id=1, source_target_pairs={{0,96},{8,104},{16,112},{24,120},{32,64},{40,72},{48,80},{56,88},{... | collective-permute-start | bytes 393224 | tf_op jit(solution)/shard_map/ppermute | solution.py:411
  54.3 11.7 %collective-permute-start.12 = (bf16[256,128]{1,0:T(8,128)(2,1)S(1)}, bf16[256,128]{1,0:T(8,128)(2,1)S(1)}, u32[]{:S(2)}, u32[]{:S(2)}) collective-permute-start(bf16[256,128]{1,0:T(8,128)(2,1)S(1)} %get-tuple-element.60), channel_id=1, source_target_pairs={{0,32},{8,40},{16,48},{24,56},{32,0},{40,8},{48,16},{56,24},{64,96... | collective-permute-start | bytes 196616 | tf_op jit(solution)/shard_map/ppermute | solution.py:411
  60.2 12.5 %collective-permute-start.22 = (bf16[256,256]{1,0:T(8,128)(2,1)S(1)}, bf16[256,256]{1,0:T(8,128)(2,1)S(1)}, u32[]{:S(2)}, u32[]{:S(2)}) collective-permute-start(bf16[256,256]{1,0:T(8,128)(2,1)S(1)} %get-tuple-element.71), channel_id=1, source_target_pairs={{0,8},{8,0},{16,24},{24,16},{32,40},{40,32},{48,56},{56,48},{64,72... | collective-permute-start | bytes 393224 | tf_op jit(solution)/shard_map/ppermute | solution.py:411
  60.3 12.4 %collective-permute-start.23 = (bf16[256,256]{1,0:T(8,128)(2,1)S(1)}, bf16[256,256]{1,0:T(8,128)(2,1)S(1)}, u32[]{:S(2)}, u32[]{:S(2)}) collective-permute-start(bf16[256,256]{1,0:T(8,128)(2,1)S(1)} %get-tuple-element.72), channel_id=1, source_target_pairs={{0,16},{8,24},{16,0},{24,8},{32,48},{40,56},{48,32},{56,40},{64,80... | collective-permute-start | bytes 393224 | tf_op jit(solution)/shard_map/ppermute | solution.py:411
  63.4 9.3 %collective-permute-start.24 = (bf16[256,256]{1,0:T(8,128)(2,1)S(1)}, bf16[256,256]{1,0:T(8,128)(2,1)S(1)}, u32[]{:S(2)}, u32[]{:S(2)}) collective-permute-start(bf16[256,256]{1,0:T(8,128)(2,1)S(1)} %get-tuple-element.73), channel_id=1, source_target_pairs={{0,24},{8,16},{16,8},{24,0},{32,56},{40,48},{48,40},{56,32},{64,88... | collective-permute-start | bytes 393224 | tf_op jit(solution)/shard_map/ppermute | solution.py:411
  65.0 5.8 %collective-permute-start.13 = (bf16[256,128]{1,0:T(8,128)(2,1)S(1)}, bf16[256,128]{1,0:T(8,128)(2,1)S(1)}, u32[]{:S(2)}, u32[]{:S(2)}) collective-permute-start(bf16[256,128]{1,0:T(8,128)(2,1)S(1)} %get-tuple-element.61), channel_id=1, source_target_pairs={{0,64},{8,72},{16,80},{24,88},{32,96},{40,104},{48,112},{56,120},{... | collective-permute-start | bytes 196616 | tf_op jit(solution)/shard_map/ppermute | solution.py:411
  66.0 5.5 %collective-permute-start.14 = (bf16[256,128]{1,0:T(8,128)(2,1)S(1)}, bf16[256,128]{1,0:T(8,128)(2,1)S(1)}, u32[]{:S(2)}, u32[]{:S(2)}) collective-permute-start(bf16[256,128]{1,0:T(8,128)(2,1)S(1)} %get-tuple-element.62), channel_id=1, source_target_pairs={{0,96},{8,104},{16,112},{24,120},{32,64},{40,72},{48,80},{56,88},{... | collective-permute-start | bytes 196616 | tf_op jit(solution)/shard_map/ppermute | solution.py:411

commit v8 on v5

--- a/solution.py
+++ b/solution.py
@@ -280,7 +280,7 @@
 
 def attend_far_kernel(
     lam, y2, z2, buf_in, stat_in, kpad_in, kturn_in, qpad_in, dq_in, dk_in, dv_in,
-    g1, g2, g3, r1, r2, r3, own_q, own_k, own_v,
+    g1, g2, g3, r1, r2, r3, v1, v2, v3, own_q, own_k, own_v,
     buf, stat, kpad, kturn, qpad, dq, dk, dv, wide_w, tall_s,
 ):
     z, y, _ = position()
@@ -303,18 +303,17 @@
         put_q(ref, slot)
         ref[ROWS : 2 * ROWS] = (dk[slot] * scale).astype(BF)
         ref[2 * ROWS :] = dv[slot].astype(BF)
-    for n, ref in enumerate((r1, r2, r3), 1):
+    for n, (ref, ref_v) in enumerate(((r1, v1), (r2, v2), (r3, v3)), 1):
         keys = jnp.bitwise_xor(z, n) < z
+        ref_v[...] = dv[SIDE + n].astype(BF)
 
         @pl.when(keys)
         def _():
-            ref[0:ROWS] = (dk[SIDE + n] * scale).astype(BF)
-            ref[ROWS:] = dv[SIDE + n].astype(BF)
+            ref[...] = (dk[SIDE + n] * scale).astype(BF)
 
         @pl.when(jnp.logical_not(keys))
         def _():
             put_q(ref, SIDE + n)
-            ref[ROWS:] = jnp.zeros((ROWS, 128), BF)
 
     own_q[0] = dq[SIDE] * scale
     own_q[1] = dq[0] * scale
@@ -343,18 +342,19 @@
 
 
 def keys_kernel(
-    own_k, own_v, y1, y2, y3, z1, z2, z3, turned_in, q_out, k_out, v_out, acc_k, acc_v
+    own_k, own_v, y1, y2, y3, z1, z2, z3, v1, v2, v3, turned_in,
+    q_out, k_out, v_out, acc_k, acc_v,
 ):
     z, _, _ = position()
     acc_k[...] = own_k[1]
     acc_v[...] = own_v[1]
-    for n, ref in enumerate((z1, z2, z3)):
-        keys = z < jnp.bitwise_xor(z, n + 1)
+    for n, (ref, ref_v) in enumerate(((z1, v1), (z2, v2), (z3, v3)), 1):
+        keys = z < jnp.bitwise_xor(z, n)
 
         @pl.when(keys)
         def _():
-            acc_k[...] += ref[0:ROWS].astype(F32)
-            acc_v[...] += ref[ROWS:].astype(F32)
+            acc_k[...] += ref[...].astype(F32)
+            acc_v[...] += ref_v[...].astype(F32)
 
     row = iota((ROWS, ROWS), 0)
     col = iota((ROWS, ROWS), 1)
@@ -543,7 +543,7 @@
     )(mix_lambda, latents, yown, ys[0], ys[2], zown, zs[0], zs[2])
     result_shapes = (
         (shape(3 * ROWS, 128),) * 3
-        + (shape(2 * ROWS, 128),) * 3
+        + (shape(ROWS, 128),) * 6
         + (shape(2, 128, ROWS, dtype=F32),)
         + (shape(2, ROWS, 128, dtype=F32),) * 2
     )
@@ -557,9 +557,10 @@
         7 * pair_flops,
         aliases={3 + n: len(result_shapes) + n for n in range(len(state_shapes))},
     )(mix_lambda, ys[1], zs[1], *state)
-    own_q, own_k, own_v = results[6:9]
+    own_q, own_k, own_v = results[9:12]
     y_back = [traded(x, "y", n) for n, x in enumerate(results[0:3], 1)]
     z_back = [traded(x, "z", n) for n, x in enumerate(results[3:6], 1)]
+    v_back = [traded(x, "z", n) for n, x in enumerate(results[6:9], 1)]
     turned_grad = call(
         queries_kernel,
         shape(ROWS, ROWS),
@@ -585,10 +586,10 @@
         (shape(2 * ROWS, 128),) * 3,
         0,
         0,
-        9,
+        12,
         [pltpu.VMEM((ROWS, 128), F32)] * 2,
         10**7,
-    )(own_k, own_v, *y_back, *z_back, turned_grad)
+    )(own_k, own_v, *y_back, *z_back, *v_back, turned_grad)
     weight_grad = call(
         total_kernel, shape(ROWS, ROWS, dtype=F32), 0, 0, 4, [], 10**6
     )(own, *[traded(x, "y", n) for n, x in enumerate(parts, 1)])

time: 68.8 us -> 73.3 us (1.065); the launches traced: 67.9 us -> 73.2 us
  starting transfers between devices: 38 us -> 42 us
  waiting for transfers between devices: 17.2 us -> 18.7 us
    ppermute x19 -> x22, starting transfers between devices: 33.5 us -> 37.9 us  [traded(): return lax.ppermute(x, 'sp', [(s, s ^ step) for s in range(SIDE * SIDE)])]
    ppermute x19 -> x22, waiting for transfers between devices: 17.2 us -> 18.7 us  [traded(): return lax.ppermute(x, 'sp', [(s, s ^ step) for s in range(SIDE * SIDE)])]
  transfers between devices with their start and end apart: 26 -> 29, of which waited for: 12 -> 11; matrix products, arithmetic and copies ran while one was open for 0% -> 0% of each run, Pallas kernels for 12% -> 12%
where the time goes in v8:
time: 73.3 us; the launch traced here: 73.2 us
  starting transfers between devices  42 us (57%)
  waiting for transfers between devices  18.7 us (26%)
  Pallas kernels  11.8 us (16%)
    ppermute x22, starting transfers between devices, traded(): return lax.ppermute(x, 'sp', [(s, s ^ step) for s in range(SIDE * SIDE)])  37.9 us
    ppermute x22, waiting for transfers between devices, traded(): return lax.ppermute(x, 'sp', [(s, s ^ step) for s in range(SIDE * SIDE)])  18.7 us
    pallas_call x7, Pallas kernels, run(): return calling(*arrays[:scalars], *held, *rest)  11.8 us
    ppermute x2, starting transfers between devices, across(): lax.ppermute(x, 'tp', [(t, t ^ 2) for t in range(lax.axis_size('tp'))])  2.03 us
  transfers between devices with their start and end apart: 29, of which 11 were waited for; matrix products, arithmetic and copies ran while one was open for 0% of the time, Pallas kernels for 12%

profile of v8, /device:TPU:0, one launch (start us, length us, event | category | flops | bytes accessed | tf_op | source)
XLA Modules:
  0.0 73.2 jit_solution(14651460307577538724)
XLA Ops:
  0.6 2.0 %shard_map.120 = (bf16[1056,128]{1,0:T(8,128)(2,1)S(1)}, bf16[1056,128]{1,0:T(8,128)(2,1)S(1)}, bf16[544,128]{1,0:T(8,128)(2,1)S(1)}, bf16[544,128]{1,0:T(8,128)...) custom-call(bf16[512,128]{1,0:T(8,128)(2,1)} %bitcast.11, ...), custom_call_target="tpu_custom_call" | custom-call | flops 100000000 | bytes 1000000 | tf_op jit(solution)/shard_map/pallas_call | solution.py:460
  2.7 4.1 %collective-permute-start.22 = (bf16[64,1024]{1,0:T(8,128)(2,1)S(1)}, bf16[64,1024]{1,0:T(8,128)(2,1)S(1)}, u32[]{:S(2)}, u32[]{:S(2)}) collective-permute-start(bf16[64,1024]{1,0:T(8,128)(2,1)S(1)} %get-tuple-element.69), channel_id=1, source_target_pairs={{0,64},{8,72},{16,80},{24,88},{32,96},{40,104},{48,112},{56,120},{... | collective-permute-start | bytes 393224 | tf_op jit(solution)/shard_map/ppermute | solution.py:413
  6.7 1.0 %collective-permute-start.4 = (bf16[544,128]{1,0:T(8,128)(2,1)S(1)}, bf16[544,128]{1,0:T(8,128)(2,1)S(1)}, u32[]{:S(2)}, u32[]{:S(2)}) collective-permute-start(bf16[544,128]{1,0:T(8,128)(2,1)S(1)} %get-tuple-element.42), channel_id=1, source_target_pairs={{0,32},{8,40},{16,48},{24,56},{32,0},{40,8},{48,16},{56,24},{64,96... | collective-permute-start | bytes 417800 | tf_op jit(solution)/shard_map/ppermute | solution.py:413
  7.8 1.6 %collective-permute-start.2 = (bf16[1056,128]{1,0:T(8,128)(2,1)S(1)}, bf16[1056,128]{1,0:T(8,128)(2,1)S(1)}, u32[]{:S(2)}, u32[]{:S(2)}) collective-permute-start(bf16[1056,128]{1,0:T(8,128)(2,1)S(1)} %get-tuple-element.39.yown), channel_id=1, source_target_pairs={{0,8},{8,0},{16,24},{24,16},{32,40},{40,32},{48,56},{56,48},{64,72... | collective-permute-start | bytes 811016 | tf_op jit(solution)/shard_map/ppermute | solution.py:413
  9.3 2.2 %collective-permute-start.3 = (bf16[1056,128]{1,0:T(8,128)(2,1)S(1)}, bf16[1056,128]{1,0:T(8,128)(2,1)S(1)}, u32[]{:S(2)}, u32[]{:S(2)}) collective-permute-start(bf16[1056,128]{1,0:T(8,128)(2,1)S(1)} %get-tuple-element.39.yown), channel_id=1, source_target_pairs={{0,24},{8,16},{16,8},{24,0},{32,56},{40,48},{48,40},{56,32},{64,88... | collective-permute-start | bytes 811016 | tf_op jit(solution)/shard_map/ppermute | solution.py:413
  11.5 1.0 %collective-permute-start.18 = (bf16[128,1024]{1,0:T(8,128)(2,1)S(1)}, bf16[128,1024]{1,0:T(8,128)(2,1)S(1)}, u32[]{:S(2)}, u32[]{:S(2)}) collective-permute-start(bf16[128,1024]{1,0:T(8,128)(2,1)S(1)} %get-tuple-element.68), channel_id=1, source_target_pairs={{0,32},{1,97},{2,34},{3,99},{4,36},{5,101},{6,38},{7,103},{8,40},{... | collective-permute-start | bytes 786440 | tf_op jit(solution)/shard_map/ppermute | solution.py:423
  12.5 0.0 collective-permute-done.22.f0
  12.5 2.3 %collective-permute-start.5 = (bf16[544,128]{1,0:T(8,128)(2,1)S(1)}, bf16[544,128]{1,0:T(8,128)(2,1)S(1)}, u32[]{:S(2)}, u32[]{:S(2)}) collective-permute-start(bf16[544,128]{1,0:T(8,128)(2,1)S(1)} %get-tuple-element.43), channel_id=1, source_target_pairs={{0,96},{8,104},{16,112},{24,120},{32,64},{40,72},{48,80},{56,88},{... | collective-permute-start | bytes 417800 | tf_op jit(solution)/shard_map/ppermute | solution.py:413
  14.8 0.0 collective-permute-done.4.z1
  14.8 3.2 %collective-permute-start = (bf16[1056,128]{1,0:T(8,128)(2,1)S(1)}, bf16[1056,128]{1,0:T(8,128)(2,1)S(1)}, u32[]{:S(2)}, u32[]{:S(2)}) collective-permute-start(bf16[1056,128]{1,0:T(8,128)(2,1)S(1)} %get-tuple-element.39.yown), channel_id=1, source_target_pairs={{0,16},{8,24},{16,0},{24,8},{32,48},{40,56},{48,32},{56,40},{64,80... | collective-permute-start | bytes 811016 | tf_op jit(solution)/shard_map/ppermute | solution.py:413
  18.0 1.9 %collective-permute-done.5.z3 = bf16[544,128]{1,0:T(8,128)(2,1)S(1)} collective-permute-done((bf16[544,128]{1,0:T(8,128)(2,1)S(1)}, bf16[544,128]{1,0:T(8,128)(2,1)S(1)}, u32[]{:S(2)}, u32[]{:S(2)}) %collective-permute-start.5) | collective-permute-done | bytes 139296 | tf_op jit(solution)/shard_map/ppermute | solution.py:413
  19.8 0.3 collective-permute-start.1
  20.2 1.5 %collective-permute-start.23 = (bf16[64,1024]{1,0:T(8,128)(2,1)S(1)}, bf16[64,1024]{1,0:T(8,128)(2,1)S(1)}, u32[]{:S(2)}, u32[]{:S(2)}) collective-permute-start(bf16[64,1024]{1,0:T(8,128)(2,1)S(1)} %collective-permute-done.22.f0), channel_id=1, source_target_pairs={{0,2},{1,3},{2,0},{3,1},{4,6},{5,7},{6,4},{7,5},{8,10},{9,11},{10,... | collective-permute-start | bytes 393224 | tf_op jit(solution)/shard_map/ppermute | solution.py:427
  21.7 0.5 collective-permute-start.19
  22.2 0.0 collective-permute-done.3.y3
  22.2 3.9 %shard_map.121 = (bf16[8,1056,128]{2,1,0:T(8,128)(2,1)S(1)}, f32[8,8,256]{2,1,0:T(8,128)S(1)}, bf16[8,512,128]{2,1,0:T(8,128)(2,1)S(1)}, bf16[8,128,512]{2,1,0:T...) custom-call(f32[2]{0:T(128)S(1)} %copy-done, ...), custom_call_target="tpu_custom_call" | custom-call | flops 838860800 | bytes 1000000 | tf_op jit(solution)/shard_map/pallas_call | solution.py:460
  26.1 0.4 collective-permute-done.1.z2
  26.6 2.9 %shard_map.122 = (bf16[768,128]{1,0:T(8,128)(2,1)S(1)}, bf16[768,128]{1,0:T(8,128)(2,1)S(1)}, bf16[768,128]{1,0:T(8,128)(2,1)S(1)}, bf16[256,128]{1,0:T(8,128)(2...) custom-call(f32[2]{0:T(128)S(1)} %copy-done, ...), custom_call_target="tpu_custom_call", output_to_operand_aliasing={{12}: (3, {}), {13}: (4, {}), {14}: (5, {}), {15}: (6, {}),... | custom-call | flops 587202560 | bytes 1000000 | tf_op jit(solution)/shard_map/pallas_call | solution.py:460
  29.5 0.8 %collective-permute-start.6 = (bf16[768,128]{1,0:T(8,128)(2,1)S(1)}, bf16[768,128]{1,0:T(8,128)(2,1)S(1)}, u32[]{:S(2)}, u32[]{:S(2)}) collective-permute-start(bf16[768,128]{1,0:T(8,128)(2,1)S(1)} %get-tuple-element.54), channel_id=1, source_target_pairs={{0,8},{8,0},{16,24},{24,16},{32,40},{40,32},{48,56},{56,48},{64,72... | collective-permute-start | bytes 589832 | tf_op jit(solution)/shard_map/ppermute | solution.py:413
  30.3 2.8 %collective-permute-start.7 = (bf16[768,128]{1,0:T(8,128)(2,1)S(1)}, bf16[768,128]{1,0:T(8,128)(2,1)S(1)}, u32[]{:S(2)}, u32[]{:S(2)}) collective-permute-start(bf16[768,128]{1,0:T(8,128)(2,1)S(1)} %get-tuple-element.55), channel_id=1, source_target_pairs={{0,16},{8,24},{16,0},{24,8},{32,48},{40,56},{48,32},{56,40},{64,80... | collective-permute-start | bytes 589832 | tf_op jit(solution)/shard_map/ppermute | solution.py:413
  33.2 1.7 %collective-permute-start.10 = (bf16[256,128]{1,0:T(8,128)(2,1)S(1)}, bf16[256,128]{1,0:T(8,128)(2,1)S(1)}, u32[]{:S(2)}, u32[]{:S(2)}) collective-permute-start(bf16[256,128]{1,0:T(8,128)(2,1)S(1)} %get-tuple-element.58), channel_id=1, source_target_pairs={{0,64},{8,72},{16,80},{24,88},{32,96},{40,104},{48,112},{56,120},{... | collective-permute-start | bytes 196616 | tf_op jit(solution)/shard_map/ppermute | solution.py:413
  34.9 3.2 %collective-permute-start.11 = (bf16[256,128]{1,0:T(8,128)(2,1)S(1)}, bf16[256,128]{1,0:T(8,128)(2,1)S(1)}, u32[]{:S(2)}, u32[]{:S(2)}) collective-permute-start(bf16[256,128]{1,0:T(8,128)(2,1)S(1)} %get-tuple-element.59), channel_id=1, source_target_pairs={{0,96},{8,104},{16,112},{24,120},{32,64},{40,72},{48,80},{56,88},{... | collective-permute-start | bytes 196616 | tf_op jit(solution)/shard_map/ppermute | solution.py:413
  38.1 0.9 %collective-permute-done.10.z2 = bf16[256,128]{1,0:T(8,128)(2,1)S(1)} collective-permute-done((bf16[256,128]{1,0:T(8,128)(2,1)S(1)}, bf16[256,128]{1,0:T(8,128)(2,1)S(1)}, u32[]{:S(2)}, u32[]{:S(2)}) %collective-permute-start.10) | collective-permute-done | bytes 65568 | tf_op jit(solution)/shard_map/ppermute | solution.py:413
  38.9 1.2 %collective-permute-start.8 = (bf16[768,128]{1,0:T(8,128)(2,1)S(1)}, bf16[768,128]{1,0:T(8,128)(2,1)S(1)}, u32[]{:S(2)}, u32[]{:S(2)}) collective-permute-start(bf16[768,128]{1,0:T(8,128)(2,1)S(1)} %get-tuple-element.56), channel_id=1, source_target_pairs={{0,24},{8,16},{16,8},{24,0},{32,56},{40,48},{48,40},{56,32},{64,88... | collective-permute-start | bytes 589832 | tf_op jit(solution)/shard_map/ppermute | solution.py:413
  40.2 0.2 collective-permute-done.11.z3
  40.4 1.1 %collective-permute-start.9 = (bf16[256,128]{1,0:T(8,128)(2,1)S(1)}, bf16[256,128]{1,0:T(8,128)(2,1)S(1)}, u32[]{:S(2)}, u32[]{:S(2)}) collective-permute-start(bf16[256,128]{1,0:T(8,128)(2,1)S(1)} %get-tuple-element.57), channel_id=1, source_target_pairs={{0,32},{8,40},{16,48},{24,56},{32,0},{40,8},{48,16},{56,24},{64,96... | collective-permute-start | bytes 196616 | tf_op jit(solution)/shard_map/ppermute | solution.py:413
  41.5 3.1 %collective-permute-done.9.z1 = bf16[256,128]{1,0:T(8,128)(2,1)S(1)} collective-permute-done((bf16[256,128]{1,0:T(8,128)(2,1)S(1)}, bf16[256,128]{1,0:T(8,128)(2,1)S(1)}, u32[]{:S(2)}, u32[]{:S(2)}) %collective-permute-start.9) | collective-permute-done | bytes 65568 | tf_op jit(solution)/shard_map/ppermute | solution.py:413
  44.7 0.5 collective-permute-start.24
  45.2 0.1 collective-permute-start.25
  45.3 0.4 collective-permute-start.21
  45.7 0.1 collective-permute-done.8.y3
  45.8 0.1 shard_map.123.turned_in.g0
  45.9 2.3 %collective-permute-start.15 = (bf16[256,256]{1,0:T(8,128)(2,1)S(1)}, bf16[256,256]{1,0:T(8,128)(2,1)S(1)}, u32[]{:S(2)}, u32[]{:S(2)}) collective-permute-start(bf16[256,256]{1,0:T(8,128)(2,1)S(1)} %shard_map.123.turned_in.g0), channel_id=1, source_target_pairs={{0,32},{8,40},{16,48},{24,56},{32,0},{40,8},{48,16},{56,24},{64,96... | collective-permute-start | bytes 393224 | tf_op jit(solution)/shard_map/ppermute | solution.py:413
  48.2 2.3 %collective-permute-start.16 = (bf16[256,256]{1,0:T(8,128)(2,1)S(1)}, bf16[256,256]{1,0:T(8,128)(2,1)S(1)}, u32[]{:S(2)}, u32[]{:S(2)}) collective-permute-start(bf16[256,256]{1,0:T(8,128)(2,1)S(1)} %shard_map.123.turned_in.g0), channel_id=1, source_target_pairs={{0,64},{8,72},{16,80},{24,88},{32,96},{40,104},{48,112},{56,120},{... | collective-permute-start | bytes 393224 | tf_op jit(solution)/shard_map/ppermute | solution.py:413
  50.5 0.5 collective-permute-start.17
  51.0 0.7 collective-permute-start.12
  51.7 0.2 collective-permute-done.15.g1
  51.9 5.8 %collective-permute-done.16.g2 = bf16[256,256]{1,0:T(8,128)(2,1)S(1)} collective-permute-done((bf16[256,256]{1,0:T(8,128)(2,1)S(1)}, bf16[256,256]{1,0:T(8,128)(2,1)S(1)}, u32[]{:S(2)}, u32[]{:S(2)}) %collective-permute-start.16) | collective-permute-done | bytes 131104 | tf_op jit(solution)/shard_map/ppermute | solution.py:413
  57.7 1.6 %collective-permute-done.17.g3 = bf16[256,256]{1,0:T(8,128)(2,1)S(1)} collective-permute-done((bf16[256,256]{1,0:T(8,128)(2,1)S(1)}, bf16[256,256]{1,0:T(8,128)(2,1)S(1)}, u32[]{:S(2)}, u32[]{:S(2)}) %collective-permute-start.17) | collective-permute-done | bytes 131104 | tf_op jit(solution)/shard_map/ppermute | solution.py:413
  59.3 0.9 %shard_map.125 = (f32[256,256]{1,0:T(8,128)S(1)}, bf16[256,256]{1,0:T(8,128)(2,1)S(1)}, bf16[256,256]{1,0:T(8,128)(2,1)S(1)}, bf16[256,256]{1,0:T(8,128)(2,1)S(1)}) custom-call(bf16[256,256]{1,0:T(8,128)(2,1)S(1)} %shard_map.123.turned_in.g0, bf16[256,256]{1,0:T(8,128)(2,1)S(1)} %collective-permute-done.15.g1, ...), custom_call_target="tpu_custom_call" | custom-call | flops 536870912 | bytes 1000000 | tf_op jit(solution)/shard_map/pallas_call | solution.py:460
  60.2 0.2 collective-permute-start.26
  60.5 1.9 %collective-permute-start.27 = (bf16[256,256]{1,0:T(8,128)(2,1)S(1)}, bf16[256,256]{1,0:T(8,128)(2,1)S(1)}, u32[]{:S(2)}, u32[]{:S(2)}) collective-permute-start(bf16[256,256]{1,0:T(8,128)(2,1)S(1)} %get-tuple-element.72), channel_id=1, source_target_pairs={{0,16},{8,24},{16,0},{24,8},{32,48},{40,56},{48,32},{56,40},{64,80... | collective-permute-start | bytes 393224 | tf_op jit(solution)/shard_map/ppermute | solution.py:413
  62.3 2.7 %collective-permute-start.28 = (bf16[256,256]{1,0:T(8,128)(2,1)S(1)}, bf16[256,256]{1,0:T(8,128)(2,1)S(1)}, u32[]{:S(2)}, u32[]{:S(2)}) collective-permute-start(bf16[256,256]{1,0:T(8,128)(2,1)S(1)} %get-tuple-element.73), channel_id=1, source_target_pairs={{0,24},{8,16},{16,8},{24,0},{32,56},{40,48},{48,40},{56,32},{64,88... | collective-permute-start | bytes 393224 | tf_op jit(solution)/shard_map/ppermute | solution.py:413
  65.0 1.8 %collective-permute-start.14 = (bf16[256,128]{1,0:T(8,128)(2,1)S(1)}, bf16[256,128]{1,0:T(8,128)(2,1)S(1)}, u32[]{:S(2)}, u32[]{:S(2)}) collective-permute-start(bf16[256,128]{1,0:T(8,128)(2,1)S(1)} %get-tuple-element.62), channel_id=1, source_target_pairs={{0,96},{8,104},{16,112},{24,120},{32,64},{40,72},{48,80},{56,88},{... | collective-permute-start | bytes 196616 | tf_op jit(solution)/shard_map/ppermute | solution.py:413
  66.8 4.1 %collective-permute-done.13.v2 = bf16[256,128]{1,0:T(8,128)(2,1)S(1)} collective-permute-done((bf16[256,128]{1,0:T(8,128)(2,1)S(1)}, bf16[256,128]{1,0:T(8,128)(2,1)S(1)}, u32[]{:S(2)}, u32[]{:S(2)}) %collective-permute-start.13) | collective-permute-done | bytes 65568 | tf_op jit(solution)/shard_map/ppermute | solution.py:413
  70.9 0.3 collective-permute-done.14.v3
  71.2 1.1 %shard_map.124 = (bf16[512,128]{1,0:T(8,128)(2,1)}, bf16[512,128]{1,0:T(8,128)(2,1)}, bf16[512,128]{1,0:T(8,128)(2,1)}) custom-call(f32[2,256,128]{2,1,0:T(8,128)S(1)} %get-tuple-element.52.own_k, f32[2,256,128]{2,1,0:T(8,128)S(1)} %get-tuple-element.53.own_v, bf16[768,128]{1,0:T(8,128)(2,1)S(1)} %collective-permute-done.6.y1, ...), custom_call_target="tpu_custom_call" | custom-call | flops 10000000 | bytes 1000000 | tf_op jit(solution)/shard_map/pallas_call | solution.py:460
  72.4 0.8 %shard_map.126 = f32[256,256]{1,0:T(8,128)} custom-call(f32[256,256]{1,0:T(8,128)S(1)} %get-tuple-element.70.own, bf16[256,256]{1,0:T(8,128)(2,1)S(1)} %collective-permute-done.26.t1, bf16[256,256]{1,0:T(8,128)(2,1)S(1)} %collective-permute-done.27.t2, bf16[256,256]{1,0:T(8,128)(2,1)S(1)} %collective-permute-done.28.t3), custom_call_target="tpu_custom_call" | custom-call | flops 1000000 | bytes 1000000 | tf_op jit(solution)/shard_map/pallas_call | solution.py:460
  (19 shorter events, 0.0 us)
Async XLA Ops:
  0.6 21.6 %copy-start = (f32[2]{0:T(128)S(1)}, f32[2]{0:T(128)}, u32[]{:S(2)}) copy-start(f32[2]{0:T(128)} %lam.3) | copy-start | bytes 28
  2.7 9.9 %collective-permute-start.22 = (bf16[64,1024]{1,0:T(8,128)(2,1)S(1)}, bf16[64,1024]{1,0:T(8,128)(2,1)S(1)}, u32[]{:S(2)}, u32[]{:S(2)}) collective-permute-start(bf16[64,1024]{1,0:T(8,128)(2,1)S(1)} %get-tuple-element.69), channel_id=1, source_target_pairs={{0,64},{8,72},{16,80},{24,88},{32,96},{40,104},{48,112},{56,120},{... | collective-permute-start | bytes 393224 | tf_op jit(solution)/shard_map/ppermute | solution.py:413
  6.7 8.0 %collective-permute-start.4 = (bf16[544,128]{1,0:T(8,128)(2,1)S(1)}, bf16[544,128]{1,0:T(8,128)(2,1)S(1)}, u32[]{:S(2)}, u32[]{:S(2)}) collective-permute-start(bf16[544,128]{1,0:T(8,128)(2,1)S(1)} %get-tuple-element.42), channel_id=1, source_target_pairs={{0,32},{8,40},{16,48},{24,56},{32,0},{40,8},{48,16},{56,24},{64,96... | collective-permute-start | bytes 417800 | tf_op jit(solution)/shard_map/ppermute | solution.py:413
  7.8 13.9 %collective-permute-start.2 = (bf16[1056,128]{1,0:T(8,128)(2,1)S(1)}, bf16[1056,128]{1,0:T(8,128)(2,1)S(1)}, u32[]{:S(2)}, u32[]{:S(2)}) collective-permute-start(bf16[1056,128]{1,0:T(8,128)(2,1)S(1)} %get-tuple-element.39.yown), channel_id=1, source_target_pairs={{0,8},{8,0},{16,24},{24,16},{32,40},{40,32},{48,56},{56,48},{64,72... | collective-permute-start | bytes 811016 | tf_op jit(solution)/shard_map/ppermute | solution.py:413
  9.3 12.9 %collective-permute-start.3 = (bf16[1056,128]{1,0:T(8,128)(2,1)S(1)}, bf16[1056,128]{1,0:T(8,128)(2,1)S(1)}, u32[]{:S(2)}, u32[]{:S(2)}) collective-permute-start(bf16[1056,128]{1,0:T(8,128)(2,1)S(1)} %get-tuple-element.39.yown), channel_id=1, source_target_pairs={{0,24},{8,16},{16,8},{24,0},{32,56},{40,48},{48,40},{56,32},{64,88... | collective-permute-start | bytes 811016 | tf_op jit(solution)/shard_map/ppermute | solution.py:413
  11.5 8.7 %collective-permute-start.18 = (bf16[128,1024]{1,0:T(8,128)(2,1)S(1)}, bf16[128,1024]{1,0:T(8,128)(2,1)S(1)}, u32[]{:S(2)}, u32[]{:S(2)}) collective-permute-start(bf16[128,1024]{1,0:T(8,128)(2,1)S(1)} %get-tuple-element.68), channel_id=1, source_target_pairs={{0,32},{1,97},{2,34},{3,99},{4,36},{5,101},{6,38},{7,103},{8,40},{... | collective-permute-start | bytes 786440 | tf_op jit(solution)/shard_map/ppermute | solution.py:423
  12.5 7.3 %collective-permute-start.5 = (bf16[544,128]{1,0:T(8,128)(2,1)S(1)}, bf16[544,128]{1,0:T(8,128)(2,1)S(1)}, u32[]{:S(2)}, u32[]{:S(2)}) collective-permute-start(bf16[544,128]{1,0:T(8,128)(2,1)S(1)} %get-tuple-element.43), channel_id=1, source_target_pairs={{0,96},{8,104},{16,112},{24,120},{32,64},{40,72},{48,80},{56,88},{... | collective-permute-start | bytes 417800 | tf_op jit(solution)/shard_map/ppermute | solution.py:413
  14.8 11.8 %collective-permute-start = (bf16[1056,128]{1,0:T(8,128)(2,1)S(1)}, bf16[1056,128]{1,0:T(8,128)(2,1)S(1)}, u32[]{:S(2)}, u32[]{:S(2)}) collective-permute-start(bf16[1056,128]{1,0:T(8,128)(2,1)S(1)} %get-tuple-element.39.yown), channel_id=1, source_target_pairs={{0,16},{8,24},{16,0},{24,8},{32,48},{40,56},{48,32},{56,40},{64,80... | collective-permute-start | bytes 811016 | tf_op jit(solution)/shard_map/ppermute | solution.py:413
  19.8 6.7 %collective-permute-start.1 = (bf16[544,128]{1,0:T(8,128)(2,1)S(1)}, bf16[544,128]{1,0:T(8,128)(2,1)S(1)}, u32[]{:S(2)}, u32[]{:S(2)}) collective-permute-start(bf16[544,128]{1,0:T(8,128)(2,1)S(1)} %get-tuple-element.40), channel_id=1, source_target_pairs={{0,64},{8,72},{16,80},{24,88},{32,96},{40,104},{48,112},{56,120},{... | collective-permute-start | bytes 417800 | tf_op jit(solution)/shard_map/ppermute | solution.py:413
  20.2 14.7 %collective-permute-start.23 = (bf16[64,1024]{1,0:T(8,128)(2,1)S(1)}, bf16[64,1024]{1,0:T(8,128)(2,1)S(1)}, u32[]{:S(2)}, u32[]{:S(2)}) collective-permute-start(bf16[64,1024]{1,0:T(8,128)(2,1)S(1)} %collective-permute-done.22.f0), channel_id=1, source_target_pairs={{0,2},{1,3},{2,0},{3,1},{4,6},{5,7},{6,4},{7,5},{8,10},{9,11},{10,... | collective-permute-start | bytes 393224 | tf_op jit(solution)/shard_map/ppermute | solution.py:427
  21.7 23.6 %collective-permute-start.19 = (bf16[128,1024]{1,0:T(8,128)(2,1)S(1)}, bf16[128,1024]{1,0:T(8,128)(2,1)S(1)}, u32[]{:S(2)}, u32[]{:S(2)}) collective-permute-start(bf16[128,1024]{1,0:T(8,128)(2,1)S(1)} %collective-permute-done.18.n0), channel_id=1, source_target_pairs={{0,2},{1,3},{2,0},{3,1},{4,6},{5,7},{6,4},{7,5},{8,10},{9,11},{10,... | collective-permute-start | bytes 786440 | tf_op jit(solution)/shard_map/ppermute | solution.py:427
  29.5 15.1 %collective-permute-start.6 = (bf16[768,128]{1,0:T(8,128)(2,1)S(1)}, bf16[768,128]{1,0:T(8,128)(2,1)S(1)}, u32[]{:S(2)}, u32[]{:S(2)}) collective-permute-start(bf16[768,128]{1,0:T(8,128)(2,1)S(1)} %get-tuple-element.54), channel_id=1, source_target_pairs={{0,8},{8,0},{16,24},{24,16},{32,40},{40,32},{48,56},{56,48},{64,72... | collective-permute-start | bytes 589832 | tf_op jit(solution)/shard_map/ppermute | solution.py:413
  30.3 14.8 %collective-permute-start.7 = (bf16[768,128]{1,0:T(8,128)(2,1)S(1)}, bf16[768,128]{1,0:T(8,128)(2,1)S(1)}, u32[]{:S(2)}, u32[]{:S(2)}) collective-permute-start(bf16[768,128]{1,0:T(8,128)(2,1)S(1)} %get-tuple-element.55), channel_id=1, source_target_pairs={{0,16},{8,24},{16,0},{24,8},{32,48},{40,56},{48,32},{56,40},{64,80... | collective-permute-start | bytes 589832 | tf_op jit(solution)/shard_map/ppermute | solution.py:413
  33.2 5.8 %collective-permute-start.10 = (bf16[256,128]{1,0:T(8,128)(2,1)S(1)}, bf16[256,128]{1,0:T(8,128)(2,1)S(1)}, u32[]{:S(2)}, u32[]{:S(2)}) collective-permute-start(bf16[256,128]{1,0:T(8,128)(2,1)S(1)} %get-tuple-element.58), channel_id=1, source_target_pairs={{0,64},{8,72},{16,80},{24,88},{32,96},{40,104},{48,112},{56,120},{... | collective-permute-start | bytes 196616 | tf_op jit(solution)/shard_map/ppermute | solution.py:413
  34.9 5.5 %collective-permute-start.11 = (bf16[256,128]{1,0:T(8,128)(2,1)S(1)}, bf16[256,128]{1,0:T(8,128)(2,1)S(1)}, u32[]{:S(2)}, u32[]{:S(2)}) collective-permute-start(bf16[256,128]{1,0:T(8,128)(2,1)S(1)} %get-tuple-element.59), channel_id=1, source_target_pairs={{0,96},{8,104},{16,112},{24,120},{32,64},{40,72},{48,80},{56,88},{... | collective-permute-start | bytes 196616 | tf_op jit(solution)/shard_map/ppermute | solution.py:413
  38.9 6.9 %collective-permute-start.8 = (bf16[768,128]{1,0:T(8,128)(2,1)S(1)}, bf16[768,128]{1,0:T(8,128)(2,1)S(1)}, u32[]{:S(2)}, u32[]{:S(2)}) collective-permute-start(bf16[768,128]{1,0:T(8,128)(2,1)S(1)} %get-tuple-element.56), channel_id=1, source_target_pairs={{0,24},{8,16},{16,8},{24,0},{32,56},{40,48},{48,40},{56,32},{64,88... | collective-permute-start | bytes 589832 | tf_op jit(solution)/shard_map/ppermute | solution.py:413
  40.4 4.3 %collective-permute-start.9 = (bf16[256,128]{1,0:T(8,128)(2,1)S(1)}, bf16[256,128]{1,0:T(8,128)(2,1)S(1)}, u32[]{:S(2)}, u32[]{:S(2)}) collective-permute-start(bf16[256,128]{1,0:T(8,128)(2,1)S(1)} %get-tuple-element.57), channel_id=1, source_target_pairs={{0,32},{8,40},{16,48},{24,56},{32,0},{40,8},{48,16},{56,24},{64,96... | collective-permute-start | bytes 196616 | tf_op jit(solution)/shard_map/ppermute | solution.py:413
  44.6 6.3 %collective-permute-start.20 = (bf16[128,1024]{1,0:T(8,128)(2,1)S(1)}, bf16[128,1024]{1,0:T(8,128)(2,1)S(1)}, u32[]{:S(2)}, u32[]{:S(2)}) collective-permute-start(bf16[128,1024]{1,0:T(8,128)(2,1)S(1)} %collective-permute-done.18.n0), channel_id=1, source_target_pairs={{0,1},{1,0},{2,3},{3,2},{4,5},{5,4},{6,7},{7,6},{8,9},{9,8},{10,11... | collective-permute-start | bytes 786440 | tf_op jit(solution)/shard_map/ppermute | solution.py:431
  44.7 3.6 %collective-permute-start.24 = (bf16[64,1024]{1,0:T(8,128)(2,1)S(1)}, bf16[64,1024]{1,0:T(8,128)(2,1)S(1)}, u32[]{:S(2)}, u32[]{:S(2)}) collective-permute-start(bf16[64,1024]{1,0:T(8,128)(2,1)S(1)} %collective-permute-done.22.f0), channel_id=1, source_target_pairs={{0,1},{1,0},{2,3},{3,2},{4,5},{5,4},{6,7},{7,6},{8,9},{9,8},{10,11... | collective-permute-start | bytes 393224 | tf_op jit(solution)/shard_map/ppermute | solution.py:431
  45.2 5.3 %collective-permute-start.25 = (bf16[64,1024]{1,0:T(8,128)(2,1)S(1)}, bf16[64,1024]{1,0:T(8,128)(2,1)S(1)}, u32[]{:S(2)}, u32[]{:S(2)}) collective-permute-start(bf16[64,1024]{1,0:T(8,128)(2,1)S(1)} %collective-permute-done.23.f1), channel_id=1, source_target_pairs={{0,1},{1,0},{2,3},{3,2},{4,5},{5,4},{6,7},{7,6},{8,9},{9,8},{10,11... | collective-permute-start | bytes 393224 | tf_op jit(solution)/shard_map/ppermute | solution.py:431
  45.3 14.1 %collective-permute-start.21 = (bf16[128,1024]{1,0:T(8,128)(2,1)S(1)}, bf16[128,1024]{1,0:T(8,128)(2,1)S(1)}, u32[]{:S(2)}, u32[]{:S(2)}) collective-permute-start(bf16[128,1024]{1,0:T(8,128)(2,1)S(1)} %collective-permute-done.19.n1), channel_id=1, source_target_pairs={{0,1},{1,0},{2,3},{3,2},{4,5},{5,4},{6,7},{7,6},{8,9},{9,8},{10,11... | collective-permute-start | bytes 786440 | tf_op jit(solution)/shard_map/ppermute | solution.py:431
  45.9 6.0 %collective-permute-start.15 = (bf16[256,256]{1,0:T(8,128)(2,1)S(1)}, bf16[256,256]{1,0:T(8,128)(2,1)S(1)}, u32[]{:S(2)}, u32[]{:S(2)}) collective-permute-start(bf16[256,256]{1,0:T(8,128)(2,1)S(1)} %shard_map.123.turned_in.g0), channel_id=1, source_target_pairs={{0,32},{8,40},{16,48},{24,56},{32,0},{40,8},{48,16},{56,24},{64,96... | collective-permute-start | bytes 393224 | tf_op jit(solution)/shard_map/ppermute | solution.py:413
  48.2 9.5 %collective-permute-start.16 = (bf16[256,256]{1,0:T(8,128)(2,1)S(1)}, bf16[256,256]{1,0:T(8,128)(2,1)S(1)}, u32[]{:S(2)}, u32[]{:S(2)}) collective-permute-start(bf16[256,256]{1,0:T(8,128)(2,1)S(1)} %shard_map.123.turned_in.g0), channel_id=1, source_target_pairs={{0,64},{8,72},{16,80},{24,88},{32,96},{40,104},{48,112},{56,120},{... | collective-permute-start | bytes 393224 | tf_op jit(solution)/shard_map/ppermute | solution.py:413
  50.5 8.8 %collective-permute-start.17 = (bf16[256,256]{1,0:T(8,128)(2,1)S(1)}, bf16[256,256]{1,0:T(8,128)(2,1)S(1)}, u32[]{:S(2)}, u32[]{:S(2)}) collective-permute-start(bf16[256,256]{1,0:T(8,128)(2,1)S(1)} %shard_map.123.turned_in.g0), channel_id=1, source_target_pairs={{0,96},{8,104},{16,112},{24,120},{32,64},{40,72},{48,80},{56,88},{... | collective-permute-start | bytes 393224 | tf_op jit(solution)/shard_map/ppermute | solution.py:413
  51.0 14.0 %collective-permute-start.12 = (bf16[256,128]{1,0:T(8,128)(2,1)S(1)}, bf16[256,128]{1,0:T(8,128)(2,1)S(1)}, u32[]{:S(2)}, u32[]{:S(2)}) collective-permute-start(bf16[256,128]{1,0:T(8,128)(2,1)S(1)} %get-tuple-element.60), channel_id=1, source_target_pairs={{0,32},{8,40},{16,48},{24,56},{32,0},{40,8},{48,16},{56,24},{64,96... | collective-permute-start | bytes 196616 | tf_op jit(solution)/shard_map/ppermute | solution.py:413
  60.2 12.1 %collective-permute-start.26 = (bf16[256,256]{1,0:T(8,128)(2,1)S(1)}, bf16[256,256]{1,0:T(8,128)(2,1)S(1)}, u32[]{:S(2)}, u32[]{:S(2)}) collective-permute-start(bf16[256,256]{1,0:T(8,128)(2,1)S(1)} %get-tuple-element.71), channel_id=1, source_target_pairs={{0,8},{8,0},{16,24},{24,16},{32,40},{40,32},{48,56},{56,48},{64,72... | collective-permute-start | bytes 393224 | tf_op jit(solution)/shard_map/ppermute | solution.py:413
  60.5 11.9 %collective-permute-start.27 = (bf16[256,256]{1,0:T(8,128)(2,1)S(1)}, bf16[256,256]{1,0:T(8,128)(2,1)S(1)}, u32[]{:S(2)}, u32[]{:S(2)}) collective-permute-start(bf16[256,256]{1,0:T(8,128)(2,1)S(1)} %get-tuple-element.72), channel_id=1, source_target_pairs={{0,16},{8,24},{16,0},{24,8},{32,48},{40,56},{48,32},{56,40},{64,80... | collective-permute-start | bytes 393224 | tf_op jit(solution)/shard_map/ppermute | solution.py:413
  62.3 10.0 %collective-permute-start.28 = (bf16[256,256]{1,0:T(8,128)(2,1)S(1)}, bf16[256,256]{1,0:T(8,128)(2,1)S(1)}, u32[]{:S(2)}, u32[]{:S(2)}) collective-permute-start(bf16[256,256]{1,0:T(8,128)(2,1)S(1)} %get-tuple-element.73), channel_id=1, source_target_pairs={{0,24},{8,16},{16,8},{24,0},{32,56},{40,48},{48,40},{56,32},{64,88... | collective-permute-start | bytes 393224 | tf_op jit(solution)/shard_map/ppermute | solution.py:413
  65.0 5.9 %collective-permute-start.13 = (bf16[256,128]{1,0:T(8,128)(2,1)S(1)}, bf16[256,128]{1,0:T(8,128)(2,1)S(1)}, u32[]{:S(2)}, u32[]{:S(2)}) collective-permute-start(bf16[256,128]{1,0:T(8,128)(2,1)S(1)} %get-tuple-element.61), channel_id=1, source_target_pairs={{0,64},{8,72},{16,80},{24,88},{32,96},{40,104},{48,112},{56,120},{... | collective-permute-start | bytes 196616 | tf_op jit(solution)/shard_map/ppermute | solution.py:413
  65.0 6.2 %collective-permute-start.14 = (bf16[256,128]{1,0:T(8,128)(2,1)S(1)}, bf16[256,128]{1,0:T(8,128)(2,1)S(1)}, u32[]{:S(2)}, u32[]{:S(2)}) collective-permute-start(bf16[256,128]{1,0:T(8,128)(2,1)S(1)} %get-tuple-element.62), channel_id=1, source_target_pairs={{0,96},{8,104},{16,112},{24,120},{32,64},{40,72},{48,80},{56,88},{... | collective-permute-start | bytes 196616 | tf_op jit(solution)/shard_map/ppermute | solution.py:413
